TPU v7x, 256 devices: a whole 4x4x8 slice. The times are simulated.
256 devices in a mesh: sp: 32 (over z, x), tp: 8 (over y, core).
Axes of the slice: x: 4, y: 4, z: 8, core: 2. Of those that a mesh axis runs over, the one named last changes fastest.
Arguments:
- tokens: bfloat16 [12288, 2048], P(('sp', 'tp')), may hold values from -6 to 6
- norm_gain: bfloat16 [2048], replicated, may hold values from 0.099609375 to 1.8984375
- query_down_weight: bfloat16 [2048, 512], replicated, may hold values from -0.125 to 0.125
- query_latent_norm_gain: bfloat16 [512], replicated, may hold values from 0.099609375 to 1.8984375
- key_value_down_weight: bfloat16 [2048, 256], replicated, may hold values from -0.125 to 0.125
- key_value_latent_gain: bfloat16 [256], replicated, may hold values from 0.099609375 to 1.8984375
- w_rope_key: bfloat16 [2048, 32], replicated, may hold values from -0.125 to 0.125
- w_pool_in: bfloat16 [2048, 512], replicated, may hold values from -0.125 to 0.125
- query_up_weight: bfloat16 [512, 2304], P(None, 'tp'), may hold values from -0.25 to 0.25
- key_value_up_weight: bfloat16 [256, 3072], P(None, 'tp'), may hold values from -0.375 to 0.375
- query_gain: bfloat16 [96], replicated, may hold values from 1 to 16
- key_gain: bfloat16 [96], replicated, may hold values from 1 to 16
- w_pool_mix: bfloat16 [8, 64, 64], P('tp'), may hold values from -0.75 to 0.75
- pool_scale: bfloat16 [512], P('tp'), may hold values from 1 to 10
- w_out_attn: bfloat16 [1536, 2048], P('tp'), may hold values from -0.3125 to 0.3125
- w_out_pool: bfloat16 [512, 2048], P('tp'), may hold values from -0.25 to 0.25
Outputs:
- mixed: bfloat16 [12288, 2048], P(('sp', 'tp'))
- row_logsum: float32 [24, 12288], P('tp', 'sp')
All inputs are finite; a program needn't handle non-finite values.
Results may differ from a plain program's by a relative error of at most 0.035.
Values may be sent and summed in bfloat16 or wider, within the bound.
No kernel may reach another device: no remote copies, remote signals or barrier semaphores. Data moves between devices by JAX's collectives and lax.ppermute only.
A program may use at most 128 MiB of HBM per device.

v0:
```python
import jax
import jax.numpy as jnp
import numpy as np
from jax import lax
from jax.experimental import pallas as pl
from jax.experimental.pallas import tpu as pltpu
from jax.sharding import Mesh, PartitionSpec as P

NOPE = 64
ROT = 32
HALF = 16
HEAD = 96
VAL = 64
HEADS = 3
QR = 512
KR = 256
EPS = 1e-06
WIDTH = 2048
ROWS = 48
BLOCK = 384
SIDE = 192
TOKENS = 12288
LOG2E = 1.4426950408889634
LN2 = 0.6931471805599453
MSG = 208
VROWS = 80
QTILE = 512
NX = 4
NY = 4
NZ = 8
NQ = NX * BLOCK

bf16 = jnp.bfloat16
f32 = jnp.float32


def trig_tables(inner_places, outer_step, outer_count):
    freqs = 10000.0 ** (-np.arange(HALF, dtype=np.float64) / HALF)
    inner = freqs[:, None] * inner_places[None, :]
    outer = freqs[:, None] * (outer_step * np.arange(outer_count, dtype=np.float64))[None, :]
    pad = np.zeros((HALF, 128 - outer_count))
    cast = lambda a: a.astype(np.float32)
    return (
        cast(np.cos(inner)),
        cast(np.sin(inner)),
        cast(np.concatenate([np.cos(outer), pad], 1)),
        cast(np.concatenate([np.sin(outer), pad], 1)),
    )


def query_tables():
    return trig_tables(np.arange(BLOCK, dtype=np.float64), BLOCK, NZ * NX)


def key_tables():
    z = np.arange(NZ, dtype=np.float64)
    places = (NX * BLOCK * z[:, None] + np.arange(ROWS, dtype=np.float64)[None, :]).reshape(-1)
    return trig_tables(places, ROWS, NX * NY * 2)


def near(x):
    return pltpu.with_memory_space_constraint(x, pltpu.VMEM)


def vmem():
    return pl.BlockSpec(memory_space=pltpu.VMEM)


def smem():
    return pl.BlockSpec(memory_space=pltpu.SMEM)


def nt(a, b):
    return lax.dot_general(a, b, (((1,), (1,)), ((), ())), preferred_element_type=f32)


def nn(a, b):
    return lax.dot_general(a, b, (((1,), (0,)), ((), ())), preferred_element_type=f32)


def params(limit=24, **kw):
    return pltpu.CompilerParams(vmem_limit_bytes=limit * 1024 * 1024, **kw)


KSTEP = 512


def latents_body(
    tok, gain, qdw, qg, kdw, kg, rw, pw, q_out, kv_out, pool_out, inv, aq, ak, ar, ap
):
    k = pl.program_id(0)

    @pl.when(k == 0)
    def _():
        x = tok[...].astype(f32)
        inv[...] = jnp.broadcast_to(
            lax.rsqrt(jnp.mean(x * x, axis=-1, keepdims=True) + EPS), (ROWS, 128)
        )
        aq[...] = jnp.zeros_like(aq)
        ak[...] = jnp.zeros_like(ak)
        ar[...] = jnp.zeros_like(ar)
        ap[...] = jnp.zeros_like(ap)

    cols = pl.ds(pl.multiple_of(k * KSTEP, KSTEP), KSTEP)
    x = tok[:, cols].astype(f32)
    normed = (x * inv[:, 0:1] * gain[cols].astype(f32).reshape(1, KSTEP)).astype(bf16)
    aq[...] += nn(normed, qdw[...])
    ak[...] += nn(normed, kdw[...])
    ar[...] += nt(normed, rw[...])
    ap[...] += nn(normed, pw[...])

    @pl.when(k == pl.num_programs(0) - 1)
    def _():
        def norm(v, g):
            return (
                v
                * lax.rsqrt(jnp.mean(v * v, axis=-1, keepdims=True) + EPS)
                * g.astype(f32).reshape(1, -1)
            ).astype(bf16)

        q = norm(aq[...], qg[...])
        kv = norm(ak[...], kg[...])
        rope = jnp.concatenate(
            [ar[...].astype(bf16), jnp.zeros((ROWS, 128 - ROT), bf16)], axis=1
        )
        pool_out[...] = ap[...].astype(bf16)
        q_out[...] = q
        for n in range(NZ):
            kv_out[n, :, 0:KR] = kv
            kv_out[n, :, KR:] = rope


def latents(tok, gain, qdw, qg, kdw, kg, rw, pw):
    steps = WIDTH // KSTEP
    whole = lambda *s: pl.BlockSpec(s, lambda k: (0,) * len(s))
    part = lambda n: pl.BlockSpec((KSTEP, n), lambda k: (k, 0))
    return pl.pallas_call(
        latents_body,
        grid=(steps,),
        in_specs=[
            whole(ROWS, WIDTH),
            whole(WIDTH),
            part(QR),
            whole(QR),
            part(KR),
            whole(KR),
            pl.BlockSpec((ROT, KSTEP), lambda k: (0, k)),
            part(512),
        ],
        out_specs=(
            whole(ROWS, QR),
            whole(NZ, ROWS, KR + 128),
            whole(ROWS, 512),
        ),
        out_shape=(
            jax.ShapeDtypeStruct((ROWS, QR), bf16),
            jax.ShapeDtypeStruct((NZ, ROWS, KR + 128), bf16),
            jax.ShapeDtypeStruct((ROWS, 512), bf16),
        ),
        scratch_shapes=[
            pltpu.VMEM((ROWS, 128), f32),
            pltpu.VMEM((ROWS, QR), f32),
            pltpu.VMEM((ROWS, KR), f32),
            pltpu.VMEM((ROWS, ROT), f32),
            pltpu.VMEM((ROWS, 512), f32),
        ],
        compiler_params=params(dimension_semantics=("arbitrary",)),
        name="latents",
    )(tok, gain, qdw, qg, kdw, kg, rw.T, pw)


def angles(coff, soff, cb, sb, idx):
    lanes = lax.broadcasted_iota(jnp.int32, (HALF, 128), 1)
    hit = lanes == idx
    cbase = jnp.sum(jnp.where(hit, cb, 0.0), axis=1, keepdims=True)
    sbase = jnp.sum(jnp.where(hit, sb, 0.0), axis=1, keepdims=True)
    return cbase * coff - sbase * soff, sbase * coff + cbase * soff


def rotated(v, cosine, sine):
    a = v[NOPE : NOPE + HALF]
    b = v[NOPE + HALF :]
    return jnp.concatenate(
        [v[:NOPE], a * cosine - b * sine, a * sine + b * cosine, jnp.zeros_like(v[:ROT])],
        axis=0,
    )


def queries_body(sc, own0, own1, own2, own3, other, wqt, qgain, coff, soff, cb, sb, out):
    c = sc[0]
    own = (own0, own1, own2, own3)
    for x in range(NX):
        mine = own[x][...]
        twin = other[x]
        rows = []
        for y in range(NY):
            piece = slice(y * ROWS, (y + 1) * ROWS)
            rows.append(jnp.where(c == 0, mine[piece], twin[piece]))
            rows.append(jnp.where(c == 0, twin[piece], mine[piece]))
        q = nt(wqt[...], jnp.concatenate(rows, axis=0))
        place = sc[2] * NX + (sc[3] + NX - x) % NX
        cosine, sine = angles(coff[...], soff[...], cb[...], sb[...], place)
        at = pl.multiple_of(((sc[3] + NX - x) % NX) * BLOCK, BLOCK)
        for h in range(HEADS):
            v = q[h * HEAD : (h + 1) * HEAD]
            inv = lax.rsqrt(jnp.mean(v * v, axis=0, keepdims=True) + EPS)
            v = v * inv * qgain[...]
            v = rotated(v, cosine, sine) * (LOG2E * HEAD**-0.5)
            out[h, :, pl.ds(at, BLOCK)] = v.astype(bf16)


def queries(sc, own, other, wqt, qgain, tables):
    return pl.pallas_call(
        queries_body,
        in_specs=[smem()] + [vmem()] * 11,
        out_specs=vmem(),
        out_shape=jax.ShapeDtypeStruct((HEADS, 128, NQ), bf16),
        compiler_params=params(),
        name="queries",
    )(sc, *own, other, wqt, qgain, *tables)


def keys_body(a0, a1, a2, a3, a4, sc, own, other, wkvt, kgain, coff, soff, cb, sb, kbuf, vbuf):
    c, x = sc[0], sc[3]
    pick = (
        lax.broadcasted_iota(jnp.int32, (ROT, 128), 0)
        == lax.broadcasted_iota(jnp.int32, (ROT, 128), 1)
    ).astype(bf16)
    ones = (lax.broadcasted_iota(jnp.int32, (VROWS - VAL, BLOCK), 0) == 0).astype(bf16)
    blocks = [(own, k, k, c) for k in range(NY)] + [(other, k, k, 1 - c) for k in range(NY)]
    for b, (ref, at, y_from, c_from) in enumerate(blocks):
        lat = ref[at]
        kv = nt(wkvt[...], lat[:, :KR])
        rope = nt(pick, lat[:, KR:])
        rope_square = jnp.sum(rope * rope, axis=0, keepdims=True)
        place = (x * NY + y_from) * 2 + c_from
        cosine, sine = angles(coff[...], soff[...], cb[...], sb[...], place)
        cols = slice(b * BLOCK, (b + 1) * BLOCK)
        for h in range(HEADS):
            plain = kv[h * 128 : h * 128 + NOPE]
            total = jnp.sum(plain * plain, axis=0, keepdims=True) + rope_square
            inv = lax.rsqrt(total * (1.0 / HEAD) + EPS)
            k = jnp.concatenate([plain, rope], axis=0) * inv * kgain[...]
            k = rotated(k, cosine, sine).astype(bf16)
            kbuf[h, cols, :] = k.T
            vbuf[h, 0:VAL, cols] = kv[h * 128 + NOPE : (h + 1) * 128].astype(bf16)
            vbuf[h, VAL:, cols] = ones


def keys_values(after, sc, own, other, wkvt, kgain, tables):
    count = 2 * NY * BLOCK
    return pl.pallas_call(
        keys_body,
        in_specs=[pl.BlockSpec(memory_space=pl.ANY)] * 5 + [smem()] + [vmem()] * 8,
        out_specs=(vmem(), vmem()),
        out_shape=(
            pltpu.VMEM((HEADS, count, 128), bf16),
            pltpu.VMEM((HEADS, VROWS, count), bf16),
        ),
        compiler_params=params(),
        name="keys",
    )(*after, sc, own, other, wkvt, kgain, *tables)


CHUNK = 256
SUB = 128
TILES = HEADS * (NQ // QTILE)


def attend_body(sizes, first, last, extra, *refs):
    refs = list(refs)
    refs = refs[extra:]
    pairs = [(refs.pop(0), refs.pop(0)) for _ in sizes]
    qt = refs.pop(0)
    if not first:
        acc_in, m_in = refs[:2]
        refs = refs[2:]
    if last:
        msg = refs.pop(0)
        acc_s, m_s = refs[2:]
    else:
        acc_s, m_s = refs[:2]
        refs = refs[2:]
    bufs = refs[:2]
    chunks = []
    base = 0
    for (kr, vr), n in zip(pairs, sizes):
        for at in range(0, n, CHUNK):
            size = min(CHUNK, n - at)
            chunks.append((base + at, size, kr, vr, at))
        base += n

    def where(i):
        per = NQ // QTILE
        return i // per, pl.ds(pl.multiple_of((i % per) * QTILE, QTILE), QTILE)

    def score(i, chunk, buf, top):
        row, size, kr, _, at = chunk
        h, col = where(i)
        for sub in range(0, size, SUB):
            s = nn(kr[h, at + sub : at + sub + SUB, :], qt[h, :, col])
            buf[row + sub : row + sub + SUB, :] = s
            top = jnp.maximum(top, jnp.max(s.reshape(SUB // 8, 8, QTILE), axis=0))
        return top

    def weigh(i, chunk, buf, m):
        row, size, _, vr, at = chunk
        h, _ = where(i)
        p = jnp.exp2(buf[row : row + size, :] - m).astype(bf16)
        return nn(vr[h, :, at : at + size], p)

    low = jnp.full((8, QTILE), -1e30, f32)

    def settle(i, top):
        m = jnp.max(top, axis=0, keepdims=True)
        if first:
            return m
        h, col = where(i)
        return jnp.maximum(m, m_in[h, :, col])

    def finish(i, m, acc):
        h, col = where(i)
        if not first:
            acc = acc + acc_in[h, :, col] * jnp.exp2(m_in[h, :, col] - m)
        acc_s[h, :, col] = acc
        m_s[h, :, col] = m

    def both(i, m, buf, nxt):
        acc = None
        top = low
        for chunk in chunks:
            part = weigh(i, chunk, buf, m)
            acc = part if acc is None else acc + part
            top = score(i + 1, chunk, nxt, top)
        finish(i, m, acc)
        return settle(i + 1, top)

    top = low
    for chunk in chunks:
        top = score(0, chunk, bufs[0], top)
    m = settle(0, top)

    def pair(j, m):
        m = both(2 * j, m, bufs[0], bufs[1])
        return both(2 * j + 1, m, bufs[1], bufs[0])

    m = lax.fori_loop(0, (TILES - 1) // 2, pair, m)
    acc = None
    for chunk in chunks:
        part = weigh(TILES - 1, chunk, bufs[0], m)
        acc = part if acc is None else acc + part
    finish(TILES - 1, m, acc)

    if last:
        for x in range(NX):
            cols = slice(x * BLOCK, (x + 1) * BLOCK)
            stats = []
            for h in range(HEADS):
                total = acc_s[h, VAL : VAL + 1, cols]
                part = acc_s[h, 0:VAL, cols] * (1.0 / total)
                msg[x, h * VAL : (h + 1) * VAL, :] = part.astype(bf16)
                lse = (m_s[h, :, cols] + jnp.log2(total)) * LN2
                hi = lse.astype(bf16)
                rest = lse - hi.astype(f32)
                mid = rest.astype(bf16)
                low_part = (rest - mid.astype(f32)).astype(bf16)
                stats += [hi.astype(f32), mid.astype(f32), low_part.astype(f32)]
            stats.append(jnp.zeros((MSG - HEADS * VAL - 9, BLOCK), f32))
            msg[x, HEADS * VAL :, :] = jnp.concatenate(stats, axis=0).astype(bf16)


def attend(pairs, qt, carry, last, after=()):
    sizes = [k.shape[1] for k, _ in pairs]
    first = carry is None
    state = (
        jax.ShapeDtypeStruct((HEADS, VROWS, NQ), f32),
        jax.ShapeDtypeStruct((HEADS, 1, NQ), f32),
    )
    if last:
        out_shape = pltpu.VMEM((NX, MSG, BLOCK), bf16)
        out_specs = vmem()
    else:
        out_shape = state
        out_specs = (vmem(), vmem())
    args = [near(a) for pair in pairs for a in pair] + [qt] + ([] if first else list(carry))
    scratch = [pltpu.VMEM((sum(sizes), QTILE), f32) for _ in range(2)]
    if last:
        scratch += [pltpu.VMEM(t.shape, t.dtype) for t in state]

    def body(*refs):
        attend_body(sizes, first, last, len(after), *refs)

    return pl.pallas_call(
        body,
        in_specs=[pl.BlockSpec(memory_space=pl.ANY)] * len(after) + [vmem()] * len(args),
        out_specs=out_specs,
        out_shape=out_shape,
        scratch_shapes=scratch,
        compiler_params=params(40),
    )(*after, *args)


def merge_body(sc, msg, keep, send, lse_out, buf):
    c = sc[0]
    for h in range(HEADS):
        logs = []
        for x in range(NX):
            tail = msg[x, HEADS * VAL :, :].astype(f32)
            r = 3 * h
            logs.append(tail[r : r + 1] + tail[r + 1 : r + 2] + tail[r + 2 : r + 3])
        top = jnp.maximum(jnp.maximum(logs[0], logs[1]), jnp.maximum(logs[2], logs[3]))
        weights = [jnp.exp(v - top) for v in logs]
        total = weights[0] + weights[1] + weights[2] + weights[3]
        lse_out[h : h + 1, :] = top + jnp.log(total)
        inv = 1.0 / total
        acc = jnp.zeros((VAL, BLOCK), f32)
        for x in range(NX):
            acc = acc + msg[x, h * VAL : (h + 1) * VAL, :].astype(f32) * (weights[x] * inv)
        buf[:, h * VAL : (h + 1) * VAL] = acc.T.astype(bf16)
    for y in range(NY):
        dst = slice(y * ROWS, (y + 1) * ROWS)
        at = pl.multiple_of(y * 2 * ROWS + c * ROWS, ROWS)
        keep[dst, :] = buf[pl.ds(at, ROWS), :]
        to = pl.multiple_of(y * 2 * ROWS + (1 - c) * ROWS, ROWS)
        send[dst, :] = buf[pl.ds(to, ROWS), :]


def merge(sc, msg):
    return pl.pallas_call(
        merge_body,
        in_specs=[smem(), vmem()],
        out_specs=(vmem(), vmem(), vmem()),
        out_shape=(
            pltpu.VMEM((SIDE, HEADS * VAL), bf16),
            pltpu.VMEM((SIDE, HEADS * VAL), bf16),
            jax.ShapeDtypeStruct((HEADS, BLOCK), f32),
        ),
        scratch_shapes=[pltpu.VMEM((BLOCK, HEADS * VAL), bf16)],
        compiler_params=params(),
        name="merge",
    )(sc, near(msg))


def pool_body(sc, own, low, high, out):
    first = ((sc[2] * NX + sc[3]) * NY * 2 + sc[1] * 2 + sc[0]) * ROWS
    x = own[...].astype(f32)
    side = jnp.zeros((8, 512), f32)
    window = jnp.concatenate(
        [side, low[...].astype(f32), x, high[...].astype(f32), side], axis=0
    )
    n = ROWS + 32
    s1 = window[0 : n - 1] + window[1:n]
    s2 = s1[0 : n - 3] + s1[2 : n - 1]
    s4 = s2[0 : n - 7] + s2[4 : n - 3]
    s8 = s4[0 : n - 15] + s4[8 : n - 7]
    w1 = s1[15 : 15 + ROWS]
    w2 = s2[14 : 14 + ROWS]
    w4 = s4[12 : 12 + ROWS]
    w8 = s8[8 : 8 + ROWS]
    group = (lax.broadcasted_iota(jnp.int32, (ROWS, 512), 1) // 64) % 4
    total = jnp.where(
        group == 0, w1, jnp.where(group == 1, w2, jnp.where(group == 2, w4, w8))
    )
    half = jnp.where(group == 0, 1, jnp.where(group == 1, 2, jnp.where(group == 2, 4, 8)))
    place = first + lax.broadcasted_iota(jnp.int32, (ROWS, 512), 0)
    count = (jnp.minimum(place + half, TOKENS) - jnp.maximum(place - half, 0)).astype(f32)
    pooled = (total / count - x).astype(bf16)
    for y in range(NY):
        out[y, :, :] = pooled[:, y * 128 : (y + 1) * 128]


def pooling(sc, own, low, high):
    return pl.pallas_call(
        pool_body,
        in_specs=[smem()] + [vmem()] * 3,
        out_specs=vmem(),
        out_shape=jax.ShapeDtypeStruct((NY, ROWS, 128), bf16),
        compiler_params=params(),
        name="pooling",
    )(sc, own, low, high)


def project_body(mine, theirs, pooled, mixw, scale, wa, wb, wp, out):
    mapped = nn(pooled[...].reshape(SIDE, 128), mixw[...])
    extra = (mapped * scale[...]).astype(bf16)
    total = nn(mine[...], wa[...]) + nn(theirs[...], wb[...]) + nn(extra, wp[...])
    for y in range(NY):
        out[y, :, :] = total[y * ROWS : (y + 1) * ROWS].astype(bf16)


def project(mine, theirs, pooled, mixw, scale, wa, wb, wp):
    args = [near(a) for a in (mine, theirs, pooled, mixw, scale, wa, wb, wp)]
    return pl.pallas_call(
        project_body,
        in_specs=[vmem()] * 8,
        out_specs=vmem(),
        out_shape=pltpu.VMEM((NY, ROWS, WIDTH), bf16),
        compiler_params=params(),
        name="project",
    )(*args)


def across(x):
    return lax.ppermute(x, "c", [(0, 1), (1, 0)])


def shifted(x, axis, places):
    count = lax.axis_size(axis)
    return lax.ppermute(x, axis, [(i, (i + places) % count) for i in range(count)])


def order_body(y_ref, a, b, c, d, out):
    y = y_ref[0]
    for k, ref in enumerate((a, b, c, d)):
        at = pl.multiple_of(((y + NY - k) % NY) * ROWS, ROWS)
        out[pl.ds(at, ROWS), :] = ref[...]


def in_order(pieces, y):
    return pl.pallas_call(
        order_body,
        in_specs=[smem()] + [vmem()] * NY,
        out_specs=vmem(),
        out_shape=jax.ShapeDtypeStruct((NY * ROWS, QR), bf16),
        compiler_params=params(),
        name="order",
    )(y.astype(jnp.int32).reshape(1), *pieces)


def shards(
    tokens,
    norm_gain,
    query_down_weight,
    query_latent_norm_gain,
    key_value_down_weight,
    key_value_latent_gain,
    w_rope_key,
    w_pool_in,
    query_up_weight,
    key_value_up_weight,
    query_gain,
    key_gain,
    w_pool_mix,
    pool_scale,
    w_out_attn,
    w_out_pool,
):
    z = lax.axis_index("z")
    x = lax.axis_index("x")
    y = lax.axis_index("y")
    c = lax.axis_index("c")
    sc = jnp.stack([c, y, z, x]).astype(jnp.int32)
    wqt = query_up_weight.T
    wkvt = key_value_up_weight.T
    qgain = query_gain.astype(f32).reshape(HEAD, 1)
    kgain = key_gain.astype(f32).reshape(HEAD, 1)

    wb = across(w_out_attn)
    wp_other = across(w_out_pool)
    mix_other = across(w_pool_mix[0])
    scale_other = across(pool_scale)
    wp = jnp.where(
        c == 0,
        jnp.concatenate([w_out_pool, wp_other], 0),
        jnp.concatenate([wp_other, w_out_pool], 0),
    )
    zero = jnp.zeros((64, 64), bf16)
    mix0 = jnp.where(c == 0, w_pool_mix[0], mix_other)
    mix1 = jnp.where(c == 0, mix_other, w_pool_mix[0])
    mixw = jnp.concatenate(
        [jnp.concatenate([mix0, zero], 1), jnp.concatenate([zero, mix1], 1)], 0
    )
    scale = jnp.where(
        c == 0,
        jnp.concatenate([pool_scale, scale_other]),
        jnp.concatenate([scale_other, pool_scale]),
    ).astype(f32).reshape(1, 128)

    q_all, kv_all, pool_in = latents(
        tokens,
        norm_gain,
        query_down_weight,
        query_latent_norm_gain,
        key_value_down_weight,
        key_value_latent_gain,
        w_rope_key,
        w_pool_in,
    )
    q_side = [q_all] + [shifted(q_all, "y", k) for k in range(1, NY)]
    kv_own = lax.all_to_all(kv_all, "z", 0, 0, tiled=True).reshape(NZ * ROWS, KR + 128)
    kv = lax.all_to_all(jnp.broadcast_to(kv_own[None], (NY, *kv_own.shape)), "y", 0, 0, tiled=True)
    q_side = in_order(q_side, lax.axis_index("y"))
    q_own = [q_side] + [shifted(q_side, "x", k) for k in range(1, NX)]

    count = NZ * NX * NY * 2
    every = ("z", "x", "y", "c")
    low = lax.ppermute(
        pool_in[ROWS - 8 :], every, [(i, i + 1) for i in range(count - 1)]
    )
    high = lax.ppermute(pool_in[:8], every, [(i + 1, i) for i in range(count - 1)])
    pooled = pooling(sc, pool_in, low, high)
    pooled = lax.all_to_all(pooled, "y", 0, 0, tiled=True)

    q_pile = jnp.stack(q_own)
    q_twin = across(q_pile)
    qt = queries(sc, q_own, q_twin, wqt, qgain, query_tables())
    kv_twin = across(kv)
    after = (pooled, wp, wb, mixw, scale)
    pair = keys_values(after, sc, kv, kv_twin, wkvt, kgain, key_tables())
    partial = attend([pair], qt, None, True)

    merged = lax.all_to_all(partial, "x", 0, 0, tiled=True)
    keep, send, row_logsum = merge(sc, merged)
    parts = project(keep, across(send), pooled, mixw, scale, w_out_attn, wb, wp)
    parts = lax.all_to_all(parts, "y", 0, 0, tiled=True)
    mixed = jnp.sum(parts.astype(f32), axis=0).astype(bf16)
    return mixed, row_logsum


def solution(mesh):
    fine = Mesh(mesh.devices.reshape(NZ, NX, NY, 2), ("z", "x", "y", "c"))
    tp = ("y", "c")
    placed = (
        P(("z", "x", "y", "c"), None),
        P(),
        P(),
        P(),
        P(),
        P(),
        P(),
        P(),
        P(None, tp),
        P(None, tp),
        P(),
        P(),
        P(tp, None, None),
        P(tp),
        P(tp, None),
        P(tp, None),
    )

    return jax.shard_map(
        shards,
        mesh=fine,
        in_specs=placed,
        out_specs=(P(("z", "x", "y", "c"), None), P(tp, ("z", "x"))),
        check_vma=False,
    )
```

profile of v0, /device:TPU:1, one launch (start us, length us, event | category | flops | bytes accessed | tf_op | source)
XLA Modules:
  0.0 155.4 jit_solution(3849040673514769966)
XLA Ops:
  0.6 1.6 %copy-done = bf16[2048,512]{1,0:T(8,128)(2,1)S(1)} copy-done((bf16[2048,512]{1,0:T(8,128)(2,1)S(1)}, bf16[2048,512]{1,0:T(8,128)(2,1)}, u32[]{:S(2)}) %copy-start) | copy-done | bytes 2097176
  2.2 1.6 %copy-done.1 = bf16[2048,512]{1,0:T(8,128)(2,1)S(1)} copy-done((bf16[2048,512]{1,0:T(8,128)(2,1)S(1)}, bf16[2048,512]{1,0:T(8,128)(2,1)}, u32[]{:S(2)}) %copy-start.1) | copy-done | bytes 2097176
  3.8 1.2 copy-done.2
  5.0 0.9 copy-done.11
  6.0 0.9 copy-done.13
  8.9 1.9 %latents.1 = (bf16[48,512]{1,0:T(8,128)(2,1)S(1)}, bf16[8,48,384]{2,1,0:T(8,128)(2,1)S(1)}, bf16[48,512]{1,0:T(8,128)(2,1)S(1)}) custom-call(bf16[48,2048]{1,0:T(8,128)(2,1)S(1)} %copy-done.11, bf16[2048]{0:T(1024)(128)(2,1)S(1)} %copy-done.27, bf16[2048,512]{1,0:T(8,128)(2,1)S(1)} %copy-done, bf16[512]{0:T(512)(128)(2,1)S(1)} %copy-done.28, ...), custom_call_target="tpu_custom_call" | custom-call | tf_op jit(solution)/shard_map/latents/pallas_call | solution.py:137
  10.8 19.8 %all_to_all.25 = bf16[8,48,384]{2,1,0:T(8,128)(2,1)S(1)} all-to-all(bf16[8,48,384]{2,1,0:T(8,128)(2,1)S(1)} %get-tuple-element.11), channel_id=1, replica_groups=mesh['z'=8,'x'=4,'y'=4,'c'=2] {'z'}, dimensions={0} | all-to-all | bytes 589824 | tf_op jit(solution)/shard_map/all_to_all | solution.py:590
  30.6 1.2 broadcast_in_dim.9
  31.7 4.3 %all-to-all-start.2 = ((bf16[4,384,384]{2,1,0:T(8,128)(2,1)}), bf16[4,384,384]{2,1,0:T(8,128)(2,1)S(1)}, u32[]{:S(2)}, u32[]{:S(2)}) async-start(bf16[4,384,384]{2,1,0:T(8,128)(2,1)} %broadcast_in_dim.9), calls=%async_computation.2 | async-start | bytes 2359296 | tf_op jit(solution)/shard_map/all_to_all | solution.py:591
  36.1 1.5 collective-permute-start.7
  37.5 2.4 %collective-permute-start.8 = (bf16[48,512]{1,0:T(8,128)(2,1)S(1)}, bf16[48,512]{1,0:T(8,128)(2,1)S(1)}, u32[]{:S(2)}, u32[]{:S(2)}) collective-permute-start(bf16[48,512]{1,0:T(8,128)(2,1)S(1)} %get-tuple-element.14.a), channel_id=1, source_target_pairs={{0,4},{2,6},{4,0},{6,2},{1,5},{3,7},{5,1},{7,3},{8,12},{10,14},{12... | collective-permute-start | bytes 147464 | tf_op jit(solution)/shard_map/ppermute | solution.py:509
  39.9 1.2 collective-permute-start.9
  41.1 6.0 %collective-permute-start = (bf16[8,512]{1,0:T(8,128)(2,1)S(1)}, bf16[8,512]{1,0:T(8,128)(2,1)S(1)}, u32[]{:S(2)}, u32[]{:S(2)}) collective-permute-start(bf16[8,512]{1,0:T(8,128)(2,1)S(1)} %get-tuple-element.19), channel_id=1, source_target_pairs={{0,1},{1,2},{2,3},{3,4},{4,5},{5,6},{6,7},{7,8},{8,9},{9,10},{10,1... | collective-permute-start | bytes 24584 | tf_op jit(solution)/shard_map/ppermute | solution.py:597
  47.1 2.4 %all-to-all-done.2.own = bf16[4,384,384]{2,1,0:T(8,128)(2,1)S(1)} async-done(((bf16[4,384,384]{2,1,0:T(8,128)(2,1)}), bf16[4,384,384]{2,1,0:T(8,128)(2,1)S(1)}, u32[]{:S(2)}, u32[]{:S(2)}) %all-to-all-start.2) | async-done | bytes 1179680 | tf_op jit(solution)/shard_map/all_to_all | solution.py:591
  49.5 5.1 %collective-permute-start.6 = (bf16[4,384,384]{2,1,0:T(8,128)(2,1)S(1)}, bf16[4,384,384]{2,1,0:T(8,128)(2,1)}, u32[]{:S(2)}, u32[]{:S(2)}) collective-permute-start(bf16[4,384,384]{2,1,0:T(8,128)(2,1)S(1)} %all-to-all-done.2.own), channel_id=1, source_target_pairs={{0,1},{1,0},{2,3},{3,2},{4,5},{5,4},{6,7},{7,6},{8,9},{9,8},{10,11... | collective-permute-start | bytes 3538952 | tf_op jit(solution)/shard_map/ppermute | solution.py:504
  54.7 1.3 collective-permute-start.10
  56.0 2.5 %collective-permute-start.11 = (bf16[192,512]{1,0:T(8,128)(2,1)S(1)}, bf16[192,512]{1,0:T(8,128)(2,1)S(1)}, u32[]{:S(2)}, u32[]{:S(2)}) collective-permute-start(bf16[192,512]{1,0:T(8,128)(2,1)S(1)} %order.1.own0), channel_id=1, source_target_pairs={{0,16},{8,24},{16,0},{24,8},{1,17},{9,25},{17,1},{25,9},{2,18},{10... | collective-permute-start | bytes 589832 | tf_op jit(solution)/shard_map/ppermute | solution.py:509
  58.5 1.2 collective-permute-start.12
  59.6 1.8 %collective-permute-done.10.own1 = bf16[192,512]{1,0:T(8,128)(2,1)S(1)} collective-permute-done((bf16[192,512]{1,0:T(8,128)(2,1)S(1)}, bf16[192,512]{1,0:T(8,128)(2,1)S(1)}, u32[]{:S(2)}, u32[]{:S(2)}) %collective-permute-start.10) | collective-permute-done | bytes 196640 | tf_op jit(solution)/shard_map/ppermute | solution.py:509
  61.5 2.4 %collective-permute-start.3 = (bf16[192,2048]{1,0:T(8,128)(2,1)}, bf16[192,2048]{1,0:T(8,128)(2,1)}, u32[]{:S(2)}, u32[]{:S(2)}) collective-permute-start(bf16[192,2048]{1,0:T(8,128)(2,1)} %wa.1), channel_id=1, source_target_pairs={{0,1},{1,0},{2,3},{3,2},{4,5},{5,4},{6,7},{7,6},{8,9},{9,8},{10,11... | collective-permute-start | bytes 2359304 | tf_op jit(solution)/shard_map/ppermute | solution.py:504
  63.8 2.8 %collective-permute-done.11.own2 = bf16[192,512]{1,0:T(8,128)(2,1)S(1)} collective-permute-done((bf16[192,512]{1,0:T(8,128)(2,1)S(1)}, bf16[192,512]{1,0:T(8,128)(2,1)S(1)}, u32[]{:S(2)}, u32[]{:S(2)}) %collective-permute-start.11) | collective-permute-done | bytes 196640 | tf_op jit(solution)/shard_map/ppermute | solution.py:509
  66.7 1.9 %collective-permute-start.5 = (bf16[64]{0:T(256)(128)(2,1)S(1)}, bf16[64]{0:T(256)(128)(2,1)S(1)}, u32[]{:S(2)}, u32[]{:S(2)}) collective-permute-start(bf16[64]{0:T(256)(128)(2,1)S(1)} %copy-done.33), channel_id=1, source_target_pairs={{0,1},{1,0},{2,3},{3,2},{4,5},{5,4},{6,7},{7,6},{8,9},{9,8},{10,11... | collective-permute-start | bytes 392 | tf_op jit(solution)/shard_map/ppermute | solution.py:504
  68.5 1.0 pad_maximum_fusion
  71.9 2.4 %collective-permute-start.1 = (bf16[8,512]{1,0:T(8,128)(2,1)S(1)}, bf16[8,512]{1,0:T(8,128)(2,1)S(1)}, u32[]{:S(2)}, u32[]{:S(2)}) collective-permute-start(bf16[8,512]{1,0:T(8,128)(2,1)S(1)} %get-tuple-element.18), channel_id=1, source_target_pairs={{1,0},{2,1},{3,2},{4,3},{5,4},{6,5},{7,6},{8,7},{9,8},{10,9},{11,1... | collective-permute-start | bytes 24584 | tf_op jit(solution)/shard_map/ppermute | solution.py:600
  75.0 1.8 %collective-permute-done.1.high = bf16[8,512]{1,0:T(8,128)(2,1)S(1)} collective-permute-done((bf16[8,512]{1,0:T(8,128)(2,1)S(1)}, bf16[8,512]{1,0:T(8,128)(2,1)S(1)}, u32[]{:S(2)}, u32[]{:S(2)}) %collective-permute-start.1) | collective-permute-done | bytes 8224 | tf_op jit(solution)/shard_map/ppermute | solution.py:600
  76.9 1.3 pooling.1
  78.2 4.2 %all-to-all-start = ((bf16[4,48,128]{2,1,0:T(8,128)(2,1)}), bf16[4,48,128]{2,1,0:T(8,128)(2,1)S(1)}, u32[]{:S(2)}, u32[]{:S(2)}) async-start(bf16[4,48,128]{2,1,0:T(8,128)(2,1)} %pooling.1), calls=%async_computation | async-start | bytes 98304 | tf_op jit(solution)/shard_map/all_to_all | solution.py:602
  82.5 1.2 maximum_select_fusion.a1.wp
  83.7 0.9 copy-done.3
  84.5 1.1 copy-done.4
  85.7 0.9 copy-done.6
  86.6 0.9 copy-done.8
  87.5 1.0 copy-done.9
  88.5 0.8 copy-done.12
  89.3 0.7 copy-done.16
  90.0 0.7 copy-done.17
  92.8 1.5 queries.1.refs_2_
  94.4 0.8 copy-done.10
  95.9 0.7 copy-done.15
  99.3 3.1 %keys.1 = (bf16[3,3072,128]{2,1,0:T(8,128)(2,1)S(1)}, bf16[3,80,3072]{2,1,0:T(8,128)(2,1)S(1)}) custom-call(bf16[4,48,128]{2,1,0:T(8,128)(2,1)S(1)} %all-to-all-done.a0.pooled, bf16[128,2048]{1,0:T(8,128)(2,1)S(1)} %maximum_select_fusion.a1.wp, bf16[192,2048]{1,0:T(8,128)(2,1)} %collective-permute-done.3.a2.wb, bf16[128,128]{1,0:T(8,128)(2,1)S(1)} %fusion.2.a3.mixw, ...), custom_call_target="tpu_custom_call" | custom-call | tf_op jit(solution)/shard_map/keys/pallas_call | solution.py:252
  102.3 15.3 %shard_map.239 = bf16[4,208,384]{2,1,0:T(8,128)(2,1)S(1)} custom-call(bf16[3,3072,128]{2,1,0:T(8,128)(2,1)S(1)} %get-tuple-element.12.refs_0_, bf16[3,80,3072]{2,1,0:T(8,128)(2,1)S(1)} %get-tuple-element.13.refs_1_, bf16[3,128,1536]{2,1,0:T(8,128)(2,1)S(1)} %queries.1.refs_2_), custom_call_target="tpu_custom_call" | custom-call | tf_op jit(solution)/shard_map/pallas_call | solution.py:393
  117.7 14.9 %all_to_all.26.msg = bf16[4,208,384]{2,1,0:T(8,128)(2,1)S(1)} all-to-all(bf16[4,208,384]{2,1,0:T(8,128)(2,1)S(1)} %shard_map.239), channel_id=1, replica_groups=mesh['z'=8,'x'=4,'y'=4,'c'=2] {'x'}, dimensions={0} | all-to-all | bytes 1277952 | tf_op jit(solution)/shard_map/all_to_all | solution.py:612
  132.6 1.4 merge.1
  134.0 1.9 %collective-permute-start.14 = (bf16[192,192]{1,0:T(8,128)(2,1)S(1)}, bf16[192,192]{1,0:T(8,128)(2,1)S(1)}, u32[]{:S(2)}, u32[]{:S(2)}) collective-permute-start(bf16[192,192]{1,0:T(8,128)(2,1)S(1)} %get-tuple-element.16), channel_id=1, source_target_pairs={{0,1},{1,0},{2,3},{3,2},{4,5},{5,4},{6,7},{7,6},{8,9},{9,8},{10,11... | collective-permute-start | bytes 221192 | tf_op jit(solution)/shard_map/ppermute | solution.py:504
  135.9 0.9 collective-permute-done.14.theirs
  136.9 2.1 %project.1 = bf16[4,48,2048]{2,1,0:T(8,128)(2,1)S(1)} custom-call(bf16[192,192]{1,0:T(8,128)(2,1)S(1)} %get-tuple-element.15.mine, bf16[192,192]{1,0:T(8,128)(2,1)S(1)} %collective-permute-done.14.theirs, bf16[4,48,128]{2,1,0:T(8,128)(2,1)S(1)} %all-to-all-done.a0.pooled, bf16[128,128]{1,0:T(8,128)(2,1)S(1)} %fusion.2.a3.mixw, f32[1,128]{1,0:T(1,128)S(1)} %copy-done.26, ...), custom_call_target="tpu_custom_call" | custom-call | tf_op jit(solution)/shard_map/project/pallas_call | solution.py:493
  139.0 15.5 %all_to_all.27 = bf16[4,48,2048]{2,1,0:T(8,128)(2,1)S(1)} all-to-all(bf16[4,48,2048]{2,1,0:T(8,128)(2,1)S(1)} %project.1), channel_id=1, replica_groups=mesh['z'=8,'x'=4,'y'=4,'c'=2] {'y'}, dimensions={0} | all-to-all | bytes 1572864 | tf_op jit(solution)/shard_map/all_to_all | solution.py:615
  154.5 0.8 reduce_sum.12
  (83 shorter events, 10.7 us)
Async XLA Ops:
  0.6 1.6 %copy-start = (bf16[2048,512]{1,0:T(8,128)(2,1)S(1)}, bf16[2048,512]{1,0:T(8,128)(2,1)}, u32[]{:S(2)}) copy-start(bf16[2048,512]{1,0:T(8,128)(2,1)} %qdw.1) | copy-start | bytes 6291460
  2.2 1.6 %copy-start.1 = (bf16[2048,512]{1,0:T(8,128)(2,1)S(1)}, bf16[2048,512]{1,0:T(8,128)(2,1)}, u32[]{:S(2)}) copy-start(bf16[2048,512]{1,0:T(8,128)(2,1)} %pw.1) | copy-start | bytes 6291460
  3.8 1.2 copy-start.2
  5.0 0.9 copy-start.11
  6.0 0.9 copy-start.13
  6.9 0.7 copy-start.27
  31.7 22.9 %copy-start.34 = (bf16[96]{0:T(256)(128)(2,1)S(1)}, bf16[96]{0:T(256)(128)(2,1)}, u32[]{:S(2)}) copy-start(bf16[96]{0:T(256)(128)(2,1)} %param.35) | copy-start | bytes 580
  31.7 27.9 %copy-start.35 = (bf16[96]{0:T(256)(128)(2,1)S(1)}, bf16[96]{0:T(256)(128)(2,1)}, u32[]{:S(2)}) copy-start(bf16[96]{0:T(256)(128)(2,1)} %param.34) | copy-start | bytes 580
  31.7 34.9 %copy-start.33 = (bf16[64]{0:T(256)(128)(2,1)S(1)}, bf16[64]{0:T(256)(128)(2,1)}, u32[]{:S(2)}) copy-start(bf16[64]{0:T(256)(128)(2,1)} %param.37) | copy-start | bytes 388
  31.7 17.8 %all-to-all-start.2 = ((bf16[4,384,384]{2,1,0:T(8,128)(2,1)}), bf16[4,384,384]{2,1,0:T(8,128)(2,1)S(1)}, u32[]{:S(2)}, u32[]{:S(2)}) async-start(bf16[4,384,384]{2,1,0:T(8,128)(2,1)} %broadcast_in_dim.9), calls=%async_computation.2 | async-start | bytes 2359296 | tf_op jit(solution)/shard_map/all_to_all | solution.py:591
  36.1 34.2 %copy-start.31 = (bf16[256,384]{1,0:T(8,128)(2,1)S(1)}, bf16[256,384]{1,0:T(8,128)(2,1)}, u32[]{:S(2)}) copy-start(bf16[256,384]{1,0:T(8,128)(2,1)} %param.33) | copy-start | bytes 589828
  36.1 38.3 %copy-start.32 = (bf16[1,64,64]{2,1,0:T(8,128)(2,1)S(1)}, bf16[1,64,64]{2,1,0:T(8,128)(2,1)}, u32[]{:S(2)}) copy-start(bf16[1,64,64]{2,1,0:T(8,128)(2,1)} %param.36) | copy-start | bytes 24580
  36.1 40.8 %copy-start.30 = (bf16[64,2048]{1,0:T(8,128)(2,1)S(1)}, bf16[64,2048]{1,0:T(8,128)(2,1)}, u32[]{:S(2)}) copy-start(bf16[64,2048]{1,0:T(8,128)(2,1)} %param.39) | copy-start | bytes 786436
  36.1 18.6 %collective-permute-start.7 = (bf16[48,512]{1,0:T(8,128)(2,1)S(1)}, bf16[48,512]{1,0:T(8,128)(2,1)S(1)}, u32[]{:S(2)}, u32[]{:S(2)}) collective-permute-start(bf16[48,512]{1,0:T(8,128)(2,1)S(1)} %get-tuple-element.14.a), channel_id=1, source_target_pairs={{0,2},{2,4},{4,6},{6,0},{1,3},{3,5},{5,7},{7,1},{8,10},{10,12},{12... | collective-permute-start | bytes 147464 | tf_op jit(solution)/shard_map/ppermute | solution.py:509
  37.5 17.1 %collective-permute-start.8 = (bf16[48,512]{1,0:T(8,128)(2,1)S(1)}, bf16[48,512]{1,0:T(8,128)(2,1)S(1)}, u32[]{:S(2)}, u32[]{:S(2)}) collective-permute-start(bf16[48,512]{1,0:T(8,128)(2,1)S(1)} %get-tuple-element.14.a), channel_id=1, source_target_pairs={{0,4},{2,6},{4,0},{6,2},{1,5},{3,7},{5,1},{7,3},{8,12},{10,14},{12... | collective-permute-start | bytes 147464 | tf_op jit(solution)/shard_map/ppermute | solution.py:509
  39.9 14.8 %collective-permute-start.9 = (bf16[48,512]{1,0:T(8,128)(2,1)S(1)}, bf16[48,512]{1,0:T(8,128)(2,1)S(1)}, u32[]{:S(2)}, u32[]{:S(2)}) collective-permute-start(bf16[48,512]{1,0:T(8,128)(2,1)S(1)} %get-tuple-element.14.a), channel_id=1, source_target_pairs={{0,6},{2,0},{4,2},{6,4},{1,7},{3,1},{5,3},{7,5},{8,14},{10,8},{12,... | collective-permute-start | bytes 147464 | tf_op jit(solution)/shard_map/ppermute | solution.py:509
  41.1 33.2 %collective-permute-start = (bf16[8,512]{1,0:T(8,128)(2,1)S(1)}, bf16[8,512]{1,0:T(8,128)(2,1)S(1)}, u32[]{:S(2)}, u32[]{:S(2)}) collective-permute-start(bf16[8,512]{1,0:T(8,128)(2,1)S(1)} %get-tuple-element.19), channel_id=1, source_target_pairs={{0,1},{1,2},{2,3},{3,4},{4,5},{5,6},{6,7},{7,8},{8,9},{9,10},{10,1... | collective-permute-start | bytes 24584 | tf_op jit(solution)/shard_map/ppermute | solution.py:597
  49.5 44.8 %collective-permute-start.6 = (bf16[4,384,384]{2,1,0:T(8,128)(2,1)S(1)}, bf16[4,384,384]{2,1,0:T(8,128)(2,1)}, u32[]{:S(2)}, u32[]{:S(2)}) collective-permute-start(bf16[4,384,384]{2,1,0:T(8,128)(2,1)S(1)} %all-to-all-done.2.own), channel_id=1, source_target_pairs={{0,1},{1,0},{2,3},{3,2},{4,5},{5,4},{6,7},{7,6},{8,9},{9,8},{10,11... | collective-permute-start | bytes 3538952 | tf_op jit(solution)/shard_map/ppermute | solution.py:504
  54.7 6.7 %collective-permute-start.10 = (bf16[192,512]{1,0:T(8,128)(2,1)S(1)}, bf16[192,512]{1,0:T(8,128)(2,1)S(1)}, u32[]{:S(2)}, u32[]{:S(2)}) collective-permute-start(bf16[192,512]{1,0:T(8,128)(2,1)S(1)} %order.1.own0), channel_id=1, source_target_pairs={{0,8},{8,16},{16,24},{24,0},{1,9},{9,17},{17,25},{25,1},{2,10},{10... | collective-permute-start | bytes 589832 | tf_op jit(solution)/shard_map/ppermute | solution.py:509
  56.0 10.7 %collective-permute-start.11 = (bf16[192,512]{1,0:T(8,128)(2,1)S(1)}, bf16[192,512]{1,0:T(8,128)(2,1)S(1)}, u32[]{:S(2)}, u32[]{:S(2)}) collective-permute-start(bf16[192,512]{1,0:T(8,128)(2,1)S(1)} %order.1.own0), channel_id=1, source_target_pairs={{0,16},{8,24},{16,0},{24,8},{1,17},{9,25},{17,1},{25,9},{2,18},{10... | collective-permute-start | bytes 589832 | tf_op jit(solution)/shard_map/ppermute | solution.py:509
  58.5 10.1 %collective-permute-start.12 = (bf16[192,512]{1,0:T(8,128)(2,1)S(1)}, bf16[192,512]{1,0:T(8,128)(2,1)S(1)}, u32[]{:S(2)}, u32[]{:S(2)}) collective-permute-start(bf16[192,512]{1,0:T(8,128)(2,1)S(1)} %order.1.own0), channel_id=1, source_target_pairs={{0,24},{8,0},{16,8},{24,16},{1,25},{9,1},{17,9},{25,17},{2,26},{10... | collective-permute-start | bytes 589832 | tf_op jit(solution)/shard_map/ppermute | solution.py:509
  61.5 32.9 %collective-permute-start.3 = (bf16[192,2048]{1,0:T(8,128)(2,1)}, bf16[192,2048]{1,0:T(8,128)(2,1)}, u32[]{:S(2)}, u32[]{:S(2)}) collective-permute-start(bf16[192,2048]{1,0:T(8,128)(2,1)} %wa.1), channel_id=1, source_target_pairs={{0,1},{1,0},{2,3},{3,2},{4,5},{5,4},{6,7},{7,6},{8,9},{9,8},{10,11... | collective-permute-start | bytes 2359304 | tf_op jit(solution)/shard_map/ppermute | solution.py:504
  66.7 3.6 %copy-start.5 = (bf16[192,512]{1,0:T(8,128)(2,1)}, bf16[192,512]{1,0:T(8,128)(2,1)S(1)}, u32[]{:S(2)}) copy-start(bf16[192,512]{1,0:T(8,128)(2,1)S(1)} %collective-permute-done.11.own2) | copy-start | bytes 589828
  66.7 5.2 %collective-permute-start.5 = (bf16[64]{0:T(256)(128)(2,1)S(1)}, bf16[64]{0:T(256)(128)(2,1)S(1)}, u32[]{:S(2)}, u32[]{:S(2)}) collective-permute-start(bf16[64]{0:T(256)(128)(2,1)S(1)} %copy-done.33), channel_id=1, source_target_pairs={{0,1},{1,0},{2,3},{3,2},{4,5},{5,4},{6,7},{7,6},{8,9},{9,8},{10,11... | collective-permute-start | bytes 392 | tf_op jit(solution)/shard_map/ppermute | solution.py:504
  69.5 0.7 copy-start.7
  70.2 13.4 %collective-permute-start.13 = (bf16[4,192,512]{2,1,0:T(8,128)(2,1)}, bf16[4,192,512]{2,1,0:T(8,128)(2,1)S(1)}, u32[]{:S(2)}, u32[]{:S(2)}) collective-permute-start(bf16[4,192,512]{2,1,0:T(8,128)(2,1)} %pad_maximum_fusion), channel_id=1, source_target_pairs={{0,1},{1,0},{2,3},{3,2},{4,5},{5,4},{6,7},{7,6},{8,9},{9,8},{10,11... | collective-permute-start | bytes 2359304 | tf_op jit(solution)/shard_map/ppermute | solution.py:504
  70.3 13.3 %copy-start.18 = (s32[4]{0:T(128)}, s32[4]{0:T(128)S(1)}, u32[]{:S(2)}) copy-start(s32[4]{0:T(128)S(1)} %pad_add_fusion.sc) | copy-start | bytes 52
  71.9 5.0 %collective-permute-start.1 = (bf16[8,512]{1,0:T(8,128)(2,1)S(1)}, bf16[8,512]{1,0:T(8,128)(2,1)S(1)}, u32[]{:S(2)}, u32[]{:S(2)}) collective-permute-start(bf16[8,512]{1,0:T(8,128)(2,1)S(1)} %get-tuple-element.18), channel_id=1, source_target_pairs={{1,0},{2,1},{3,2},{4,3},{5,4},{6,5},{7,6},{8,7},{9,8},{10,9},{11,1... | collective-permute-start | bytes 24584 | tf_op jit(solution)/shard_map/ppermute | solution.py:600
  74.3 8.0 %collective-permute-start.4 = (bf16[64,64]{1,0:T(8,128)(2,1)S(1)}, bf16[64,64]{1,0:T(8,128)(2,1)S(1)}, u32[]{:S(2)}, u32[]{:S(2)}) collective-permute-start(bf16[64,64]{1,0:T(8,128)(2,1)S(1)} %bitcast.31), channel_id=1, source_target_pairs={{0,1},{1,0},{2,3},{3,2},{4,5},{5,4},{6,7},{7,6},{8,9},{9,8},{10,11... | collective-permute-start | bytes 24584 | tf_op jit(solution)/shard_map/ppermute | solution.py:504
  76.9 5.6 %collective-permute-start.2 = (bf16[64,2048]{1,0:T(8,128)(2,1)S(1)}, bf16[64,2048]{1,0:T(8,128)(2,1)}, u32[]{:S(2)}, u32[]{:S(2)}) collective-permute-start(bf16[64,2048]{1,0:T(8,128)(2,1)S(1)} %copy-done.30), channel_id=1, source_target_pairs={{0,1},{1,0},{2,3},{3,2},{4,5},{5,4},{6,7},{7,6},{8,9},{9,8},{10,11... | collective-permute-start | bytes 786440 | tf_op jit(solution)/shard_map/ppermute | solution.py:504
  78.2 16.1 %all-to-all-start = ((bf16[4,48,128]{2,1,0:T(8,128)(2,1)}), bf16[4,48,128]{2,1,0:T(8,128)(2,1)S(1)}, u32[]{:S(2)}, u32[]{:S(2)}) async-start(bf16[4,48,128]{2,1,0:T(8,128)(2,1)} %pooling.1), calls=%async_computation | async-start | bytes 98304 | tf_op jit(solution)/shard_map/all_to_all | solution.py:602
  83.6 0.9 copy-start.3
  84.5 1.1 copy-start.4
  85.7 0.9 copy-start.6
  86.6 0.9 copy-start.8
  87.5 1.0 copy-start.9
  88.5 0.8 copy-start.12
  89.3 0.7 copy-start.16
  90.0 0.7 copy-start.17
  91.4 0.7 copy-start.24
  92.1 0.7 copy-start.25
  94.3 0.8 copy-start.10
  95.1 0.7 copy-start.14
  95.9 0.7 copy-start.15
  97.3 0.7 copy-start.22
  98.0 0.7 copy-start.23
  102.3 30.2 %copy-start.21 = (s32[4]{0:T(128)S(1)}, s32[4]{0:T(128)}, u32[]{:S(2)}) copy-start(s32[4]{0:T(128)} %copy-done.18) | copy-start | bytes 52
  134.0 2.9 %collective-permute-start.14 = (bf16[192,192]{1,0:T(8,128)(2,1)S(1)}, bf16[192,192]{1,0:T(8,128)(2,1)S(1)}, u32[]{:S(2)}, u32[]{:S(2)}) collective-permute-start(bf16[192,192]{1,0:T(8,128)(2,1)S(1)} %get-tuple-element.16), channel_id=1, source_target_pairs={{0,1},{1,0},{2,3},{3,2},{4,5},{5,4},{6,7},{7,6},{8,9},{9,8},{10,11... | collective-permute-start | bytes 221192 | tf_op jit(solution)/shard_map/ppermute | solution.py:504
  (5 other events, 3.2 us)
where the time goes:
time: 157 us; the launch traced here: 155 us
  blocking collectives  50.1 us (32%)
  starting transfers between devices  38.3 us (24%)
  Pallas kernels  26.7 us (17%)
  local copies, waits for them, and re-layouts  25.8 us (16%)
  waiting for transfers between devices  9.86 us (6%)
  other arithmetic  3.73 us (2%)
    unnamed x73, local copies, waits for them, and re-layouts  23.2 us
    all_to_all x1, blocking collectives, shards(): lax.all_to_all(kv_all, 'z', 0, 0, tiled=True).reshape(NZ * ROWS, KR + 128)  19.8 us
    all_to_all x1, blocking collectives, shards(): parts = lax.all_to_all(parts, 'y', 0, 0, tiled=True)  15.5 us
    pallas_call x1, Pallas kernels, attend(): pl.pallas_call(body, in_specs=[pl.BlockSpec(memory_space=pl.ANY)] * len(a...  15.3 us
    all_to_all x1, blocking collectives, shards(): merged = lax.all_to_all(partial, 'x', 0, 0, tiled=True)  14.9 us
    ppermute x7, starting transfers between devices, across(): return lax.ppermute(x, 'c', [(0, 1), (1, 0)])  11.4 us
    ppermute x6, starting transfers between devices, shifted(): lax.ppermute(x, axis, [(i, (i + places) % count) for i in range(count)])  9.93 us
    ppermute x1, starting transfers between devices, shards(): lax.ppermute(pool_in[ROWS - 8:], every, [(i, i + 1) for i in range(count...  6.03 us
  transfers between devices with their start and end apart: 17, of which 5 were waited for; matrix products, arithmetic and copies ran while one was open for 3% of the time, Pallas kernels for 2%

commit v1 on v0

--- a/solution.py
+++ b/solution.py
@@ -40,12 +40,8 @@
     outer = freqs[:, None] * (outer_step * np.arange(outer_count, dtype=np.float64))[None, :]
     pad = np.zeros((HALF, 128 - outer_count))
     cast = lambda a: a.astype(np.float32)
-    return (
-        cast(np.cos(inner)),
-        cast(np.sin(inner)),
-        cast(np.concatenate([np.cos(outer), pad], 1)),
-        cast(np.concatenate([np.sin(outer), pad], 1)),
-    )
+    parts = [np.cos(inner), np.sin(inner), np.cos(outer), pad, np.sin(outer), pad]
+    return cast(np.concatenate(parts, 1))
 
 
 def query_tables():
@@ -66,10 +62,6 @@
     return pl.BlockSpec(memory_space=pltpu.VMEM)
 
 
-def smem():
-    return pl.BlockSpec(memory_space=pltpu.SMEM)
-
-
 def nt(a, b):
     return lax.dot_general(a, b, (((1,), (1,)), ((), ())), preferred_element_type=f32)
 
@@ -78,15 +70,15 @@
     return lax.dot_general(a, b, (((1,), (0,)), ((), ())), preferred_element_type=f32)
 
 
-def params(limit=24, **kw):
+def params(limit=56, **kw):
     return pltpu.CompilerParams(vmem_limit_bytes=limit * 1024 * 1024, **kw)
 
 
-KSTEP = 512
+KSTEP = 1024
 
 
 def latents_body(
-    tok, gain, qdw, qg, kdw, kg, rw, pw, q_out, kv_out, pool_out, inv, aq, ak, ar, ap
+    tok, gain, qdw, qg, kdw, kg, rw, pw, m0, m1, m2, m3, kv_out, inv, aq, ak, ar, ap, pb
 ):
     k = pl.program_id(0)
 
@@ -123,8 +115,12 @@
         rope = jnp.concatenate(
             [ar[...].astype(bf16), jnp.zeros((ROWS, 128 - ROT), bf16)], axis=1
         )
-        pool_out[...] = ap[...].astype(bf16)
-        q_out[...] = q
+        pb[...] = ap[...].astype(bf16)
+        y = lax.axis_index("y")
+        for n, out in enumerate((m0, m1, m2, m3)):
+            cols = pl.ds(pl.multiple_of(((y + n) % NY) * 128, 128), 128)
+            out[:, 0:QR] = q
+            out[:, QR:] = pb[:, cols]
         for n in range(NZ):
             kv_out[n, :, 0:KR] = kv
             kv_out[n, :, KR:] = rope
@@ -148,14 +144,12 @@
             part(512),
         ],
         out_specs=(
-            whole(ROWS, QR),
+            *[whole(ROWS, QR + 128)] * NY,
             whole(NZ, ROWS, KR + 128),
-            whole(ROWS, 512),
         ),
         out_shape=(
-            jax.ShapeDtypeStruct((ROWS, QR), bf16),
+            *[jax.ShapeDtypeStruct((ROWS, QR + 128), bf16)] * NY,
             jax.ShapeDtypeStruct((NZ, ROWS, KR + 128), bf16),
-            jax.ShapeDtypeStruct((ROWS, 512), bf16),
         ),
         scratch_shapes=[
             pltpu.VMEM((ROWS, 128), f32),
@@ -163,18 +157,32 @@
             pltpu.VMEM((ROWS, KR), f32),
             pltpu.VMEM((ROWS, ROT), f32),
             pltpu.VMEM((ROWS, 512), f32),
+            pltpu.VMEM((ROWS, 512), bf16),
         ],
         compiler_params=params(dimension_semantics=("arbitrary",)),
         name="latents",
     )(tok, gain, qdw, qg, kdw, kg, rw.T, pw)
 
 
-def angles(coff, soff, cb, sb, idx):
+def angles(table, idx):
     lanes = lax.broadcasted_iota(jnp.int32, (HALF, 128), 1)
     hit = lanes == idx
+    coff = table[:, 0:BLOCK]
+    soff = table[:, BLOCK : 2 * BLOCK]
+    cb = table[:, 2 * BLOCK : 2 * BLOCK + 128]
+    sb = table[:, 2 * BLOCK + 128 :]
     cbase = jnp.sum(jnp.where(hit, cb, 0.0), axis=1, keepdims=True)
     sbase = jnp.sum(jnp.where(hit, sb, 0.0), axis=1, keepdims=True)
     return cbase * coff - sbase * soff, sbase * coff + cbase * soff
+
+
+def column(gain):
+    row = jnp.broadcast_to(gain[...].astype(f32).reshape(1, HEAD), (8, HEAD)).astype(bf16)
+    eye = (
+        lax.broadcasted_iota(jnp.int32, (HEAD, HEAD), 0)
+        == lax.broadcasted_iota(jnp.int32, (HEAD, HEAD), 1)
+    ).astype(bf16)
+    return nt(eye, row)[:, 0:1]
 
 
 def rotated(v, cosine, sine):
@@ -186,8 +194,11 @@
     )
 
 
-def queries_body(sc, own0, own1, own2, own3, other, wqt, qgain, coff, soff, cb, sb, out):
-    c = sc[0]
+def queries_body(own0, own1, own2, own3, other, wqt, gain, table, out):
+    c = lax.axis_index("c")
+    z = lax.axis_index("z")
+    here = lax.axis_index("x")
+    qgain = column(gain)
     own = (own0, own1, own2, own3)
     for x in range(NX):
         mine = own[x][...]
@@ -198,30 +209,34 @@
             rows.append(jnp.where(c == 0, mine[piece], twin[piece]))
             rows.append(jnp.where(c == 0, twin[piece], mine[piece]))
         q = nt(wqt[...], jnp.concatenate(rows, axis=0))
-        place = sc[2] * NX + (sc[3] + NX - x) % NX
-        cosine, sine = angles(coff[...], soff[...], cb[...], sb[...], place)
-        at = pl.multiple_of(((sc[3] + NX - x) % NX) * BLOCK, BLOCK)
+        block = (here + NX - x) % NX
+        place = z * NX + block
+        cosine, sine = angles(table, place)
+        at = pl.multiple_of(block * BLOCK, BLOCK)
         for h in range(HEADS):
             v = q[h * HEAD : (h + 1) * HEAD]
             inv = lax.rsqrt(jnp.mean(v * v, axis=0, keepdims=True) + EPS)
-            v = v * inv * qgain[...]
+            v = v * inv * qgain
             v = rotated(v, cosine, sine) * (LOG2E * HEAD**-0.5)
             out[h, :, pl.ds(at, BLOCK)] = v.astype(bf16)
 
 
-def queries(sc, own, other, wqt, qgain, tables):
+def queries(own, other, wqt, qgain, table):
     return pl.pallas_call(
         queries_body,
-        in_specs=[smem()] + [vmem()] * 11,
+        in_specs=[vmem()] * 8,
         out_specs=vmem(),
-        out_shape=jax.ShapeDtypeStruct((HEADS, 128, NQ), bf16),
+        out_shape=pltpu.VMEM((HEADS, 128, NQ), bf16),
         compiler_params=params(),
         name="queries",
-    )(sc, *own, other, wqt, qgain, *tables)
-
-
-def keys_body(a0, a1, a2, a3, a4, sc, own, other, wkvt, kgain, coff, soff, cb, sb, kbuf, vbuf):
-    c, x = sc[0], sc[3]
+    )(*own, other, wqt, qgain, table)
+
+
+def keys_body(count, *refs):
+    own, other, wkvt, gain, table, kbuf, vbuf = refs[count:]
+    c = lax.axis_index("c")
+    x = lax.axis_index("x")
+    kgain = column(gain)
     pick = (
         lax.broadcasted_iota(jnp.int32, (ROT, 128), 0)
         == lax.broadcasted_iota(jnp.int32, (ROT, 128), 1)
@@ -234,24 +249,28 @@
         rope = nt(pick, lat[:, KR:])
         rope_square = jnp.sum(rope * rope, axis=0, keepdims=True)
         place = (x * NY + y_from) * 2 + c_from
-        cosine, sine = angles(coff[...], soff[...], cb[...], sb[...], place)
+        cosine, sine = angles(table, place)
         cols = slice(b * BLOCK, (b + 1) * BLOCK)
         for h in range(HEADS):
             plain = kv[h * 128 : h * 128 + NOPE]
             total = jnp.sum(plain * plain, axis=0, keepdims=True) + rope_square
             inv = lax.rsqrt(total * (1.0 / HEAD) + EPS)
-            k = jnp.concatenate([plain, rope], axis=0) * inv * kgain[...]
+            k = jnp.concatenate([plain, rope], axis=0) * inv * kgain
             k = rotated(k, cosine, sine).astype(bf16)
             kbuf[h, cols, :] = k.T
             vbuf[h, 0:VAL, cols] = kv[h * 128 + NOPE : (h + 1) * 128].astype(bf16)
             vbuf[h, VAL:, cols] = ones
 
 
-def keys_values(after, sc, own, other, wkvt, kgain, tables):
+def keys_values(after, own, other, wkvt, kgain, table):
     count = 2 * NY * BLOCK
-    return pl.pallas_call(
-        keys_body,
-        in_specs=[pl.BlockSpec(memory_space=pl.ANY)] * 5 + [smem()] + [vmem()] * 8,
+
+    def body(*refs):
+        keys_body(len(after), *refs)
+
+    return pl.pallas_call(
+        body,
+        in_specs=[pl.BlockSpec(memory_space=pl.ANY)] * len(after) + [vmem()] * 5,
         out_specs=(vmem(), vmem()),
         out_shape=(
             pltpu.VMEM((HEADS, count, 128), bf16),
@@ -259,7 +278,7 @@
         ),
         compiler_params=params(),
         name="keys",
-    )(*after, sc, own, other, wkvt, kgain, *tables)
+    )(*after, own, other, wkvt, kgain, table)
 
 
 CHUNK = 256
@@ -382,7 +401,8 @@
     else:
         out_shape = state
         out_specs = (vmem(), vmem())
-    args = [near(a) for pair in pairs for a in pair] + [qt] + ([] if first else list(carry))
+    args = [near(a) for pair in pairs for a in pair] + [near(qt)]
+    args += [] if first else list(carry)
     scratch = [pltpu.VMEM((sum(sizes), QTILE), f32) for _ in range(2)]
     if last:
         scratch += [pltpu.VMEM(t.shape, t.dtype) for t in state]
@@ -400,8 +420,8 @@
     )(*after, *args)
 
 
-def merge_body(sc, msg, keep, send, lse_out, buf):
-    c = sc[0]
+def merge_body(msg, keep, send, lse_out, buf):
+    c = lax.axis_index("c")
     for h in range(HEADS):
         logs = []
         for x in range(NX):
@@ -425,10 +445,10 @@
         send[dst, :] = buf[pl.ds(to, ROWS), :]
 
 
-def merge(sc, msg):
+def merge(msg):
     return pl.pallas_call(
         merge_body,
-        in_specs=[smem(), vmem()],
+        in_specs=[vmem()],
         out_specs=(vmem(), vmem(), vmem()),
         out_shape=(
             pltpu.VMEM((SIDE, HEADS * VAL), bf16),
@@ -436,66 +456,76 @@
             jax.ShapeDtypeStruct((HEADS, BLOCK), f32),
         ),
         scratch_shapes=[pltpu.VMEM((BLOCK, HEADS * VAL), bf16)],
-        compiler_params=params(),
+        compiler_params=params(24),
         name="merge",
-    )(sc, near(msg))
-
-
-def pool_body(sc, own, low, high, out):
-    first = ((sc[2] * NX + sc[3]) * NY * 2 + sc[1] * 2 + sc[0]) * ROWS
-    x = own[...].astype(f32)
-    side = jnp.zeros((8, 512), f32)
-    window = jnp.concatenate(
-        [side, low[...].astype(f32), x, high[...].astype(f32), side], axis=0
-    )
-    n = ROWS + 32
-    s1 = window[0 : n - 1] + window[1:n]
-    s2 = s1[0 : n - 3] + s1[2 : n - 1]
-    s4 = s2[0 : n - 7] + s2[4 : n - 3]
-    s8 = s4[0 : n - 15] + s4[8 : n - 7]
-    w1 = s1[15 : 15 + ROWS]
-    w2 = s2[14 : 14 + ROWS]
-    w4 = s4[12 : 12 + ROWS]
-    w8 = s8[8 : 8 + ROWS]
-    group = (lax.broadcasted_iota(jnp.int32, (ROWS, 512), 1) // 64) % 4
-    total = jnp.where(
-        group == 0, w1, jnp.where(group == 1, w2, jnp.where(group == 2, w4, w8))
-    )
-    half = jnp.where(group == 0, 1, jnp.where(group == 1, 2, jnp.where(group == 2, 4, 8)))
-    place = first + lax.broadcasted_iota(jnp.int32, (ROWS, 512), 0)
-    count = (jnp.minimum(place + half, TOKENS) - jnp.maximum(place - half, 0)).astype(f32)
-    pooled = (total / count - x).astype(bf16)
+    )(near(msg))
+
+
+def pool_body(own, other, low, high, mixw, scale, out, xs):
+    c, y0, z, x0 = [lax.axis_index(n) for n in "cyzx"]
+    xs[0:8, :] = jnp.zeros((8, 128), f32)
+    xs[8:16, :] = low[...].astype(f32)
+    xs[16 + BLOCK : 24 + BLOCK, :] = high[...].astype(f32)
+    xs[24 + BLOCK : 32 + BLOCK, :] = jnp.zeros((8, 128), f32)
     for y in range(NY):
-        out[y, :, :] = pooled[:, y * 128 : (y + 1) * 128]
-
-
-def pooling(sc, own, low, high):
+        src = slice(y * ROWS, (y + 1) * ROWS)
+        at = pl.multiple_of(16 + y * 2 * ROWS + c * ROWS, 16)
+        xs[pl.ds(at, ROWS), :] = own[src, :].astype(f32)
+        to = pl.multiple_of(16 + y * 2 * ROWS + (1 - c) * ROWS, 16)
+        xs[pl.ds(to, ROWS), :] = other[src, :].astype(f32)
+    lane = lax.broadcasted_iota(jnp.int32, (ROWS, 128), 1)
+    second = lane >= 64
+    wide = (y0 % 2) == 1
+    half = jnp.where(wide, jnp.where(second, 8, 4), jnp.where(second, 2, 1))
+    for y in range(NY):
+        row0 = y * 2 * ROWS + c * ROWS
+        window = xs[pl.ds(pl.multiple_of(row0, 16), ROWS + 32), :]
+        n = ROWS + 32
+        x = window[16 : 16 + ROWS]
+        s1 = window[0 : n - 1] + window[1:n]
+        s2 = s1[0 : n - 3] + s1[2 : n - 1]
+        s4 = s2[0 : n - 7] + s2[4 : n - 3]
+        s8 = s4[0 : n - 15] + s4[8 : n - 7]
+        w1 = s1[15 : 15 + ROWS]
+        w2 = s2[14 : 14 + ROWS]
+        w4 = s4[12 : 12 + ROWS]
+        w8 = s8[8 : 8 + ROWS]
+        total = jnp.where(wide, jnp.where(second, w8, w4), jnp.where(second, w2, w1))
+        place = (
+            (z * NX + x0) * BLOCK + row0 + lax.broadcasted_iota(jnp.int32, (ROWS, 128), 0)
+        )
+        count = (jnp.minimum(place + half, TOKENS) - jnp.maximum(place - half, 0)).astype(f32)
+        pooled = (total / count - x).astype(bf16)
+        mapped = nn(pooled, mixw[...])
+        out[y * ROWS : (y + 1) * ROWS, :] = (mapped * scale[...]).astype(bf16)
+
+
+def pooling(own, other, low, high, mixw, scale):
     return pl.pallas_call(
         pool_body,
-        in_specs=[smem()] + [vmem()] * 3,
+        in_specs=[vmem()] * 6,
         out_specs=vmem(),
-        out_shape=jax.ShapeDtypeStruct((NY, ROWS, 128), bf16),
+        out_shape=jax.ShapeDtypeStruct((SIDE, 128), bf16),
+        scratch_shapes=[pltpu.VMEM((BLOCK + 32, 128), f32)],
         compiler_params=params(),
         name="pooling",
-    )(sc, own, low, high)
-
-
-def project_body(mine, theirs, pooled, mixw, scale, wa, wb, wp, out):
-    mapped = nn(pooled[...].reshape(SIDE, 128), mixw[...])
-    extra = (mapped * scale[...]).astype(bf16)
-    total = nn(mine[...], wa[...]) + nn(theirs[...], wb[...]) + nn(extra, wp[...])
+    )(own, other, low, high, mixw, scale)
+
+
+def project_body(mine, theirs, pooled, wa, wb, wp, out):
+    total = nn(mine[...], wa[...]) + nn(theirs[...], wb[...]) + nn(pooled[...], wp[...])
     for y in range(NY):
         out[y, :, :] = total[y * ROWS : (y + 1) * ROWS].astype(bf16)
 
 
-def project(mine, theirs, pooled, mixw, scale, wa, wb, wp):
-    args = [near(a) for a in (mine, theirs, pooled, mixw, scale, wa, wb, wp)]
+def project(mine, theirs, pooled, wa, wb, wp):
+    args = [near(a) for a in (mine, theirs, pooled, wa, wb, wp)]
     return pl.pallas_call(
         project_body,
-        in_specs=[vmem()] * 8,
+        in_specs=[vmem()] * 6,
         out_specs=vmem(),
         out_shape=pltpu.VMEM((NY, ROWS, WIDTH), bf16),
-        compiler_params=params(),
+        compiler_params=params(24),
         name="project",
     )(*args)
 
@@ -509,22 +539,26 @@
     return lax.ppermute(x, axis, [(i, (i + places) % count) for i in range(count)])
 
 
-def order_body(y_ref, a, b, c, d, out):
-    y = y_ref[0]
+def order_body(a, b, c, d, q_out, pool_out):
+    y = lax.axis_index("y")
     for k, ref in enumerate((a, b, c, d)):
         at = pl.multiple_of(((y + NY - k) % NY) * ROWS, ROWS)
-        out[pl.ds(at, ROWS), :] = ref[...]
-
-
-def in_order(pieces, y):
+        q_out[pl.ds(at, ROWS), :] = ref[:, 0:QR]
+        pool_out[pl.ds(at, ROWS), :] = ref[:, QR:]
+
+
+def in_order(pieces):
     return pl.pallas_call(
         order_body,
-        in_specs=[smem()] + [vmem()] * NY,
-        out_specs=vmem(),
-        out_shape=jax.ShapeDtypeStruct((NY * ROWS, QR), bf16),
+        in_specs=[vmem()] * NY,
+        out_specs=(vmem(), vmem()),
+        out_shape=(
+            jax.ShapeDtypeStruct((NY * ROWS, QR), bf16),
+            jax.ShapeDtypeStruct((NY * ROWS, 128), bf16),
+        ),
         compiler_params=params(),
         name="order",
-    )(y.astype(jnp.int32).reshape(1), *pieces)
+    )(*pieces)
 
 
 def shards(
@@ -545,15 +579,9 @@
     w_out_attn,
     w_out_pool,
 ):
-    z = lax.axis_index("z")
-    x = lax.axis_index("x")
-    y = lax.axis_index("y")
     c = lax.axis_index("c")
-    sc = jnp.stack([c, y, z, x]).astype(jnp.int32)
     wqt = query_up_weight.T
     wkvt = key_value_up_weight.T
-    qgain = query_gain.astype(f32).reshape(HEAD, 1)
-    kgain = key_gain.astype(f32).reshape(HEAD, 1)
 
     wb = across(w_out_attn)
     wp_other = across(w_out_pool)
@@ -576,7 +604,7 @@
         jnp.concatenate([scale_other, pool_scale]),
     ).astype(f32).reshape(1, 128)
 
-    q_all, kv_all, pool_in = latents(
+    *messages, kv_all = latents(
         tokens,
         norm_gain,
         query_down_weight,
@@ -586,32 +614,32 @@
         w_rope_key,
         w_pool_in,
     )
-    q_side = [q_all] + [shifted(q_all, "y", k) for k in range(1, NY)]
+    pieces = [messages[0]] + [shifted(messages[k], "y", k) for k in range(1, NY)]
     kv_own = lax.all_to_all(kv_all, "z", 0, 0, tiled=True).reshape(NZ * ROWS, KR + 128)
-    kv = lax.all_to_all(jnp.broadcast_to(kv_own[None], (NY, *kv_own.shape)), "y", 0, 0, tiled=True)
-    q_side = in_order(q_side, lax.axis_index("y"))
+    kv = lax.all_to_all(
+        jnp.broadcast_to(kv_own[None], (NY, *kv_own.shape)), "y", 0, 0, tiled=True
+    )
+    q_side, pool_own = in_order(pieces)
     q_own = [q_side] + [shifted(q_side, "x", k) for k in range(1, NX)]
 
-    count = NZ * NX * NY * 2
-    every = ("z", "x", "y", "c")
-    low = lax.ppermute(
-        pool_in[ROWS - 8 :], every, [(i, i + 1) for i in range(count - 1)]
-    )
-    high = lax.ppermute(pool_in[:8], every, [(i + 1, i) for i in range(count - 1)])
-    pooled = pooling(sc, pool_in, low, high)
-    pooled = lax.all_to_all(pooled, "y", 0, 0, tiled=True)
+    pool_other = across(pool_own)
+    tail_rows = jnp.where(c == 1, pool_own[SIDE - 8 :], pool_other[SIDE - 8 :])
+    head_rows = jnp.where(c == 0, pool_own[:8], pool_other[:8])
+    count = NZ * NX
+    low = lax.ppermute(tail_rows, ("z", "x"), [(i, i + 1) for i in range(count - 1)])
+    high = lax.ppermute(head_rows, ("z", "x"), [(i + 1, i) for i in range(count - 1)])
+    pooled = pooling(pool_own, pool_other, low, high, mixw, scale)
 
     q_pile = jnp.stack(q_own)
     q_twin = across(q_pile)
-    qt = queries(sc, q_own, q_twin, wqt, qgain, query_tables())
+    qt = queries(q_own, q_twin, wqt, query_gain, query_tables())
     kv_twin = across(kv)
-    after = (pooled, wp, wb, mixw, scale)
-    pair = keys_values(after, sc, kv, kv_twin, wkvt, kgain, key_tables())
+    pair = keys_values((pooled, wp, wb), kv, kv_twin, wkvt, key_gain, key_tables())
     partial = attend([pair], qt, None, True)
 
     merged = lax.all_to_all(partial, "x", 0, 0, tiled=True)
-    keep, send, row_logsum = merge(sc, merged)
-    parts = project(keep, across(send), pooled, mixw, scale, w_out_attn, wb, wp)
+    keep, send, row_logsum = merge(merged)
+    parts = project(keep, across(send), pooled, w_out_attn, wb, wp)
     parts = lax.all_to_all(parts, "y", 0, 0, tiled=True)
     mixed = jnp.sum(parts.astype(f32), axis=0).astype(bf16)
     return mixed, row_logsum

time: 157 us -> 139 us (0.89)
  local copies, waits for them, and re-layouts: 25.8 us -> 5.02 us
  waiting for transfers between devices: 9.86 us -> 15.7 us
  starting transfers between devices: 38.3 us -> 32.7 us
  Pallas kernels: 26.7 us -> 30.4 us
  blocking collectives: 50.1 us -> 47.8 us
  other arithmetic: 3.73 us -> 5.84 us
    unnamed x73 -> x45, local copies, waits for them, and re-layouts: 23.2 us -> 3.89 us
    all_to_all x1, waiting for transfers between devices: 2.38 us -> 8.41 us  [shards(): lax.all_to_all(jnp.broadcast_to(kv_own[None], (NY, *kv_own.shape)), 'y',...]
    ppermute x2, starting transfers between devices: 8.42 us -> 3.49 us  [the longest x1 2.03 us: shards(): lax.ppermute(tail_rows, ('z', 'x'), [(i, i + 1) for i in range(count - 1)])]
    all_to_all x1 -> x0, starting transfers between devices: 4.18 us -> none  [shards(): pooled = lax.all_to_all(pooled, 'y', 0, 0, tiled=True)]
    ppermute x7 -> x8, starting transfers between devices: 11.4 us -> 15 us  [across(): return lax.ppermute(x, 'c', [(0, 1), (1, 0)])]
    pallas_call x1, Pallas kernels: 1.89 us -> 4.25 us  [latents(): pl.pallas_call(latents_body, grid=(steps,), in_specs=[whole(ROWS, WIDTH),...]
    ppermute x6, waiting for transfers between devices: 4.67 us -> 2.36 us  [shifted(): lax.ppermute(x, axis, [(i, (i + places) % count) for i in range(count)])]
  transfers between devices with their start and end apart: 17 -> 17, of which waited for: 5 -> 6; matrix products, arithmetic and copies ran while one was open for 3% -> 4% of each run, Pallas kernels for 2% -> 4%
where the time goes in v1:
time: 139 us; the launch traced here: 138 us
  blocking collectives  47.8 us (34%)
  starting transfers between devices  32.7 us (24%)
  Pallas kernels  30.4 us (22%)
  waiting for transfers between devices  15.7 us (11%)
  other arithmetic  5.84 us (4%)
  local copies, waits for them, and re-layouts  5.02 us (4%)
    all_to_all x1, blocking collectives, shards(): lax.all_to_all(kv_all, 'z', 0, 0, tiled=True).reshape(NZ * ROWS, KR + 128)  20 us
    pallas_call x1, Pallas kernels, attend(): pl.pallas_call(body, in_specs=[pl.BlockSpec(memory_space=pl.ANY)] * len(a...  15.3 us
    ppermute x8, starting transfers between devices, across(): return lax.ppermute(x, 'c', [(0, 1), (1, 0)])  15 us
    all_to_all x1, blocking collectives, shards(): parts = lax.all_to_all(parts, 'y', 0, 0, tiled=True)  14.4 us
    all_to_all x1, blocking collectives, shards(): merged = lax.all_to_all(partial, 'x', 0, 0, tiled=True)  13.4 us
    ppermute x6, starting transfers between devices, shifted(): lax.ppermute(x, axis, [(i, (i + places) % count) for i in range(count)])  9.85 us
    all_to_all x1, waiting for transfers between devices, shards(): lax.all_to_all(jnp.broadcast_to(kv_own[None], (NY, *kv_own.shape)), 'y',...  8.41 us
    all_to_all x1, starting transfers between devices, shards(): lax.all_to_all(jnp.broadcast_to(kv_own[None], (NY, *kv_own.shape)), 'y',...  4.33 us
  transfers between devices with their start and end apart: 17, of which 6 were waited for; matrix products, arithmetic and copies ran while one was open for 4% of the time, Pallas kernels for 4%

profile of v1, /device:TPU:1, one launch (start us, length us, event | category | flops | bytes accessed | tf_op | source)
XLA Modules:
  0.0 138.3 jit_solution(15926483974237336111)
XLA Ops:
  0.6 4.3 %latents.1 = (bf16[48,640]{1,0:T(8,128)(2,1)}, bf16[48,640]{1,0:T(8,128)(2,1)}, bf16[48,640]{1,0:T(8,128)(2,1)}, bf16[48,640]{1,0:T(8,128)(2,1)}, bf16[8,48,384]{2,1,0:T(8,128)(2,1)}) custom-call(bf16[48,2048]{1,0:T(8,128)(2,1)} %tok.1, bf16[2048]{0:T(1024)(128)(2,1)} %gain.2, bf16[2048,512]{1,0:T(8,128)(2,1)} %qdw.1, bf16[512]{0:T(512)(128)(2,1)} %qg.1, ...), custom_call_target="tpu_custom_call" | custom-call | tf_op jit(solution)/shard_map/latents/pallas_call | solution.py:133
  4.9 20.0 %all_to_all.20 = bf16[8,48,384]{2,1,0:T(8,128)(2,1)S(1)} all-to-all(bf16[8,48,384]{2,1,0:T(8,128)(2,1)} %get-tuple-element.19), channel_id=1, replica_groups=mesh['z'=8,'x'=4,'y'=4,'c'=2] {'z'}, dimensions={0} | all-to-all | bytes 589824 | tf_op jit(solution)/shard_map/all_to_all | solution.py:618
  24.9 1.1 broadcast_in_dim.9
  26.0 4.3 %all-to-all-start.1 = ((bf16[4,384,384]{2,1,0:T(8,128)(2,1)}), bf16[4,384,384]{2,1,0:T(8,128)(2,1)S(1)}, u32[]{:S(2)}, u32[]{:S(2)}) async-start(bf16[4,384,384]{2,1,0:T(8,128)(2,1)} %broadcast_in_dim.9), calls=%async_computation.1 | async-start | bytes 2359296 | tf_op jit(solution)/shard_map/all_to_all | solution.py:619
  30.4 1.5 %collective-permute-start = (bf16[48,640]{1,0:T(8,128)(2,1)S(1)}, bf16[48,640]{1,0:T(8,128)(2,1)S(1)}, u32[]{:S(2)}, u32[]{:S(2)}) collective-permute-start(bf16[48,640]{1,0:T(8,128)(2,1)S(1)} %copy-done.21), channel_id=1, source_target_pairs={{0,2},{2,4},{4,6},{6,0},{1,3},{3,5},{5,7},{7,1},{8,10},{10,12},{12... | collective-permute-start | bytes 184328 | tf_op jit(solution)/shard_map/ppermute | solution.py:539
  31.8 2.4 %collective-permute-start.1 = (bf16[48,640]{1,0:T(8,128)(2,1)S(1)}, bf16[48,640]{1,0:T(8,128)(2,1)S(1)}, u32[]{:S(2)}, u32[]{:S(2)}) collective-permute-start(bf16[48,640]{1,0:T(8,128)(2,1)S(1)} %copy-done.20), channel_id=1, source_target_pairs={{0,4},{2,6},{4,0},{6,2},{1,5},{3,7},{5,1},{7,3},{8,12},{10,14},{12... | collective-permute-start | bytes 184328 | tf_op jit(solution)/shard_map/ppermute | solution.py:539
  34.2 1.2 collective-permute-start.2
  35.4 8.4 %all-to-all-done.1.refs_3_ = bf16[4,384,384]{2,1,0:T(8,128)(2,1)S(1)} async-done(((bf16[4,384,384]{2,1,0:T(8,128)(2,1)}), bf16[4,384,384]{2,1,0:T(8,128)(2,1)S(1)}, u32[]{:S(2)}, u32[]{:S(2)}) %all-to-all-start.1) | async-done | bytes 1179680 | tf_op jit(solution)/shard_map/all_to_all | solution.py:619
  43.8 5.3 %collective-permute-start.10 = (bf16[4,384,384]{2,1,0:T(8,128)(2,1)S(1)}, bf16[4,384,384]{2,1,0:T(8,128)(2,1)}, u32[]{:S(2)}, u32[]{:S(2)}) collective-permute-start(bf16[4,384,384]{2,1,0:T(8,128)(2,1)S(1)} %all-to-all-done.1.refs_3_), channel_id=1, source_target_pairs={{0,1},{1,0},{2,3},{3,2},{4,5},{5,4},{6,7},{7,6},{8,9},{9,8},{10,11... | collective-permute-start | bytes 3538952 | tf_op jit(solution)/shard_map/ppermute | solution.py:534
  49.2 0.6 copy-done.11
  49.8 0.0 copy-done.12
  49.8 0.0 copy-done.13
  49.8 1.6 %order.1 = (bf16[192,512]{1,0:T(8,128)(2,1)}, bf16[192,128]{1,0:T(8,128)(2,1)}) custom-call(bf16[48,640]{1,0:T(8,128)(2,1)} %get-tuple-element.14.a, bf16[48,640]{1,0:T(8,128)(2,1)} %copy-done.11, bf16[48,640]{1,0:T(8,128)(2,1)} %copy-done.12, bf16[48,640]{1,0:T(8,128)(2,1)} %copy-done.13), custom_call_target="tpu_custom_call" | custom-call | tf_op jit(solution)/shard_map/order/pallas_call | solution.py:551
  51.5 1.2 collective-permute-start.11
  52.7 2.5 %collective-permute-start.12 = (bf16[192,512]{1,0:T(8,128)(2,1)}, bf16[192,512]{1,0:T(8,128)(2,1)S(1)}, u32[]{:S(2)}, u32[]{:S(2)}) collective-permute-start(bf16[192,512]{1,0:T(8,128)(2,1)} %get-tuple-element.22.own0), channel_id=1, source_target_pairs={{0,16},{8,24},{16,0},{24,8},{1,17},{9,25},{17,1},{25,9},{2,18},{10... | collective-permute-start | bytes 589832 | tf_op jit(solution)/shard_map/ppermute | solution.py:539
  55.1 1.1 collective-permute-start.13
  56.3 2.1 %collective-permute-start.7 = (bf16[64]{0:T(256)(128)(2,1)S(1)}, bf16[64]{0:T(256)(128)(2,1)S(1)}, u32[]{:S(2)}, u32[]{:S(2)}) collective-permute-start(bf16[64]{0:T(256)(128)(2,1)S(1)} %copy-done.18), channel_id=1, source_target_pairs={{0,1},{1,0},{2,3},{3,2},{4,5},{5,4},{6,7},{7,6},{8,9},{9,8},{10,11... | collective-permute-start | bytes 392 | tf_op jit(solution)/shard_map/ppermute | solution.py:534
  58.4 0.8 copy.20
  59.2 0.3 collective-permute-start.6
  59.6 0.7 fusion.3.scale
  60.2 0.7 collective-permute-start.8
  60.9 2.3 %collective-permute-done.12.own2 = bf16[192,512]{1,0:T(8,128)(2,1)S(1)} collective-permute-done((bf16[192,512]{1,0:T(8,128)(2,1)}, bf16[192,512]{1,0:T(8,128)(2,1)S(1)}, u32[]{:S(2)}, u32[]{:S(2)}) %collective-permute-start.12) | collective-permute-done | bytes 196640 | tf_op jit(solution)/shard_map/ppermute | solution.py:539
  63.3 2.1 %collective-permute-start.9 = (bf16[192,2048]{1,0:T(8,128)(2,1)S(1)}, bf16[192,2048]{1,0:T(8,128)(2,1)S(1)}, u32[]{:S(2)}, u32[]{:S(2)}) collective-permute-start(bf16[192,2048]{1,0:T(8,128)(2,1)S(1)} %copy-done.3), channel_id=1, source_target_pairs={{0,1},{1,0},{2,3},{3,2},{4,5},{5,4},{6,7},{7,6},{8,9},{9,8},{10,11... | collective-permute-start | bytes 2359304 | tf_op jit(solution)/shard_map/ppermute | solution.py:534
  65.4 0.1 collective-permute-start.3
  65.5 1.0 pad_maximum_fusion
  66.5 0.8 collective-permute-done.3.other
  67.4 0.4 collective-permute-start.14
  67.8 0.7 slice_select_fusion
  68.4 2.0 %collective-permute-start.4 = (bf16[8,128]{1,0:T(8,128)(2,1)S(1)}, bf16[8,128]{1,0:T(8,128)(2,1)S(1)}, u32[]{:S(2)}, u32[]{:S(2)}) collective-permute-start(bf16[8,128]{1,0:T(8,128)(2,1)S(1)} %get-tuple-element.27), channel_id=1, source_target_pairs={{0,8},{8,16},{16,24},{24,32},{32,40},{40,48},{48,56},{56,64},{64,7... | collective-permute-start | bytes 6152 | tf_op jit(solution)/shard_map/ppermute | solution.py:629
  70.5 0.7 collective-permute-done.4.low
  71.2 1.5 %collective-permute-start.5 = (bf16[8,128]{1,0:T(8,128)(2,1)S(1)}, bf16[8,128]{1,0:T(8,128)(2,1)S(1)}, u32[]{:S(2)}, u32[]{:S(2)}) collective-permute-start(bf16[8,128]{1,0:T(8,128)(2,1)S(1)} %get-tuple-element.26), channel_id=1, source_target_pairs={{8,0},{16,8},{24,16},{32,24},{40,32},{48,40},{56,48},{64,56},{72,6... | collective-permute-start | bytes 6152 | tf_op jit(solution)/shard_map/ppermute | solution.py:630
  72.7 0.7 fusion.2.mixw
  73.4 2.4 %collective-permute-done.5.high = bf16[8,128]{1,0:T(8,128)(2,1)S(1)} collective-permute-done((bf16[8,128]{1,0:T(8,128)(2,1)S(1)}, bf16[8,128]{1,0:T(8,128)(2,1)S(1)}, u32[]{:S(2)}, u32[]{:S(2)}) %collective-permute-start.5) | collective-permute-done | bytes 2080 | tf_op jit(solution)/shard_map/ppermute | solution.py:630
  75.8 0.6 copy-done.17
  76.3 1.7 %pooling.1.refs_0_.pooled = bf16[192,128]{1,0:T(8,128)(2,1)} custom-call(bf16[192,128]{1,0:T(8,128)(2,1)} %get-tuple-element.18.own, bf16[192,128]{1,0:T(8,128)(2,1)} %copy-done.14, bf16[8,128]{1,0:T(8,128)(2,1)} %copy-done.16, bf16[8,128]{1,0:T(8,128)(2,1)} %copy-done.17, bf16[128,128]{1,0:T(8,128)(2,1)} %fusion.2.mixw, f32[1,128]{1,0:T(1,128)} %fusion.3.scale), custom_call_target="tpu_custom_call" | custom-call | tf_op jit(solution)/shard_map/pooling/pallas_call | solution.py:504
  78.1 1.9 %maximum_select_fusion.refs_1_.wp = bf16[128,2048]{1,0:T(8,128)(2,1)} fusion(bf16[64,2048]{1,0:T(8,128)(2,1)S(1)} %collective-permute-done.8, bf16[64,2048]{1,0:T(8,128)(2,1)} %param.33, pred[]{:T(512)S(6)} %eq.5), kind=kLoop, calls=%fused_computation.1 | loop fusion | flops 2359296 | bytes 1048577 | tf_op jit(solution)/shard_map/jit(_where)/select_n | solution.py:590
  80.0 0.9 copy-done.9
  80.9 2.4 %queries.1.refs_2_ = bf16[3,128,1536]{2,1,0:T(8,128)(2,1)S(1)} custom-call(bf16[192,512]{1,0:T(8,128)(2,1)} %get-tuple-element.22.own0, bf16[192,512]{1,0:T(8,128)(2,1)} %copy-done.6, bf16[192,512]{1,0:T(8,128)(2,1)} %copy-done.7, bf16[192,512]{1,0:T(8,128)(2,1)} %copy-done.8, bf16[4,192,512]{2,1,0:T(8,128)(2,1)} %copy-done.9, bf16[288,512]{1,0:T(8,128)(2,1)} %bitcast.19, ...), custom_call_target="tpu_custom_call" | custom-call | tf_op jit(solution)/shard_map/queries/pallas_call | solution.py:225
  83.4 0.9 copy-done.1
  84.3 3.4 %keys.1 = (bf16[3,3072,128]{2,1,0:T(8,128)(2,1)S(1)}, bf16[3,80,3072]{2,1,0:T(8,128)(2,1)S(1)}) custom-call(bf16[192,128]{1,0:T(8,128)(2,1)} %pooling.1.refs_0_.pooled, bf16[128,2048]{1,0:T(8,128)(2,1)} %maximum_select_fusion.refs_1_.wp, bf16[192,2048]{1,0:T(8,128)(2,1)} %copy-done.1, bf16[4,384,384]{2,1,0:T(8,128)(2,1)} %copy-done.5, ...), custom_call_target="tpu_custom_call" | custom-call | tf_op jit(solution)/shard_map/keys/pallas_call | solution.py:271
  87.7 15.3 %shard_map.185 = bf16[4,208,384]{2,1,0:T(8,128)(2,1)S(1)} custom-call(bf16[3,3072,128]{2,1,0:T(8,128)(2,1)S(1)} %get-tuple-element.20.refs_0_, bf16[3,80,3072]{2,1,0:T(8,128)(2,1)S(1)} %get-tuple-element.21.refs_1_, bf16[3,128,1536]{2,1,0:T(8,128)(2,1)S(1)} %queries.1.refs_2_), custom_call_target="tpu_custom_call" | custom-call | tf_op jit(solution)/shard_map/pallas_call | solution.py:413
  103.1 13.4 %all_to_all.21.msg = bf16[4,208,384]{2,1,0:T(8,128)(2,1)S(1)} all-to-all(bf16[4,208,384]{2,1,0:T(8,128)(2,1)S(1)} %shard_map.185), channel_id=1, replica_groups=mesh['z'=8,'x'=4,'y'=4,'c'=2] {'x'}, dimensions={0} | all-to-all | bytes 1277952 | tf_op jit(solution)/shard_map/all_to_all | solution.py:640
  116.5 0.9 merge.1
  117.4 3.9 %collective-permute-start.15 = (bf16[192,192]{1,0:T(8,128)(2,1)S(1)}, bf16[192,192]{1,0:T(8,128)(2,1)S(1)}, u32[]{:S(2)}, u32[]{:S(2)}) collective-permute-start(bf16[192,192]{1,0:T(8,128)(2,1)S(1)} %get-tuple-element.24), channel_id=1, source_target_pairs={{0,1},{1,0},{2,3},{3,2},{4,5},{5,4},{6,7},{7,6},{8,9},{9,8},{10,11... | collective-permute-start | bytes 221192 | tf_op jit(solution)/shard_map/ppermute | solution.py:534
  121.3 0.9 collective-permute-done.15.theirs
  122.3 0.8 project.1
  123.0 14.4 %all_to_all.22 = bf16[4,48,2048]{2,1,0:T(8,128)(2,1)S(1)} all-to-all(bf16[4,48,2048]{2,1,0:T(8,128)(2,1)S(1)} %project.1), channel_id=1, replica_groups=mesh['z'=8,'x'=4,'y'=4,'c'=2] {'y'}, dimensions={0} | all-to-all | bytes 1572864 | tf_op jit(solution)/shard_map/all_to_all | solution.py:643
  137.5 0.8 reduce_sum.12
  (50 shorter events, 0.1 us)
Async XLA Ops:
  26.0 4.4 %copy-start.21 = (bf16[48,640]{1,0:T(8,128)(2,1)S(1)}, bf16[48,640]{1,0:T(8,128)(2,1)}, u32[]{:S(2)}) copy-start(bf16[48,640]{1,0:T(8,128)(2,1)} %get-tuple-element.15) | copy-start | bytes 184324
  26.0 5.8 %copy-start.20 = (bf16[48,640]{1,0:T(8,128)(2,1)S(1)}, bf16[48,640]{1,0:T(8,128)(2,1)}, u32[]{:S(2)}) copy-start(bf16[48,640]{1,0:T(8,128)(2,1)} %get-tuple-element.16) | copy-start | bytes 184324
  26.0 8.2 %copy-start.19 = (bf16[48,640]{1,0:T(8,128)(2,1)S(1)}, bf16[48,640]{1,0:T(8,128)(2,1)}, u32[]{:S(2)}) copy-start(bf16[48,640]{1,0:T(8,128)(2,1)} %get-tuple-element.17) | copy-start | bytes 184324
  26.0 30.3 %copy-start.18 = (bf16[64]{0:T(256)(128)(2,1)S(1)}, bf16[64]{0:T(256)(128)(2,1)}, u32[]{:S(2)}) copy-start(bf16[64]{0:T(256)(128)(2,1)} %param.31) | copy-start | bytes 388
  26.0 32.4 %copy-start.10 = (bf16[256,384]{1,0:T(8,128)(2,1)S(1)}, bf16[256,384]{1,0:T(8,128)(2,1)}, u32[]{:S(2)}) copy-start(bf16[256,384]{1,0:T(8,128)(2,1)} %param.27) | copy-start | bytes 589828
  26.0 33.2 %copy-start.15 = (bf16[1,64,64]{2,1,0:T(8,128)(2,1)S(1)}, bf16[1,64,64]{2,1,0:T(8,128)(2,1)}, u32[]{:S(2)}) copy-start(bf16[1,64,64]{2,1,0:T(8,128)(2,1)} %param.30) | copy-start | bytes 24580
  26.0 37.3 %copy-start.3 = (bf16[192,2048]{1,0:T(8,128)(2,1)S(1)}, bf16[192,2048]{1,0:T(8,128)(2,1)}, u32[]{:S(2)}) copy-start(bf16[192,2048]{1,0:T(8,128)(2,1)} %wa.1) | copy-start | bytes 2359300
  26.0 17.8 %all-to-all-start.1 = ((bf16[4,384,384]{2,1,0:T(8,128)(2,1)}), bf16[4,384,384]{2,1,0:T(8,128)(2,1)S(1)}, u32[]{:S(2)}, u32[]{:S(2)}) async-start(bf16[4,384,384]{2,1,0:T(8,128)(2,1)} %broadcast_in_dim.9), calls=%async_computation.1 | async-start | bytes 2359296 | tf_op jit(solution)/shard_map/all_to_all | solution.py:619
  30.4 18.8 %collective-permute-start = (bf16[48,640]{1,0:T(8,128)(2,1)S(1)}, bf16[48,640]{1,0:T(8,128)(2,1)S(1)}, u32[]{:S(2)}, u32[]{:S(2)}) collective-permute-start(bf16[48,640]{1,0:T(8,128)(2,1)S(1)} %copy-done.21), channel_id=1, source_target_pairs={{0,2},{2,4},{4,6},{6,0},{1,3},{3,5},{5,7},{7,1},{8,10},{10,12},{12... | collective-permute-start | bytes 184328 | tf_op jit(solution)/shard_map/ppermute | solution.py:539
  31.8 17.3 %collective-permute-start.1 = (bf16[48,640]{1,0:T(8,128)(2,1)S(1)}, bf16[48,640]{1,0:T(8,128)(2,1)S(1)}, u32[]{:S(2)}, u32[]{:S(2)}) collective-permute-start(bf16[48,640]{1,0:T(8,128)(2,1)S(1)} %copy-done.20), channel_id=1, source_target_pairs={{0,4},{2,6},{4,0},{6,2},{1,5},{3,7},{5,1},{7,3},{8,12},{10,14},{12... | collective-permute-start | bytes 184328 | tf_op jit(solution)/shard_map/ppermute | solution.py:539
  34.2 14.9 %collective-permute-start.2 = (bf16[48,640]{1,0:T(8,128)(2,1)S(1)}, bf16[48,640]{1,0:T(8,128)(2,1)S(1)}, u32[]{:S(2)}, u32[]{:S(2)}) collective-permute-start(bf16[48,640]{1,0:T(8,128)(2,1)S(1)} %copy-done.19), channel_id=1, source_target_pairs={{0,6},{2,0},{4,2},{6,4},{1,7},{3,1},{5,3},{7,5},{8,14},{10,8},{12,... | collective-permute-start | bytes 184328 | tf_op jit(solution)/shard_map/ppermute | solution.py:539
  43.8 36.2 %copy-start.5 = (bf16[4,384,384]{2,1,0:T(8,128)(2,1)}, bf16[4,384,384]{2,1,0:T(8,128)(2,1)S(1)}, u32[]{:S(2)}) copy-start(bf16[4,384,384]{2,1,0:T(8,128)(2,1)S(1)} %all-to-all-done.1.refs_3_) | copy-start | bytes 3538948
  43.8 39.6 %collective-permute-start.10 = (bf16[4,384,384]{2,1,0:T(8,128)(2,1)S(1)}, bf16[4,384,384]{2,1,0:T(8,128)(2,1)}, u32[]{:S(2)}, u32[]{:S(2)}) collective-permute-start(bf16[4,384,384]{2,1,0:T(8,128)(2,1)S(1)} %all-to-all-done.1.refs_3_), channel_id=1, source_target_pairs={{0,1},{1,0},{2,3},{3,2},{4,5},{5,4},{6,7},{7,6},{8,9},{9,8},{10,11... | collective-permute-start | bytes 3538952 | tf_op jit(solution)/shard_map/ppermute | solution.py:534
  49.1 0.6 copy-start.11
  49.2 0.6 copy-start.12
  49.2 0.7 copy-start.13
  51.5 8.8 %collective-permute-start.11 = (bf16[192,512]{1,0:T(8,128)(2,1)}, bf16[192,512]{1,0:T(8,128)(2,1)S(1)}, u32[]{:S(2)}, u32[]{:S(2)}) collective-permute-start(bf16[192,512]{1,0:T(8,128)(2,1)} %get-tuple-element.22.own0), channel_id=1, source_target_pairs={{0,8},{8,16},{16,24},{24,0},{1,9},{9,17},{17,25},{25,1},{2,10},{10... | collective-permute-start | bytes 589832 | tf_op jit(solution)/shard_map/ppermute | solution.py:539
  52.7 10.6 %collective-permute-start.12 = (bf16[192,512]{1,0:T(8,128)(2,1)}, bf16[192,512]{1,0:T(8,128)(2,1)S(1)}, u32[]{:S(2)}, u32[]{:S(2)}) collective-permute-start(bf16[192,512]{1,0:T(8,128)(2,1)} %get-tuple-element.22.own0), channel_id=1, source_target_pairs={{0,16},{8,24},{16,0},{24,8},{1,17},{9,25},{17,1},{25,9},{2,18},{10... | collective-permute-start | bytes 589832 | tf_op jit(solution)/shard_map/ppermute | solution.py:539
  55.1 10.3 %collective-permute-start.13 = (bf16[192,512]{1,0:T(8,128)(2,1)}, bf16[192,512]{1,0:T(8,128)(2,1)S(1)}, u32[]{:S(2)}, u32[]{:S(2)}) collective-permute-start(bf16[192,512]{1,0:T(8,128)(2,1)} %get-tuple-element.22.own0), channel_id=1, source_target_pairs={{0,24},{8,0},{16,8},{24,16},{1,25},{9,1},{17,9},{25,17},{2,26},{10... | collective-permute-start | bytes 589832 | tf_op jit(solution)/shard_map/ppermute | solution.py:539
  56.3 2.9 %collective-permute-start.7 = (bf16[64]{0:T(256)(128)(2,1)S(1)}, bf16[64]{0:T(256)(128)(2,1)S(1)}, u32[]{:S(2)}, u32[]{:S(2)}) collective-permute-start(bf16[64]{0:T(256)(128)(2,1)S(1)} %copy-done.18), channel_id=1, source_target_pairs={{0,1},{1,0},{2,3},{3,2},{4,5},{5,4},{6,7},{7,6},{8,9},{9,8},{10,11... | collective-permute-start | bytes 392 | tf_op jit(solution)/shard_map/ppermute | solution.py:534
  59.2 9.2 %collective-permute-start.6 = (bf16[64,64]{1,0:T(8,128)(2,1)S(1)}, bf16[64,64]{1,0:T(8,128)(2,1)S(1)}, u32[]{:S(2)}, u32[]{:S(2)}) collective-permute-start(bf16[64,64]{1,0:T(8,128)(2,1)S(1)} %bitcast.21), channel_id=1, source_target_pairs={{0,1},{1,0},{2,3},{3,2},{4,5},{5,4},{6,7},{7,6},{8,9},{9,8},{10,11... | collective-permute-start | bytes 24584 | tf_op jit(solution)/shard_map/ppermute | solution.py:534
  60.2 19.8 %copy-start.6 = (bf16[192,512]{1,0:T(8,128)(2,1)}, bf16[192,512]{1,0:T(8,128)(2,1)S(1)}, u32[]{:S(2)}) copy-start(bf16[192,512]{1,0:T(8,128)(2,1)S(1)} %collective-permute-done.11.own1) | copy-start | bytes 589828
  60.2 17.8 %collective-permute-start.8 = (bf16[64,2048]{1,0:T(8,128)(2,1)}, bf16[64,2048]{1,0:T(8,128)(2,1)S(1)}, u32[]{:S(2)}, u32[]{:S(2)}) collective-permute-start(bf16[64,2048]{1,0:T(8,128)(2,1)} %param.33), channel_id=1, source_target_pairs={{0,1},{1,0},{2,3},{3,2},{4,5},{5,4},{6,7},{7,6},{8,9},{9,8},{10,11... | collective-permute-start | bytes 786440 | tf_op jit(solution)/shard_map/ppermute | solution.py:534
  63.3 16.7 %copy-start.7 = (bf16[192,512]{1,0:T(8,128)(2,1)}, bf16[192,512]{1,0:T(8,128)(2,1)S(1)}, u32[]{:S(2)}) copy-start(bf16[192,512]{1,0:T(8,128)(2,1)S(1)} %collective-permute-done.12.own2) | copy-start | bytes 589828
  63.3 20.1 %collective-permute-start.9 = (bf16[192,2048]{1,0:T(8,128)(2,1)S(1)}, bf16[192,2048]{1,0:T(8,128)(2,1)S(1)}, u32[]{:S(2)}, u32[]{:S(2)}) collective-permute-start(bf16[192,2048]{1,0:T(8,128)(2,1)S(1)} %copy-done.3), channel_id=1, source_target_pairs={{0,1},{1,0},{2,3},{3,2},{4,5},{5,4},{6,7},{7,6},{8,9},{9,8},{10,11... | collective-permute-start | bytes 2359304 | tf_op jit(solution)/shard_map/ppermute | solution.py:534
  65.4 14.6 %copy-start.8 = (bf16[192,512]{1,0:T(8,128)(2,1)}, bf16[192,512]{1,0:T(8,128)(2,1)S(1)}, u32[]{:S(2)}) copy-start(bf16[192,512]{1,0:T(8,128)(2,1)S(1)} %collective-permute-done.13.own3) | copy-start | bytes 589828
  65.4 2.0 %collective-permute-start.3 = (bf16[192,128]{1,0:T(8,128)(2,1)}, bf16[192,128]{1,0:T(8,128)(2,1)S(1)}, u32[]{:S(2)}, u32[]{:S(2)}) collective-permute-start(bf16[192,128]{1,0:T(8,128)(2,1)} %get-tuple-element.18.own), channel_id=1, source_target_pairs={{0,1},{1,0},{2,3},{3,2},{4,5},{5,4},{6,7},{7,6},{8,9},{9,8},{10,11... | collective-permute-start | bytes 147464 | tf_op jit(solution)/shard_map/ppermute | solution.py:534
  67.4 8.4 %copy-start.14 = (bf16[192,128]{1,0:T(8,128)(2,1)}, bf16[192,128]{1,0:T(8,128)(2,1)S(1)}, u32[]{:S(2)}) copy-start(bf16[192,128]{1,0:T(8,128)(2,1)S(1)} %collective-permute-done.3.other) | copy-start | bytes 147460
  67.4 12.6 %collective-permute-start.14 = (bf16[4,192,512]{2,1,0:T(8,128)(2,1)S(1)}, bf16[4,192,512]{2,1,0:T(8,128)(2,1)S(1)}, u32[]{:S(2)}, u32[]{:S(2)}) collective-permute-start(bf16[4,192,512]{2,1,0:T(8,128)(2,1)S(1)} %pad_maximum_fusion), channel_id=1, source_target_pairs={{0,1},{1,0},{2,3},{3,2},{4,5},{5,4},{6,7},{7,6},{8,9},{9,8},{10,11... | collective-permute-start | bytes 2359304 | tf_op jit(solution)/shard_map/ppermute | solution.py:534
  68.4 2.8 %collective-permute-start.4 = (bf16[8,128]{1,0:T(8,128)(2,1)S(1)}, bf16[8,128]{1,0:T(8,128)(2,1)S(1)}, u32[]{:S(2)}, u32[]{:S(2)}) collective-permute-start(bf16[8,128]{1,0:T(8,128)(2,1)S(1)} %get-tuple-element.27), channel_id=1, source_target_pairs={{0,8},{8,16},{16,24},{24,32},{32,40},{40,48},{48,56},{56,64},{64,7... | collective-permute-start | bytes 6152 | tf_op jit(solution)/shard_map/ppermute | solution.py:629
  71.2 4.6 %copy-start.16 = (bf16[8,128]{1,0:T(8,128)(2,1)}, bf16[8,128]{1,0:T(8,128)(2,1)S(1)}, u32[]{:S(2)}) copy-start(bf16[8,128]{1,0:T(8,128)(2,1)S(1)} %collective-permute-done.4.low) | copy-start | bytes 6148
  71.2 4.6 %collective-permute-start.5 = (bf16[8,128]{1,0:T(8,128)(2,1)S(1)}, bf16[8,128]{1,0:T(8,128)(2,1)S(1)}, u32[]{:S(2)}, u32[]{:S(2)}) collective-permute-start(bf16[8,128]{1,0:T(8,128)(2,1)S(1)} %get-tuple-element.26), channel_id=1, source_target_pairs={{8,0},{16,8},{24,16},{32,24},{40,32},{48,40},{56,48},{64,56},{72,6... | collective-permute-start | bytes 6152 | tf_op jit(solution)/shard_map/ppermute | solution.py:630
  75.8 0.6 copy-start.17
  80.0 0.9 copy-start.9
  83.4 0.9 copy-start.1
  103.0 19.2 %copy-start = (bf16[128,2048]{1,0:T(8,128)(2,1)S(1)}, bf16[128,2048]{1,0:T(8,128)(2,1)}, u32[]{:S(2)}) copy-start(bf16[128,2048]{1,0:T(8,128)(2,1)} %maximum_select_fusion.refs_1_.wp) | copy-start | bytes 1572868
  103.0 19.2 %copy-start.2 = (bf16[192,2048]{1,0:T(8,128)(2,1)S(1)}, bf16[192,2048]{1,0:T(8,128)(2,1)}, u32[]{:S(2)}) copy-start(bf16[192,2048]{1,0:T(8,128)(2,1)} %copy-done.1) | copy-start | bytes 2359300
  103.0 19.2 %copy-start.4 = (bf16[192,128]{1,0:T(8,128)(2,1)S(1)}, bf16[192,128]{1,0:T(8,128)(2,1)}, u32[]{:S(2)}) copy-start(bf16[192,128]{1,0:T(8,128)(2,1)} %pooling.1.refs_0_.pooled) | copy-start | bytes 147460
  117.4 4.9 %collective-permute-start.15 = (bf16[192,192]{1,0:T(8,128)(2,1)S(1)}, bf16[192,192]{1,0:T(8,128)(2,1)S(1)}, u32[]{:S(2)}, u32[]{:S(2)}) collective-permute-start(bf16[192,192]{1,0:T(8,128)(2,1)S(1)} %get-tuple-element.24), channel_id=1, source_target_pairs={{0,1},{1,0},{2,3},{3,2},{4,5},{5,4},{6,7},{7,6},{8,9},{9,8},{10,11... | collective-permute-start | bytes 221192 | tf_op jit(solution)/shard_map/ppermute | solution.py:534

commit v2 on v0

v2 whole, which is shorter than its diff:
```python
import jax
import jax.numpy as jnp
import numpy as np
from jax import lax
from jax.experimental import pallas as pl
from jax.experimental.pallas import tpu as pltpu
from jax.sharding import Mesh, PartitionSpec as P

NOPE = 64
ROT = 32
HALF = 16
HEAD = 96
VAL = 64
HEADS = 3
QR = 512
KR = 256
EPS = 1e-06
WIDTH = 2048
ROWS = 48
BLOCK = 384
TOKENS = 12288
LOG2E = 1.4426950408889634
LN2 = 0.6931471805599453
MSG = 256
VROWS = 80
QTILE = 512
NX = 4
NY = 4
NZ = 8
NQ = NX * BLOCK

bf16 = jnp.bfloat16
f32 = jnp.float32


def trig_tables(inner_places, outer_step, outer_count):
    freqs = 10000.0 ** (-np.arange(HALF, dtype=np.float64) / HALF)
    inner = freqs[:, None] * inner_places[None, :]
    outer = freqs[:, None] * (outer_step * np.arange(outer_count, dtype=np.float64))[None, :]
    pad = np.zeros((HALF, 128 - outer_count))
    cast = lambda a: a.astype(np.float32)
    parts = [np.cos(inner), np.sin(inner), np.cos(outer), pad, np.sin(outer), pad]
    return cast(np.concatenate(parts, 1))


def query_tables():
    return trig_tables(np.arange(BLOCK, dtype=np.float64), BLOCK, NZ * NX)


def key_tables():
    z = np.arange(NZ, dtype=np.float64)
    places = (NX * BLOCK * z[:, None] + np.arange(ROWS, dtype=np.float64)[None, :]).reshape(-1)
    return trig_tables(places, ROWS, NX * NY * 2)


def near(x):
    return pltpu.with_memory_space_constraint(x, pltpu.VMEM)


def vmem():
    return pl.BlockSpec(memory_space=pltpu.VMEM)


def nt(a, b):
    return lax.dot_general(a, b, (((1,), (1,)), ((), ())), preferred_element_type=f32)


def nn(a, b):
    return lax.dot_general(a, b, (((1,), (0,)), ((), ())), preferred_element_type=f32)


def params(limit=56, **kw):
    return pltpu.CompilerParams(vmem_limit_bytes=limit * 1024 * 1024, **kw)


KSTEP = 1024


def latents_body(
    tok, gain, qdw, qg, kdw, kg, rw, pw, q_out, kv_out, pool_out, inv, aq, ak, ar, ap
):
    k = pl.program_id(0)

    @pl.when(k == 0)
    def _():
        x = tok[...].astype(f32)
        inv[...] = jnp.broadcast_to(
            lax.rsqrt(jnp.mean(x * x, axis=-1, keepdims=True) + EPS), (ROWS, 128)
        )
        aq[...] = jnp.zeros_like(aq)
        ak[...] = jnp.zeros_like(ak)
        ar[...] = jnp.zeros_like(ar)
        ap[...] = jnp.zeros_like(ap)

    cols = pl.ds(pl.multiple_of(k * KSTEP, KSTEP), KSTEP)
    x = tok[:, cols].astype(f32)
    normed = (x * inv[:, 0:1] * gain[cols].astype(f32).reshape(1, KSTEP)).astype(bf16)
    aq[...] += nn(normed, qdw[...])
    ak[...] += nn(normed, kdw[...])
    ar[...] += nt(normed, rw[...])
    ap[...] += nn(normed, pw[...])

    @pl.when(k == pl.num_programs(0) - 1)
    def _():
        def norm(v, g):
            return (
                v
                * lax.rsqrt(jnp.mean(v * v, axis=-1, keepdims=True) + EPS)
                * g.astype(f32).reshape(1, -1)
            ).astype(bf16)

        q = norm(aq[...], qg[...])
        kv = norm(ak[...], kg[...])
        rope = jnp.concatenate(
            [ar[...].astype(bf16), jnp.zeros((ROWS, 128 - ROT), bf16)], axis=1
        )
        q_out[...] = q
        pool_out[...] = ap[...].astype(bf16)
        for n in range(NZ):
            kv_out[n, :, 0:KR] = kv
            kv_out[n, :, KR:] = rope


def latents(tok, gain, qdw, qg, kdw, kg, rw, pw):
    steps = WIDTH // KSTEP
    whole = lambda *s: pl.BlockSpec(s, lambda k: (0,) * len(s))
    part = lambda n: pl.BlockSpec((KSTEP, n), lambda k: (k, 0))
    return pl.pallas_call(
        latents_body,
        grid=(steps,),
        in_specs=[
            whole(ROWS, WIDTH),
            whole(WIDTH),
            part(QR),
            whole(QR),
            part(KR),
            whole(KR),
            pl.BlockSpec((ROT, KSTEP), lambda k: (0, k)),
            part(512),
        ],
        out_specs=(
            whole(ROWS, QR),
            whole(NZ, ROWS, KR + 128),
            whole(ROWS, 512),
        ),
        out_shape=(
            jax.ShapeDtypeStruct((ROWS, QR), bf16),
            jax.ShapeDtypeStruct((NZ, ROWS, KR + 128), bf16),
            jax.ShapeDtypeStruct((ROWS, 512), bf16),
        ),
        scratch_shapes=[
            pltpu.VMEM((ROWS, 128), f32),
            pltpu.VMEM((ROWS, QR), f32),
            pltpu.VMEM((ROWS, KR), f32),
            pltpu.VMEM((ROWS, ROT), f32),
            pltpu.VMEM((ROWS, 512), f32),
        ],
        compiler_params=params(dimension_semantics=("arbitrary",)),
        name="latents",
    )(tok, gain, qdw, qg, kdw, kg, rw.T, pw)


def angles(table, idx):
    lanes = lax.broadcasted_iota(jnp.int32, (HALF, 128), 1)
    hit = lanes == idx
    coff = table[:, 0:BLOCK]
    soff = table[:, BLOCK : 2 * BLOCK]
    cb = table[:, 2 * BLOCK : 2 * BLOCK + 128]
    sb = table[:, 2 * BLOCK + 128 :]
    cbase = jnp.sum(jnp.where(hit, cb, 0.0), axis=1, keepdims=True)
    sbase = jnp.sum(jnp.where(hit, sb, 0.0), axis=1, keepdims=True)
    return cbase * coff - sbase * soff, sbase * coff + cbase * soff


def column(gain):
    row = jnp.broadcast_to(gain[...].astype(f32).reshape(1, HEAD), (8, HEAD)).astype(bf16)
    eye = (
        lax.broadcasted_iota(jnp.int32, (HEAD, HEAD), 0)
        == lax.broadcasted_iota(jnp.int32, (HEAD, HEAD), 1)
    ).astype(bf16)
    return nt(eye, row)[:, 0:1]


def rotated(v, cosine, sine):
    a = v[NOPE : NOPE + HALF]
    b = v[NOPE + HALF :]
    return jnp.concatenate(
        [v[:NOPE], a * cosine - b * sine, a * sine + b * cosine, jnp.zeros_like(v[:ROT])],
        axis=0,
    )


def queries_body(own0, own1, own2, own3, two0, two1, two2, two3, wqt, gain, table, out):
    c = lax.axis_index("c")
    z = lax.axis_index("z")
    here = lax.axis_index("x")
    qgain = column(gain)
    own = (own0, own1, own2, own3)
    other = (two0, two1, two2, two3)
    for x in range(NX):
        mine = own[x][...]
        twin = other[x][...]
        rows = []
        for y in range(NY):
            piece = slice(y * ROWS, (y + 1) * ROWS)
            rows.append(jnp.where(c == 0, mine[piece], twin[piece]))
            rows.append(jnp.where(c == 0, twin[piece], mine[piece]))
        q = nt(wqt[...], jnp.concatenate(rows, axis=0))
        block = (here + NX - x) % NX
        place = z * NX + block
        cosine, sine = angles(table, place)
        at = pl.multiple_of(block * BLOCK, BLOCK)
        for h in range(HEADS):
            v = q[h * HEAD : (h + 1) * HEAD]
            inv = lax.rsqrt(jnp.mean(v * v, axis=0, keepdims=True) + EPS)
            v = v * inv * qgain
            v = rotated(v, cosine, sine) * (LOG2E * HEAD**-0.5)
            out[h, :, pl.ds(at, BLOCK)] = v.astype(bf16)


def queries(own, other, wqt, qgain, table):
    return pl.pallas_call(
        queries_body,
        in_specs=[vmem()] * 11,
        out_specs=vmem(),
        out_shape=pltpu.VMEM((HEADS, 128, NQ), bf16),
        compiler_params=params(),
        name="queries",
    )(*own, *other, wqt, qgain, table)


def keys_body(count, *refs):
    own, other, wkvt, gain, table, kbuf, vbuf = refs[count:]
    c = lax.axis_index("c")
    x = lax.axis_index("x")
    kgain = column(gain)
    pick = (
        lax.broadcasted_iota(jnp.int32, (ROT, 128), 0)
        == lax.broadcasted_iota(jnp.int32, (ROT, 128), 1)
    ).astype(bf16)
    ones = (lax.broadcasted_iota(jnp.int32, (VROWS - VAL, BLOCK), 0) == 0).astype(bf16)
    blocks = [(own, k, k, c) for k in range(NY)] + [(other, k, k, 1 - c) for k in range(NY)]
    for b, (ref, at, y_from, c_from) in enumerate(blocks):
        lat = ref[at]
        kv = nt(wkvt[...], lat[:, :KR])
        rope = nt(pick, lat[:, KR:])
        rope_square = jnp.sum(rope * rope, axis=0, keepdims=True)
        place = (x * NY + y_from) * 2 + c_from
        cosine, sine = angles(table, place)
        cols = slice(b * BLOCK, (b + 1) * BLOCK)
        for h in range(HEADS):
            plain = kv[h * 128 : h * 128 + NOPE]
            total = jnp.sum(plain * plain, axis=0, keepdims=True) + rope_square
            inv = lax.rsqrt(total * (1.0 / HEAD) + EPS)
            k = jnp.concatenate([plain, rope], axis=0) * inv * kgain
            k = rotated(k, cosine, sine).astype(bf16)
            kbuf[h, cols, :] = k.T
            vbuf[h, 0:VAL, cols] = kv[h * 128 + NOPE : (h + 1) * 128].astype(bf16)
            vbuf[h, VAL:, cols] = ones


def keys_values(after, own, other, wkvt, kgain, table):
    count = 2 * NY * BLOCK

    def body(*refs):
        keys_body(len(after), *refs)

    return pl.pallas_call(
        body,
        in_specs=[pl.BlockSpec(memory_space=pl.ANY)] * len(after) + [vmem()] * 5,
        out_specs=(vmem(), vmem()),
        out_shape=(
            pltpu.VMEM((HEADS, count, 128), bf16),
            pltpu.VMEM((HEADS, VROWS, count), bf16),
        ),
        compiler_params=params(),
        name="keys",
    )(*after, own, other, wkvt, kgain, table)


CHUNK = 256
SUB = 128
TILES = HEADS * (NQ // QTILE)


def attend_body(kbuf, vbuf, qt, msg, l0, l1, l2, l3, buf0, buf1, acc_s, m_s, logs):
    bufs = (buf0, buf1)
    pairs = [(kbuf, vbuf)]
    sizes = [kbuf.shape[1]]
    chunks = []
    base = 0
    for (kr, vr), n in zip(pairs, sizes):
        for at in range(0, n, CHUNK):
            size = min(CHUNK, n - at)
            chunks.append((base + at, size, kr, vr, at))
        base += n

    def where(i):
        per = NQ // QTILE
        return i // per, pl.ds(pl.multiple_of((i % per) * QTILE, QTILE), QTILE)

    def score(i, chunk, buf, top):
        row, size, kr, _, at = chunk
        h, col = where(i)
        for sub in range(0, size, SUB):
            s = nn(kr[h, at + sub : at + sub + SUB, :], qt[h, :, col])
            buf[row + sub : row + sub + SUB, :] = s
            top = jnp.maximum(top, jnp.max(s.reshape(SUB // 8, 8, QTILE), axis=0))
        return top

    def weigh(i, chunk, buf, m):
        row, size, _, vr, at = chunk
        h, _ = where(i)
        p = jnp.exp2(buf[row : row + size, :] - m).astype(bf16)
        return nn(vr[h, :, at : at + size], p)

    low = jnp.full((8, QTILE), -1e30, f32)

    def settle(top):
        return jnp.max(top, axis=0, keepdims=True)

    def finish(i, m, acc):
        h, col = where(i)
        acc_s[h, :, col] = acc
        m_s[h, :, col] = m

    def both(i, m, buf, nxt):
        acc = None
        top = low
        for chunk in chunks:
            part = weigh(i, chunk, buf, m)
            acc = part if acc is None else acc + part
            top = score(i + 1, chunk, nxt, top)
        finish(i, m, acc)
        return settle(top)

    top = low
    for chunk in chunks:
        top = score(0, chunk, bufs[0], top)
    m = settle(top)

    def pair(j, m):
        m = both(2 * j, m, bufs[0], bufs[1])
        return both(2 * j + 1, m, bufs[1], bufs[0])

    m = lax.fori_loop(0, (TILES - 1) // 2, pair, m)
    acc = None
    for chunk in chunks:
        part = weigh(TILES - 1, chunk, bufs[0], m)
        acc = part if acc is None else acc + part
    finish(TILES - 1, m, acc)

    for x in range(NX):
        cols = slice(x * BLOCK, (x + 1) * BLOCK)
        parts = []
        stats = []
        for h in range(HEADS):
            total = acc_s[h, VAL : VAL + 1, cols]
            parts.append((acc_s[h, 0:VAL, cols] * (1.0 / total)).astype(bf16))
            lse = (m_s[h, :, cols] + jnp.log2(total)) * LN2
            logs[x, h : h + 1, :] = lse
            hi = lse.astype(bf16)
            rest = lse - hi.astype(f32)
            mid = rest.astype(bf16)
            low_part = (rest - mid.astype(f32)).astype(bf16)
            stats += [hi.astype(f32), mid.astype(f32), low_part.astype(f32)]
        stats.append(jnp.zeros((MSG - HEADS * VAL - 9, BLOCK), f32))
        parts.append(jnp.concatenate(stats, axis=0).astype(bf16))
        rows = jnp.concatenate(parts, axis=0).T
        for y in range(NY):
            msg[x * NY + y, :, :] = rows[y * 2 * ROWS : (y + 1) * 2 * ROWS]
    here = lax.axis_index("x")
    for k, ref in enumerate((l0, l1, l2, l3)):
        ref[...] = logs[(here + k) % NX]


def attend(kbuf, vbuf, qt):
    return pl.pallas_call(
        attend_body,
        in_specs=[vmem()] * 3,
        out_specs=(vmem(),) * 5,
        out_shape=(
            jax.ShapeDtypeStruct((NX * NY, 2 * ROWS, MSG), bf16),
            *[jax.ShapeDtypeStruct((8, BLOCK), f32)] * NX,
        ),
        scratch_shapes=[
            pltpu.VMEM((kbuf.shape[1], QTILE), f32),
            pltpu.VMEM((kbuf.shape[1], QTILE), f32),
            pltpu.VMEM((HEADS, VROWS, NQ), f32),
            pltpu.VMEM((HEADS, 1, NQ), f32),
            pltpu.VMEM((NX, 8, BLOCK), f32),
        ],
        compiler_params=params(40),
        name="attend",
    )(near(kbuf), near(vbuf), near(qt))


def logsum_body(a, b, c, d, out):
    logs = [r[0:HEADS, :] for r in (a, b, c, d)]
    top = jnp.maximum(jnp.maximum(logs[0], logs[1]), jnp.maximum(logs[2], logs[3]))
    total = sum(jnp.exp(v - top) for v in logs)
    out[...] = top + jnp.log(total)


def logsums(parts):
    return pl.pallas_call(
        logsum_body,
        in_specs=[vmem()] * NX,
        out_specs=vmem(),
        out_shape=jax.ShapeDtypeStruct((HEADS, BLOCK), f32),
        compiler_params=params(),
        name="logsums",
    )(*parts)


PLACES = (0, -1, 1, 2)


def pool_body(own, low, high, keep, send, buf):
    z, here, y0, c = [lax.axis_index(n) for n in "zxyc"]
    first = ((z * NX + here) * NY * 2 + y0 * 2 + c) * ROWS
    x = own[...].astype(f32)
    side = jnp.zeros((8, 512), f32)
    window = jnp.concatenate(
        [side, low[...].astype(f32), x, high[...].astype(f32), side], axis=0
    )
    n = ROWS + 32
    s1 = window[0 : n - 1] + window[1:n]
    s2 = s1[0 : n - 3] + s1[2 : n - 1]
    s4 = s2[0 : n - 7] + s2[4 : n - 3]
    s8 = s4[0 : n - 15] + s4[8 : n - 7]
    w1 = s1[15 : 15 + ROWS]
    w2 = s2[14 : 14 + ROWS]
    w4 = s4[12 : 12 + ROWS]
    w8 = s8[8 : 8 + ROWS]
    group = (lax.broadcasted_iota(jnp.int32, (ROWS, 512), 1) // 64) % 4
    total = jnp.where(
        group == 0, w1, jnp.where(group == 1, w2, jnp.where(group == 2, w4, w8))
    )
    half = jnp.where(group == 0, 1, jnp.where(group == 1, 2, jnp.where(group == 2, 4, 8)))
    place = first + lax.broadcasted_iota(jnp.int32, (ROWS, 512), 0)
    count = (jnp.minimum(place + half, TOKENS) - jnp.maximum(place - half, 0)).astype(f32)
    buf[...] = (total / count - x).astype(bf16)
    even, odd = [], []
    for d in PLACES:
        at = pl.multiple_of(((y0 + NY + d) % NY) * 128, 128)
        tile = buf[:, pl.ds(at, 128)]
        even.append(tile[:, 0:64])
        odd.append(tile[:, 64:128])
    even = jnp.concatenate(even, axis=1)
    odd = jnp.concatenate(odd, axis=1)
    keep[...] = jnp.where(c == 0, even, odd)
    send[...] = jnp.where(c == 0, odd, even)


def pooling(own, low, high):
    return pl.pallas_call(
        pool_body,
        in_specs=[vmem()] * 3,
        out_specs=(vmem(), vmem()),
        out_shape=(
            jax.ShapeDtypeStruct((ROWS, 256), bf16),
            jax.ShapeDtypeStruct((ROWS, 256), bf16),
        ),
        scratch_shapes=[pltpu.VMEM((ROWS, 512), bf16)],
        compiler_params=params(),
        name="pooling",
    )(own, low, high)


NSTEP = 512


def project_body(got, mine, theirs, *refs):
    wa, wp = refs[0:5], refs[5:10]
    keep, send, att, pool = refs[10:]
    y0 = lax.axis_index("y")
    c = lax.axis_index("c")

    @pl.when(pl.program_id(0) == 0)
    def _():
        row = lax.broadcasted_iota(jnp.int32, (128, HEADS * VAL), 0)
        head = lax.broadcasted_iota(jnp.int32, (128, HEADS * VAL), 1) // VAL
        spread = ((row >= 64 + 3 * head) & (row < 67 + 3 * head)).astype(bf16)
        for n, d in enumerate(PLACES):
            slots = [x * NY + (y0 + NY + d) % NY for x in range(NX)]
            logs = [nn(got[slot, :, 128:256], spread) for slot in slots]
            top = jnp.maximum(
                jnp.maximum(logs[0], logs[1]), jnp.maximum(logs[2], logs[3])
            )
            weights = [jnp.exp(v - top) for v in logs]
            total = weights[0] + weights[1] + weights[2] + weights[3]
            acc = jnp.zeros((2 * ROWS, HEADS * VAL), f32)
            for slot, w in zip(slots, weights):
                acc = acc + got[slot, :, 0 : HEADS * VAL].astype(f32) * w
            att[n, :, :] = (acc / total).astype(bf16)
        pool[0:ROWS, :] = jnp.where(c == 0, mine[...], theirs[...])
        pool[ROWS:, :] = jnp.where(c == 0, theirs[...], mine[...])

    total = nn(pool[...], jnp.concatenate([w[...] for w in wp], axis=0))
    for n in range(3):
        total = total + nn(att[n], wa[n][...])
    total = total + nn(att[3], jnp.concatenate([wa[3][...], wa[4][...]], axis=0))
    first, second = total[0:ROWS], total[ROWS:]
    keep[...] = jnp.where(c == 0, first, second)
    send[...] = jnp.where(c == 0, second, first).astype(bf16)


def project(got, mine, theirs, wa, wp):
    whole = lambda *s: pl.BlockSpec(s, lambda k: (0,) * len(s))
    part = lambda n: pl.BlockSpec((n, NSTEP), lambda k: (0, k))
    weights = [*wa, *wp]
    return pl.pallas_call(
        project_body,
        grid=(WIDTH // NSTEP,),
        in_specs=[whole(*got.shape), whole(*mine.shape), whole(*theirs.shape)]
        + [part(w.shape[0]) for w in weights],
        out_specs=(part(ROWS), part(ROWS)),
        out_shape=(
            jax.ShapeDtypeStruct((ROWS, WIDTH), f32),
            jax.ShapeDtypeStruct((ROWS, WIDTH), bf16),
        ),
        scratch_shapes=[
            pltpu.VMEM((NY, 2 * ROWS, HEADS * VAL), bf16),
            pltpu.VMEM((2 * ROWS, 256), bf16),
        ],
        compiler_params=params(dimension_semantics=("arbitrary",)),
        name="project",
    )(got, mine, theirs, *weights)


def across(x):
    return lax.ppermute(x, "c", [(0, 1), (1, 0)])


def shifted(x, axis, places):
    count = lax.axis_size(axis)
    return lax.ppermute(x, axis, [(i, (i + places) % count) for i in range(count)])


def order_body(a, b, c, d, q_out):
    y = lax.axis_index("y")
    for k, ref in enumerate((a, b, c, d)):
        at = pl.multiple_of(((y + NY - k) % NY) * ROWS, ROWS)
        q_out[pl.ds(at, ROWS), :] = ref[...]


def in_order(pieces):
    return pl.pallas_call(
        order_body,
        in_specs=[vmem()] * NY,
        out_specs=vmem(),
        out_shape=jax.ShapeDtypeStruct((NY * ROWS, QR), bf16),
        compiler_params=params(),
        name="order",
    )(*pieces)


def shards(
    tokens,
    norm_gain,
    query_down_weight,
    query_latent_norm_gain,
    key_value_down_weight,
    key_value_latent_gain,
    w_rope_key,
    w_pool_in,
    query_up_weight,
    key_value_up_weight,
    query_gain,
    key_gain,
    w_pool_mix,
    pool_scale,
    w_out_attn,
    w_out_pool,
):
    wqt = query_up_weight.T
    wkvt = key_value_up_weight.T

    q_all, kv_all, pool_in = latents(
        tokens,
        norm_gain,
        query_down_weight,
        query_latent_norm_gain,
        key_value_down_weight,
        key_value_latent_gain,
        w_rope_key,
        w_pool_in,
    )
    pieces = [q_all] + [shifted(q_all, "y", k) for k in range(1, NY)]
    kv_own = lax.all_to_all(kv_all, "z", 0, 0, tiled=True).reshape(NZ * ROWS, KR + 128)

    count = NZ * NX * NY * 2
    every = ("z", "x", "y", "c")
    low = lax.ppermute(
        pool_in[ROWS - 8 :], every, [(i, i + 1) for i in range(count - 1)]
    )
    high = lax.ppermute(pool_in[:8], every, [(i + 1, i) for i in range(count - 1)])
    pool_mine, pool_send = pooling(pool_in, low, high)
    pool_theirs = across(pool_send)

    folded = jnp.dot(
        w_pool_mix[0],
        (pool_scale.astype(f32)[:, None] * w_out_pool.astype(f32)).astype(bf16),
        preferred_element_type=f32,
    ).astype(bf16)
    wa1 = shifted(w_out_attn, "y", 1)
    wa3 = shifted(w_out_attn, "y", NY - 1)
    wp1 = shifted(folded, "y", 1)
    wp3 = shifted(folded, "y", NY - 1)
    half = HEADS * VAL // 2
    wa2a = shifted(wa1[:half], "y", 1)
    wa2b = shifted(wa3[half:], "y", NY - 1)
    wp2a = shifted(wp1[:32], "y", 1)
    wp2b = shifted(wp3[32:], "y", NY - 1)

    kv = lax.all_to_all(
        jnp.broadcast_to(kv_own[None], (NY, *kv_own.shape)), "y", 0, 0, tiled=True
    )
    q_side = in_order(pieces)
    q_own = [q_side] + [shifted(q_side, "x", k) for k in range(1, NX)]
    tag = q_own[1][:8, :128] + q_own[2][:8, :128] + q_own[3][:8, :128]
    q_twin = [across(q) for q in q_own]
    kv_twin = across(kv)
    qt = queries(q_own, q_twin, wqt, query_gain, query_tables())
    pair = keys_values((tag,), kv, kv_twin, wkvt, key_gain, key_tables())
    message, *logs = attend(*pair, qt)

    got = lax.all_to_all(message, ("x", "y"), 0, 0, tiled=True)
    logs = [logs[0]] + [shifted(logs[k], "x", k) for k in range(1, NX)]
    row_logsum = logsums(logs)
    keep, send = project(
        got,
        pool_mine,
        pool_theirs,
        (w_out_attn, wa1, wa3, wa2a, wa2b),
        (folded, wp1, wp3, wp2a, wp2b),
    )
    mixed = (keep + across(send).astype(f32)).astype(bf16)
    return mixed, row_logsum


def solution(mesh):
    fine = Mesh(mesh.devices.reshape(NZ, NX, NY, 2), ("z", "x", "y", "c"))
    tp = ("y", "c")
    placed = (
        P(("z", "x", "y", "c"), None),
        P(),
        P(),
        P(),
        P(),
        P(),
        P(),
        P(),
        P(None, tp),
        P(None, tp),
        P(),
        P(),
        P(tp, None, None),
        P(tp),
        P(tp, None),
        P(tp, None),
    )

    return jax.shard_map(
        shards,
        mesh=fine,
        in_specs=placed,
        out_specs=(P(("z", "x", "y", "c"), None), P(tp, ("z", "x"))),
        check_vma=False,
    )
```

time: 157 us -> 158 us (level)
  local copies, waits for them, and re-layouts: 25.8 us -> 6.98 us
  waiting for transfers between devices: 9.86 us -> 24.2 us
  blocking collectives: 50.1 us -> 37.5 us
  Pallas kernels: 26.7 us -> 36.7 us
  starting transfers between devices: 38.3 us -> 46.8 us
    unnamed x73 -> x65, local copies, waits for them, and re-layouts: 23.2 us -> 5.08 us
    ppermute x6 -> x17, starting transfers between devices: 9.93 us -> 25 us  [shifted(): lax.ppermute(x, axis, [(i, (i + places) % count) for i in range(count)])]
    all_to_all x2 -> x1, blocking collectives: 30.4 us -> 17.6 us  [shards(): lax.all_to_all(jnp.broadcast_to(kv_own[None], (NY, *kv_own.shape)), 'y',...]
    ppermute x6 -> x17, waiting for transfers between devices: 4.67 us -> 16.9 us  [shifted(): lax.ppermute(x, axis, [(i, (i + places) % count) for i in range(count)])]
    pallas_call x7, Pallas kernels: 24.8 us -> 32.5 us  [the longest x1 16.5 us: attend(): pl.pallas_call(attend_body, in_specs=[vmem()] * 3, out_specs=(vmem(),) *...]
    all_to_all x2 -> x1, starting transfers between devices: 8.51 us -> 4.68 us  [shards(): got = lax.all_to_all(message, ('x', 'y'), 0, 0, tiled=True)]
    ppermute x1, starting transfers between devices: 6.03 us -> 2.29 us  [shards(): lax.ppermute(pool_in[ROWS - 8:], every, [(i, i + 1) for i in range(count...]
    all_to_all x2 -> x1, waiting for transfers between devices: 2.38 us -> 0.01 us  [shards(): got = lax.all_to_all(message, ('x', 'y'), 0, 0, tiled=True)]
  transfers between devices with their start and end apart: 17 -> 27, of which waited for: 5 -> 13; matrix products, arithmetic and copies ran while one was open for 3% -> 2% of each run, Pallas kernels for 2% -> 17%
where the time goes in v2:
time: 158 us; the launch traced here: 156 us
  starting transfers between devices  46.8 us (30%)
  blocking collectives  37.5 us (24%)
  Pallas kernels  36.7 us (23%)
  waiting for transfers between devices  24.2 us (15%)
  local copies, waits for them, and re-layouts  6.98 us (4%)
  other arithmetic  2.29 us (1%)
    ppermute x17, starting transfers between devices, shifted(): lax.ppermute(x, axis, [(i, (i + places) % count) for i in range(count)])  25 us
    all_to_all x1, blocking collectives, shards(): lax.all_to_all(kv_all, 'z', 0, 0, tiled=True).reshape(NZ * ROWS, KR + 128)  20 us
    all_to_all x1, blocking collectives, shards(): lax.all_to_all(jnp.broadcast_to(kv_own[None], (NY, *kv_own.shape)), 'y',...  17.6 us
    ppermute x17, waiting for transfers between devices, shifted(): lax.ppermute(x, axis, [(i, (i + places) % count) for i in range(count)])  16.9 us
    pallas_call x1, Pallas kernels, attend(): pl.pallas_call(attend_body, in_specs=[vmem()] * 3, out_specs=(vmem(),) *...  16.5 us
    ppermute x7, starting transfers between devices, across(): return lax.ppermute(x, 'c', [(0, 1), (1, 0)])  12.7 us
    pallas_call x1, Pallas kernels, project(): pl.pallas_call(project_body, grid=(WIDTH // NSTEP,), in_specs=[whole(*got...  5.58 us
    unnamed x65, local copies, waits for them, and re-layouts  5.08 us
  transfers between devices with their start and end apart: 27, of which 13 were waited for; matrix products, arithmetic and copies ran while one was open for 2% of the time, Pallas kernels for 17%

profile of v2, /device:TPU:1, one launch (start us, length us, event | category | flops | bytes accessed | tf_op | source)
XLA Modules:
  0.0 155.7 jit_solution(10397046666681453850)
XLA Ops:
  0.6 4.2 %latents.1 = (bf16[48,512]{1,0:T(8,128)(2,1)}, bf16[8,48,384]{2,1,0:T(8,128)(2,1)}, bf16[48,512]{1,0:T(8,128)(2,1)}) custom-call(bf16[48,2048]{1,0:T(8,128)(2,1)} %tok.1, bf16[2048]{0:T(1024)(128)(2,1)} %gain.2, bf16[2048,512]{1,0:T(8,128)(2,1)} %qdw.1, bf16[512]{0:T(512)(128)(2,1)} %qg.1, bf16[2048,256]{1,0:T(8,128)(2,1)} %kdw.1, bf16[256]{0:T(256)(128)(2,1)} %kg.1, ...), custom_call_target="tpu_custom_call" | custom-call | tf_op jit(solution)/shard_map/latents/pallas_call | solution.py:128
  4.9 20.0 %all_to_all.15 = bf16[8,48,384]{2,1,0:T(8,128)(2,1)S(1)} all-to-all(bf16[8,48,384]{2,1,0:T(8,128)(2,1)} %get-tuple-element.17), channel_id=1, replica_groups=mesh['z'=8,'x'=4,'y'=4,'c'=2] {'z'}, dimensions={0} | all-to-all | bytes 589824 | tf_op jit(solution)/shard_map/all_to_all | solution.py:591
  25.0 17.6 %all_to_all.16.refs_1_ = bf16[4,384,384]{2,1,0:T(8,128)(2,1)S(1)} all-to-all(bf16[4,384,384]{2,1,0:T(8,128)(2,1)S(1)} %broadcast_in_dim.9), channel_id=1, replica_groups=mesh['z'=8,'x'=4,'y'=4,'c'=2] {'y'}, dimensions={0} | all-to-all | bytes 2359296 | tf_op jit(solution)/shard_map/all_to_all | solution.py:617
  42.5 4.0 %collective-permute-start.6 = (bf16[4,384,384]{2,1,0:T(8,128)(2,1)S(1)}, bf16[4,384,384]{2,1,0:T(8,128)(2,1)}, u32[]{:S(2)}, u32[]{:S(2)}) collective-permute-start(bf16[4,384,384]{2,1,0:T(8,128)(2,1)S(1)} %all_to_all.16.refs_1_), channel_id=1, source_target_pairs={{0,1},{1,0},{2,3},{3,2},{4,5},{5,4},{6,7},{7,6},{8,9},{9,8},{10,11... | collective-permute-start | bytes 3538952 | tf_op jit(solution)/shard_map/ppermute | solution.py:533
  46.8 1.8 %collective-permute-start.1 = (bf16[48,512]{1,0:T(8,128)(2,1)S(1)}, bf16[48,512]{1,0:T(8,128)(2,1)S(1)}, u32[]{:S(2)}, u32[]{:S(2)}) collective-permute-start(bf16[48,512]{1,0:T(8,128)(2,1)S(1)} %copy-done.21), channel_id=1, source_target_pairs={{0,4},{2,6},{4,0},{6,2},{1,5},{3,7},{5,1},{7,3},{8,12},{10,14},{12... | collective-permute-start | bytes 147464 | tf_op jit(solution)/shard_map/ppermute | solution.py:538
  48.6 0.6 collective-permute-start.2
  49.2 1.5 collective-permute-done.b
  50.7 0.7 collective-permute-done.1.c
  51.4 0.9 collective-permute-done.2.d
  52.3 0.6 copy-done.24
  52.9 1.6 %order.1.own0 = bf16[192,512]{1,0:T(8,128)(2,1)} custom-call(bf16[48,512]{1,0:T(8,128)(2,1)} %get-tuple-element.16.a, bf16[48,512]{1,0:T(8,128)(2,1)} %copy-done.22, bf16[48,512]{1,0:T(8,128)(2,1)} %copy-done.23, bf16[48,512]{1,0:T(8,128)(2,1)} %copy-done.24), custom_call_target="tpu_custom_call" | custom-call | tf_op jit(solution)/shard_map/order/pallas_call | solution.py:549
  54.5 1.2 collective-permute-start.3
  55.7 1.5 collective-permute-start.5
  57.2 1.5 collective-permute-start.4
  58.7 2.1 %collective-permute-start.7 = (bf16[192,512]{1,0:T(8,128)(2,1)}, bf16[192,512]{1,0:T(8,128)(2,1)S(1)}, u32[]{:S(2)}, u32[]{:S(2)}) collective-permute-start(bf16[192,512]{1,0:T(8,128)(2,1)} %order.1.own0), channel_id=1, source_target_pairs={{0,1},{1,0},{2,3},{3,2},{4,5},{5,4},{6,7},{7,6},{8,9},{9,8},{10,11... | collective-permute-start | bytes 589832 | tf_op jit(solution)/shard_map/ppermute | solution.py:533
  61.1 2.9 %collective-permute-start.8 = (bf16[192,512]{1,0:T(8,128)(2,1)S(1)}, bf16[192,512]{1,0:T(8,128)(2,1)S(1)}, u32[]{:S(2)}, u32[]{:S(2)}) collective-permute-start(bf16[192,512]{1,0:T(8,128)(2,1)S(1)} %collective-permute-done.3.own1), channel_id=1, source_target_pairs={{0,1},{1,0},{2,3},{3,2},{4,5},{5,4},{6,7},{7,6},{8,9},{9,8},{10,11... | collective-permute-start | bytes 589832 | tf_op jit(solution)/shard_map/ppermute | solution.py:533
  64.0 1.0 collective-permute-start.14
  65.0 1.3 collective-permute-done.4.own2
  66.3 1.4 collective-permute-start.15
  67.7 0.8 copy.20
  68.5 3.2 %collective-permute-start.9 = (bf16[192,512]{1,0:T(8,128)(2,1)S(1)}, bf16[192,512]{1,0:T(8,128)(2,1)S(1)}, u32[]{:S(2)}, u32[]{:S(2)}) collective-permute-start(bf16[192,512]{1,0:T(8,128)(2,1)S(1)} %collective-permute-done.4.own2), channel_id=1, source_target_pairs={{0,1},{1,0},{2,3},{3,2},{4,5},{5,4},{6,7},{7,6},{8,9},{9,8},{10,11... | collective-permute-start | bytes 589832 | tf_op jit(solution)/shard_map/ppermute | solution.py:533
  73.8 2.5 %queries.1.qt = bf16[3,128,1536]{2,1,0:T(8,128)(2,1)S(1)} custom-call(bf16[192,512]{1,0:T(8,128)(2,1)} %order.1.own0, bf16[192,512]{1,0:T(8,128)(2,1)} %copy-done.11, bf16[192,512]{1,0:T(8,128)(2,1)} %copy-done.13, bf16[192,512]{1,0:T(8,128)(2,1)} %copy-done.12, bf16[192,512]{1,0:T(8,128)(2,1)} %copy-done.14, bf16[192,512]{1,0:T(8,128)(2,1)} %copy-done.15, ...), custom_call_target="tpu_custom_call" | custom-call | tf_op jit(solution)/shard_map/queries/pallas_call | solution.py:222
  76.3 3.4 %keys.1 = (bf16[3,3072,128]{2,1,0:T(8,128)(2,1)S(1)}, bf16[3,80,3072]{2,1,0:T(8,128)(2,1)S(1)}) custom-call(bf16[8,128]{1,0:T(8,128)(2,1)} %slice_add_fusion.refs_0_, bf16[4,384,384]{2,1,0:T(8,128)(2,1)} %copy-done.2, bf16[4,384,384]{2,1,0:T(8,128)(2,1)} %collective-permute-done.6.refs_2_, bf16[384,256]{1,0:T(8,128)(2,1)} %bitcast.10, bf16[96]{0:T(256)(128)(2,1)} %refs_4_.1, ...), custom_call_target="tpu_custom_call" | custom-call | tf_op jit(solution)/shard_map/keys/pallas_call | solution.py:268
  79.7 16.5 %attend.1 = (bf16[16,96,256]{2,1,0:T(8,128)(2,1)}, f32[8,384]{1,0:T(8,128)S(1)}, f32[8,384]{1,0:T(8,128)S(1)}, f32[8,384]{1,0:T(8,128)S(1)}, f32[8,384]{1,0:T(8,128)S(1)}) custom-call(bf16[3,3072,128]{2,1,0:T(8,128)(2,1)S(1)} %get-tuple-element.18.kbuf, bf16[3,80,3072]{2,1,0:T(8,128)(2,1)S(1)} %get-tuple-element.19.vbuf, bf16[3,128,1536]{2,1,0:T(8,128)(2,1)S(1)} %queries.1.qt), custom_call_target="tpu_custom_call" | custom-call | tf_op jit(solution)/shard_map/attend/pallas_call | solution.py:378
  96.2 0.6 copy-done.1
  96.7 4.7 %all-to-all-start.2 = ((bf16[16,96,256]{2,1,0:T(8,128)(2,1)}), bf16[16,96,256]{2,1,0:T(8,128)(2,1)S(1)}, u32[]{:S(2)}, u32[]{:S(2)}) async-start(bf16[16,96,256]{2,1,0:T(8,128)(2,1)} %get-tuple-element.20), calls=%async_computation.2 | async-start | bytes 1572864 | tf_op jit(solution)/shard_map/all_to_all | solution.py:629
  101.8 1.4 collective-permute-start.18
  103.2 1.3 collective-permute-start.19
  104.8 1.0 slice.40
  105.8 2.6 %collective-permute-start.17 = (bf16[96,2048]{1,0:T(8,128)(2,1)S(1)}, bf16[96,2048]{1,0:T(8,128)(2,1)S(1)}, u32[]{:S(2)}, u32[]{:S(2)}) collective-permute-start(bf16[96,2048]{1,0:T(8,128)(2,1)S(1)} %slice.40), channel_id=1, source_target_pairs={{0,6},{2,0},{4,2},{6,4},{1,7},{3,1},{5,3},{7,5},{8,14},{10,8},{12,... | collective-permute-start | bytes 1179656 | tf_op jit(solution)/shard_map/ppermute | solution.py:538
  108.4 10.6 %collective-permute-done.18.refs_6_ = bf16[64,2048]{1,0:T(8,128)(2,1)S(1)} collective-permute-done((bf16[64,2048]{1,0:T(8,128)(2,1)S(1)}, bf16[64,2048]{1,0:T(8,128)(2,1)S(1)}, u32[]{:S(2)}, u32[]{:S(2)}) %collective-permute-start.18) | collective-permute-done | bytes 262176 | tf_op jit(solution)/shard_map/ppermute | solution.py:538
  119.1 2.9 %collective-permute-start.21 = (bf16[32,2048]{1,0:T(8,128)(2,1)S(1)}, bf16[32,2048]{1,0:T(8,128)(2,1)S(1)}, u32[]{:S(2)}, u32[]{:S(2)}) collective-permute-start(bf16[32,2048]{1,0:T(8,128)(2,1)S(1)} %slice.42), channel_id=1, source_target_pairs={{0,6},{2,0},{4,2},{6,4},{1,7},{3,1},{5,3},{7,5},{8,14},{10,8},{12,... | collective-permute-start | bytes 393224 | tf_op jit(solution)/shard_map/ppermute | solution.py:538
  122.1 0.7 fusion.3
  122.8 2.3 %collective-permute-start.11 = (bf16[8,512]{1,0:T(8,128)(2,1)S(1)}, bf16[8,512]{1,0:T(8,128)(2,1)S(1)}, u32[]{:S(2)}, u32[]{:S(2)}) collective-permute-start(bf16[8,512]{1,0:T(8,128)(2,1)S(1)} %get-tuple-element.31), channel_id=1, source_target_pairs={{0,1},{1,2},{2,3},{3,4},{4,5},{5,6},{6,7},{7,8},{8,9},{9,10},{10,1... | collective-permute-start | bytes 24584 | tf_op jit(solution)/shard_map/ppermute | solution.py:595
  125.1 1.6 %collective-permute-done.11.low = bf16[8,512]{1,0:T(8,128)(2,1)S(1)} collective-permute-done((bf16[8,512]{1,0:T(8,128)(2,1)S(1)}, bf16[8,512]{1,0:T(8,128)(2,1)S(1)}, u32[]{:S(2)}, u32[]{:S(2)}) %collective-permute-start.11) | collective-permute-done | bytes 8224 | tf_op jit(solution)/shard_map/ppermute | solution.py:595
  126.7 2.0 %collective-permute-start.12 = (bf16[8,512]{1,0:T(8,128)(2,1)S(1)}, bf16[8,512]{1,0:T(8,128)(2,1)S(1)}, u32[]{:S(2)}, u32[]{:S(2)}) collective-permute-start(bf16[8,512]{1,0:T(8,128)(2,1)S(1)} %get-tuple-element.30), channel_id=1, source_target_pairs={{1,0},{2,1},{3,2},{4,3},{5,4},{6,5},{7,6},{8,7},{9,8},{10,9},{11,1... | collective-permute-start | bytes 24584 | tf_op jit(solution)/shard_map/ppermute | solution.py:598
  128.8 3.7 %collective-permute-done.12.high = bf16[8,512]{1,0:T(8,128)(2,1)S(1)} collective-permute-done((bf16[8,512]{1,0:T(8,128)(2,1)S(1)}, bf16[8,512]{1,0:T(8,128)(2,1)S(1)}, u32[]{:S(2)}, u32[]{:S(2)}) %collective-permute-start.12) | collective-permute-done | bytes 8224 | tf_op jit(solution)/shard_map/ppermute | solution.py:598
  133.0 1.7 %pooling.1 = (bf16[48,256]{1,0:T(8,128)(2,1)}, bf16[48,256]{1,0:T(8,128)(2,1)}) custom-call(bf16[48,512]{1,0:T(8,128)(2,1)} %get-tuple-element.21.own, bf16[8,512]{1,0:T(8,128)(2,1)} %copy-done.29, bf16[8,512]{1,0:T(8,128)(2,1)} %copy-done.30), custom_call_target="tpu_custom_call" | custom-call | tf_op jit(solution)/shard_map/pooling/pallas_call | solution.py:457
  134.7 1.4 collective-permute-done.13.theirs
  137.3 5.6 %project.1 = (f32[48,2048]{1,0:T(8,128)}, bf16[48,2048]{1,0:T(8,128)(2,1)}) custom-call(bf16[16,96,256]{2,1,0:T(8,128)(2,1)} %copy-done.3, bf16[48,256]{1,0:T(8,128)(2,1)} %get-tuple-element.22.mine, bf16[48,256]{1,0:T(8,128)(2,1)} %copy-done.25, bf16[192,2048]{1,0:T(8,128)(2,1)} %refs_0_.1, bf16[192,2048]{1,0:T(8,128)(2,1)} %copy-done.4, ...), custom_call_target="tpu_custom_call" | custom-call | tf_op jit(solution)/shard_map/project/pallas_call | solution.py:513
  143.2 3.7 %collective-permute-start.23 = (f32[8,384]{1,0:T(8,128)S(1)}, f32[8,384]{1,0:T(8,128)S(1)}, u32[]{:S(2)}, u32[]{:S(2)}) collective-permute-start(f32[8,384]{1,0:T(8,128)S(1)} %get-tuple-element.27), channel_id=1, source_target_pairs={{0,8},{8,16},{16,24},{24,0},{1,9},{9,17},{17,25},{25,1},{2,10},{10... | collective-permute-start | bytes 36872 | tf_op jit(solution)/shard_map/ppermute | solution.py:538
  146.9 2.3 %collective-permute-start.24 = (f32[8,384]{1,0:T(8,128)S(1)}, f32[8,384]{1,0:T(8,128)S(1)}, u32[]{:S(2)}, u32[]{:S(2)}) collective-permute-start(f32[8,384]{1,0:T(8,128)S(1)} %get-tuple-element.28), channel_id=1, source_target_pairs={{0,16},{8,24},{16,0},{24,8},{1,17},{9,25},{17,1},{25,9},{2,18},{10... | collective-permute-start | bytes 36872 | tf_op jit(solution)/shard_map/ppermute | solution.py:538
  149.1 1.2 collective-permute-start.25
  150.3 0.6 collective-permute-done.24.c
  151.0 1.0 collective-permute-done.25.d
  152.0 0.6 copy-done.28
  152.6 1.4 logsums.1
  154.0 1.7 %add_convert_fusion = bf16[48,2048]{1,0:T(8,128)(2,1)} fusion(f32[48,2048]{1,0:T(8,128)} %get-tuple-element.24, bf16[48,2048]{1,0:T(8,128)(2,1)S(1)} %collective-permute-done.22), kind=kLoop, calls=%fused_computation.3 | loop fusion | flops 294912 | bytes 786432 | tf_op jit(solution)/shard_map/convert_element_type | solution.py:639
  (91 shorter events, 5.5 us)
Async XLA Ops:
  0.6 100.8 %copy-start = (bf16[1,64,64]{2,1,0:T(8,128)(2,1)S(1)}, bf16[1,64,64]{2,1,0:T(8,128)(2,1)}, u32[]{:S(2)}) copy-start(bf16[1,64,64]{2,1,0:T(8,128)(2,1)} %param.30) | copy-start | bytes 24580
  24.9 21.6 %copy-start.21 = (bf16[48,512]{1,0:T(8,128)(2,1)S(1)}, bf16[48,512]{1,0:T(8,128)(2,1)}, u32[]{:S(2)}) copy-start(bf16[48,512]{1,0:T(8,128)(2,1)} %get-tuple-element.16.a) | copy-start | bytes 147460
  24.9 42.7 %copy-start.18 = (bf16[256,384]{1,0:T(8,128)(2,1)S(1)}, bf16[256,384]{1,0:T(8,128)(2,1)}, u32[]{:S(2)}) copy-start(bf16[256,384]{1,0:T(8,128)(2,1)} %param.27) | copy-start | bytes 589828
  25.0 43.5 %copy-start.31 = (bf16[64]{0:T(256)(128)(2,1)S(1)}, bf16[64]{0:T(256)(128)(2,1)}, u32[]{:S(2)}) copy-start(bf16[64]{0:T(256)(128)(2,1)} %param.31) | copy-start | bytes 388
  42.5 33.8 %copy-start.2 = (bf16[4,384,384]{2,1,0:T(8,128)(2,1)}, bf16[4,384,384]{2,1,0:T(8,128)(2,1)S(1)}, u32[]{:S(2)}) copy-start(bf16[4,384,384]{2,1,0:T(8,128)(2,1)S(1)} %all_to_all.16.refs_1_) | copy-start | bytes 3538948
  42.5 33.8 %collective-permute-start.6 = (bf16[4,384,384]{2,1,0:T(8,128)(2,1)S(1)}, bf16[4,384,384]{2,1,0:T(8,128)(2,1)}, u32[]{:S(2)}, u32[]{:S(2)}) collective-permute-start(bf16[4,384,384]{2,1,0:T(8,128)(2,1)S(1)} %all_to_all.16.refs_1_), channel_id=1, source_target_pairs={{0,1},{1,0},{2,3},{3,2},{4,5},{5,4},{6,7},{7,6},{8,9},{9,8},{10,11... | collective-permute-start | bytes 3538952 | tf_op jit(solution)/shard_map/ppermute | solution.py:533
  46.5 4.2 %collective-permute-start = (bf16[48,512]{1,0:T(8,128)(2,1)S(1)}, bf16[48,512]{1,0:T(8,128)(2,1)S(1)}, u32[]{:S(2)}, u32[]{:S(2)}) collective-permute-start(bf16[48,512]{1,0:T(8,128)(2,1)S(1)} %copy-done.21), channel_id=1, source_target_pairs={{0,2},{2,4},{4,6},{6,0},{1,3},{3,5},{5,7},{7,1},{8,10},{10,12},{12... | collective-permute-start | bytes 147464 | tf_op jit(solution)/shard_map/ppermute | solution.py:538
  46.8 4.5 %collective-permute-start.1 = (bf16[48,512]{1,0:T(8,128)(2,1)S(1)}, bf16[48,512]{1,0:T(8,128)(2,1)S(1)}, u32[]{:S(2)}, u32[]{:S(2)}) collective-permute-start(bf16[48,512]{1,0:T(8,128)(2,1)S(1)} %copy-done.21), channel_id=1, source_target_pairs={{0,4},{2,6},{4,0},{6,2},{1,5},{3,7},{5,1},{7,3},{8,12},{10,14},{12... | collective-permute-start | bytes 147464 | tf_op jit(solution)/shard_map/ppermute | solution.py:538
  48.6 3.7 %collective-permute-start.2 = (bf16[48,512]{1,0:T(8,128)(2,1)S(1)}, bf16[48,512]{1,0:T(8,128)(2,1)S(1)}, u32[]{:S(2)}, u32[]{:S(2)}) collective-permute-start(bf16[48,512]{1,0:T(8,128)(2,1)S(1)} %copy-done.21), channel_id=1, source_target_pairs={{0,6},{2,0},{4,2},{6,4},{1,7},{3,1},{5,3},{7,5},{8,14},{10,8},{12,... | collective-permute-start | bytes 147464 | tf_op jit(solution)/shard_map/ppermute | solution.py:538
  50.7 1.6 %copy-start.22 = (bf16[48,512]{1,0:T(8,128)(2,1)}, bf16[48,512]{1,0:T(8,128)(2,1)S(1)}, u32[]{:S(2)}) copy-start(bf16[48,512]{1,0:T(8,128)(2,1)S(1)} %collective-permute-done.b) | copy-start | bytes 147460
  51.4 1.0 copy-start.23
  54.5 6.6 %collective-permute-start.3 = (bf16[192,512]{1,0:T(8,128)(2,1)}, bf16[192,512]{1,0:T(8,128)(2,1)S(1)}, u32[]{:S(2)}, u32[]{:S(2)}) collective-permute-start(bf16[192,512]{1,0:T(8,128)(2,1)} %order.1.own0), channel_id=1, source_target_pairs={{0,8},{8,16},{16,24},{24,0},{1,9},{9,17},{17,25},{25,1},{2,10},{10... | collective-permute-start | bytes 589832 | tf_op jit(solution)/shard_map/ppermute | solution.py:538
  55.7 8.3 %collective-permute-start.5 = (bf16[192,512]{1,0:T(8,128)(2,1)}, bf16[192,512]{1,0:T(8,128)(2,1)S(1)}, u32[]{:S(2)}, u32[]{:S(2)}) collective-permute-start(bf16[192,512]{1,0:T(8,128)(2,1)} %order.1.own0), channel_id=1, source_target_pairs={{0,24},{8,0},{16,8},{24,16},{1,25},{9,1},{17,9},{25,17},{2,26},{10... | collective-permute-start | bytes 589832 | tf_op jit(solution)/shard_map/ppermute | solution.py:538
  57.2 9.1 %collective-permute-start.4 = (bf16[192,512]{1,0:T(8,128)(2,1)}, bf16[192,512]{1,0:T(8,128)(2,1)S(1)}, u32[]{:S(2)}, u32[]{:S(2)}) collective-permute-start(bf16[192,512]{1,0:T(8,128)(2,1)} %order.1.own0), channel_id=1, source_target_pairs={{0,16},{8,24},{16,0},{24,8},{1,17},{9,25},{17,1},{25,9},{2,18},{10... | collective-permute-start | bytes 589832 | tf_op jit(solution)/shard_map/ppermute | solution.py:538
  58.7 9.8 %collective-permute-start.7 = (bf16[192,512]{1,0:T(8,128)(2,1)}, bf16[192,512]{1,0:T(8,128)(2,1)S(1)}, u32[]{:S(2)}, u32[]{:S(2)}) collective-permute-start(bf16[192,512]{1,0:T(8,128)(2,1)} %order.1.own0), channel_id=1, source_target_pairs={{0,1},{1,0},{2,3},{3,2},{4,5},{5,4},{6,7},{7,6},{8,9},{9,8},{10,11... | collective-permute-start | bytes 589832 | tf_op jit(solution)/shard_map/ppermute | solution.py:533
  61.1 12.0 %copy-start.11 = (bf16[192,512]{1,0:T(8,128)(2,1)}, bf16[192,512]{1,0:T(8,128)(2,1)S(1)}, u32[]{:S(2)}) copy-start(bf16[192,512]{1,0:T(8,128)(2,1)S(1)} %collective-permute-done.3.own1) | copy-start | bytes 589828
  61.1 10.6 %collective-permute-start.8 = (bf16[192,512]{1,0:T(8,128)(2,1)S(1)}, bf16[192,512]{1,0:T(8,128)(2,1)S(1)}, u32[]{:S(2)}, u32[]{:S(2)}) collective-permute-start(bf16[192,512]{1,0:T(8,128)(2,1)S(1)} %collective-permute-done.3.own1), channel_id=1, source_target_pairs={{0,1},{1,0},{2,3},{3,2},{4,5},{5,4},{6,7},{7,6},{8,9},{9,8},{10,11... | collective-permute-start | bytes 589832 | tf_op jit(solution)/shard_map/ppermute | solution.py:533
  64.0 9.1 %copy-start.12 = (bf16[192,512]{1,0:T(8,128)(2,1)}, bf16[192,512]{1,0:T(8,128)(2,1)S(1)}, u32[]{:S(2)}) copy-start(bf16[192,512]{1,0:T(8,128)(2,1)S(1)} %collective-permute-done.5.own3) | copy-start | bytes 589828
  64.0 40.5 %collective-permute-start.14 = (bf16[192,2048]{1,0:T(8,128)(2,1)}, bf16[192,2048]{1,0:T(8,128)(2,1)S(1)}, u32[]{:S(2)}, u32[]{:S(2)}) collective-permute-start(bf16[192,2048]{1,0:T(8,128)(2,1)} %refs_0_.1), channel_id=1, source_target_pairs={{0,2},{2,4},{4,6},{6,0},{1,3},{3,5},{5,7},{7,1},{8,10},{10,12},{12... | collective-permute-start | bytes 2359304 | tf_op jit(solution)/shard_map/ppermute | solution.py:538
  66.3 6.8 %copy-start.13 = (bf16[192,512]{1,0:T(8,128)(2,1)}, bf16[192,512]{1,0:T(8,128)(2,1)S(1)}, u32[]{:S(2)}) copy-start(bf16[192,512]{1,0:T(8,128)(2,1)S(1)} %collective-permute-done.4.own2) | copy-start | bytes 589828
  66.3 38.5 %collective-permute-start.15 = (bf16[192,2048]{1,0:T(8,128)(2,1)}, bf16[192,2048]{1,0:T(8,128)(2,1)}, u32[]{:S(2)}, u32[]{:S(2)}) collective-permute-start(bf16[192,2048]{1,0:T(8,128)(2,1)} %refs_0_.1), channel_id=1, source_target_pairs={{0,6},{2,0},{4,2},{6,4},{1,7},{3,1},{5,3},{7,5},{8,14},{10,8},{12,... | collective-permute-start | bytes 2359304 | tf_op jit(solution)/shard_map/ppermute | solution.py:538
  68.5 4.6 %copy-start.14 = (bf16[192,512]{1,0:T(8,128)(2,1)}, bf16[192,512]{1,0:T(8,128)(2,1)S(1)}, u32[]{:S(2)}) copy-start(bf16[192,512]{1,0:T(8,128)(2,1)S(1)} %collective-permute-done.7.two0) | copy-start | bytes 589828
  68.5 4.2 %collective-permute-start.9 = (bf16[192,512]{1,0:T(8,128)(2,1)S(1)}, bf16[192,512]{1,0:T(8,128)(2,1)S(1)}, u32[]{:S(2)}, u32[]{:S(2)}) collective-permute-start(bf16[192,512]{1,0:T(8,128)(2,1)S(1)} %collective-permute-done.4.own2), channel_id=1, source_target_pairs={{0,1},{1,0},{2,3},{3,2},{4,5},{5,4},{6,7},{7,6},{8,9},{9,8},{10,11... | collective-permute-start | bytes 589832 | tf_op jit(solution)/shard_map/ppermute | solution.py:533
  71.7 1.5 copy-start.15
  71.7 1.4 collective-permute-start.10
  96.7 4.7 %copy-start.10 = (bf16[64,2048]{1,0:T(8,128)(2,1)S(1)}, bf16[64,2048]{1,0:T(8,128)(2,1)}, u32[]{:S(2)}) copy-start(bf16[64,2048]{1,0:T(8,128)(2,1)} %param.33) | copy-start | bytes 786436
  96.7 39.4 %all-to-all-start.2 = ((bf16[16,96,256]{2,1,0:T(8,128)(2,1)}), bf16[16,96,256]{2,1,0:T(8,128)(2,1)S(1)}, u32[]{:S(2)}, u32[]{:S(2)}) async-start(bf16[16,96,256]{2,1,0:T(8,128)(2,1)} %get-tuple-element.20), calls=%async_computation.2 | async-start | bytes 1572864 | tf_op jit(solution)/shard_map/all_to_all | solution.py:629
  101.7 34.4 %copy-start.5 = (bf16[64,2048]{1,0:T(8,128)(2,1)}, bf16[64,2048]{1,0:T(8,128)(2,1)S(1)}, u32[]{:S(2)}) copy-start(bf16[64,2048]{1,0:T(8,128)(2,1)S(1)} %fusion.refs_5_) | copy-start | bytes 786436
  101.8 17.2 %collective-permute-start.18 = (bf16[64,2048]{1,0:T(8,128)(2,1)S(1)}, bf16[64,2048]{1,0:T(8,128)(2,1)S(1)}, u32[]{:S(2)}, u32[]{:S(2)}) collective-permute-start(bf16[64,2048]{1,0:T(8,128)(2,1)S(1)} %fusion.refs_5_), channel_id=1, source_target_pairs={{0,2},{2,4},{4,6},{6,0},{1,3},{3,5},{5,7},{7,1},{8,10},{10,12},{12... | collective-permute-start | bytes 786440 | tf_op jit(solution)/shard_map/ppermute | solution.py:538
  103.2 15.9 %collective-permute-start.19 = (bf16[64,2048]{1,0:T(8,128)(2,1)S(1)}, bf16[64,2048]{1,0:T(8,128)(2,1)S(1)}, u32[]{:S(2)}, u32[]{:S(2)}) collective-permute-start(bf16[64,2048]{1,0:T(8,128)(2,1)S(1)} %fusion.refs_5_), channel_id=1, source_target_pairs={{0,6},{2,0},{4,2},{6,4},{1,7},{3,1},{5,3},{7,5},{8,14},{10,8},{12,... | collective-permute-start | bytes 786440 | tf_op jit(solution)/shard_map/ppermute | solution.py:538
  104.5 31.7 %copy-start.4 = (bf16[192,2048]{1,0:T(8,128)(2,1)}, bf16[192,2048]{1,0:T(8,128)(2,1)S(1)}, u32[]{:S(2)}) copy-start(bf16[192,2048]{1,0:T(8,128)(2,1)S(1)} %collective-permute-done.14.refs_1_) | copy-start | bytes 2359300
  104.5 31.6 %collective-permute-start.16 = (bf16[96,2048]{1,0:T(8,128)(2,1)S(1)}, bf16[96,2048]{1,0:T(8,128)(2,1)S(1)}, u32[]{:S(2)}, u32[]{:S(2)}) collective-permute-start(bf16[96,2048]{1,0:T(8,128)(2,1)S(1)} %slice.39), channel_id=1, source_target_pairs={{0,2},{2,4},{4,6},{6,0},{1,3},{3,5},{5,7},{7,1},{8,10},{10,12},{12... | collective-permute-start | bytes 1179656 | tf_op jit(solution)/shard_map/ppermute | solution.py:538
  105.8 30.3 %collective-permute-start.17 = (bf16[96,2048]{1,0:T(8,128)(2,1)S(1)}, bf16[96,2048]{1,0:T(8,128)(2,1)S(1)}, u32[]{:S(2)}, u32[]{:S(2)}) collective-permute-start(bf16[96,2048]{1,0:T(8,128)(2,1)S(1)} %slice.40), channel_id=1, source_target_pairs={{0,6},{2,0},{4,2},{6,4},{1,7},{3,1},{5,3},{7,5},{8,14},{10,8},{12,... | collective-permute-start | bytes 1179656 | tf_op jit(solution)/shard_map/ppermute | solution.py:538
  119.0 17.2 %copy-start.6 = (bf16[64,2048]{1,0:T(8,128)(2,1)}, bf16[64,2048]{1,0:T(8,128)(2,1)S(1)}, u32[]{:S(2)}) copy-start(bf16[64,2048]{1,0:T(8,128)(2,1)S(1)} %collective-permute-done.18.refs_6_) | copy-start | bytes 786436
  119.0 17.1 %collective-permute-start.20 = (bf16[32,2048]{1,0:T(8,128)(2,1)S(1)}, bf16[32,2048]{1,0:T(8,128)(2,1)S(1)}, u32[]{:S(2)}, u32[]{:S(2)}) collective-permute-start(bf16[32,2048]{1,0:T(8,128)(2,1)S(1)} %slice.41), channel_id=1, source_target_pairs={{0,2},{2,4},{4,6},{6,0},{1,3},{3,5},{5,7},{7,1},{8,10},{10,12},{12... | collective-permute-start | bytes 393224 | tf_op jit(solution)/shard_map/ppermute | solution.py:538
  119.1 17.1 %copy-start.7 = (bf16[64,2048]{1,0:T(8,128)(2,1)}, bf16[64,2048]{1,0:T(8,128)(2,1)S(1)}, u32[]{:S(2)}) copy-start(bf16[64,2048]{1,0:T(8,128)(2,1)S(1)} %collective-permute-done.19.refs_7_) | copy-start | bytes 786436
  119.1 17.0 %collective-permute-start.21 = (bf16[32,2048]{1,0:T(8,128)(2,1)S(1)}, bf16[32,2048]{1,0:T(8,128)(2,1)S(1)}, u32[]{:S(2)}, u32[]{:S(2)}) collective-permute-start(bf16[32,2048]{1,0:T(8,128)(2,1)S(1)} %slice.42), channel_id=1, source_target_pairs={{0,6},{2,0},{4,2},{6,4},{1,7},{3,1},{5,3},{7,5},{8,14},{10,8},{12,... | collective-permute-start | bytes 393224 | tf_op jit(solution)/shard_map/ppermute | solution.py:538
  122.8 3.9 %collective-permute-start.11 = (bf16[8,512]{1,0:T(8,128)(2,1)S(1)}, bf16[8,512]{1,0:T(8,128)(2,1)S(1)}, u32[]{:S(2)}, u32[]{:S(2)}) collective-permute-start(bf16[8,512]{1,0:T(8,128)(2,1)S(1)} %get-tuple-element.31), channel_id=1, source_target_pairs={{0,1},{1,2},{2,3},{3,4},{4,5},{5,6},{6,7},{7,8},{8,9},{9,10},{10,1... | collective-permute-start | bytes 24584 | tf_op jit(solution)/shard_map/ppermute | solution.py:595
  126.7 5.7 %copy-start.29 = (bf16[8,512]{1,0:T(8,128)(2,1)}, bf16[8,512]{1,0:T(8,128)(2,1)S(1)}, u32[]{:S(2)}) copy-start(bf16[8,512]{1,0:T(8,128)(2,1)S(1)} %collective-permute-done.11.low) | copy-start | bytes 24580
  126.7 5.7 %collective-permute-start.12 = (bf16[8,512]{1,0:T(8,128)(2,1)S(1)}, bf16[8,512]{1,0:T(8,128)(2,1)S(1)}, u32[]{:S(2)}, u32[]{:S(2)}) collective-permute-start(bf16[8,512]{1,0:T(8,128)(2,1)S(1)} %get-tuple-element.30), channel_id=1, source_target_pairs={{1,0},{2,1},{3,2},{4,3},{5,4},{6,5},{7,6},{8,7},{9,8},{10,9},{11,1... | collective-permute-start | bytes 24584 | tf_op jit(solution)/shard_map/ppermute | solution.py:598
  134.7 1.4 collective-permute-start.13
  136.2 1.2 copy-start.3
  142.9 11.0 %collective-permute-start.22 = (bf16[48,2048]{1,0:T(8,128)(2,1)}, bf16[48,2048]{1,0:T(8,128)(2,1)S(1)}, u32[]{:S(2)}, u32[]{:S(2)}) collective-permute-start(bf16[48,2048]{1,0:T(8,128)(2,1)} %get-tuple-element.25), channel_id=1, source_target_pairs={{0,1},{1,0},{2,3},{3,2},{4,5},{5,4},{6,7},{7,6},{8,9},{9,8},{10,11... | collective-permute-start | bytes 589832 | tf_op jit(solution)/shard_map/ppermute | solution.py:533
  143.2 7.2 %collective-permute-start.23 = (f32[8,384]{1,0:T(8,128)S(1)}, f32[8,384]{1,0:T(8,128)S(1)}, u32[]{:S(2)}, u32[]{:S(2)}) collective-permute-start(f32[8,384]{1,0:T(8,128)S(1)} %get-tuple-element.27), channel_id=1, source_target_pairs={{0,8},{8,16},{16,24},{24,0},{1,9},{9,17},{17,25},{25,1},{2,10},{10... | collective-permute-start | bytes 36872 | tf_op jit(solution)/shard_map/ppermute | solution.py:538
  146.9 4.1 %collective-permute-start.24 = (f32[8,384]{1,0:T(8,128)S(1)}, f32[8,384]{1,0:T(8,128)S(1)}, u32[]{:S(2)}, u32[]{:S(2)}) collective-permute-start(f32[8,384]{1,0:T(8,128)S(1)} %get-tuple-element.28), channel_id=1, source_target_pairs={{0,16},{8,24},{16,0},{24,8},{1,17},{9,25},{17,1},{25,9},{2,18},{10... | collective-permute-start | bytes 36872 | tf_op jit(solution)/shard_map/ppermute | solution.py:538
  149.1 2.8 %collective-permute-start.25 = (f32[8,384]{1,0:T(8,128)S(1)}, f32[8,384]{1,0:T(8,128)S(1)}, u32[]{:S(2)}, u32[]{:S(2)}) collective-permute-start(f32[8,384]{1,0:T(8,128)S(1)} %get-tuple-element.29), channel_id=1, source_target_pairs={{0,24},{8,0},{16,8},{24,16},{1,25},{9,1},{17,9},{25,17},{2,26},{10... | collective-permute-start | bytes 36872 | tf_op jit(solution)/shard_map/ppermute | solution.py:538
  150.3 1.7 %copy-start.26 = (f32[8,384]{1,0:T(8,128)}, f32[8,384]{1,0:T(8,128)S(1)}, u32[]{:S(2)}) copy-start(f32[8,384]{1,0:T(8,128)S(1)} %collective-permute-done.23.b) | copy-start | bytes 36868
  151.0 1.0 copy-start.27
  (11 other events, 7.5 us)

commit v3 on v2

--- a/solution.py
+++ b/solution.py
@@ -468,65 +468,65 @@
     )(own, low, high)
 
 
-NSTEP = 512
-
-
-def project_body(got, mine, theirs, *refs):
-    wa, wp = refs[0:5], refs[5:10]
-    keep, send, att, pool = refs[10:]
+def project_body(got, mine, theirs, w0, w1, w3, w2a, w2b, keep, send, wbuf, sems):
     y0 = lax.axis_index("y")
     c = lax.axis_index("c")
-
-    @pl.when(pl.program_id(0) == 0)
-    def _():
-        row = lax.broadcasted_iota(jnp.int32, (128, HEADS * VAL), 0)
-        head = lax.broadcasted_iota(jnp.int32, (128, HEADS * VAL), 1) // VAL
-        spread = ((row >= 64 + 3 * head) & (row < 67 + 3 * head)).astype(bf16)
-        for n, d in enumerate(PLACES):
-            slots = [x * NY + (y0 + NY + d) % NY for x in range(NX)]
-            logs = [nn(got[slot, :, 128:256], spread) for slot in slots]
-            top = jnp.maximum(
-                jnp.maximum(logs[0], logs[1]), jnp.maximum(logs[2], logs[3])
-            )
-            weights = [jnp.exp(v - top) for v in logs]
-            total = weights[0] + weights[1] + weights[2] + weights[3]
-            acc = jnp.zeros((2 * ROWS, HEADS * VAL), f32)
-            for slot, w in zip(slots, weights):
-                acc = acc + got[slot, :, 0 : HEADS * VAL].astype(f32) * w
-            att[n, :, :] = (acc / total).astype(bf16)
-        pool[0:ROWS, :] = jnp.where(c == 0, mine[...], theirs[...])
-        pool[ROWS:, :] = jnp.where(c == 0, theirs[...], mine[...])
-
-    total = nn(pool[...], jnp.concatenate([w[...] for w in wp], axis=0))
-    for n in range(3):
-        total = total + nn(att[n], wa[n][...])
-    total = total + nn(att[3], jnp.concatenate([wa[3][...], wa[4][...]], axis=0))
-    first, second = total[0:ROWS], total[ROWS:]
-    keep[...] = jnp.where(c == 0, first, second)
-    send[...] = jnp.where(c == 0, second, first).astype(bf16)
-
-
-def project(got, mine, theirs, wa, wp):
-    whole = lambda *s: pl.BlockSpec(s, lambda k: (0,) * len(s))
-    part = lambda n: pl.BlockSpec((n, NSTEP), lambda k: (0, k))
-    weights = [*wa, *wp]
+    places = ((w0, 0, 0), (w1, 1, 0), (w3, 2, 0), (w2a, 3, 0), (w2b, 3, 128))
+    copies = []
+    for n, (ref, slot, at) in enumerate(places):
+        rows = ref.shape[0]
+        copies.append(
+            pltpu.make_async_copy(ref, wbuf.at[slot, at : at + rows], sems.at[n])
+        )
+    for copy in copies:
+        copy.start()
+    row = lax.broadcasted_iota(jnp.int32, (128, HEADS * VAL), 0)
+    head = lax.broadcasted_iota(jnp.int32, (128, HEADS * VAL), 1) // VAL
+    spread = ((row >= 64 + 3 * head) & (row < 67 + 3 * head)).astype(bf16)
+    inputs = []
+    for n, d in enumerate(PLACES):
+        slots = [x * NY + (y0 + NY + d) % NY for x in range(NX)]
+        logs = [nn(got[slot, :, 128:256], spread) for slot in slots]
+        top = jnp.maximum(jnp.maximum(logs[0], logs[1]), jnp.maximum(logs[2], logs[3]))
+        weights = [jnp.exp(v - top) for v in logs]
+        total = weights[0] + weights[1] + weights[2] + weights[3]
+        acc = jnp.zeros((2 * ROWS, HEADS * VAL), f32)
+        for slot, w in zip(slots, weights):
+            acc = acc + got[slot, :, 0 : HEADS * VAL].astype(f32) * w
+        own = mine[:, n * 64 : (n + 1) * 64]
+        twin = theirs[:, n * 64 : (n + 1) * 64]
+        pool = jnp.concatenate(
+            [jnp.where(c == 0, own, twin), jnp.where(c == 0, twin, own)], axis=0
+        )
+        inputs.append(jnp.concatenate([(acc / total).astype(bf16), pool], axis=1))
+    for copy in copies:
+        copy.wait()
+    for col in range(0, WIDTH, 512):
+        cols = slice(col, col + 512)
+        result = nn(inputs[0], wbuf[0, :, cols])
+        for n in range(1, NY):
+            result = result + nn(inputs[n], wbuf[n, :, cols])
+        first, second = result[0:ROWS], result[ROWS:]
+        keep[:, cols] = jnp.where(c == 0, first, second)
+        send[:, cols] = jnp.where(c == 0, second, first).astype(bf16)
+
+
+def project(got, mine, theirs, weights):
     return pl.pallas_call(
         project_body,
-        grid=(WIDTH // NSTEP,),
-        in_specs=[whole(*got.shape), whole(*mine.shape), whole(*theirs.shape)]
-        + [part(w.shape[0]) for w in weights],
-        out_specs=(part(ROWS), part(ROWS)),
+        in_specs=[vmem()] * 3 + [pl.BlockSpec(memory_space=pl.ANY)] * 5,
+        out_specs=(vmem(), vmem()),
         out_shape=(
-            jax.ShapeDtypeStruct((ROWS, WIDTH), f32),
-            jax.ShapeDtypeStruct((ROWS, WIDTH), bf16),
+            pltpu.VMEM((ROWS, WIDTH), f32),
+            pltpu.VMEM((ROWS, WIDTH), bf16),
         ),
         scratch_shapes=[
-            pltpu.VMEM((NY, 2 * ROWS, HEADS * VAL), bf16),
-            pltpu.VMEM((2 * ROWS, 256), bf16),
+            pltpu.VMEM((NY, 256, WIDTH), bf16),
+            pltpu.SemaphoreType.DMA((5,)),
         ],
-        compiler_params=params(dimension_semantics=("arbitrary",)),
+        compiler_params=params(40),
         name="project",
-    )(got, mine, theirs, *weights)
+    )(near(got), near(mine), near(theirs), *weights)
 
 
 def across(x):
@@ -604,39 +604,30 @@
         (pool_scale.astype(f32)[:, None] * w_out_pool.astype(f32)).astype(bf16),
         preferred_element_type=f32,
     ).astype(bf16)
-    wa1 = shifted(w_out_attn, "y", 1)
-    wa3 = shifted(w_out_attn, "y", NY - 1)
-    wp1 = shifted(folded, "y", 1)
-    wp3 = shifted(folded, "y", NY - 1)
-    half = HEADS * VAL // 2
-    wa2a = shifted(wa1[:half], "y", 1)
-    wa2b = shifted(wa3[half:], "y", NY - 1)
-    wp2a = shifted(wp1[:32], "y", 1)
-    wp2b = shifted(wp3[32:], "y", NY - 1)
+    w0 = jnp.concatenate([w_out_attn, folded], axis=0)
+    w1 = shifted(w0, "y", 1)
+    w3 = shifted(w0, "y", NY - 1)
+    w1_half, w3_half = lax.optimization_barrier((w1[:128], w3[128:]))
+    w2a = shifted(w1_half, "y", 1)
+    w2b = shifted(w3_half, "y", NY - 1)
 
     kv = lax.all_to_all(
         jnp.broadcast_to(kv_own[None], (NY, *kv_own.shape)), "y", 0, 0, tiled=True
     )
     q_side = in_order(pieces)
     q_own = [q_side] + [shifted(q_side, "x", k) for k in range(1, NX)]
-    tag = q_own[1][:8, :128] + q_own[2][:8, :128] + q_own[3][:8, :128]
     q_twin = [across(q) for q in q_own]
     kv_twin = across(kv)
     qt = queries(q_own, q_twin, wqt, query_gain, query_tables())
-    pair = keys_values((tag,), kv, kv_twin, wkvt, key_gain, key_tables())
+    pair = keys_values((), kv, kv_twin, wkvt, key_gain, key_tables())
     message, *logs = attend(*pair, qt)
 
     got = lax.all_to_all(message, ("x", "y"), 0, 0, tiled=True)
     logs = [logs[0]] + [shifted(logs[k], "x", k) for k in range(1, NX)]
     row_logsum = logsums(logs)
-    keep, send = project(
-        got,
-        pool_mine,
-        pool_theirs,
-        (w_out_attn, wa1, wa3, wa2a, wa2b),
-        (folded, wp1, wp3, wp2a, wp2b),
-    )
-    mixed = (keep + across(send).astype(f32)).astype(bf16)
+    keep, send = project(got, pool_mine, pool_theirs, (w0, w1, w3, w2a, w2b))
+    received = across(send)
+    mixed = (keep + received.astype(f32)).astype(bf16)
     return mixed, row_logsum
 
 

time: 158 us -> 143 us (0.905)
  blocking collectives: 37.5 us -> 20.1 us
  waiting for transfers between devices: 24.2 us -> 32.8 us
  local copies, waits for them, and re-layouts: 6.98 us -> 11.9 us
  Pallas kernels: 36.7 us -> 32.2 us
  starting transfers between devices: 46.8 us -> 42.6 us
    all_to_all x1 -> x0, blocking collectives: 17.6 us -> none  [shards(): lax.all_to_all(jnp.broadcast_to(kv_own[None], (NY, *kv_own.shape)), 'y',...]
    ppermute x1, waiting for transfers between devices: 1.62 us -> 10.5 us  [shards(): lax.ppermute(pool_in[ROWS - 8:], every, [(i, i + 1) for i in range(count...]
    all_to_all x0 -> x1, waiting for transfers between devices: none -> 8.4 us  [shards(): lax.all_to_all(jnp.broadcast_to(kv_own[None], (NY, *kv_own.shape)), 'y',...]
    ppermute x17 -> x13, waiting for transfers between devices: 16.9 us -> 9.15 us  [shifted(): lax.ppermute(x, axis, [(i, (i + places) % count) for i in range(count)])]
    ppermute x17 -> x13, starting transfers between devices: 25 us -> 20.1 us  [shifted(): lax.ppermute(x, axis, [(i, (i + places) % count) for i in range(count)])]
    all_to_all x0 -> x1, starting transfers between devices: none -> 4.17 us  [shards(): lax.all_to_all(jnp.broadcast_to(kv_own[None], (NY, *kv_own.shape)), 'y',...]
    ppermute x7, starting transfers between devices: 12.7 us -> 8.61 us  [across(): return lax.ppermute(x, 'c', [(0, 1), (1, 0)])]
    unnamed x65 -> x45, local copies, waits for them, and re-layouts: 5.08 us -> 8.91 us
  transfers between devices with their start and end apart: 27 -> 24, of which waited for: 13 -> 10; matrix products, arithmetic and copies ran while one was open for 2% -> 3% of each run, Pallas kernels for 17% -> 18%
where the time goes in v3:
time: 143 us; the launch traced here: 142 us
  starting transfers between devices  42.6 us (30%)
  waiting for transfers between devices  32.8 us (23%)
  Pallas kernels  32.2 us (23%)
  blocking collectives  20.1 us (14%)
  local copies, waits for them, and re-layouts  11.9 us (8%)
    all_to_all x1, blocking collectives, shards(): lax.all_to_all(kv_all, 'z', 0, 0, tiled=True).reshape(NZ * ROWS, KR + 128)  20.1 us
    ppermute x13, starting transfers between devices, shifted(): lax.ppermute(x, axis, [(i, (i + places) % count) for i in range(count)])  20.1 us
    pallas_call x1, Pallas kernels, attend(): pl.pallas_call(attend_body, in_specs=[vmem()] * 3, out_specs=(vmem(),) *...  15.4 us
    ppermute x1, waiting for transfers between devices, shards(): lax.ppermute(pool_in[ROWS - 8:], every, [(i, i + 1) for i in range(count...  10.5 us
    ppermute x13, waiting for transfers between devices, shifted(): lax.ppermute(x, axis, [(i, (i + places) % count) for i in range(count)])  9.15 us
    unnamed x45, local copies, waits for them, and re-layouts  8.91 us
    ppermute x7, starting transfers between devices, across(): return lax.ppermute(x, 'c', [(0, 1), (1, 0)])  8.61 us
    all_to_all x1, waiting for transfers between devices, shards(): lax.all_to_all(jnp.broadcast_to(kv_own[None], (NY, *kv_own.shape)), 'y',...  8.4 us
  transfers between devices with their start and end apart: 24, of which 10 were waited for; matrix products, arithmetic and copies ran while one was open for 3% of the time, Pallas kernels for 18%

profile of v3, /device:TPU:1, one launch (start us, length us, event | category | flops | bytes accessed | tf_op | source)
XLA Modules:
  0.0 141.7 jit_solution(11446959892052533804)
XLA Ops:
  0.6 4.2 %latents.1 = (bf16[48,512]{1,0:T(8,128)(2,1)}, bf16[8,48,384]{2,1,0:T(8,128)(2,1)}, bf16[48,512]{1,0:T(8,128)(2,1)}) custom-call(bf16[48,2048]{1,0:T(8,128)(2,1)} %tok.1, bf16[2048]{0:T(1024)(128)(2,1)} %gain.2, bf16[2048,512]{1,0:T(8,128)(2,1)} %qdw.1, bf16[512]{0:T(512)(128)(2,1)} %qg.1, bf16[2048,256]{1,0:T(8,128)(2,1)} %kdw.1, bf16[256]{0:T(256)(128)(2,1)} %kg.1, ...), custom_call_target="tpu_custom_call" | custom-call | tf_op jit(solution)/shard_map/latents/pallas_call | solution.py:128
  4.8 20.1 %all_to_all.15 = bf16[8,48,384]{2,1,0:T(8,128)(2,1)S(1)} all-to-all(bf16[8,48,384]{2,1,0:T(8,128)(2,1)} %get-tuple-element.18), channel_id=1, replica_groups=mesh['z'=8,'x'=4,'y'=4,'c'=2] {'z'}, dimensions={0} | all-to-all | bytes 589824 | tf_op jit(solution)/shard_map/all_to_all | solution.py:591
  25.0 1.2 broadcast_in_dim.9
  26.1 4.2 %all-to-all-start.1 = ((bf16[4,384,384]{2,1,0:T(8,128)(2,1)}), bf16[4,384,384]{2,1,0:T(8,128)(2,1)S(1)}, u32[]{:S(2)}, u32[]{:S(2)}) async-start(bf16[4,384,384]{2,1,0:T(8,128)(2,1)} %broadcast_in_dim.9), calls=%async_computation.1 | async-start | bytes 2359296 | tf_op jit(solution)/shard_map/all_to_all | solution.py:614
  30.3 1.5 %collective-permute-start.1 = (bf16[48,512]{1,0:T(8,128)(2,1)S(1)}, bf16[48,512]{1,0:T(8,128)(2,1)S(1)}, u32[]{:S(2)}, u32[]{:S(2)}) collective-permute-start(bf16[48,512]{1,0:T(8,128)(2,1)S(1)} %copy-done.12), channel_id=1, source_target_pairs={{0,2},{2,4},{4,6},{6,0},{1,3},{3,5},{5,7},{7,1},{8,10},{10,12},{12... | collective-permute-start | bytes 147464 | tf_op jit(solution)/shard_map/ppermute | solution.py:538
  31.8 2.4 %collective-permute-start.2 = (bf16[48,512]{1,0:T(8,128)(2,1)S(1)}, bf16[48,512]{1,0:T(8,128)(2,1)S(1)}, u32[]{:S(2)}, u32[]{:S(2)}) collective-permute-start(bf16[48,512]{1,0:T(8,128)(2,1)S(1)} %copy-done.12), channel_id=1, source_target_pairs={{0,4},{2,6},{4,0},{6,2},{1,5},{3,7},{5,1},{7,3},{8,12},{10,14},{12... | collective-permute-start | bytes 147464 | tf_op jit(solution)/shard_map/ppermute | solution.py:538
  34.2 1.2 collective-permute-start.3
  35.4 8.4 %all-to-all-done.1.refs_0_ = bf16[4,384,384]{2,1,0:T(8,128)(2,1)S(1)} async-done(((bf16[4,384,384]{2,1,0:T(8,128)(2,1)}), bf16[4,384,384]{2,1,0:T(8,128)(2,1)S(1)}, u32[]{:S(2)}, u32[]{:S(2)}) %all-to-all-start.1) | async-done | bytes 1179680 | tf_op jit(solution)/shard_map/all_to_all | solution.py:614
  43.8 5.1 %collective-permute-start = (bf16[4,384,384]{2,1,0:T(8,128)(2,1)S(1)}, bf16[4,384,384]{2,1,0:T(8,128)(2,1)}, u32[]{:S(2)}, u32[]{:S(2)}) collective-permute-start(bf16[4,384,384]{2,1,0:T(8,128)(2,1)S(1)} %all-to-all-done.1.refs_0_), channel_id=1, source_target_pairs={{0,1},{1,0},{2,3},{3,2},{4,5},{5,4},{6,7},{7,6},{8,9},{9,8},{10,11... | collective-permute-start | bytes 3538952 | tf_op jit(solution)/shard_map/ppermute | solution.py:533
  49.6 2.4 %collective-permute-start.15 = (bf16[256,2048]{1,0:T(8,128)(2,1)S(1)}, bf16[256,2048]{1,0:T(8,128)(2,1)}, u32[]{:S(2)}, u32[]{:S(2)}) collective-permute-start(bf16[256,2048]{1,0:T(8,128)(2,1)S(1)} %pad_maximum_fusion.w0), channel_id=1, source_target_pairs={{0,6},{2,0},{4,2},{6,4},{1,7},{3,1},{5,3},{7,5},{8,14},{10,8},{12,... | collective-permute-start | bytes 3145736 | tf_op jit(solution)/shard_map/ppermute | solution.py:538
  52.0 0.6 copy-done.14
  52.6 0.6 copy-done.15
  53.2 1.6 %order.1.own0 = bf16[192,512]{1,0:T(8,128)(2,1)} custom-call(bf16[48,512]{1,0:T(8,128)(2,1)} %get-tuple-element.21.a, bf16[48,512]{1,0:T(8,128)(2,1)} %copy-done.13, bf16[48,512]{1,0:T(8,128)(2,1)} %copy-done.14, bf16[48,512]{1,0:T(8,128)(2,1)} %copy-done.15), custom_call_target="tpu_custom_call" | custom-call | tf_op jit(solution)/shard_map/order/pallas_call | solution.py:549
  54.8 1.2 collective-permute-start.4
  56.0 2.4 %collective-permute-start.5 = (bf16[192,512]{1,0:T(8,128)(2,1)}, bf16[192,512]{1,0:T(8,128)(2,1)}, u32[]{:S(2)}, u32[]{:S(2)}) collective-permute-start(bf16[192,512]{1,0:T(8,128)(2,1)} %order.1.own0), channel_id=1, source_target_pairs={{0,16},{8,24},{16,0},{24,8},{1,17},{9,25},{17,1},{25,9},{2,18},{10... | collective-permute-start | bytes 589832 | tf_op jit(solution)/shard_map/ppermute | solution.py:538
  58.5 3.6 %collective-permute-done.4.own1 = bf16[192,512]{1,0:T(8,128)(2,1)S(1)} collective-permute-done((bf16[192,512]{1,0:T(8,128)(2,1)}, bf16[192,512]{1,0:T(8,128)(2,1)S(1)}, u32[]{:S(2)}, u32[]{:S(2)}) %collective-permute-start.4) | collective-permute-done | bytes 196640 | tf_op jit(solution)/shard_map/ppermute | solution.py:538
  62.1 1.4 collective-permute-start.6
  63.5 3.9 %collective-permute-done.5.own2 = bf16[192,512]{1,0:T(8,128)(2,1)} collective-permute-done((bf16[192,512]{1,0:T(8,128)(2,1)}, bf16[192,512]{1,0:T(8,128)(2,1)}, u32[]{:S(2)}, u32[]{:S(2)}) %collective-permute-start.5) | collective-permute-done | bytes 196640 | tf_op jit(solution)/shard_map/ppermute | solution.py:538
  67.4 1.4 %collective-permute-start.7 = (bf16[192,512]{1,0:T(8,128)(2,1)}, bf16[192,512]{1,0:T(8,128)(2,1)S(1)}, u32[]{:S(2)}, u32[]{:S(2)}) collective-permute-start(bf16[192,512]{1,0:T(8,128)(2,1)} %order.1.own0), channel_id=1, source_target_pairs={{0,1},{1,0},{2,3},{3,2},{4,5},{5,4},{6,7},{7,6},{8,9},{9,8},{10,11... | collective-permute-start | bytes 589832 | tf_op jit(solution)/shard_map/ppermute | solution.py:533
  68.8 0.9 collective-permute-start.8
  70.8 0.7 copy-done.11
  71.8 1.7 %copy.20 = bf16[256,384]{0,1:T(8,128)(2,1)} copy(bf16[256,384]{1,0:T(8,128)(2,1)} %param.27) | data formatting | bytes 393216 | tf_op args[9]
  73.6 2.5 %queries.1.qt = bf16[3,128,1536]{2,1,0:T(8,128)(2,1)S(1)} custom-call(bf16[192,512]{1,0:T(8,128)(2,1)} %order.1.own0, bf16[192,512]{1,0:T(8,128)(2,1)} %copy-done.9, bf16[192,512]{1,0:T(8,128)(2,1)} %collective-permute-done.5.own2, bf16[192,512]{1,0:T(8,128)(2,1)} %collective-permute-done.6.own3, bf16[192,512]{1,0:T(8,128)(2,1)} %copy-done.10, ...), custom_call_target="tpu_custom_call" | custom-call | tf_op jit(solution)/shard_map/queries/pallas_call | solution.py:222
  76.1 3.4 %keys.1 = (bf16[3,3072,128]{2,1,0:T(8,128)(2,1)S(1)}, bf16[3,80,3072]{2,1,0:T(8,128)(2,1)S(1)}) custom-call(bf16[4,384,384]{2,1,0:T(8,128)(2,1)} %copy-done.6, bf16[4,384,384]{2,1,0:T(8,128)(2,1)} %collective-permute-done.refs_1_, bf16[384,256]{1,0:T(8,128)(2,1)} %bitcast.10, bf16[96]{0:T(256)(128)(2,1)} %refs_3_.1, f32[16,1024]{1,0:T(8,128)} %constant.5.clone.refs_4_), custom_call_target="tpu_custom_call" | custom-call | tf_op jit(solution)/shard_map/keys/pallas_call | solution.py:268
  79.5 15.4 %attend.1 = (bf16[16,96,256]{2,1,0:T(8,128)(2,1)S(1)}, f32[8,384]{1,0:T(8,128)S(1)}, f32[8,384]{1,0:T(8,128)S(1)}, f32[8,384]{1,0:T(8,128)S(1)}, f32[8,384]{1,0:T(8,128)S(1)}) custom-call(bf16[3,3072,128]{2,1,0:T(8,128)(2,1)S(1)} %get-tuple-element.19.kbuf, bf16[3,80,3072]{2,1,0:T(8,128)(2,1)S(1)} %get-tuple-element.20.vbuf, bf16[3,128,1536]{2,1,0:T(8,128)(2,1)S(1)} %queries.1.qt), custom_call_target="tpu_custom_call" | custom-call | tf_op jit(solution)/shard_map/attend/pallas_call | solution.py:378
  94.9 0.9 copy-done.1
  96.4 4.7 %all-to-all-start.2 = ((bf16[16,96,256]{2,1,0:T(8,128)(2,1)}), bf16[16,96,256]{2,1,0:T(8,128)(2,1)S(1)}, u32[]{:S(2)}, u32[]{:S(2)}) async-start(bf16[16,96,256]{2,1,0:T(8,128)(2,1)} %copy-done.1), calls=%async_computation.2 | async-start | bytes 1572864 | tf_op jit(solution)/shard_map/all_to_all | solution.py:625
  101.1 1.1 slice.17
  102.2 1.4 %collective-permute-start.16 = (bf16[128,2048]{1,0:T(8,128)(2,1)S(1)}, bf16[128,2048]{1,0:T(8,128)(2,1)S(1)}, u32[]{:S(2)}, u32[]{:S(2)}) collective-permute-start(bf16[128,2048]{1,0:T(8,128)(2,1)S(1)} %slice.16), channel_id=1, source_target_pairs={{0,2},{2,4},{4,6},{6,0},{1,3},{3,5},{5,7},{7,1},{8,10},{10,12},{12... | collective-permute-start | bytes 1572872 | tf_op jit(solution)/shard_map/ppermute | solution.py:538
  103.6 1.3 collective-permute-start.17
  105.0 0.7 fusion.3
  105.7 3.2 %collective-permute-start.11 = (bf16[8,512]{1,0:T(8,128)(2,1)S(1)}, bf16[8,512]{1,0:T(8,128)(2,1)S(1)}, u32[]{:S(2)}, u32[]{:S(2)}) collective-permute-start(bf16[8,512]{1,0:T(8,128)(2,1)S(1)} %get-tuple-element.35), channel_id=1, source_target_pairs={{0,1},{1,2},{2,3},{3,4},{4,5},{5,6},{6,7},{7,8},{8,9},{9,10},{10,1... | collective-permute-start | bytes 24584 | tf_op jit(solution)/shard_map/ppermute | solution.py:595
  108.9 1.9 %collective-permute-start.12 = (bf16[8,512]{1,0:T(8,128)(2,1)S(1)}, bf16[8,512]{1,0:T(8,128)(2,1)S(1)}, u32[]{:S(2)}, u32[]{:S(2)}) collective-permute-start(bf16[8,512]{1,0:T(8,128)(2,1)S(1)} %get-tuple-element.34), channel_id=1, source_target_pairs={{1,0},{2,1},{3,2},{4,3},{5,4},{6,5},{7,6},{8,7},{9,8},{10,9},{11,1... | collective-permute-start | bytes 24584 | tf_op jit(solution)/shard_map/ppermute | solution.py:598
  110.8 10.5 %collective-permute-done.11.low = bf16[8,512]{1,0:T(8,128)(2,1)S(1)} collective-permute-done((bf16[8,512]{1,0:T(8,128)(2,1)S(1)}, bf16[8,512]{1,0:T(8,128)(2,1)S(1)}, u32[]{:S(2)}, u32[]{:S(2)}) %collective-permute-start.11) | collective-permute-done | bytes 8224 | tf_op jit(solution)/shard_map/ppermute | solution.py:595
  121.3 2.7 %collective-permute-done.12.high = bf16[8,512]{1,0:T(8,128)(2,1)S(1)} collective-permute-done((bf16[8,512]{1,0:T(8,128)(2,1)S(1)}, bf16[8,512]{1,0:T(8,128)(2,1)S(1)}, u32[]{:S(2)}, u32[]{:S(2)}) %collective-permute-start.12) | collective-permute-done | bytes 8224 | tf_op jit(solution)/shard_map/ppermute | solution.py:598
  124.0 0.6 copy-done.20
  124.6 1.7 %pooling.1 = (bf16[48,256]{1,0:T(8,128)(2,1)}, bf16[48,256]{1,0:T(8,128)(2,1)}) custom-call(bf16[48,512]{1,0:T(8,128)(2,1)} %get-tuple-element.23.own, bf16[8,512]{1,0:T(8,128)(2,1)} %copy-done.19, bf16[8,512]{1,0:T(8,128)(2,1)} %copy-done.20), custom_call_target="tpu_custom_call" | custom-call | tf_op jit(solution)/shard_map/pooling/pallas_call | solution.py:457
  126.3 1.4 collective-permute-done.13.theirs
  127.7 0.8 copy-done.2
  128.5 1.0 copy-done.3
  129.5 0.7 copy-done.4
  130.2 2.2 %project.1 = (f32[48,2048]{1,0:T(8,128)S(1)}, bf16[48,2048]{1,0:T(8,128)(2,1)S(1)}) custom-call(bf16[16,96,256]{2,1,0:T(8,128)(2,1)S(1)} %all-to-all-done.2.got, bf16[48,256]{1,0:T(8,128)(2,1)S(1)} %copy-done.4, bf16[48,256]{1,0:T(8,128)(2,1)S(1)} %collective-permute-done.13.theirs, bf16[256,2048]{1,0:T(8,128)(2,1)S(1)} %pad_maximum_fusion.w0, ...), custom_call_target="tpu_custom_call" | custom-call | tf_op jit(solution)/shard_map/project/pallas_call | solution.py:515
  132.9 0.8 collective-permute-start.19
  133.7 2.4 %collective-permute-start.20 = (f32[8,384]{1,0:T(8,128)S(1)}, f32[8,384]{1,0:T(8,128)S(1)}, u32[]{:S(2)}, u32[]{:S(2)}) collective-permute-start(f32[8,384]{1,0:T(8,128)S(1)} %get-tuple-element.32), channel_id=1, source_target_pairs={{0,16},{8,24},{16,0},{24,8},{1,17},{9,25},{17,1},{25,9},{2,18},{10... | collective-permute-start | bytes 36872 | tf_op jit(solution)/shard_map/ppermute | solution.py:538
  136.1 1.3 collective-permute-start.21
  137.8 1.2 collective-permute-done.21.d
  139.6 1.4 logsums.1
  141.0 0.7 add_convert_fusion
  (62 shorter events, 4.4 us)
Async XLA Ops:
  0.6 48.2 %copy-start = (bf16[1,64,64]{2,1,0:T(8,128)(2,1)S(1)}, bf16[1,64,64]{2,1,0:T(8,128)(2,1)}, u32[]{:S(2)}) copy-start(bf16[1,64,64]{2,1,0:T(8,128)(2,1)} %param.30) | copy-start | bytes 24580
  4.8 25.5 %copy-start.12 = (bf16[48,512]{1,0:T(8,128)(2,1)S(1)}, bf16[48,512]{1,0:T(8,128)(2,1)}, u32[]{:S(2)}) copy-start(bf16[48,512]{1,0:T(8,128)(2,1)} %get-tuple-element.21.a) | copy-start | bytes 147460
  4.8 30.5 %copy-start.21 = (bf16[64]{0:T(256)(128)(2,1)S(1)}, bf16[64]{0:T(256)(128)(2,1)}, u32[]{:S(2)}) copy-start(bf16[64]{0:T(256)(128)(2,1)} %param.31) | copy-start | bytes 388
  4.8 44.0 %copy-start.8 = (bf16[64,2048]{1,0:T(8,128)(2,1)S(1)}, bf16[64,2048]{1,0:T(8,128)(2,1)}, u32[]{:S(2)}) copy-start(bf16[64,2048]{1,0:T(8,128)(2,1)} %param.33) | copy-start | bytes 786436
  25.0 24.2 %copy-start.7 = (bf16[192,2048]{1,0:T(8,128)(2,1)S(1)}, bf16[192,2048]{1,0:T(8,128)(2,1)}, u32[]{:S(2)}) copy-start(bf16[192,2048]{1,0:T(8,128)(2,1)} %param.32) | copy-start | bytes 2359300
  26.1 17.6 %all-to-all-start.1 = ((bf16[4,384,384]{2,1,0:T(8,128)(2,1)}), bf16[4,384,384]{2,1,0:T(8,128)(2,1)S(1)}, u32[]{:S(2)}, u32[]{:S(2)}) async-start(bf16[4,384,384]{2,1,0:T(8,128)(2,1)} %broadcast_in_dim.9), calls=%async_computation.1 | async-start | bytes 2359296 | tf_op jit(solution)/shard_map/all_to_all | solution.py:614
  30.3 19.3 %collective-permute-start.1 = (bf16[48,512]{1,0:T(8,128)(2,1)S(1)}, bf16[48,512]{1,0:T(8,128)(2,1)S(1)}, u32[]{:S(2)}, u32[]{:S(2)}) collective-permute-start(bf16[48,512]{1,0:T(8,128)(2,1)S(1)} %copy-done.12), channel_id=1, source_target_pairs={{0,2},{2,4},{4,6},{6,0},{1,3},{3,5},{5,7},{7,1},{8,10},{10,12},{12... | collective-permute-start | bytes 147464 | tf_op jit(solution)/shard_map/ppermute | solution.py:538
  31.8 20.2 %collective-permute-start.2 = (bf16[48,512]{1,0:T(8,128)(2,1)S(1)}, bf16[48,512]{1,0:T(8,128)(2,1)S(1)}, u32[]{:S(2)}, u32[]{:S(2)}) collective-permute-start(bf16[48,512]{1,0:T(8,128)(2,1)S(1)} %copy-done.12), channel_id=1, source_target_pairs={{0,4},{2,6},{4,0},{6,2},{1,5},{3,7},{5,1},{7,3},{8,12},{10,14},{12... | collective-permute-start | bytes 147464 | tf_op jit(solution)/shard_map/ppermute | solution.py:538
  34.2 17.8 %collective-permute-start.3 = (bf16[48,512]{1,0:T(8,128)(2,1)S(1)}, bf16[48,512]{1,0:T(8,128)(2,1)S(1)}, u32[]{:S(2)}, u32[]{:S(2)}) collective-permute-start(bf16[48,512]{1,0:T(8,128)(2,1)S(1)} %copy-done.12), channel_id=1, source_target_pairs={{0,6},{2,0},{4,2},{6,4},{1,7},{3,1},{5,3},{7,5},{8,14},{10,8},{12,... | collective-permute-start | bytes 147464 | tf_op jit(solution)/shard_map/ppermute | solution.py:538
  43.8 32.3 %copy-start.6 = (bf16[4,384,384]{2,1,0:T(8,128)(2,1)}, bf16[4,384,384]{2,1,0:T(8,128)(2,1)S(1)}, u32[]{:S(2)}) copy-start(bf16[4,384,384]{2,1,0:T(8,128)(2,1)S(1)} %all-to-all-done.1.refs_0_) | copy-start | bytes 3538948
  43.8 32.3 %collective-permute-start = (bf16[4,384,384]{2,1,0:T(8,128)(2,1)S(1)}, bf16[4,384,384]{2,1,0:T(8,128)(2,1)}, u32[]{:S(2)}, u32[]{:S(2)}) collective-permute-start(bf16[4,384,384]{2,1,0:T(8,128)(2,1)S(1)} %all-to-all-done.1.refs_0_), channel_id=1, source_target_pairs={{0,1},{1,0},{2,3},{3,2},{4,5},{5,4},{6,7},{7,6},{8,9},{9,8},{10,11... | collective-permute-start | bytes 3538952 | tf_op jit(solution)/shard_map/ppermute | solution.py:533
  49.2 51.8 %collective-permute-start.14 = (bf16[256,2048]{1,0:T(8,128)(2,1)S(1)}, bf16[256,2048]{1,0:T(8,128)(2,1)S(1)}, u32[]{:S(2)}, u32[]{:S(2)}) collective-permute-start(bf16[256,2048]{1,0:T(8,128)(2,1)S(1)} %pad_maximum_fusion.w0), channel_id=1, source_target_pairs={{0,2},{2,4},{4,6},{6,0},{1,3},{3,5},{5,7},{7,1},{8,10},{10,12},{12... | collective-permute-start | bytes 3145736 | tf_op jit(solution)/shard_map/ppermute | solution.py:538
  49.6 2.4 %copy-start.13 = (bf16[48,512]{1,0:T(8,128)(2,1)}, bf16[48,512]{1,0:T(8,128)(2,1)S(1)}, u32[]{:S(2)}) copy-start(bf16[48,512]{1,0:T(8,128)(2,1)S(1)} %collective-permute-done.1.b) | copy-start | bytes 147460
  49.6 51.5 %collective-permute-start.15 = (bf16[256,2048]{1,0:T(8,128)(2,1)S(1)}, bf16[256,2048]{1,0:T(8,128)(2,1)}, u32[]{:S(2)}, u32[]{:S(2)}) collective-permute-start(bf16[256,2048]{1,0:T(8,128)(2,1)S(1)} %pad_maximum_fusion.w0), channel_id=1, source_target_pairs={{0,6},{2,0},{4,2},{6,4},{1,7},{3,1},{5,3},{7,5},{8,14},{10,8},{12,... | collective-permute-start | bytes 3145736 | tf_op jit(solution)/shard_map/ppermute | solution.py:538
  52.0 0.6 copy-start.14
  52.6 0.6 copy-start.15
  54.8 7.3 %collective-permute-start.4 = (bf16[192,512]{1,0:T(8,128)(2,1)}, bf16[192,512]{1,0:T(8,128)(2,1)S(1)}, u32[]{:S(2)}, u32[]{:S(2)}) collective-permute-start(bf16[192,512]{1,0:T(8,128)(2,1)} %order.1.own0), channel_id=1, source_target_pairs={{0,8},{8,16},{16,24},{24,0},{1,9},{9,17},{17,25},{25,1},{2,10},{10... | collective-permute-start | bytes 589832 | tf_op jit(solution)/shard_map/ppermute | solution.py:538
  56.0 11.4 %collective-permute-start.5 = (bf16[192,512]{1,0:T(8,128)(2,1)}, bf16[192,512]{1,0:T(8,128)(2,1)}, u32[]{:S(2)}, u32[]{:S(2)}) collective-permute-start(bf16[192,512]{1,0:T(8,128)(2,1)} %order.1.own0), channel_id=1, source_target_pairs={{0,16},{8,24},{16,0},{24,8},{1,17},{9,25},{17,1},{25,9},{2,18},{10... | collective-permute-start | bytes 589832 | tf_op jit(solution)/shard_map/ppermute | solution.py:538
  62.1 11.5 %copy-start.9 = (bf16[192,512]{1,0:T(8,128)(2,1)}, bf16[192,512]{1,0:T(8,128)(2,1)S(1)}, u32[]{:S(2)}) copy-start(bf16[192,512]{1,0:T(8,128)(2,1)S(1)} %collective-permute-done.4.own1) | copy-start | bytes 589828
  62.1 6.7 %collective-permute-start.6 = (bf16[192,512]{1,0:T(8,128)(2,1)}, bf16[192,512]{1,0:T(8,128)(2,1)}, u32[]{:S(2)}, u32[]{:S(2)}) collective-permute-start(bf16[192,512]{1,0:T(8,128)(2,1)} %order.1.own0), channel_id=1, source_target_pairs={{0,24},{8,0},{16,8},{24,16},{1,25},{9,1},{17,9},{25,17},{2,26},{10... | collective-permute-start | bytes 589832 | tf_op jit(solution)/shard_map/ppermute | solution.py:538
  67.4 2.7 %collective-permute-start.7 = (bf16[192,512]{1,0:T(8,128)(2,1)}, bf16[192,512]{1,0:T(8,128)(2,1)S(1)}, u32[]{:S(2)}, u32[]{:S(2)}) collective-permute-start(bf16[192,512]{1,0:T(8,128)(2,1)} %order.1.own0), channel_id=1, source_target_pairs={{0,1},{1,0},{2,3},{3,2},{4,5},{5,4},{6,7},{7,6},{8,9},{9,8},{10,11... | collective-permute-start | bytes 589832 | tf_op jit(solution)/shard_map/ppermute | solution.py:533
  68.8 2.0 %collective-permute-start.8 = (bf16[192,512]{1,0:T(8,128)(2,1)S(1)}, bf16[192,512]{1,0:T(8,128)(2,1)S(1)}, u32[]{:S(2)}, u32[]{:S(2)}) collective-permute-start(bf16[192,512]{1,0:T(8,128)(2,1)S(1)} %collective-permute-done.4.own1), channel_id=1, source_target_pairs={{0,1},{1,0},{2,3},{3,2},{4,5},{5,4},{6,7},{7,6},{8,9},{9,8},{10,11... | collective-permute-start | bytes 589832 | tf_op jit(solution)/shard_map/ppermute | solution.py:533
  70.1 0.7 copy-start.10
  70.1 3.5 %collective-permute-start.9 = (bf16[192,512]{1,0:T(8,128)(2,1)}, bf16[192,512]{1,0:T(8,128)(2,1)}, u32[]{:S(2)}, u32[]{:S(2)}) collective-permute-start(bf16[192,512]{1,0:T(8,128)(2,1)} %collective-permute-done.5.own2), channel_id=1, source_target_pairs={{0,1},{1,0},{2,3},{3,2},{4,5},{5,4},{6,7},{7,6},{8,9},{9,8},{10,11... | collective-permute-start | bytes 589832 | tf_op jit(solution)/shard_map/ppermute | solution.py:533
  70.8 0.7 copy-start.11
  71.5 2.1 %collective-permute-start.10 = (bf16[192,512]{1,0:T(8,128)(2,1)}, bf16[192,512]{1,0:T(8,128)(2,1)}, u32[]{:S(2)}, u32[]{:S(2)}) collective-permute-start(bf16[192,512]{1,0:T(8,128)(2,1)} %collective-permute-done.6.own3), channel_id=1, source_target_pairs={{0,1},{1,0},{2,3},{3,2},{4,5},{5,4},{6,7},{7,6},{8,9},{9,8},{10,11... | collective-permute-start | bytes 589832 | tf_op jit(solution)/shard_map/ppermute | solution.py:533
  94.9 0.9 copy-start.1
  95.8 0.6 copy-start.5
  96.4 32.1 %all-to-all-start.2 = ((bf16[16,96,256]{2,1,0:T(8,128)(2,1)}), bf16[16,96,256]{2,1,0:T(8,128)(2,1)S(1)}, u32[]{:S(2)}, u32[]{:S(2)}) async-start(bf16[16,96,256]{2,1,0:T(8,128)(2,1)} %copy-done.1), calls=%async_computation.2 | async-start | bytes 1572864 | tf_op jit(solution)/shard_map/all_to_all | solution.py:625
  102.2 25.5 %collective-permute-start.16 = (bf16[128,2048]{1,0:T(8,128)(2,1)S(1)}, bf16[128,2048]{1,0:T(8,128)(2,1)S(1)}, u32[]{:S(2)}, u32[]{:S(2)}) collective-permute-start(bf16[128,2048]{1,0:T(8,128)(2,1)S(1)} %slice.16), channel_id=1, source_target_pairs={{0,2},{2,4},{4,6},{6,0},{1,3},{3,5},{5,7},{7,1},{8,10},{10,12},{12... | collective-permute-start | bytes 1572872 | tf_op jit(solution)/shard_map/ppermute | solution.py:538
  103.6 24.0 %collective-permute-start.17 = (bf16[128,2048]{1,0:T(8,128)(2,1)S(1)}, bf16[128,2048]{1,0:T(8,128)(2,1)S(1)}, u32[]{:S(2)}, u32[]{:S(2)}) collective-permute-start(bf16[128,2048]{1,0:T(8,128)(2,1)S(1)} %slice.17), channel_id=1, source_target_pairs={{0,6},{2,0},{4,2},{6,4},{1,7},{3,1},{5,3},{7,5},{8,14},{10,8},{12,... | collective-permute-start | bytes 1572872 | tf_op jit(solution)/shard_map/ppermute | solution.py:538
  105.7 15.7 %collective-permute-start.11 = (bf16[8,512]{1,0:T(8,128)(2,1)S(1)}, bf16[8,512]{1,0:T(8,128)(2,1)S(1)}, u32[]{:S(2)}, u32[]{:S(2)}) collective-permute-start(bf16[8,512]{1,0:T(8,128)(2,1)S(1)} %get-tuple-element.35), channel_id=1, source_target_pairs={{0,1},{1,2},{2,3},{3,4},{4,5},{5,6},{6,7},{7,8},{8,9},{9,10},{10,1... | collective-permute-start | bytes 24584 | tf_op jit(solution)/shard_map/ppermute | solution.py:595
  108.9 15.1 %collective-permute-start.12 = (bf16[8,512]{1,0:T(8,128)(2,1)S(1)}, bf16[8,512]{1,0:T(8,128)(2,1)S(1)}, u32[]{:S(2)}, u32[]{:S(2)}) collective-permute-start(bf16[8,512]{1,0:T(8,128)(2,1)S(1)} %get-tuple-element.34), channel_id=1, source_target_pairs={{1,0},{2,1},{3,2},{4,3},{5,4},{6,5},{7,6},{8,7},{9,8},{10,9},{11,1... | collective-permute-start | bytes 24584 | tf_op jit(solution)/shard_map/ppermute | solution.py:598
  121.3 2.7 %copy-start.19 = (bf16[8,512]{1,0:T(8,128)(2,1)}, bf16[8,512]{1,0:T(8,128)(2,1)S(1)}, u32[]{:S(2)}) copy-start(bf16[8,512]{1,0:T(8,128)(2,1)S(1)} %collective-permute-done.11.low) | copy-start | bytes 24580
  124.0 0.6 copy-start.20
  126.3 1.4 collective-permute-start.13
  127.7 0.8 copy-start.2
  128.5 1.0 copy-start.3
  129.5 0.7 copy-start.4
  132.5 8.5 %collective-permute-start.18 = (bf16[48,2048]{1,0:T(8,128)(2,1)S(1)}, bf16[48,2048]{1,0:T(8,128)(2,1)S(1)}, u32[]{:S(2)}, u32[]{:S(2)}) collective-permute-start(bf16[48,2048]{1,0:T(8,128)(2,1)S(1)} %get-tuple-element.29), channel_id=1, source_target_pairs={{0,1},{1,0},{2,3},{3,2},{4,5},{5,4},{6,7},{7,6},{8,9},{9,8},{10,11... | collective-permute-start | bytes 589832 | tf_op jit(solution)/shard_map/ppermute | solution.py:533
  132.9 4.5 %collective-permute-start.19 = (f32[8,384]{1,0:T(8,128)S(1)}, f32[8,384]{1,0:T(8,128)S(1)}, u32[]{:S(2)}, u32[]{:S(2)}) collective-permute-start(f32[8,384]{1,0:T(8,128)S(1)} %get-tuple-element.31), channel_id=1, source_target_pairs={{0,8},{8,16},{16,24},{24,0},{1,9},{9,17},{17,25},{25,1},{2,10},{10... | collective-permute-start | bytes 36872 | tf_op jit(solution)/shard_map/ppermute | solution.py:538
  133.7 4.0 %collective-permute-start.20 = (f32[8,384]{1,0:T(8,128)S(1)}, f32[8,384]{1,0:T(8,128)S(1)}, u32[]{:S(2)}, u32[]{:S(2)}) collective-permute-start(f32[8,384]{1,0:T(8,128)S(1)} %get-tuple-element.32), channel_id=1, source_target_pairs={{0,16},{8,24},{16,0},{24,8},{1,17},{9,25},{17,1},{25,9},{2,18},{10... | collective-permute-start | bytes 36872 | tf_op jit(solution)/shard_map/ppermute | solution.py:538
  136.1 2.8 %collective-permute-start.21 = (f32[8,384]{1,0:T(8,128)S(1)}, f32[8,384]{1,0:T(8,128)S(1)}, u32[]{:S(2)}, u32[]{:S(2)}) collective-permute-start(f32[8,384]{1,0:T(8,128)S(1)} %get-tuple-element.33), channel_id=1, source_target_pairs={{0,24},{8,0},{16,8},{24,16},{1,25},{9,1},{17,9},{25,17},{2,26},{10... | collective-permute-start | bytes 36872 | tf_op jit(solution)/shard_map/ppermute | solution.py:538
  137.4 1.6 %copy-start.16 = (f32[8,384]{1,0:T(8,128)}, f32[8,384]{1,0:T(8,128)S(1)}, u32[]{:S(2)}) copy-start(f32[8,384]{1,0:T(8,128)S(1)} %collective-permute-done.19.b) | copy-start | bytes 36868
  137.8 1.2 copy-start.17
  139.0 0.6 copy-start.18

commit v4 on v3

--- a/solution.py
+++ b/solution.py
@@ -190,22 +190,25 @@
     )
 
 
-def queries_body(own0, own1, own2, own3, two0, two1, two2, two3, wqt, gain, table, out):
+def queries_body(
+    own0, own1, own2, own3, two0, two1, two2, two3, wqt, gain, table, out, lat
+):
     c = lax.axis_index("c")
     z = lax.axis_index("z")
     here = lax.axis_index("x")
     qgain = column(gain)
     own = (own0, own1, own2, own3)
     other = (two0, two1, two2, two3)
+    y = lax.axis_index("y")
     for x in range(NX):
-        mine = own[x][...]
-        twin = other[x][...]
-        rows = []
-        for y in range(NY):
-            piece = slice(y * ROWS, (y + 1) * ROWS)
-            rows.append(jnp.where(c == 0, mine[piece], twin[piece]))
-            rows.append(jnp.where(c == 0, twin[piece], mine[piece]))
-        q = nt(wqt[...], jnp.concatenate(rows, axis=0))
+        for k in range(NY):
+            piece = slice(k * ROWS, (k + 1) * ROWS)
+            at = ((y + NY - k) % NY) * 2 * ROWS
+            first = pl.multiple_of(at + c * ROWS, ROWS)
+            lat[x, pl.ds(first, ROWS), :] = own[x][piece]
+            second = pl.multiple_of(at + (1 - c) * ROWS, ROWS)
+            lat[x, pl.ds(second, ROWS), :] = other[x][piece]
+        q = nt(wqt[...], lat[x])
         block = (here + NX - x) % NX
         place = z * NX + block
         cosine, sine = angles(table, place)
@@ -224,6 +227,7 @@
         in_specs=[vmem()] * 11,
         out_specs=vmem(),
         out_shape=pltpu.VMEM((HEADS, 128, NQ), bf16),
+        scratch_shapes=[pltpu.VMEM((NX, BLOCK, QR), bf16)],
         compiler_params=params(),
         name="queries",
     )(*own, *other, wqt, qgain, table)
@@ -283,7 +287,9 @@
 TILES = HEADS * (NQ // QTILE)
 
 
-def attend_body(kbuf, vbuf, qt, msg, l0, l1, l2, l3, buf0, buf1, acc_s, m_s, logs):
+def attend_body(
+    kbuf, vbuf, qt, out, l0, l1, l2, l3, buf0, buf1, acc_s, m_s, logs, msg, sems
+):
     bufs = (buf0, buf1)
     pairs = [(kbuf, vbuf)]
     sizes = [kbuf.shape[1]]
@@ -369,16 +375,23 @@
         rows = jnp.concatenate(parts, axis=0).T
         for y in range(NY):
             msg[x * NY + y, :, :] = rows[y * 2 * ROWS : (y + 1) * 2 * ROWS]
+        pltpu.make_async_copy(
+            msg.at[x * NY : (x + 1) * NY], out.at[x * NY : (x + 1) * NY], sems.at[x]
+        ).start()
     here = lax.axis_index("x")
     for k, ref in enumerate((l0, l1, l2, l3)):
         ref[...] = logs[(here + k) % NX]
+    for x in range(NX):
+        pltpu.make_async_copy(
+            msg.at[x * NY : (x + 1) * NY], out.at[x * NY : (x + 1) * NY], sems.at[x]
+        ).wait()
 
 
 def attend(kbuf, vbuf, qt):
     return pl.pallas_call(
         attend_body,
         in_specs=[vmem()] * 3,
-        out_specs=(vmem(),) * 5,
+        out_specs=(pl.BlockSpec(memory_space=pl.ANY), *[vmem()] * 4),
         out_shape=(
             jax.ShapeDtypeStruct((NX * NY, 2 * ROWS, MSG), bf16),
             *[jax.ShapeDtypeStruct((8, BLOCK), f32)] * NX,
@@ -389,6 +402,8 @@
             pltpu.VMEM((HEADS, VROWS, NQ), f32),
             pltpu.VMEM((HEADS, 1, NQ), f32),
             pltpu.VMEM((NX, 8, BLOCK), f32),
+            pltpu.VMEM((NX * NY, 2 * ROWS, MSG), bf16),
+            pltpu.SemaphoreType.DMA((NX,)),
         ],
         compiler_params=params(40),
         name="attend",
@@ -468,15 +483,16 @@
     )(own, low, high)
 
 
-def project_body(got, mine, theirs, w0, w1, w3, w2a, w2b, keep, send, wbuf, sems):
+def project_body(got, mine, theirs, *refs):
+    sources = refs[:8]
+    keep, send, wbuf, sems = refs[8:]
     y0 = lax.axis_index("y")
     c = lax.axis_index("c")
-    places = ((w0, 0, 0), (w1, 1, 0), (w3, 2, 0), (w2a, 3, 0), (w2b, 3, 128))
     copies = []
-    for n, (ref, slot, at) in enumerate(places):
-        rows = ref.shape[0]
+    for n, ref in enumerate(sources):
+        at = 128 * (n % 2)
         copies.append(
-            pltpu.make_async_copy(ref, wbuf.at[slot, at : at + rows], sems.at[n])
+            pltpu.make_async_copy(ref, wbuf.at[n // 2, at : at + 128], sems.at[n])
         )
     for copy in copies:
         copy.start()
@@ -514,7 +530,7 @@
 def project(got, mine, theirs, weights):
     return pl.pallas_call(
         project_body,
-        in_specs=[vmem()] * 3 + [pl.BlockSpec(memory_space=pl.ANY)] * 5,
+        in_specs=[vmem()] * 3 + [pl.BlockSpec(memory_space=pl.ANY)] * 8,
         out_specs=(vmem(), vmem()),
         out_shape=(
             pltpu.VMEM((ROWS, WIDTH), f32),
@@ -522,7 +538,7 @@
         ),
         scratch_shapes=[
             pltpu.VMEM((NY, 256, WIDTH), bf16),
-            pltpu.SemaphoreType.DMA((5,)),
+            pltpu.SemaphoreType.DMA((8,)),
         ],
         compiler_params=params(40),
         name="project",
@@ -536,24 +552,6 @@
 def shifted(x, axis, places):
     count = lax.axis_size(axis)
     return lax.ppermute(x, axis, [(i, (i + places) % count) for i in range(count)])
-
-
-def order_body(a, b, c, d, q_out):
-    y = lax.axis_index("y")
-    for k, ref in enumerate((a, b, c, d)):
-        at = pl.multiple_of(((y + NY - k) % NY) * ROWS, ROWS)
-        q_out[pl.ds(at, ROWS), :] = ref[...]
-
-
-def in_order(pieces):
-    return pl.pallas_call(
-        order_body,
-        in_specs=[vmem()] * NY,
-        out_specs=vmem(),
-        out_shape=jax.ShapeDtypeStruct((NY * ROWS, QR), bf16),
-        compiler_params=params(),
-        name="order",
-    )(*pieces)
 
 
 def shards(
@@ -604,17 +602,20 @@
         (pool_scale.astype(f32)[:, None] * w_out_pool.astype(f32)).astype(bf16),
         preferred_element_type=f32,
     ).astype(bf16)
-    w0 = jnp.concatenate([w_out_attn, folded], axis=0)
-    w1 = shifted(w0, "y", 1)
-    w3 = shifted(w0, "y", NY - 1)
-    w1_half, w3_half = lax.optimization_barrier((w1[:128], w3[128:]))
-    w2a = shifted(w1_half, "y", 1)
-    w2b = shifted(w3_half, "y", NY - 1)
+    upper = w_out_attn[:128]
+    lower = jnp.concatenate([w_out_attn[128:], folded], axis=0)
+    upper1 = shifted(upper, "y", 1)
+    lower3 = shifted(lower, "y", NY - 1)
+    lower1 = shifted(lower, "y", 1)
+    upper3 = shifted(upper, "y", NY - 1)
+    upper2 = shifted(upper1, "y", 1)
+    lower2 = shifted(lower3, "y", NY - 1)
+    pieces_w = (upper, lower, upper1, lower1, upper3, lower3, upper2, lower2)
 
     kv = lax.all_to_all(
         jnp.broadcast_to(kv_own[None], (NY, *kv_own.shape)), "y", 0, 0, tiled=True
     )
-    q_side = in_order(pieces)
+    q_side = jnp.concatenate(pieces, axis=0)
     q_own = [q_side] + [shifted(q_side, "x", k) for k in range(1, NX)]
     q_twin = [across(q) for q in q_own]
     kv_twin = across(kv)
@@ -625,7 +626,7 @@
     got = lax.all_to_all(message, ("x", "y"), 0, 0, tiled=True)
     logs = [logs[0]] + [shifted(logs[k], "x", k) for k in range(1, NX)]
     row_logsum = logsums(logs)
-    keep, send = project(got, pool_mine, pool_theirs, (w0, w1, w3, w2a, w2b))
+    keep, send = project(got, pool_mine, pool_theirs, pieces_w)
     received = across(send)
     mixed = (keep + received.astype(f32)).astype(bf16)
     return mixed, row_logsum

time: 143 us -> 158 us (1.10)
  waiting for transfers between devices: 32.8 us -> 41.9 us
  starting transfers between devices: 42.6 us -> 46.5 us
  local copies, waits for them, and re-layouts: 11.9 us -> 15.6 us
    ppermute x1, waiting for transfers between devices: 10.5 us -> 23.4 us  [shards(): lax.ppermute(pool_in[ROWS - 8:], every, [(i, i + 1) for i in range(count...]
    unnamed x45 -> x60, local copies, waits for them, and re-layouts: 8.91 us -> 13.7 us
    ppermute x13 -> x15, waiting for transfers between devices: 9.15 us -> 4.7 us  [shifted(): lax.ppermute(x, axis, [(i, (i + places) % count) for i in range(count)])]
    ppermute x7, starting transfers between devices: 8.61 us -> 11.9 us  [across(): return lax.ppermute(x, 'c', [(0, 1), (1, 0)])]
    ppermute x13 -> x15, starting transfers between devices: 20.1 us -> 22.7 us  [shifted(): lax.ppermute(x, axis, [(i, (i + places) % count) for i in range(count)])]
    pallas_call x2 -> x1, Pallas kernels: 16.9 us -> 16.2 us  [attend(): pl.pallas_call(attend_body, in_specs=[vmem()] * 3, out_specs=(pl.BlockSpe...]
  transfers between devices with their start and end apart: 24 -> 26, of which waited for: 10 -> 7; matrix products, arithmetic and copies ran while one was open for 3% -> 2% of each run, Pallas kernels for 18% -> 16%
where the time goes in v4:
time: 158 us; the launch traced here: 157 us
  starting transfers between devices  46.5 us (29%)
  waiting for transfers between devices  41.9 us (27%)
  Pallas kernels  31.1 us (20%)
  blocking collectives  20 us (13%)
  local copies, waits for them, and re-layouts  15.6 us (10%)
    ppermute x1, waiting for transfers between devices, shards(): lax.ppermute(pool_in[ROWS - 8:], every, [(i, i + 1) for i in range(count...  23.4 us
    ppermute x15, starting transfers between devices, shifted(): lax.ppermute(x, axis, [(i, (i + places) % count) for i in range(count)])  22.7 us
    all_to_all x1, blocking collectives, shards(): lax.all_to_all(kv_all, 'z', 0, 0, tiled=True).reshape(NZ * ROWS, KR + 128)  20 us
    pallas_call x1, Pallas kernels, attend(): pl.pallas_call(attend_body, in_specs=[vmem()] * 3, out_specs=(pl.BlockSpe...  16.2 us
    unnamed x60, local copies, waits for them, and re-layouts  13.7 us
    ppermute x7, starting transfers between devices, across(): return lax.ppermute(x, 'c', [(0, 1), (1, 0)])  11.9 us
    all_to_all x1, waiting for transfers between devices, shards(): lax.all_to_all(jnp.broadcast_to(kv_own[None], (NY, *kv_own.shape)), 'y',...  8.56 us
    ppermute x15, waiting for transfers between devices, shifted(): lax.ppermute(x, axis, [(i, (i + places) % count) for i in range(count)])  4.7 us
  transfers between devices with their start and end apart: 26, of which 7 were waited for; matrix products, arithmetic and copies ran while one was open for 2% of the time, Pallas kernels for 16%

profile of v4, /device:TPU:1, one launch (start us, length us, event | category | flops | bytes accessed | tf_op | source)
XLA Modules:
  0.0 157.0 jit_solution(21866953811158641)
XLA Ops:
  0.6 4.2 %latents.1 = (bf16[48,512]{1,0:T(8,128)(2,1)}, bf16[8,48,384]{2,1,0:T(8,128)(2,1)}, bf16[48,512]{1,0:T(8,128)(2,1)}) custom-call(bf16[48,2048]{1,0:T(8,128)(2,1)} %tok.1, bf16[2048]{0:T(1024)(128)(2,1)} %gain.2, bf16[2048,512]{1,0:T(8,128)(2,1)} %qdw.1, bf16[512]{0:T(512)(128)(2,1)} %qg.1, bf16[2048,256]{1,0:T(8,128)(2,1)} %kdw.1, bf16[256]{0:T(256)(128)(2,1)} %kg.1, ...), custom_call_target="tpu_custom_call" | custom-call | tf_op jit(solution)/shard_map/latents/pallas_call | solution.py:128
  4.8 20.0 %all_to_all.15 = bf16[8,48,384]{2,1,0:T(8,128)(2,1)S(1)} all-to-all(bf16[8,48,384]{2,1,0:T(8,128)(2,1)} %get-tuple-element.16), channel_id=1, replica_groups=mesh['z'=8,'x'=4,'y'=4,'c'=2] {'z'}, dimensions={0} | all-to-all | bytes 589824 | tf_op jit(solution)/shard_map/all_to_all | solution.py:589
  24.8 1.1 broadcast_in_dim.9
  25.9 4.4 %all-to-all-start.1 = ((bf16[4,384,384]{2,1,0:T(8,128)(2,1)}), bf16[4,384,384]{2,1,0:T(8,128)(2,1)}, u32[]{:S(2)}, u32[]{:S(2)}) async-start(bf16[4,384,384]{2,1,0:T(8,128)(2,1)} %broadcast_in_dim.9), calls=%async_computation.1 | async-start | bytes 2359296 | tf_op jit(solution)/shard_map/all_to_all | solution.py:615
  30.4 1.4 collective-permute-start.1
  31.8 2.5 %collective-permute-start.2 = (bf16[48,512]{1,0:T(8,128)(2,1)S(1)}, bf16[48,512]{1,0:T(8,128)(2,1)S(1)}, u32[]{:S(2)}, u32[]{:S(2)}) collective-permute-start(bf16[48,512]{1,0:T(8,128)(2,1)S(1)} %copy-done.21), channel_id=1, source_target_pairs={{0,4},{2,6},{4,0},{6,2},{1,5},{3,7},{5,1},{7,3},{8,12},{10,14},{12... | collective-permute-start | bytes 147464 | tf_op jit(solution)/shard_map/ppermute | solution.py:554
  34.3 1.1 collective-permute-start.3
  35.4 8.6 %all-to-all-done.1.refs_0_ = bf16[4,384,384]{2,1,0:T(8,128)(2,1)} async-done(((bf16[4,384,384]{2,1,0:T(8,128)(2,1)}), bf16[4,384,384]{2,1,0:T(8,128)(2,1)}, u32[]{:S(2)}, u32[]{:S(2)}) %all-to-all-start.1) | async-done | bytes 1179680 | tf_op jit(solution)/shard_map/all_to_all | solution.py:615
  44.0 5.0 %collective-permute-start = (bf16[4,384,384]{2,1,0:T(8,128)(2,1)}, bf16[4,384,384]{2,1,0:T(8,128)(2,1)}, u32[]{:S(2)}, u32[]{:S(2)}) collective-permute-start(bf16[4,384,384]{2,1,0:T(8,128)(2,1)} %all-to-all-done.1.refs_0_), channel_id=1, source_target_pairs={{0,1},{1,0},{2,3},{3,2},{4,5},{5,4},{6,7},{7,6},{8,9},{9,8},{10,11... | collective-permute-start | bytes 3538952 | tf_op jit(solution)/shard_map/ppermute | solution.py:549
  49.0 1.3 collective-permute-start.4
  50.6 2.5 %collective-permute-start.5 = (bf16[192,512]{1,0:T(8,128)(2,1)S(1)}, bf16[192,512]{1,0:T(8,128)(2,1)S(1)}, u32[]{:S(2)}, u32[]{:S(2)}) collective-permute-start(bf16[192,512]{1,0:T(8,128)(2,1)S(1)} %constant_dynamic-update-slice_fusion.own0), channel_id=1, source_target_pairs={{0,16},{8,24},{16,0},{24,8},{1,17},{9,25},{17,1},{25,9},{2,18},{10... | collective-permute-start | bytes 589832 | tf_op jit(solution)/shard_map/ppermute | solution.py:554
  53.2 1.1 collective-permute-start.6
  54.3 1.7 %collective-permute-start.7 = (bf16[192,512]{1,0:T(8,128)(2,1)S(1)}, bf16[192,512]{1,0:T(8,128)(2,1)S(1)}, u32[]{:S(2)}, u32[]{:S(2)}) collective-permute-start(bf16[192,512]{1,0:T(8,128)(2,1)S(1)} %constant_dynamic-update-slice_fusion.own0), channel_id=1, source_target_pairs={{0,1},{1,0},{2,3},{3,2},{4,5},{5,4},{6,7},{7,6},{8,9},{9,8},{10,11... | collective-permute-start | bytes 589832 | tf_op jit(solution)/shard_map/ppermute | solution.py:549
  56.0 2.0 %collective-permute-start.8 = (bf16[192,512]{1,0:T(8,128)(2,1)S(1)}, bf16[192,512]{1,0:T(8,128)(2,1)S(1)}, u32[]{:S(2)}, u32[]{:S(2)}) collective-permute-start(bf16[192,512]{1,0:T(8,128)(2,1)S(1)} %collective-permute-done.4.own1), channel_id=1, source_target_pairs={{0,1},{1,0},{2,3},{3,2},{4,5},{5,4},{6,7},{7,6},{8,9},{9,8},{10,11... | collective-permute-start | bytes 589832 | tf_op jit(solution)/shard_map/ppermute | solution.py:549
  58.1 3.0 %collective-permute-done.5.own2 = bf16[192,512]{1,0:T(8,128)(2,1)S(1)} collective-permute-done((bf16[192,512]{1,0:T(8,128)(2,1)S(1)}, bf16[192,512]{1,0:T(8,128)(2,1)S(1)}, u32[]{:S(2)}, u32[]{:S(2)}) %collective-permute-start.5) | collective-permute-done | bytes 196640 | tf_op jit(solution)/shard_map/ppermute | solution.py:554
  61.1 0.8 collective-permute-start.14
  61.9 1.8 %collective-permute-start.17 = (bf16[128,2048]{1,0:T(8,128)(2,1)S(1)}, bf16[128,2048]{1,0:T(8,128)(2,1)S(1)}, u32[]{:S(2)}, u32[]{:S(2)}) collective-permute-start(bf16[128,2048]{1,0:T(8,128)(2,1)S(1)} %pad_maximum_fusion.refs_1_), channel_id=1, source_target_pairs={{0,6},{2,0},{4,2},{6,4},{1,7},{3,1},{5,3},{7,5},{8,14},{10,8},{12,... | collective-permute-start | bytes 1572872 | tf_op jit(solution)/shard_map/ppermute | solution.py:554
  63.8 2.3 %collective-permute-start.9 = (bf16[192,512]{1,0:T(8,128)(2,1)S(1)}, bf16[192,512]{1,0:T(8,128)(2,1)S(1)}, u32[]{:S(2)}, u32[]{:S(2)}) collective-permute-start(bf16[192,512]{1,0:T(8,128)(2,1)S(1)} %collective-permute-done.5.own2), channel_id=1, source_target_pairs={{0,1},{1,0},{2,3},{3,2},{4,5},{5,4},{6,7},{7,6},{8,9},{9,8},{10,11... | collective-permute-start | bytes 589832 | tf_op jit(solution)/shard_map/ppermute | solution.py:549
  67.4 1.7 %copy.20 = bf16[256,384]{0,1:T(8,128)(2,1)} copy(bf16[256,384]{1,0:T(8,128)(2,1)} %param.27) | data formatting | bytes 393216 | tf_op args[9]
  70.5 2.5 %queries.1.qt = bf16[3,128,1536]{2,1,0:T(8,128)(2,1)S(1)} custom-call(bf16[192,512]{1,0:T(8,128)(2,1)} %copy-done.12, bf16[192,512]{1,0:T(8,128)(2,1)} %copy-done.14, bf16[192,512]{1,0:T(8,128)(2,1)} %copy-done.15, bf16[192,512]{1,0:T(8,128)(2,1)} %copy-done.16, bf16[192,512]{1,0:T(8,128)(2,1)} %copy-done.17, bf16[192,512]{1,0:T(8,128)(2,1)} %copy-done.18, ...), custom_call_target="tpu_custom_call" | custom-call | tf_op jit(solution)/shard_map/queries/pallas_call | solution.py:225
  73.1 3.4 %keys.1 = (bf16[3,3072,128]{2,1,0:T(8,128)(2,1)S(1)}, bf16[3,80,3072]{2,1,0:T(8,128)(2,1)S(1)}) custom-call(bf16[4,384,384]{2,1,0:T(8,128)(2,1)} %all-to-all-done.1.refs_0_, bf16[4,384,384]{2,1,0:T(8,128)(2,1)} %collective-permute-done.refs_1_, bf16[384,256]{1,0:T(8,128)(2,1)} %bitcast.10, bf16[96]{0:T(256)(128)(2,1)} %refs_3_.1, ...), custom_call_target="tpu_custom_call" | custom-call | tf_op jit(solution)/shard_map/keys/pallas_call | solution.py:272
  76.5 16.2 %attend.1 = (bf16[16,96,256]{2,1,0:T(8,128)(2,1)}, f32[8,384]{1,0:T(8,128)S(1)}, f32[8,384]{1,0:T(8,128)S(1)}, f32[8,384]{1,0:T(8,128)S(1)}, f32[8,384]{1,0:T(8,128)S(1)}) custom-call(bf16[3,3072,128]{2,1,0:T(8,128)(2,1)S(1)} %get-tuple-element.17.kbuf, bf16[3,80,3072]{2,1,0:T(8,128)(2,1)S(1)} %get-tuple-element.18.vbuf, bf16[3,128,1536]{2,1,0:T(8,128)(2,1)S(1)} %queries.1.qt), custom_call_target="tpu_custom_call" | custom-call | tf_op jit(solution)/shard_map/attend/pallas_call | solution.py:391
  93.2 3.6 %all-to-all-start.2 = ((bf16[16,96,256]{2,1,0:T(8,128)(2,1)}), bf16[16,96,256]{2,1,0:T(8,128)(2,1)S(1)}, u32[]{:S(2)}, u32[]{:S(2)}) async-start(bf16[16,96,256]{2,1,0:T(8,128)(2,1)} %get-tuple-element.20), calls=%async_computation.2 | async-start | bytes 1572864 | tf_op jit(solution)/shard_map/all_to_all | solution.py:626
  96.9 1.2 collective-permute-start.15
  98.1 1.5 collective-permute-start.16
  99.6 2.7 %collective-permute-start.19 = (bf16[128,2048]{1,0:T(8,128)(2,1)S(1)}, bf16[128,2048]{1,0:T(8,128)(2,1)S(1)}, u32[]{:S(2)}, u32[]{:S(2)}) collective-permute-start(bf16[128,2048]{1,0:T(8,128)(2,1)S(1)} %collective-permute-done.17.refs_5_), channel_id=1, source_target_pairs={{0,6},{2,0},{4,2},{6,4},{1,7},{3,1},{5,3},{7,5},{8,14},{10,8},{12,... | collective-permute-start | bytes 1572872 | tf_op jit(solution)/shard_map/ppermute | solution.py:554
  102.3 0.7 fusion.3
  103.0 1.9 %collective-permute-start.11 = (bf16[8,512]{1,0:T(8,128)(2,1)S(1)}, bf16[8,512]{1,0:T(8,128)(2,1)S(1)}, u32[]{:S(2)}, u32[]{:S(2)}) collective-permute-start(bf16[8,512]{1,0:T(8,128)(2,1)S(1)} %get-tuple-element.31), channel_id=1, source_target_pairs={{0,1},{1,2},{2,3},{3,4},{4,5},{5,6},{6,7},{7,8},{8,9},{9,10},{10,1... | collective-permute-start | bytes 24584 | tf_op jit(solution)/shard_map/ppermute | solution.py:593
  105.0 23.4 %collective-permute-done.11.low = bf16[8,512]{1,0:T(8,128)(2,1)S(1)} collective-permute-done((bf16[8,512]{1,0:T(8,128)(2,1)S(1)}, bf16[8,512]{1,0:T(8,128)(2,1)S(1)}, u32[]{:S(2)}, u32[]{:S(2)}) %collective-permute-start.11) | collective-permute-done | bytes 8224 | tf_op jit(solution)/shard_map/ppermute | solution.py:593
  128.4 1.9 %collective-permute-start.12 = (bf16[8,512]{1,0:T(8,128)(2,1)S(1)}, bf16[8,512]{1,0:T(8,128)(2,1)S(1)}, u32[]{:S(2)}, u32[]{:S(2)}) collective-permute-start(bf16[8,512]{1,0:T(8,128)(2,1)S(1)} %get-tuple-element.30), channel_id=1, source_target_pairs={{1,0},{2,1},{3,2},{4,3},{5,4},{6,5},{7,6},{8,7},{9,8},{10,9},{11,1... | collective-permute-start | bytes 24584 | tf_op jit(solution)/shard_map/ppermute | solution.py:596
  130.3 3.8 %collective-permute-done.12.high = bf16[8,512]{1,0:T(8,128)(2,1)S(1)} collective-permute-done((bf16[8,512]{1,0:T(8,128)(2,1)S(1)}, bf16[8,512]{1,0:T(8,128)(2,1)S(1)}, u32[]{:S(2)}, u32[]{:S(2)}) %collective-permute-start.12) | collective-permute-done | bytes 8224 | tf_op jit(solution)/shard_map/ppermute | solution.py:596
  134.7 1.7 %pooling.1 = (bf16[48,256]{1,0:T(8,128)(2,1)}, bf16[48,256]{1,0:T(8,128)(2,1)}) custom-call(bf16[48,512]{1,0:T(8,128)(2,1)} %get-tuple-element.21.own, bf16[8,512]{1,0:T(8,128)(2,1)} %copy-done.25, bf16[8,512]{1,0:T(8,128)(2,1)} %copy-done.26), custom_call_target="tpu_custom_call" | custom-call | tf_op jit(solution)/shard_map/pooling/pallas_call | solution.py:472
  136.4 1.4 collective-permute-done.13.theirs
  137.8 0.8 copy-done.1
  138.6 0.8 copy-done.3
  139.4 0.8 copy-done.5
  140.2 0.8 copy-done.7
  141.0 1.0 copy-done.2
  142.1 1.0 copy-done.4
  143.1 1.0 copy-done.6
  144.1 1.0 copy-done.8
  145.2 0.7 copy-done.9
  145.9 1.8 %project.1 = (f32[48,2048]{1,0:T(8,128)S(1)}, bf16[48,2048]{1,0:T(8,128)(2,1)S(1)}) custom-call(bf16[16,96,256]{2,1,0:T(8,128)(2,1)S(1)} %all-to-all-done.2.got, bf16[48,256]{1,0:T(8,128)(2,1)S(1)} %copy-done.9, bf16[48,256]{1,0:T(8,128)(2,1)S(1)} %collective-permute-done.13.theirs, bf16[128,2048]{1,0:T(8,128)(2,1)S(1)} %slice.14.refs_0_, ...), custom_call_target="tpu_custom_call" | custom-call | tf_op jit(solution)/shard_map/project/pallas_call | solution.py:531
  148.0 1.0 collective-permute-start.21
  149.0 2.4 %collective-permute-start.22 = (f32[8,384]{1,0:T(8,128)S(1)}, f32[8,384]{1,0:T(8,128)S(1)}, u32[]{:S(2)}, u32[]{:S(2)}) collective-permute-start(f32[8,384]{1,0:T(8,128)S(1)} %get-tuple-element.28), channel_id=1, source_target_pairs={{0,16},{8,24},{16,0},{24,8},{1,17},{9,25},{17,1},{25,9},{2,18},{10... | collective-permute-start | bytes 36872 | tf_op jit(solution)/shard_map/ppermute | solution.py:554
  151.5 1.2 collective-permute-start.23
  153.1 1.2 collective-permute-done.23.d
  154.9 1.4 logsums.1
  (82 shorter events, 6.3 us)
Async XLA Ops:
  0.6 49.7 %copy-start = (bf16[1,64,64]{2,1,0:T(8,128)(2,1)S(1)}, bf16[1,64,64]{2,1,0:T(8,128)(2,1)}, u32[]{:S(2)}) copy-start(bf16[1,64,64]{2,1,0:T(8,128)(2,1)} %param.30) | copy-start | bytes 24580
  25.9 4.5 %copy-start.21 = (bf16[48,512]{1,0:T(8,128)(2,1)S(1)}, bf16[48,512]{1,0:T(8,128)(2,1)}, u32[]{:S(2)}) copy-start(bf16[48,512]{1,0:T(8,128)(2,1)} %get-tuple-element.19) | copy-start | bytes 147460
  25.9 23.0 %copy-start.27 = (bf16[64]{0:T(256)(128)(2,1)S(1)}, bf16[64]{0:T(256)(128)(2,1)}, u32[]{:S(2)}) copy-start(bf16[64]{0:T(256)(128)(2,1)} %param.31) | copy-start | bytes 388
  25.9 24.4 %copy-start.13 = (bf16[64,2048]{1,0:T(8,128)(2,1)S(1)}, bf16[64,2048]{1,0:T(8,128)(2,1)}, u32[]{:S(2)}) copy-start(bf16[64,2048]{1,0:T(8,128)(2,1)} %param.33) | copy-start | bytes 786436
  25.9 32.1 %slice-start = ((bf16[192,2048]{1,0:T(8,128)(2,1)}), bf16[64,2048]{1,0:T(8,128)(2,1)S(1)}, s32[]{:S(2)}) async-start(bf16[192,2048]{1,0:T(8,128)(2,1)} %param.32), calls=%async_computation.3 | async-start | bytes 524288 | tf_op jit(solution)/shard_map/slice | solution.py:606
  25.9 18.0 %all-to-all-start.1 = ((bf16[4,384,384]{2,1,0:T(8,128)(2,1)}), bf16[4,384,384]{2,1,0:T(8,128)(2,1)}, u32[]{:S(2)}, u32[]{:S(2)}) async-start(bf16[4,384,384]{2,1,0:T(8,128)(2,1)} %broadcast_in_dim.9), calls=%async_computation.1 | async-start | bytes 2359296 | tf_op jit(solution)/shard_map/all_to_all | solution.py:615
  30.4 27.7 %copy-start.11 = (bf16[192,2048]{1,0:T(8,128)(2,1)S(1)}, bf16[192,2048]{1,0:T(8,128)(2,1)}, u32[]{:S(2)}) copy-start(bf16[192,2048]{1,0:T(8,128)(2,1)} %param.32) | copy-start | bytes 2359300
  30.4 18.6 %collective-permute-start.1 = (bf16[48,512]{1,0:T(8,128)(2,1)S(1)}, bf16[48,512]{1,0:T(8,128)(2,1)S(1)}, u32[]{:S(2)}, u32[]{:S(2)}) collective-permute-start(bf16[48,512]{1,0:T(8,128)(2,1)S(1)} %copy-done.21), channel_id=1, source_target_pairs={{0,2},{2,4},{4,6},{6,0},{1,3},{3,5},{5,7},{7,1},{8,10},{10,12},{12... | collective-permute-start | bytes 147464 | tf_op jit(solution)/shard_map/ppermute | solution.py:554
  31.8 17.2 %collective-permute-start.2 = (bf16[48,512]{1,0:T(8,128)(2,1)S(1)}, bf16[48,512]{1,0:T(8,128)(2,1)S(1)}, u32[]{:S(2)}, u32[]{:S(2)}) collective-permute-start(bf16[48,512]{1,0:T(8,128)(2,1)S(1)} %copy-done.21), channel_id=1, source_target_pairs={{0,4},{2,6},{4,0},{6,2},{1,5},{3,7},{5,1},{7,3},{8,12},{10,14},{12... | collective-permute-start | bytes 147464 | tf_op jit(solution)/shard_map/ppermute | solution.py:554
  34.3 14.7 %collective-permute-start.3 = (bf16[48,512]{1,0:T(8,128)(2,1)S(1)}, bf16[48,512]{1,0:T(8,128)(2,1)S(1)}, u32[]{:S(2)}, u32[]{:S(2)}) collective-permute-start(bf16[48,512]{1,0:T(8,128)(2,1)S(1)} %copy-done.21), channel_id=1, source_target_pairs={{0,6},{2,0},{4,2},{6,4},{1,7},{3,1},{5,3},{7,5},{8,14},{10,8},{12,... | collective-permute-start | bytes 147464 | tf_op jit(solution)/shard_map/ppermute | solution.py:554
  44.0 29.1 %collective-permute-start = (bf16[4,384,384]{2,1,0:T(8,128)(2,1)}, bf16[4,384,384]{2,1,0:T(8,128)(2,1)}, u32[]{:S(2)}, u32[]{:S(2)}) collective-permute-start(bf16[4,384,384]{2,1,0:T(8,128)(2,1)} %all-to-all-done.1.refs_0_), channel_id=1, source_target_pairs={{0,1},{1,0},{2,3},{3,2},{4,5},{5,4},{6,7},{7,6},{8,9},{9,8},{10,11... | collective-permute-start | bytes 3538952 | tf_op jit(solution)/shard_map/ppermute | solution.py:549
  49.0 20.2 %copy-start.12 = (bf16[192,512]{1,0:T(8,128)(2,1)}, bf16[192,512]{1,0:T(8,128)(2,1)S(1)}, u32[]{:S(2)}) copy-start(bf16[192,512]{1,0:T(8,128)(2,1)S(1)} %constant_dynamic-update-slice_fusion.own0) | copy-start | bytes 589828
  49.0 7.0 %collective-permute-start.4 = (bf16[192,512]{1,0:T(8,128)(2,1)S(1)}, bf16[192,512]{1,0:T(8,128)(2,1)S(1)}, u32[]{:S(2)}, u32[]{:S(2)}) collective-permute-start(bf16[192,512]{1,0:T(8,128)(2,1)S(1)} %constant_dynamic-update-slice_fusion.own0), channel_id=1, source_target_pairs={{0,8},{8,16},{16,24},{24,0},{1,9},{9,17},{17,25},{25,1},{2,10},{10... | collective-permute-start | bytes 589832 | tf_op jit(solution)/shard_map/ppermute | solution.py:554
  50.6 10.5 %collective-permute-start.5 = (bf16[192,512]{1,0:T(8,128)(2,1)S(1)}, bf16[192,512]{1,0:T(8,128)(2,1)S(1)}, u32[]{:S(2)}, u32[]{:S(2)}) collective-permute-start(bf16[192,512]{1,0:T(8,128)(2,1)S(1)} %constant_dynamic-update-slice_fusion.own0), channel_id=1, source_target_pairs={{0,16},{8,24},{16,0},{24,8},{1,17},{9,25},{17,1},{25,9},{2,18},{10... | collective-permute-start | bytes 589832 | tf_op jit(solution)/shard_map/ppermute | solution.py:554
  53.2 8.8 %collective-permute-start.6 = (bf16[192,512]{1,0:T(8,128)(2,1)S(1)}, bf16[192,512]{1,0:T(8,128)(2,1)S(1)}, u32[]{:S(2)}, u32[]{:S(2)}) collective-permute-start(bf16[192,512]{1,0:T(8,128)(2,1)S(1)} %constant_dynamic-update-slice_fusion.own0), channel_id=1, source_target_pairs={{0,24},{8,0},{16,8},{24,16},{1,25},{9,1},{17,9},{25,17},{2,26},{10... | collective-permute-start | bytes 589832 | tf_op jit(solution)/shard_map/ppermute | solution.py:554
  54.3 9.5 %collective-permute-start.7 = (bf16[192,512]{1,0:T(8,128)(2,1)S(1)}, bf16[192,512]{1,0:T(8,128)(2,1)S(1)}, u32[]{:S(2)}, u32[]{:S(2)}) collective-permute-start(bf16[192,512]{1,0:T(8,128)(2,1)S(1)} %constant_dynamic-update-slice_fusion.own0), channel_id=1, source_target_pairs={{0,1},{1,0},{2,3},{3,2},{4,5},{5,4},{6,7},{7,6},{8,9},{9,8},{10,11... | collective-permute-start | bytes 589832 | tf_op jit(solution)/shard_map/ppermute | solution.py:549
  56.0 13.2 %copy-start.14 = (bf16[192,512]{1,0:T(8,128)(2,1)}, bf16[192,512]{1,0:T(8,128)(2,1)S(1)}, u32[]{:S(2)}) copy-start(bf16[192,512]{1,0:T(8,128)(2,1)S(1)} %collective-permute-done.4.own1) | copy-start | bytes 589828
  56.0 10.1 %collective-permute-start.8 = (bf16[192,512]{1,0:T(8,128)(2,1)S(1)}, bf16[192,512]{1,0:T(8,128)(2,1)S(1)}, u32[]{:S(2)}, u32[]{:S(2)}) collective-permute-start(bf16[192,512]{1,0:T(8,128)(2,1)S(1)} %collective-permute-done.4.own1), channel_id=1, source_target_pairs={{0,1},{1,0},{2,3},{3,2},{4,5},{5,4},{6,7},{7,6},{8,9},{9,8},{10,11... | collective-permute-start | bytes 589832 | tf_op jit(solution)/shard_map/ppermute | solution.py:549
  61.1 8.1 %copy-start.15 = (bf16[192,512]{1,0:T(8,128)(2,1)}, bf16[192,512]{1,0:T(8,128)(2,1)S(1)}, u32[]{:S(2)}) copy-start(bf16[192,512]{1,0:T(8,128)(2,1)S(1)} %collective-permute-done.5.own2) | copy-start | bytes 589828
  61.1 38.5 %collective-permute-start.14 = (bf16[128,2048]{1,0:T(8,128)(2,1)S(1)}, bf16[128,2048]{1,0:T(8,128)(2,1)S(1)}, u32[]{:S(2)}, u32[]{:S(2)}) collective-permute-start(bf16[128,2048]{1,0:T(8,128)(2,1)S(1)} %slice.14.refs_0_), channel_id=1, source_target_pairs={{0,2},{2,4},{4,6},{6,0},{1,3},{3,5},{5,7},{7,1},{8,10},{10,12},{12... | collective-permute-start | bytes 1572872 | tf_op jit(solution)/shard_map/ppermute | solution.py:554
  61.9 7.3 %copy-start.16 = (bf16[192,512]{1,0:T(8,128)(2,1)}, bf16[192,512]{1,0:T(8,128)(2,1)S(1)}, u32[]{:S(2)}) copy-start(bf16[192,512]{1,0:T(8,128)(2,1)S(1)} %collective-permute-done.6.own3) | copy-start | bytes 589828
  61.9 37.7 %collective-permute-start.17 = (bf16[128,2048]{1,0:T(8,128)(2,1)S(1)}, bf16[128,2048]{1,0:T(8,128)(2,1)S(1)}, u32[]{:S(2)}, u32[]{:S(2)}) collective-permute-start(bf16[128,2048]{1,0:T(8,128)(2,1)S(1)} %pad_maximum_fusion.refs_1_), channel_id=1, source_target_pairs={{0,6},{2,0},{4,2},{6,4},{1,7},{3,1},{5,3},{7,5},{8,14},{10,8},{12,... | collective-permute-start | bytes 1572872 | tf_op jit(solution)/shard_map/ppermute | solution.py:554
  63.8 2.3 %copy-start.17 = (bf16[192,512]{1,0:T(8,128)(2,1)}, bf16[192,512]{1,0:T(8,128)(2,1)S(1)}, u32[]{:S(2)}) copy-start(bf16[192,512]{1,0:T(8,128)(2,1)S(1)} %collective-permute-done.7.two0) | copy-start | bytes 589828
  63.8 5.4 %collective-permute-start.9 = (bf16[192,512]{1,0:T(8,128)(2,1)S(1)}, bf16[192,512]{1,0:T(8,128)(2,1)S(1)}, u32[]{:S(2)}, u32[]{:S(2)}) collective-permute-start(bf16[192,512]{1,0:T(8,128)(2,1)S(1)} %collective-permute-done.5.own2), channel_id=1, source_target_pairs={{0,1},{1,0},{2,3},{3,2},{4,5},{5,4},{6,7},{7,6},{8,9},{9,8},{10,11... | collective-permute-start | bytes 589832 | tf_op jit(solution)/shard_map/ppermute | solution.py:549
  66.8 2.4 %collective-permute-start.10 = (bf16[192,512]{1,0:T(8,128)(2,1)S(1)}, bf16[192,512]{1,0:T(8,128)(2,1)S(1)}, u32[]{:S(2)}, u32[]{:S(2)}) collective-permute-start(bf16[192,512]{1,0:T(8,128)(2,1)S(1)} %collective-permute-done.6.own3), channel_id=1, source_target_pairs={{0,1},{1,0},{2,3},{3,2},{4,5},{5,4},{6,7},{7,6},{8,9},{9,8},{10,11... | collective-permute-start | bytes 589832 | tf_op jit(solution)/shard_map/ppermute | solution.py:549
  93.2 47.8 %all-to-all-start.2 = ((bf16[16,96,256]{2,1,0:T(8,128)(2,1)}), bf16[16,96,256]{2,1,0:T(8,128)(2,1)S(1)}, u32[]{:S(2)}, u32[]{:S(2)}) async-start(bf16[16,96,256]{2,1,0:T(8,128)(2,1)} %get-tuple-element.20), calls=%async_computation.2 | async-start | bytes 1572864 | tf_op jit(solution)/shard_map/all_to_all | solution.py:626
  96.9 40.9 %collective-permute-start.15 = (bf16[128,2048]{1,0:T(8,128)(2,1)S(1)}, bf16[128,2048]{1,0:T(8,128)(2,1)S(1)}, u32[]{:S(2)}, u32[]{:S(2)}) collective-permute-start(bf16[128,2048]{1,0:T(8,128)(2,1)S(1)} %pad_maximum_fusion.refs_1_), channel_id=1, source_target_pairs={{0,2},{2,4},{4,6},{6,0},{1,3},{3,5},{5,7},{7,1},{8,10},{10,12},{12... | collective-permute-start | bytes 1572872 | tf_op jit(solution)/shard_map/ppermute | solution.py:554
  98.1 40.5 %collective-permute-start.16 = (bf16[128,2048]{1,0:T(8,128)(2,1)S(1)}, bf16[128,2048]{1,0:T(8,128)(2,1)S(1)}, u32[]{:S(2)}, u32[]{:S(2)}) collective-permute-start(bf16[128,2048]{1,0:T(8,128)(2,1)S(1)} %slice.14.refs_0_), channel_id=1, source_target_pairs={{0,6},{2,0},{4,2},{6,4},{1,7},{3,1},{5,3},{7,5},{8,14},{10,8},{12,... | collective-permute-start | bytes 1572872 | tf_op jit(solution)/shard_map/ppermute | solution.py:554
  99.6 39.8 %collective-permute-start.18 = (bf16[128,2048]{1,0:T(8,128)(2,1)S(1)}, bf16[128,2048]{1,0:T(8,128)(2,1)S(1)}, u32[]{:S(2)}, u32[]{:S(2)}) collective-permute-start(bf16[128,2048]{1,0:T(8,128)(2,1)S(1)} %collective-permute-done.14.refs_2_), channel_id=1, source_target_pairs={{0,2},{2,4},{4,6},{6,0},{1,3},{3,5},{5,7},{7,1},{8,10},{10,12},{12... | collective-permute-start | bytes 1572872 | tf_op jit(solution)/shard_map/ppermute | solution.py:554
  99.6 40.6 %collective-permute-start.19 = (bf16[128,2048]{1,0:T(8,128)(2,1)S(1)}, bf16[128,2048]{1,0:T(8,128)(2,1)S(1)}, u32[]{:S(2)}, u32[]{:S(2)}) collective-permute-start(bf16[128,2048]{1,0:T(8,128)(2,1)S(1)} %collective-permute-done.17.refs_5_), channel_id=1, source_target_pairs={{0,6},{2,0},{4,2},{6,4},{1,7},{3,1},{5,3},{7,5},{8,14},{10,8},{12,... | collective-permute-start | bytes 1572872 | tf_op jit(solution)/shard_map/ppermute | solution.py:554
  103.0 25.4 %collective-permute-start.11 = (bf16[8,512]{1,0:T(8,128)(2,1)S(1)}, bf16[8,512]{1,0:T(8,128)(2,1)S(1)}, u32[]{:S(2)}, u32[]{:S(2)}) collective-permute-start(bf16[8,512]{1,0:T(8,128)(2,1)S(1)} %get-tuple-element.31), channel_id=1, source_target_pairs={{0,1},{1,2},{2,3},{3,4},{4,5},{5,6},{6,7},{7,8},{8,9},{9,10},{10,1... | collective-permute-start | bytes 24584 | tf_op jit(solution)/shard_map/ppermute | solution.py:593
  128.4 5.7 %copy-start.25 = (bf16[8,512]{1,0:T(8,128)(2,1)}, bf16[8,512]{1,0:T(8,128)(2,1)S(1)}, u32[]{:S(2)}) copy-start(bf16[8,512]{1,0:T(8,128)(2,1)S(1)} %collective-permute-done.11.low) | copy-start | bytes 24580
  128.4 5.7 %collective-permute-start.12 = (bf16[8,512]{1,0:T(8,128)(2,1)S(1)}, bf16[8,512]{1,0:T(8,128)(2,1)S(1)}, u32[]{:S(2)}, u32[]{:S(2)}) collective-permute-start(bf16[8,512]{1,0:T(8,128)(2,1)S(1)} %get-tuple-element.30), channel_id=1, source_target_pairs={{1,0},{2,1},{3,2},{4,3},{5,4},{6,5},{7,6},{8,7},{9,8},{10,9},{11,1... | collective-permute-start | bytes 24584 | tf_op jit(solution)/shard_map/ppermute | solution.py:596
  136.3 1.4 collective-permute-start.13
  137.8 0.8 copy-start.1
  138.6 0.8 copy-start.3
  139.4 0.8 copy-start.5
  140.2 0.8 copy-start.7
  141.0 1.0 copy-start.2
  142.1 1.0 copy-start.4
  143.1 1.0 copy-start.6
  144.1 1.0 copy-start.8
  147.7 8.6 %collective-permute-start.20 = (bf16[48,2048]{1,0:T(8,128)(2,1)S(1)}, bf16[48,2048]{1,0:T(8,128)(2,1)S(1)}, u32[]{:S(2)}, u32[]{:S(2)}) collective-permute-start(bf16[48,2048]{1,0:T(8,128)(2,1)S(1)} %get-tuple-element.25), channel_id=1, source_target_pairs={{0,1},{1,0},{2,3},{3,2},{4,5},{5,4},{6,7},{7,6},{8,9},{9,8},{10,11... | collective-permute-start | bytes 589832 | tf_op jit(solution)/shard_map/ppermute | solution.py:549
  148.0 4.7 %collective-permute-start.21 = (f32[8,384]{1,0:T(8,128)S(1)}, f32[8,384]{1,0:T(8,128)S(1)}, u32[]{:S(2)}, u32[]{:S(2)}) collective-permute-start(f32[8,384]{1,0:T(8,128)S(1)} %get-tuple-element.27), channel_id=1, source_target_pairs={{0,8},{8,16},{16,24},{24,0},{1,9},{9,17},{17,25},{25,1},{2,10},{10... | collective-permute-start | bytes 36872 | tf_op jit(solution)/shard_map/ppermute | solution.py:554
  149.0 4.0 %collective-permute-start.22 = (f32[8,384]{1,0:T(8,128)S(1)}, f32[8,384]{1,0:T(8,128)S(1)}, u32[]{:S(2)}, u32[]{:S(2)}) collective-permute-start(f32[8,384]{1,0:T(8,128)S(1)} %get-tuple-element.28), channel_id=1, source_target_pairs={{0,16},{8,24},{16,0},{24,8},{1,17},{9,25},{17,1},{25,9},{2,18},{10... | collective-permute-start | bytes 36872 | tf_op jit(solution)/shard_map/ppermute | solution.py:554
  151.5 2.8 %collective-permute-start.23 = (f32[8,384]{1,0:T(8,128)S(1)}, f32[8,384]{1,0:T(8,128)S(1)}, u32[]{:S(2)}, u32[]{:S(2)}) collective-permute-start(f32[8,384]{1,0:T(8,128)S(1)} %get-tuple-element.29), channel_id=1, source_target_pairs={{0,24},{8,0},{16,8},{24,16},{1,25},{9,1},{17,9},{25,17},{2,26},{10... | collective-permute-start | bytes 36872 | tf_op jit(solution)/shard_map/ppermute | solution.py:554
  152.6 1.7 %copy-start.22 = (f32[8,384]{1,0:T(8,128)}, f32[8,384]{1,0:T(8,128)S(1)}, u32[]{:S(2)}) copy-start(f32[8,384]{1,0:T(8,128)S(1)} %collective-permute-done.21.b) | copy-start | bytes 36868
  153.1 1.2 copy-start.23
  (7 other events, 4.6 us)

commit v5 on v4

--- a/solution.py
+++ b/solution.py
@@ -111,14 +111,14 @@
 
         q = norm(aq[...], qg[...])
         kv = norm(ak[...], kg[...])
-        rope = jnp.concatenate(
-            [ar[...].astype(bf16), jnp.zeros((ROWS, 128 - ROT), bf16)], axis=1
-        )
+        groups = [ar[8 * g : 8 * g + 8, :] for g in range(ROWS // 8)]
+        groups.append(jnp.zeros((8, KR - ROT * (ROWS // 8)), f32))
+        rope = jnp.concatenate(groups, axis=1).astype(bf16)
         q_out[...] = q
         pool_out[...] = ap[...].astype(bf16)
         for n in range(NZ):
-            kv_out[n, :, 0:KR] = kv
-            kv_out[n, :, KR:] = rope
+            kv_out[n, 0:ROWS, :] = kv
+            kv_out[n, ROWS:, :] = rope
 
 
 def latents(tok, gain, qdw, qg, kdw, kg, rw, pw):
@@ -140,12 +140,12 @@
         ],
         out_specs=(
             whole(ROWS, QR),
-            whole(NZ, ROWS, KR + 128),
+            whole(NZ, ROWS + 8, KR),
             whole(ROWS, 512),
         ),
         out_shape=(
             jax.ShapeDtypeStruct((ROWS, QR), bf16),
-            jax.ShapeDtypeStruct((NZ, ROWS, KR + 128), bf16),
+            jax.ShapeDtypeStruct((NZ, ROWS + 8, KR), bf16),
             jax.ShapeDtypeStruct((ROWS, 512), bf16),
         ),
         scratch_shapes=[
@@ -191,7 +191,7 @@
 
 
 def queries_body(
-    own0, own1, own2, own3, two0, two1, two2, two3, wqt, gain, table, out, lat
+    early, own0, own1, own2, own3, two0, two1, two2, two3, wqt, gain, table, out, lat
 ):
     c = lax.axis_index("c")
     z = lax.axis_index("z")
@@ -221,16 +221,16 @@
             out[h, :, pl.ds(at, BLOCK)] = v.astype(bf16)
 
 
-def queries(own, other, wqt, qgain, table):
+def queries(early, own, other, wqt, qgain, table):
     return pl.pallas_call(
         queries_body,
-        in_specs=[vmem()] * 11,
+        in_specs=[pl.BlockSpec(memory_space=pl.ANY)] + [vmem()] * 11,
         out_specs=vmem(),
         out_shape=pltpu.VMEM((HEADS, 128, NQ), bf16),
         scratch_shapes=[pltpu.VMEM((NX, BLOCK, QR), bf16)],
         compiler_params=params(),
         name="queries",
-    )(*own, *other, wqt, qgain, table)
+    )(early, *own, *other, wqt, qgain, table)
 
 
 def keys_body(count, *refs):
@@ -239,15 +239,21 @@
     x = lax.axis_index("x")
     kgain = column(gain)
     pick = (
-        lax.broadcasted_iota(jnp.int32, (ROT, 128), 0)
-        == lax.broadcasted_iota(jnp.int32, (ROT, 128), 1)
+        lax.broadcasted_iota(jnp.int32, (ROT, KR), 0)
+        == lax.broadcasted_iota(jnp.int32, (ROT, KR), 1) % ROT
     ).astype(bf16)
+    group = lax.broadcasted_iota(jnp.int32, (8, KR), 1) // ROT
     ones = (lax.broadcasted_iota(jnp.int32, (VROWS - VAL, BLOCK), 0) == 0).astype(bf16)
     blocks = [(own, k, k, c) for k in range(NY)] + [(other, k, k, 1 - c) for k in range(NY)]
     for b, (ref, at, y_from, c_from) in enumerate(blocks):
-        lat = ref[at]
-        kv = nt(wkvt[...], lat[:, :KR])
-        rope = nt(pick, lat[:, KR:])
+        lat, spread = [], []
+        for z in range(NZ):
+            row = z * (ROWS + 8)
+            lat.append(ref[at, row : row + ROWS, :])
+            packed = ref[at, row + ROWS : row + ROWS + 8, :].astype(f32)
+            spread += [jnp.where(group == g, packed, 0.0) for g in range(ROWS // 8)]
+        kv = nt(wkvt[...], jnp.concatenate(lat, axis=0))
+        rope = nt(pick, jnp.concatenate(spread, axis=0).astype(bf16))
         rope_square = jnp.sum(rope * rope, axis=0, keepdims=True)
         place = (x * NY + y_from) * 2 + c_from
         cosine, sine = angles(table, place)
@@ -283,7 +289,7 @@
 
 
 CHUNK = 256
-SUB = 128
+SUB = 256
 TILES = HEADS * (NQ // QTILE)
 
 
@@ -334,9 +340,9 @@
         acc = None
         top = low
         for chunk in chunks:
+            top = score(i + 1, chunk, nxt, top)
             part = weigh(i, chunk, buf, m)
             acc = part if acc is None else acc + part
-            top = score(i + 1, chunk, nxt, top)
         finish(i, m, acc)
         return settle(top)
 
@@ -586,7 +592,7 @@
         w_pool_in,
     )
     pieces = [q_all] + [shifted(q_all, "y", k) for k in range(1, NY)]
-    kv_own = lax.all_to_all(kv_all, "z", 0, 0, tiled=True).reshape(NZ * ROWS, KR + 128)
+    kv_own = lax.all_to_all(kv_all, "z", 0, 0, tiled=True).reshape(NZ * (ROWS + 8), KR)
 
     count = NZ * NX * NY * 2
     every = ("z", "x", "y", "c")
@@ -619,7 +625,7 @@
     q_own = [q_side] + [shifted(q_side, "x", k) for k in range(1, NX)]
     q_twin = [across(q) for q in q_own]
     kv_twin = across(kv)
-    qt = queries(q_own, q_twin, wqt, query_gain, query_tables())
+    qt = queries(wkvt, q_own, q_twin, wqt, query_gain, query_tables())
     pair = keys_values((), kv, kv_twin, wkvt, key_gain, key_tables())
     message, *logs = attend(*pair, qt)
 

time: 158 us -> 153 us (0.968)
  waiting for transfers between devices: 41.9 us -> 39.5 us
  local copies, waits for them, and re-layouts: 15.6 us -> 13.9 us
    all_to_all x1, waiting for transfers between devices: 8.56 us -> 2.15 us  [shards(): lax.all_to_all(jnp.broadcast_to(kv_own[None], (NY, *kv_own.shape)), 'y',...]
    ppermute x15, waiting for transfers between devices: 4.7 us -> 8.96 us  [shifted(): lax.ppermute(x, axis, [(i, (i + places) % count) for i in range(count)])]
  transfers between devices with their start and end apart: 26 -> 26, of which waited for: 7 -> 10; matrix products, arithmetic and copies ran while one was open for 2% -> 1% of each run, Pallas kernels for 16% -> 16%
where the time goes in v5:
time: 153 us; the launch traced here: 151 us
  starting transfers between devices  46.7 us (31%)
  waiting for transfers between devices  39.5 us (26%)
  Pallas kernels  30.5 us (20%)
  blocking collectives  19 us (12%)
  local copies, waits for them, and re-layouts  13.9 us (9%)
    ppermute x15, starting transfers between devices, shifted(): lax.ppermute(x, axis, [(i, (i + places) % count) for i in range(count)])  23 us
    ppermute x1, waiting for transfers between devices, shards(): lax.ppermute(pool_in[ROWS - 8:], every, [(i, i + 1) for i in range(count...  22.7 us
    all_to_all x1, blocking collectives, shards(): lax.all_to_all(kv_all, 'z', 0, 0, tiled=True).reshape(NZ * (ROWS + 8), KR)  19 us
    pallas_call x1, Pallas kernels, attend(): pl.pallas_call(attend_body, in_specs=[vmem()] * 3, out_specs=(pl.BlockSpe...  15.8 us
    unnamed x60, local copies, waits for them, and re-layouts  12.1 us
    ppermute x7, starting transfers between devices, across(): return lax.ppermute(x, 'c', [(0, 1), (1, 0)])  11.5 us
    ppermute x15, waiting for transfers between devices, shifted(): lax.ppermute(x, axis, [(i, (i + places) % count) for i in range(count)])  8.96 us
    all_to_all x1, starting transfers between devices, shards(): lax.all_to_all(jnp.broadcast_to(kv_own[None], (NY, *kv_own.shape)), 'y',...  4.36 us
  transfers between devices with their start and end apart: 26, of which 10 were waited for; matrix products, arithmetic and copies ran while one was open for 1% of the time, Pallas kernels for 16%

profile of v5, /device:TPU:1, one launch (start us, length us, event | category | flops | bytes accessed | tf_op | source)
XLA Modules:
  0.0 151.4 jit_solution(2276651092441636565)
XLA Ops:
  0.6 4.1 %latents.1 = (bf16[48,512]{1,0:T(8,128)(2,1)}, bf16[8,56,256]{2,1,0:T(8,128)(2,1)}, bf16[48,512]{1,0:T(8,128)(2,1)}) custom-call(bf16[48,2048]{1,0:T(8,128)(2,1)} %tok.1, bf16[2048]{0:T(1024)(128)(2,1)} %gain.2, bf16[2048,512]{1,0:T(8,128)(2,1)} %qdw.1, bf16[512]{0:T(512)(128)(2,1)} %qg.1, bf16[2048,256]{1,0:T(8,128)(2,1)} %kdw.1, bf16[256]{0:T(256)(128)(2,1)} %kg.1, ...), custom_call_target="tpu_custom_call" | custom-call | tf_op jit(solution)/shard_map/latents/pallas_call | solution.py:128
  4.8 19.0 %all_to_all.15 = bf16[8,56,256]{2,1,0:T(8,128)(2,1)S(1)} all-to-all(bf16[8,56,256]{2,1,0:T(8,128)(2,1)} %get-tuple-element.16), channel_id=1, replica_groups=mesh['z'=8,'x'=4,'y'=4,'c'=2] {'z'}, dimensions={0} | all-to-all | bytes 458752 | tf_op jit(solution)/shard_map/all_to_all | solution.py:595
  23.8 1.0 broadcast_in_dim.9
  24.8 4.4 %all-to-all-start.1 = ((bf16[4,448,256]{2,1,0:T(8,128)(2,1)}), bf16[4,448,256]{2,1,0:T(8,128)(2,1)}, u32[]{:S(2)}, u32[]{:S(2)}) async-start(bf16[4,448,256]{2,1,0:T(8,128)(2,1)} %broadcast_in_dim.9), calls=%async_computation.1 | async-start | bytes 1835008 | tf_op jit(solution)/shard_map/all_to_all | solution.py:621
  29.2 1.4 collective-permute-start.1
  30.6 2.6 %collective-permute-start.2 = (bf16[48,512]{1,0:T(8,128)(2,1)S(1)}, bf16[48,512]{1,0:T(8,128)(2,1)S(1)}, u32[]{:S(2)}, u32[]{:S(2)}) collective-permute-start(bf16[48,512]{1,0:T(8,128)(2,1)S(1)} %copy-done.21), channel_id=1, source_target_pairs={{0,4},{2,6},{4,0},{6,2},{1,5},{3,7},{5,1},{7,3},{8,12},{10,14},{12... | collective-permute-start | bytes 147464 | tf_op jit(solution)/shard_map/ppermute | solution.py:560
  33.2 1.1 collective-permute-start.3
  34.2 3.7 %collective-permute-done.1 = bf16[48,512]{1,0:T(8,128)(2,1)S(1)} collective-permute-done((bf16[48,512]{1,0:T(8,128)(2,1)S(1)}, bf16[48,512]{1,0:T(8,128)(2,1)S(1)}, u32[]{:S(2)}, u32[]{:S(2)}) %collective-permute-start.1) | collective-permute-done | bytes 49184 | tf_op jit(solution)/shard_map/ppermute | solution.py:560
  38.0 2.1 %all-to-all-done.1.refs_0_ = bf16[4,448,256]{2,1,0:T(8,128)(2,1)} async-done(((bf16[4,448,256]{2,1,0:T(8,128)(2,1)}), bf16[4,448,256]{2,1,0:T(8,128)(2,1)}, u32[]{:S(2)}, u32[]{:S(2)}) %all-to-all-start.1) | async-done | bytes 917536 | tf_op jit(solution)/shard_map/all_to_all | solution.py:621
  40.1 5.1 %collective-permute-start = (bf16[4,448,256]{2,1,0:T(8,128)(2,1)}, bf16[4,448,256]{2,1,0:T(8,128)(2,1)}, u32[]{:S(2)}, u32[]{:S(2)}) collective-permute-start(bf16[4,448,256]{2,1,0:T(8,128)(2,1)} %all-to-all-done.1.refs_0_), channel_id=1, source_target_pairs={{0,1},{1,0},{2,3},{3,2},{4,5},{5,4},{6,7},{7,6},{8,9},{9,8},{10,11... | collective-permute-start | bytes 2752520 | tf_op jit(solution)/shard_map/ppermute | solution.py:555
  45.2 1.3 collective-permute-start.4
  46.8 2.5 %collective-permute-start.5 = (bf16[192,512]{1,0:T(8,128)(2,1)S(1)}, bf16[192,512]{1,0:T(8,128)(2,1)S(1)}, u32[]{:S(2)}, u32[]{:S(2)}) collective-permute-start(bf16[192,512]{1,0:T(8,128)(2,1)S(1)} %constant_dynamic-update-slice_fusion.own0), channel_id=1, source_target_pairs={{0,16},{8,24},{16,0},{24,8},{1,17},{9,25},{17,1},{25,9},{2,18},{10... | collective-permute-start | bytes 589832 | tf_op jit(solution)/shard_map/ppermute | solution.py:560
  49.4 1.2 collective-permute-start.6
  50.5 1.6 %collective-permute-start.7 = (bf16[192,512]{1,0:T(8,128)(2,1)S(1)}, bf16[192,512]{1,0:T(8,128)(2,1)S(1)}, u32[]{:S(2)}, u32[]{:S(2)}) collective-permute-start(bf16[192,512]{1,0:T(8,128)(2,1)S(1)} %constant_dynamic-update-slice_fusion.own0), channel_id=1, source_target_pairs={{0,1},{1,0},{2,3},{3,2},{4,5},{5,4},{6,7},{7,6},{8,9},{9,8},{10,11... | collective-permute-start | bytes 589832 | tf_op jit(solution)/shard_map/ppermute | solution.py:555
  52.3 1.8 %collective-permute-start.8 = (bf16[192,512]{1,0:T(8,128)(2,1)S(1)}, bf16[192,512]{1,0:T(8,128)(2,1)S(1)}, u32[]{:S(2)}, u32[]{:S(2)}) collective-permute-start(bf16[192,512]{1,0:T(8,128)(2,1)S(1)} %collective-permute-done.4.own1), channel_id=1, source_target_pairs={{0,1},{1,0},{2,3},{3,2},{4,5},{5,4},{6,7},{7,6},{8,9},{9,8},{10,11... | collective-permute-start | bytes 589832 | tf_op jit(solution)/shard_map/ppermute | solution.py:555
  54.2 3.3 %collective-permute-done.5.own2 = bf16[192,512]{1,0:T(8,128)(2,1)S(1)} collective-permute-done((bf16[192,512]{1,0:T(8,128)(2,1)S(1)}, bf16[192,512]{1,0:T(8,128)(2,1)S(1)}, u32[]{:S(2)}, u32[]{:S(2)}) %collective-permute-start.5) | collective-permute-done | bytes 196640 | tf_op jit(solution)/shard_map/ppermute | solution.py:560
  57.8 2.3 %collective-permute-start.17 = (bf16[128,2048]{1,0:T(8,128)(2,1)S(1)}, bf16[128,2048]{1,0:T(8,128)(2,1)S(1)}, u32[]{:S(2)}, u32[]{:S(2)}) collective-permute-start(bf16[128,2048]{1,0:T(8,128)(2,1)S(1)} %pad_maximum_fusion.refs_1_), channel_id=1, source_target_pairs={{0,6},{2,0},{4,2},{6,4},{1,7},{3,1},{5,3},{7,5},{8,14},{10,8},{12,... | collective-permute-start | bytes 1572872 | tf_op jit(solution)/shard_map/ppermute | solution.py:560
  60.1 2.2 %collective-permute-start.9 = (bf16[192,512]{1,0:T(8,128)(2,1)S(1)}, bf16[192,512]{1,0:T(8,128)(2,1)S(1)}, u32[]{:S(2)}, u32[]{:S(2)}) collective-permute-start(bf16[192,512]{1,0:T(8,128)(2,1)S(1)} %collective-permute-done.5.own2), channel_id=1, source_target_pairs={{0,1},{1,0},{2,3},{3,2},{4,5},{5,4},{6,7},{7,6},{8,9},{9,8},{10,11... | collective-permute-start | bytes 589832 | tf_op jit(solution)/shard_map/ppermute | solution.py:555
  63.6 0.8 copy.20
  65.6 2.5 %queries.1.qt = bf16[3,128,1536]{2,1,0:T(8,128)(2,1)S(1)} custom-call(bf16[384,256]{1,0:T(8,128)(2,1)} %bitcast.9, bf16[192,512]{1,0:T(8,128)(2,1)} %copy-done.12, bf16[192,512]{1,0:T(8,128)(2,1)} %copy-done.15, bf16[192,512]{1,0:T(8,128)(2,1)} %copy-done.16, bf16[192,512]{1,0:T(8,128)(2,1)} %collective-permute-done.6.own3, bf16[192,512]{1,0:T(8,128)(2,1)} %copy-done.17, ...), custom_call_target="tpu_custom_call" | custom-call | tf_op jit(solution)/shard_map/queries/pallas_call | solution.py:225
  68.1 3.2 %keys.1 = (bf16[3,3072,128]{2,1,0:T(8,128)(2,1)S(1)}, bf16[3,80,3072]{2,1,0:T(8,128)(2,1)S(1)}) custom-call(bf16[4,448,256]{2,1,0:T(8,128)(2,1)} %all-to-all-done.1.refs_0_, bf16[4,448,256]{2,1,0:T(8,128)(2,1)} %collective-permute-done.refs_1_, bf16[384,256]{1,0:T(8,128)(2,1)} %bitcast.10, bf16[96]{0:T(256)(128)(2,1)} %refs_3_.1, ...), custom_call_target="tpu_custom_call" | custom-call | tf_op jit(solution)/shard_map/keys/pallas_call | solution.py:278
  71.4 15.8 %attend.1 = (bf16[16,96,256]{2,1,0:T(8,128)(2,1)}, f32[8,384]{1,0:T(8,128)S(1)}, f32[8,384]{1,0:T(8,128)S(1)}, f32[8,384]{1,0:T(8,128)S(1)}, f32[8,384]{1,0:T(8,128)S(1)}) custom-call(bf16[3,3072,128]{2,1,0:T(8,128)(2,1)S(1)} %get-tuple-element.17.kbuf, bf16[3,80,3072]{2,1,0:T(8,128)(2,1)S(1)} %get-tuple-element.18.vbuf, bf16[3,128,1536]{2,1,0:T(8,128)(2,1)S(1)} %queries.1.qt), custom_call_target="tpu_custom_call" | custom-call | tf_op jit(solution)/shard_map/attend/pallas_call | solution.py:397
  87.7 3.6 %all-to-all-start.2 = ((bf16[16,96,256]{2,1,0:T(8,128)(2,1)}), bf16[16,96,256]{2,1,0:T(8,128)(2,1)S(1)}, u32[]{:S(2)}, u32[]{:S(2)}) async-start(bf16[16,96,256]{2,1,0:T(8,128)(2,1)} %get-tuple-element.20), calls=%async_computation.2 | async-start | bytes 1572864 | tf_op jit(solution)/shard_map/all_to_all | solution.py:632
  91.3 1.2 collective-permute-start.15
  92.6 1.5 collective-permute-start.16
  94.1 2.7 %collective-permute-start.19 = (bf16[128,2048]{1,0:T(8,128)(2,1)S(1)}, bf16[128,2048]{1,0:T(8,128)(2,1)S(1)}, u32[]{:S(2)}, u32[]{:S(2)}) collective-permute-start(bf16[128,2048]{1,0:T(8,128)(2,1)S(1)} %collective-permute-done.17.refs_5_), channel_id=1, source_target_pairs={{0,6},{2,0},{4,2},{6,4},{1,7},{3,1},{5,3},{7,5},{8,14},{10,8},{12,... | collective-permute-start | bytes 1572872 | tf_op jit(solution)/shard_map/ppermute | solution.py:560
  96.8 0.7 fusion.3
  97.5 2.3 %collective-permute-start.11 = (bf16[8,512]{1,0:T(8,128)(2,1)S(1)}, bf16[8,512]{1,0:T(8,128)(2,1)S(1)}, u32[]{:S(2)}, u32[]{:S(2)}) collective-permute-start(bf16[8,512]{1,0:T(8,128)(2,1)S(1)} %get-tuple-element.31), channel_id=1, source_target_pairs={{0,1},{1,2},{2,3},{3,4},{4,5},{5,6},{6,7},{7,8},{8,9},{9,10},{10,1... | collective-permute-start | bytes 24584 | tf_op jit(solution)/shard_map/ppermute | solution.py:599
  99.8 22.7 %collective-permute-done.11.low = bf16[8,512]{1,0:T(8,128)(2,1)S(1)} collective-permute-done((bf16[8,512]{1,0:T(8,128)(2,1)S(1)}, bf16[8,512]{1,0:T(8,128)(2,1)S(1)}, u32[]{:S(2)}, u32[]{:S(2)}) %collective-permute-start.11) | collective-permute-done | bytes 8224 | tf_op jit(solution)/shard_map/ppermute | solution.py:599
  122.5 1.9 %collective-permute-start.12 = (bf16[8,512]{1,0:T(8,128)(2,1)S(1)}, bf16[8,512]{1,0:T(8,128)(2,1)S(1)}, u32[]{:S(2)}, u32[]{:S(2)}) collective-permute-start(bf16[8,512]{1,0:T(8,128)(2,1)S(1)} %get-tuple-element.30), channel_id=1, source_target_pairs={{1,0},{2,1},{3,2},{4,3},{5,4},{6,5},{7,6},{8,7},{9,8},{10,9},{11,1... | collective-permute-start | bytes 24584 | tf_op jit(solution)/shard_map/ppermute | solution.py:602
  124.4 3.8 %collective-permute-done.12.high = bf16[8,512]{1,0:T(8,128)(2,1)S(1)} collective-permute-done((bf16[8,512]{1,0:T(8,128)(2,1)S(1)}, bf16[8,512]{1,0:T(8,128)(2,1)S(1)}, u32[]{:S(2)}, u32[]{:S(2)}) %collective-permute-start.12) | collective-permute-done | bytes 8224 | tf_op jit(solution)/shard_map/ppermute | solution.py:602
  128.8 1.7 %pooling.1 = (bf16[48,256]{1,0:T(8,128)(2,1)}, bf16[48,256]{1,0:T(8,128)(2,1)}) custom-call(bf16[48,512]{1,0:T(8,128)(2,1)} %get-tuple-element.21.own, bf16[8,512]{1,0:T(8,128)(2,1)} %copy-done.25, bf16[8,512]{1,0:T(8,128)(2,1)} %copy-done.26), custom_call_target="tpu_custom_call" | custom-call | tf_op jit(solution)/shard_map/pooling/pallas_call | solution.py:478
  130.5 1.4 collective-permute-done.13.theirs
  131.9 0.8 copy-done.1
  132.7 0.8 copy-done.3
  133.5 0.8 copy-done.5
  134.3 0.8 copy-done.7
  135.1 1.0 copy-done.2
  136.2 1.0 copy-done.4
  137.2 1.0 copy-done.6
  138.3 1.0 copy-done.8
  139.3 0.7 copy-done.9
  140.0 1.8 %project.1 = (f32[48,2048]{1,0:T(8,128)S(1)}, bf16[48,2048]{1,0:T(8,128)(2,1)S(1)}) custom-call(bf16[16,96,256]{2,1,0:T(8,128)(2,1)S(1)} %all-to-all-done.2.got, bf16[48,256]{1,0:T(8,128)(2,1)S(1)} %copy-done.9, bf16[48,256]{1,0:T(8,128)(2,1)S(1)} %collective-permute-done.13.theirs, bf16[128,2048]{1,0:T(8,128)(2,1)S(1)} %slice.14.refs_0_, ...), custom_call_target="tpu_custom_call" | custom-call | tf_op jit(solution)/shard_map/project/pallas_call | solution.py:537
  142.1 1.3 collective-permute-start.21
  143.4 2.5 %collective-permute-start.22 = (f32[8,384]{1,0:T(8,128)S(1)}, f32[8,384]{1,0:T(8,128)S(1)}, u32[]{:S(2)}, u32[]{:S(2)}) collective-permute-start(f32[8,384]{1,0:T(8,128)S(1)} %get-tuple-element.28), channel_id=1, source_target_pairs={{0,16},{8,24},{16,0},{24,8},{1,17},{9,25},{17,1},{25,9},{2,18},{10... | collective-permute-start | bytes 36872 | tf_op jit(solution)/shard_map/ppermute | solution.py:560
  145.9 1.1 collective-permute-start.23
  147.5 1.3 collective-permute-done.23.d
  149.3 1.4 logsums.1
  (82 shorter events, 6.8 us)
Async XLA Ops:
  0.6 45.9 %copy-start = (bf16[1,64,64]{2,1,0:T(8,128)(2,1)S(1)}, bf16[1,64,64]{2,1,0:T(8,128)(2,1)}, u32[]{:S(2)}) copy-start(bf16[1,64,64]{2,1,0:T(8,128)(2,1)} %param.30) | copy-start | bytes 24580
  4.8 24.4 %copy-start.21 = (bf16[48,512]{1,0:T(8,128)(2,1)S(1)}, bf16[48,512]{1,0:T(8,128)(2,1)}, u32[]{:S(2)}) copy-start(bf16[48,512]{1,0:T(8,128)(2,1)} %get-tuple-element.19) | copy-start | bytes 147460
  4.8 29.4 %copy-start.27 = (bf16[64]{0:T(256)(128)(2,1)S(1)}, bf16[64]{0:T(256)(128)(2,1)}, u32[]{:S(2)}) copy-start(bf16[64]{0:T(256)(128)(2,1)} %param.31) | copy-start | bytes 388
  4.8 41.7 %copy-start.13 = (bf16[64,2048]{1,0:T(8,128)(2,1)S(1)}, bf16[64,2048]{1,0:T(8,128)(2,1)}, u32[]{:S(2)}) copy-start(bf16[64,2048]{1,0:T(8,128)(2,1)} %param.33) | copy-start | bytes 786436
  23.8 30.3 %slice-start = ((bf16[192,2048]{1,0:T(8,128)(2,1)}), bf16[64,2048]{1,0:T(8,128)(2,1)S(1)}, s32[]{:S(2)}) async-start(bf16[192,2048]{1,0:T(8,128)(2,1)} %param.32), calls=%async_computation.3 | async-start | bytes 524288 | tf_op jit(solution)/shard_map/slice | solution.py:612
  24.8 29.3 %copy-start.11 = (bf16[192,2048]{1,0:T(8,128)(2,1)S(1)}, bf16[192,2048]{1,0:T(8,128)(2,1)}, u32[]{:S(2)}) copy-start(bf16[192,2048]{1,0:T(8,128)(2,1)} %param.32) | copy-start | bytes 2359300
  24.8 15.3 %all-to-all-start.1 = ((bf16[4,448,256]{2,1,0:T(8,128)(2,1)}), bf16[4,448,256]{2,1,0:T(8,128)(2,1)}, u32[]{:S(2)}, u32[]{:S(2)}) async-start(bf16[4,448,256]{2,1,0:T(8,128)(2,1)} %broadcast_in_dim.9), calls=%async_computation.1 | async-start | bytes 1835008 | tf_op jit(solution)/shard_map/all_to_all | solution.py:621
  29.2 34.5 %copy-start.14 = (bf16[256,384]{1,0:T(8,128)(2,1)S(1)}, bf16[256,384]{1,0:T(8,128)(2,1)}, u32[]{:S(2)}) copy-start(bf16[256,384]{1,0:T(8,128)(2,1)} %param.27) | copy-start | bytes 589828
  29.2 8.8 %collective-permute-start.1 = (bf16[48,512]{1,0:T(8,128)(2,1)S(1)}, bf16[48,512]{1,0:T(8,128)(2,1)S(1)}, u32[]{:S(2)}, u32[]{:S(2)}) collective-permute-start(bf16[48,512]{1,0:T(8,128)(2,1)S(1)} %copy-done.21), channel_id=1, source_target_pairs={{0,2},{2,4},{4,6},{6,0},{1,3},{3,5},{5,7},{7,1},{8,10},{10,12},{12... | collective-permute-start | bytes 147464 | tf_op jit(solution)/shard_map/ppermute | solution.py:560
  30.6 14.6 %collective-permute-start.2 = (bf16[48,512]{1,0:T(8,128)(2,1)S(1)}, bf16[48,512]{1,0:T(8,128)(2,1)S(1)}, u32[]{:S(2)}, u32[]{:S(2)}) collective-permute-start(bf16[48,512]{1,0:T(8,128)(2,1)S(1)} %copy-done.21), channel_id=1, source_target_pairs={{0,4},{2,6},{4,0},{6,2},{1,5},{3,7},{5,1},{7,3},{8,12},{10,14},{12... | collective-permute-start | bytes 147464 | tf_op jit(solution)/shard_map/ppermute | solution.py:560
  33.2 12.1 %collective-permute-start.3 = (bf16[48,512]{1,0:T(8,128)(2,1)S(1)}, bf16[48,512]{1,0:T(8,128)(2,1)S(1)}, u32[]{:S(2)}, u32[]{:S(2)}) collective-permute-start(bf16[48,512]{1,0:T(8,128)(2,1)S(1)} %copy-done.21), channel_id=1, source_target_pairs={{0,6},{2,0},{4,2},{6,4},{1,7},{3,1},{5,3},{7,5},{8,14},{10,8},{12,... | collective-permute-start | bytes 147464 | tf_op jit(solution)/shard_map/ppermute | solution.py:560
  40.1 28.0 %collective-permute-start = (bf16[4,448,256]{2,1,0:T(8,128)(2,1)}, bf16[4,448,256]{2,1,0:T(8,128)(2,1)}, u32[]{:S(2)}, u32[]{:S(2)}) collective-permute-start(bf16[4,448,256]{2,1,0:T(8,128)(2,1)} %all-to-all-done.1.refs_0_), channel_id=1, source_target_pairs={{0,1},{1,0},{2,3},{3,2},{4,5},{5,4},{6,7},{7,6},{8,9},{9,8},{10,11... | collective-permute-start | bytes 2752520 | tf_op jit(solution)/shard_map/ppermute | solution.py:555
  45.2 20.4 %copy-start.12 = (bf16[192,512]{1,0:T(8,128)(2,1)}, bf16[192,512]{1,0:T(8,128)(2,1)S(1)}, u32[]{:S(2)}) copy-start(bf16[192,512]{1,0:T(8,128)(2,1)S(1)} %constant_dynamic-update-slice_fusion.own0) | copy-start | bytes 589828
  45.2 7.0 %collective-permute-start.4 = (bf16[192,512]{1,0:T(8,128)(2,1)S(1)}, bf16[192,512]{1,0:T(8,128)(2,1)S(1)}, u32[]{:S(2)}, u32[]{:S(2)}) collective-permute-start(bf16[192,512]{1,0:T(8,128)(2,1)S(1)} %constant_dynamic-update-slice_fusion.own0), channel_id=1, source_target_pairs={{0,8},{8,16},{16,24},{24,0},{1,9},{9,17},{17,25},{25,1},{2,10},{10... | collective-permute-start | bytes 589832 | tf_op jit(solution)/shard_map/ppermute | solution.py:560
  46.8 10.6 %collective-permute-start.5 = (bf16[192,512]{1,0:T(8,128)(2,1)S(1)}, bf16[192,512]{1,0:T(8,128)(2,1)S(1)}, u32[]{:S(2)}, u32[]{:S(2)}) collective-permute-start(bf16[192,512]{1,0:T(8,128)(2,1)S(1)} %constant_dynamic-update-slice_fusion.own0), channel_id=1, source_target_pairs={{0,16},{8,24},{16,0},{24,8},{1,17},{9,25},{17,1},{25,9},{2,18},{10... | collective-permute-start | bytes 589832 | tf_op jit(solution)/shard_map/ppermute | solution.py:560
  49.4 8.5 %collective-permute-start.6 = (bf16[192,512]{1,0:T(8,128)(2,1)S(1)}, bf16[192,512]{1,0:T(8,128)(2,1)}, u32[]{:S(2)}, u32[]{:S(2)}) collective-permute-start(bf16[192,512]{1,0:T(8,128)(2,1)S(1)} %constant_dynamic-update-slice_fusion.own0), channel_id=1, source_target_pairs={{0,24},{8,0},{16,8},{24,16},{1,25},{9,1},{17,9},{25,17},{2,26},{10... | collective-permute-start | bytes 589832 | tf_op jit(solution)/shard_map/ppermute | solution.py:560
  50.5 9.6 %collective-permute-start.7 = (bf16[192,512]{1,0:T(8,128)(2,1)S(1)}, bf16[192,512]{1,0:T(8,128)(2,1)S(1)}, u32[]{:S(2)}, u32[]{:S(2)}) collective-permute-start(bf16[192,512]{1,0:T(8,128)(2,1)S(1)} %constant_dynamic-update-slice_fusion.own0), channel_id=1, source_target_pairs={{0,1},{1,0},{2,3},{3,2},{4,5},{5,4},{6,7},{7,6},{8,9},{9,8},{10,11... | collective-permute-start | bytes 589832 | tf_op jit(solution)/shard_map/ppermute | solution.py:555
  52.3 12.7 %copy-start.15 = (bf16[192,512]{1,0:T(8,128)(2,1)}, bf16[192,512]{1,0:T(8,128)(2,1)S(1)}, u32[]{:S(2)}) copy-start(bf16[192,512]{1,0:T(8,128)(2,1)S(1)} %collective-permute-done.4.own1) | copy-start | bytes 589828
  52.3 10.0 %collective-permute-start.8 = (bf16[192,512]{1,0:T(8,128)(2,1)S(1)}, bf16[192,512]{1,0:T(8,128)(2,1)S(1)}, u32[]{:S(2)}, u32[]{:S(2)}) collective-permute-start(bf16[192,512]{1,0:T(8,128)(2,1)S(1)} %collective-permute-done.4.own1), channel_id=1, source_target_pairs={{0,1},{1,0},{2,3},{3,2},{4,5},{5,4},{6,7},{7,6},{8,9},{9,8},{10,11... | collective-permute-start | bytes 589832 | tf_op jit(solution)/shard_map/ppermute | solution.py:555
  57.4 7.5 %copy-start.16 = (bf16[192,512]{1,0:T(8,128)(2,1)}, bf16[192,512]{1,0:T(8,128)(2,1)S(1)}, u32[]{:S(2)}) copy-start(bf16[192,512]{1,0:T(8,128)(2,1)S(1)} %collective-permute-done.5.own2) | copy-start | bytes 589828
  57.4 36.7 %collective-permute-start.14 = (bf16[128,2048]{1,0:T(8,128)(2,1)S(1)}, bf16[128,2048]{1,0:T(8,128)(2,1)S(1)}, u32[]{:S(2)}, u32[]{:S(2)}) collective-permute-start(bf16[128,2048]{1,0:T(8,128)(2,1)S(1)} %slice.14.refs_0_), channel_id=1, source_target_pairs={{0,2},{2,4},{4,6},{6,0},{1,3},{3,5},{5,7},{7,1},{8,10},{10,12},{12... | collective-permute-start | bytes 1572872 | tf_op jit(solution)/shard_map/ppermute | solution.py:560
  57.8 36.3 %collective-permute-start.17 = (bf16[128,2048]{1,0:T(8,128)(2,1)S(1)}, bf16[128,2048]{1,0:T(8,128)(2,1)S(1)}, u32[]{:S(2)}, u32[]{:S(2)}) collective-permute-start(bf16[128,2048]{1,0:T(8,128)(2,1)S(1)} %pad_maximum_fusion.refs_1_), channel_id=1, source_target_pairs={{0,6},{2,0},{4,2},{6,4},{1,7},{3,1},{5,3},{7,5},{8,14},{10,8},{12,... | collective-permute-start | bytes 1572872 | tf_op jit(solution)/shard_map/ppermute | solution.py:560
  60.1 2.2 %copy-start.17 = (bf16[192,512]{1,0:T(8,128)(2,1)}, bf16[192,512]{1,0:T(8,128)(2,1)S(1)}, u32[]{:S(2)}) copy-start(bf16[192,512]{1,0:T(8,128)(2,1)S(1)} %collective-permute-done.7.two0) | copy-start | bytes 589828
  60.1 4.3 %collective-permute-start.9 = (bf16[192,512]{1,0:T(8,128)(2,1)S(1)}, bf16[192,512]{1,0:T(8,128)(2,1)S(1)}, u32[]{:S(2)}, u32[]{:S(2)}) collective-permute-start(bf16[192,512]{1,0:T(8,128)(2,1)S(1)} %collective-permute-done.5.own2), channel_id=1, source_target_pairs={{0,1},{1,0},{2,3},{3,2},{4,5},{5,4},{6,7},{7,6},{8,9},{9,8},{10,11... | collective-permute-start | bytes 589832 | tf_op jit(solution)/shard_map/ppermute | solution.py:555
  63.0 2.0 %collective-permute-start.10 = (bf16[192,512]{1,0:T(8,128)(2,1)}, bf16[192,512]{1,0:T(8,128)(2,1)S(1)}, u32[]{:S(2)}, u32[]{:S(2)}) collective-permute-start(bf16[192,512]{1,0:T(8,128)(2,1)} %collective-permute-done.6.own3), channel_id=1, source_target_pairs={{0,1},{1,0},{2,3},{3,2},{4,5},{5,4},{6,7},{7,6},{8,9},{9,8},{10,11... | collective-permute-start | bytes 589832 | tf_op jit(solution)/shard_map/ppermute | solution.py:555
  87.7 47.4 %all-to-all-start.2 = ((bf16[16,96,256]{2,1,0:T(8,128)(2,1)}), bf16[16,96,256]{2,1,0:T(8,128)(2,1)S(1)}, u32[]{:S(2)}, u32[]{:S(2)}) async-start(bf16[16,96,256]{2,1,0:T(8,128)(2,1)} %get-tuple-element.20), calls=%async_computation.2 | async-start | bytes 1572864 | tf_op jit(solution)/shard_map/all_to_all | solution.py:632
  91.3 40.5 %collective-permute-start.15 = (bf16[128,2048]{1,0:T(8,128)(2,1)S(1)}, bf16[128,2048]{1,0:T(8,128)(2,1)S(1)}, u32[]{:S(2)}, u32[]{:S(2)}) collective-permute-start(bf16[128,2048]{1,0:T(8,128)(2,1)S(1)} %pad_maximum_fusion.refs_1_), channel_id=1, source_target_pairs={{0,2},{2,4},{4,6},{6,0},{1,3},{3,5},{5,7},{7,1},{8,10},{10,12},{12... | collective-permute-start | bytes 1572872 | tf_op jit(solution)/shard_map/ppermute | solution.py:560
  92.6 40.1 %collective-permute-start.16 = (bf16[128,2048]{1,0:T(8,128)(2,1)S(1)}, bf16[128,2048]{1,0:T(8,128)(2,1)S(1)}, u32[]{:S(2)}, u32[]{:S(2)}) collective-permute-start(bf16[128,2048]{1,0:T(8,128)(2,1)S(1)} %slice.14.refs_0_), channel_id=1, source_target_pairs={{0,6},{2,0},{4,2},{6,4},{1,7},{3,1},{5,3},{7,5},{8,14},{10,8},{12,... | collective-permute-start | bytes 1572872 | tf_op jit(solution)/shard_map/ppermute | solution.py:560
  94.1 39.4 %collective-permute-start.18 = (bf16[128,2048]{1,0:T(8,128)(2,1)S(1)}, bf16[128,2048]{1,0:T(8,128)(2,1)S(1)}, u32[]{:S(2)}, u32[]{:S(2)}) collective-permute-start(bf16[128,2048]{1,0:T(8,128)(2,1)S(1)} %collective-permute-done.14.refs_2_), channel_id=1, source_target_pairs={{0,2},{2,4},{4,6},{6,0},{1,3},{3,5},{5,7},{7,1},{8,10},{10,12},{12... | collective-permute-start | bytes 1572872 | tf_op jit(solution)/shard_map/ppermute | solution.py:560
  94.1 40.2 %collective-permute-start.19 = (bf16[128,2048]{1,0:T(8,128)(2,1)S(1)}, bf16[128,2048]{1,0:T(8,128)(2,1)S(1)}, u32[]{:S(2)}, u32[]{:S(2)}) collective-permute-start(bf16[128,2048]{1,0:T(8,128)(2,1)S(1)} %collective-permute-done.17.refs_5_), channel_id=1, source_target_pairs={{0,6},{2,0},{4,2},{6,4},{1,7},{3,1},{5,3},{7,5},{8,14},{10,8},{12,... | collective-permute-start | bytes 1572872 | tf_op jit(solution)/shard_map/ppermute | solution.py:560
  97.5 25.0 %collective-permute-start.11 = (bf16[8,512]{1,0:T(8,128)(2,1)S(1)}, bf16[8,512]{1,0:T(8,128)(2,1)S(1)}, u32[]{:S(2)}, u32[]{:S(2)}) collective-permute-start(bf16[8,512]{1,0:T(8,128)(2,1)S(1)} %get-tuple-element.31), channel_id=1, source_target_pairs={{0,1},{1,2},{2,3},{3,4},{4,5},{5,6},{6,7},{7,8},{8,9},{9,10},{10,1... | collective-permute-start | bytes 24584 | tf_op jit(solution)/shard_map/ppermute | solution.py:599
  122.5 5.7 %copy-start.25 = (bf16[8,512]{1,0:T(8,128)(2,1)}, bf16[8,512]{1,0:T(8,128)(2,1)S(1)}, u32[]{:S(2)}) copy-start(bf16[8,512]{1,0:T(8,128)(2,1)S(1)} %collective-permute-done.11.low) | copy-start | bytes 24580
  122.5 5.7 %collective-permute-start.12 = (bf16[8,512]{1,0:T(8,128)(2,1)S(1)}, bf16[8,512]{1,0:T(8,128)(2,1)S(1)}, u32[]{:S(2)}, u32[]{:S(2)}) collective-permute-start(bf16[8,512]{1,0:T(8,128)(2,1)S(1)} %get-tuple-element.30), channel_id=1, source_target_pairs={{1,0},{2,1},{3,2},{4,3},{5,4},{6,5},{7,6},{8,7},{9,8},{10,9},{11,1... | collective-permute-start | bytes 24584 | tf_op jit(solution)/shard_map/ppermute | solution.py:602
  130.5 1.4 collective-permute-start.13
  131.9 0.8 copy-start.1
  132.7 0.8 copy-start.3
  133.5 0.8 copy-start.5
  134.3 0.8 copy-start.7
  135.1 1.0 copy-start.2
  136.2 1.0 copy-start.4
  137.2 1.0 copy-start.6
  138.3 1.0 copy-start.8
  141.9 8.9 %collective-permute-start.20 = (bf16[48,2048]{1,0:T(8,128)(2,1)S(1)}, bf16[48,2048]{1,0:T(8,128)(2,1)S(1)}, u32[]{:S(2)}, u32[]{:S(2)}) collective-permute-start(bf16[48,2048]{1,0:T(8,128)(2,1)S(1)} %get-tuple-element.25), channel_id=1, source_target_pairs={{0,1},{1,0},{2,3},{3,2},{4,5},{5,4},{6,7},{7,6},{8,9},{9,8},{10,11... | collective-permute-start | bytes 589832 | tf_op jit(solution)/shard_map/ppermute | solution.py:555
  142.1 4.9 %collective-permute-start.21 = (f32[8,384]{1,0:T(8,128)S(1)}, f32[8,384]{1,0:T(8,128)S(1)}, u32[]{:S(2)}, u32[]{:S(2)}) collective-permute-start(f32[8,384]{1,0:T(8,128)S(1)} %get-tuple-element.27), channel_id=1, source_target_pairs={{0,8},{8,16},{16,24},{24,0},{1,9},{9,17},{17,25},{25,1},{2,10},{10... | collective-permute-start | bytes 36872 | tf_op jit(solution)/shard_map/ppermute | solution.py:560
  143.4 4.0 %collective-permute-start.22 = (f32[8,384]{1,0:T(8,128)S(1)}, f32[8,384]{1,0:T(8,128)S(1)}, u32[]{:S(2)}, u32[]{:S(2)}) collective-permute-start(f32[8,384]{1,0:T(8,128)S(1)} %get-tuple-element.28), channel_id=1, source_target_pairs={{0,16},{8,24},{16,0},{24,8},{1,17},{9,25},{17,1},{25,9},{2,18},{10... | collective-permute-start | bytes 36872 | tf_op jit(solution)/shard_map/ppermute | solution.py:560
  145.9 2.8 %collective-permute-start.23 = (f32[8,384]{1,0:T(8,128)S(1)}, f32[8,384]{1,0:T(8,128)S(1)}, u32[]{:S(2)}, u32[]{:S(2)}) collective-permute-start(f32[8,384]{1,0:T(8,128)S(1)} %get-tuple-element.29), channel_id=1, source_target_pairs={{0,24},{8,0},{16,8},{24,16},{1,25},{9,1},{17,9},{25,17},{2,26},{10... | collective-permute-start | bytes 36872 | tf_op jit(solution)/shard_map/ppermute | solution.py:560
  147.0 1.7 %copy-start.22 = (f32[8,384]{1,0:T(8,128)}, f32[8,384]{1,0:T(8,128)S(1)}, u32[]{:S(2)}) copy-start(f32[8,384]{1,0:T(8,128)S(1)} %collective-permute-done.21.b) | copy-start | bytes 36868
  147.5 1.3 copy-start.23
  (7 other events, 4.5 us)

commit v6 on v5

--- a/solution.py
+++ b/solution.py
@@ -397,7 +397,7 @@
     return pl.pallas_call(
         attend_body,
         in_specs=[vmem()] * 3,
-        out_specs=(pl.BlockSpec(memory_space=pl.ANY), *[vmem()] * 4),
+        out_specs=(pl.BlockSpec(memory_space=pltpu.MemorySpace.HBM), *[vmem()] * 4),
         out_shape=(
             jax.ShapeDtypeStruct((NX * NY, 2 * ROWS, MSG), bf16),
             *[jax.ShapeDtypeStruct((8, BLOCK), f32)] * NX,
@@ -411,7 +411,7 @@
             pltpu.VMEM((NX * NY, 2 * ROWS, MSG), bf16),
             pltpu.SemaphoreType.DMA((NX,)),
         ],
-        compiler_params=params(40),
+        compiler_params=params(56),
         name="attend",
     )(near(kbuf), near(vbuf), near(qt))
 
@@ -490,15 +490,24 @@
 
 
 def project_body(got, mine, theirs, *refs):
-    sources = refs[:8]
-    keep, send, wbuf, sems = refs[8:]
+    upper, lower, upper1, lower3, onward, backward, keep, send, wbuf, sems = refs
     y0 = lax.axis_index("y")
     c = lax.axis_index("c")
     copies = []
-    for n, ref in enumerate(sources):
-        at = 128 * (n % 2)
+    moves = (
+        (upper, 0, 0),
+        (lower, 0, 1),
+        (upper1, 1, 0),
+        (onward.at[0:128], 1, 1),
+        (backward.at[0:128], 2, 0),
+        (lower3, 2, 1),
+        (onward.at[128:256], 3, 0),
+        (backward.at[128:256], 3, 1),
+    )
+    for n, (ref, slot, part) in enumerate(moves):
+        at = 128 * part
         copies.append(
-            pltpu.make_async_copy(ref, wbuf.at[n // 2, at : at + 128], sems.at[n])
+            pltpu.make_async_copy(ref, wbuf.at[slot, at : at + 128], sems.at[n])
         )
     for copy in copies:
         copy.start()
@@ -536,7 +545,7 @@
 def project(got, mine, theirs, weights):
     return pl.pallas_call(
         project_body,
-        in_specs=[vmem()] * 3 + [pl.BlockSpec(memory_space=pl.ANY)] * 8,
+        in_specs=[vmem()] * 3 + [pl.BlockSpec(memory_space=pl.ANY)] * 6,
         out_specs=(vmem(), vmem()),
         out_shape=(
             pltpu.VMEM((ROWS, WIDTH), f32),
@@ -548,7 +557,7 @@
         ],
         compiler_params=params(40),
         name="project",
-    )(near(got), near(mine), near(theirs), *weights)
+    )(near(got), mine, near(theirs), *weights)
 
 
 def across(x):
@@ -612,11 +621,11 @@
     lower = jnp.concatenate([w_out_attn[128:], folded], axis=0)
     upper1 = shifted(upper, "y", 1)
     lower3 = shifted(lower, "y", NY - 1)
-    lower1 = shifted(lower, "y", 1)
-    upper3 = shifted(upper, "y", NY - 1)
-    upper2 = shifted(upper1, "y", 1)
-    lower2 = shifted(lower3, "y", NY - 1)
-    pieces_w = (upper, lower, upper1, lower1, upper3, lower3, upper2, lower2)
+    onward = jnp.concatenate([lower, upper1], axis=0)
+    backward = jnp.concatenate([upper, lower3], axis=0)
+    onward = shifted(onward, "y", 1)
+    backward = shifted(backward, "y", NY - 1)
+    pieces_w = (upper, lower, upper1, lower3, onward, backward)
 
     kv = lax.all_to_all(
         jnp.broadcast_to(kv_own[None], (NY, *kv_own.shape)), "y", 0, 0, tiled=True

time: 153 us -> 121 us (0.79)
  blocking collectives: 19 us -> 0 us
  waiting for transfers between devices: 39.5 us -> 24.9 us
  local copies, waits for them, and re-layouts: 13.9 us -> 4.65 us
  starting transfers between devices: 46.7 us -> 54.1 us
  other arithmetic: 0.76 us -> 2.91 us
  Pallas kernels: 30.5 us -> 32.1 us
    ppermute x1, waiting for transfers between devices: 22.7 us -> 0.01 us  [shards(): lax.ppermute(pool_in[ROWS - 8:], every, [(i, i + 1) for i in range(count...]
    all_to_all x1 -> x0, blocking collectives: 19 us -> none  [shards(): lax.all_to_all(kv_all, 'z', 0, 0, tiled=True).reshape(NZ * (ROWS + 8), KR)]
    unnamed x60 -> x46, local copies, waits for them, and re-layouts: 12.1 us -> 2.83 us
    all_to_all x0 -> x1, starting transfers between devices: none -> 9 us  [shards(): lax.all_to_all(kv_all, 'z', 0, 0, tiled=True).reshape(NZ * (ROWS + 8), KR)]
    all_to_all x1, waiting for transfers between devices: 2.15 us -> 7.79 us  [shards(): lax.all_to_all(jnp.broadcast_to(kv_own[None], (NY, *kv_own.shape)), 'y',...]
    all_to_all x0 -> x1, waiting for transfers between devices: none -> 4.23 us  [shards(): lax.all_to_all(kv_all, 'z', 0, 0, tiled=True).reshape(NZ * (ROWS + 8), KR)]
    ppermute x7, starting transfers between devices: 11.5 us -> 8.16 us  [across(): return lax.ppermute(x, 'c', [(0, 1), (1, 0)])]
    ppermute x15 -> x13, waiting for transfers between devices: 8.96 us -> 6.69 us  [shifted(): lax.ppermute(x, axis, [(i, (i + places) % count) for i in range(count)])]
  transfers between devices with their start and end apart: 26 -> 25, of which waited for: 10 -> 9; matrix products, arithmetic and copies ran while one was open for 1% -> 4% of each run, Pallas kernels for 16% -> 21%
where the time goes in v6:
time: 121 us; the launch traced here: 120 us
  starting transfers between devices  54.1 us (45%)
  Pallas kernels  32.1 us (27%)
  waiting for transfers between devices  24.9 us (21%)
  local copies, waits for them, and re-layouts  4.65 us (4%)
  other arithmetic  2.91 us (2%)
    ppermute x13, starting transfers between devices, shifted(): lax.ppermute(x, axis, [(i, (i + places) % count) for i in range(count)])  21.9 us
    pallas_call x1, Pallas kernels, attend(): pl.pallas_call(attend_body, in_specs=[vmem()] * 3, out_specs=(pl.BlockSpe...  16.4 us
    all_to_all x1, starting transfers between devices, shards(): lax.all_to_all(kv_all, 'z', 0, 0, tiled=True).reshape(NZ * (ROWS + 8), KR)  9 us
    ppermute x7, starting transfers between devices, across(): return lax.ppermute(x, 'c', [(0, 1), (1, 0)])  8.16 us
    all_to_all x1, waiting for transfers between devices, shards(): lax.all_to_all(jnp.broadcast_to(kv_own[None], (NY, *kv_own.shape)), 'y',...  7.79 us
    ppermute x13, waiting for transfers between devices, shifted(): lax.ppermute(x, axis, [(i, (i + places) % count) for i in range(count)])  6.69 us
    all_to_all x1, starting transfers between devices, shards(): got = lax.all_to_all(message, ('x', 'y'), 0, 0, tiled=True)  4.69 us
    all_to_all x1, starting transfers between devices, shards(): lax.all_to_all(jnp.broadcast_to(kv_own[None], (NY, *kv_own.shape)), 'y',...  4.38 us
  transfers between devices with their start and end apart: 25, of which 9 were waited for; matrix products, arithmetic and copies ran while one was open for 4% of the time, Pallas kernels for 21%

profile of v6, /device:TPU:1, one launch (start us, length us, event | category | flops | bytes accessed | tf_op | source)
XLA Modules:
  0.0 119.8 jit_solution(6016092748517520977)
XLA Ops:
  0.7 4.2 %latents.1 = (bf16[48,512]{1,0:T(8,128)(2,1)}, bf16[8,56,256]{2,1,0:T(8,128)(2,1)}, bf16[48,512]{1,0:T(8,128)(2,1)}) custom-call(bf16[48,2048]{1,0:T(8,128)(2,1)} %tok.1, bf16[2048]{0:T(1024)(128)(2,1)} %gain.2, bf16[2048,512]{1,0:T(8,128)(2,1)} %qdw.1, bf16[512]{0:T(512)(128)(2,1)} %qg.1, bf16[2048,256]{1,0:T(8,128)(2,1)} %kdw.1, bf16[256]{0:T(256)(128)(2,1)} %kg.1, ...), custom_call_target="tpu_custom_call" | custom-call | tf_op jit(solution)/shard_map/latents/pallas_call | solution.py:128
  4.9 9.0 %all-to-all-start = ((bf16[8,56,256]{2,1,0:T(8,128)(2,1)}), bf16[8,56,256]{2,1,0:T(8,128)(2,1)S(1)}, u32[]{:S(2)}, u32[]{:S(2)}) async-start(bf16[8,56,256]{2,1,0:T(8,128)(2,1)} %get-tuple-element.16), calls=%async_computation | async-start | bytes 458752 | tf_op jit(solution)/shard_map/all_to_all | solution.py:604
  13.9 1.4 %collective-permute-start.1 = (bf16[48,512]{1,0:T(8,128)(2,1)}, bf16[48,512]{1,0:T(8,128)(2,1)S(1)}, u32[]{:S(2)}, u32[]{:S(2)}) collective-permute-start(bf16[48,512]{1,0:T(8,128)(2,1)} %get-tuple-element.19), channel_id=1, source_target_pairs={{0,2},{2,4},{4,6},{6,0},{1,3},{3,5},{5,7},{7,1},{8,10},{10,12},{12... | collective-permute-start | bytes 147464 | tf_op jit(solution)/shard_map/ppermute | solution.py:569
  15.3 2.6 %collective-permute-start.2 = (bf16[48,512]{1,0:T(8,128)(2,1)}, bf16[48,512]{1,0:T(8,128)(2,1)S(1)}, u32[]{:S(2)}, u32[]{:S(2)}) collective-permute-start(bf16[48,512]{1,0:T(8,128)(2,1)} %get-tuple-element.19), channel_id=1, source_target_pairs={{0,4},{2,6},{4,0},{6,2},{1,5},{3,7},{5,1},{7,3},{8,12},{10,14},{12... | collective-permute-start | bytes 147464 | tf_op jit(solution)/shard_map/ppermute | solution.py:569
  17.9 1.1 collective-permute-start.3
  19.0 0.5 collective-permute-start.14
  19.5 4.2 %all-to-all-done = bf16[8,56,256]{2,1,0:T(8,128)(2,1)S(1)} async-done(((bf16[8,56,256]{2,1,0:T(8,128)(2,1)}), bf16[8,56,256]{2,1,0:T(8,128)(2,1)S(1)}, u32[]{:S(2)}, u32[]{:S(2)}) %all-to-all-start) | async-done | bytes 229408 | tf_op jit(solution)/shard_map/all_to_all | solution.py:604
  23.7 1.0 broadcast_in_dim.9
  24.8 4.4 %all-to-all-start.1 = ((bf16[4,448,256]{2,1,0:T(8,128)(2,1)}), bf16[4,448,256]{2,1,0:T(8,128)(2,1)}, u32[]{:S(2)}, u32[]{:S(2)}) async-start(bf16[4,448,256]{2,1,0:T(8,128)(2,1)} %broadcast_in_dim.9), calls=%async_computation.1 | async-start | bytes 1835008 | tf_op jit(solution)/shard_map/all_to_all | solution.py:630
  29.5 2.8 %collective-permute-start.15 = (bf16[128,2048]{1,0:T(8,128)(2,1)S(1)}, bf16[128,2048]{1,0:T(8,128)(2,1)S(1)}, u32[]{:S(2)}, u32[]{:S(2)}) collective-permute-start(bf16[128,2048]{1,0:T(8,128)(2,1)S(1)} %pad_maximum_fusion.2.refs_1_), channel_id=1, source_target_pairs={{0,6},{2,0},{4,2},{6,4},{1,7},{3,1},{5,3},{7,5},{8,14},{10,8},{12,... | collective-permute-start | bytes 1572872 | tf_op jit(solution)/shard_map/ppermute | solution.py:569
  32.4 7.8 %all-to-all-done.1.refs_0_ = bf16[4,448,256]{2,1,0:T(8,128)(2,1)} async-done(((bf16[4,448,256]{2,1,0:T(8,128)(2,1)}), bf16[4,448,256]{2,1,0:T(8,128)(2,1)}, u32[]{:S(2)}, u32[]{:S(2)}) %all-to-all-start.1) | async-done | bytes 917536 | tf_op jit(solution)/shard_map/all_to_all | solution.py:630
  40.1 4.4 %collective-permute-start = (bf16[4,448,256]{2,1,0:T(8,128)(2,1)}, bf16[4,448,256]{2,1,0:T(8,128)(2,1)}, u32[]{:S(2)}, u32[]{:S(2)}) collective-permute-start(bf16[4,448,256]{2,1,0:T(8,128)(2,1)} %all-to-all-done.1.refs_0_), channel_id=1, source_target_pairs={{0,1},{1,0},{2,3},{3,2},{4,5},{5,4},{6,7},{7,6},{8,9},{9,8},{10,11... | collective-permute-start | bytes 2752520 | tf_op jit(solution)/shard_map/ppermute | solution.py:564
  44.6 1.3 %collective-permute-start.4 = (bf16[192,512]{1,0:T(8,128)(2,1)S(1)}, bf16[192,512]{1,0:T(8,128)(2,1)S(1)}, u32[]{:S(2)}, u32[]{:S(2)}) collective-permute-start(bf16[192,512]{1,0:T(8,128)(2,1)S(1)} %constant_dynamic-update-slice_fusion.own0), channel_id=1, source_target_pairs={{0,8},{8,16},{16,24},{24,0},{1,9},{9,17},{17,25},{25,1},{2,10},{10... | collective-permute-start | bytes 589832 | tf_op jit(solution)/shard_map/ppermute | solution.py:569
  45.9 2.4 %collective-permute-start.5 = (bf16[192,512]{1,0:T(8,128)(2,1)S(1)}, bf16[192,512]{1,0:T(8,128)(2,1)S(1)}, u32[]{:S(2)}, u32[]{:S(2)}) collective-permute-start(bf16[192,512]{1,0:T(8,128)(2,1)S(1)} %constant_dynamic-update-slice_fusion.own0), channel_id=1, source_target_pairs={{0,16},{8,24},{16,0},{24,8},{1,17},{9,25},{17,1},{25,9},{2,18},{10... | collective-permute-start | bytes 589832 | tf_op jit(solution)/shard_map/ppermute | solution.py:569
  48.3 1.2 collective-permute-start.6
  49.5 1.1 pad_maximum_fusion
  50.6 1.8 %collective-permute-done.4.own1 = bf16[192,512]{1,0:T(8,128)(2,1)S(1)} collective-permute-done((bf16[192,512]{1,0:T(8,128)(2,1)S(1)}, bf16[192,512]{1,0:T(8,128)(2,1)S(1)}, u32[]{:S(2)}, u32[]{:S(2)}) %collective-permute-start.4) | collective-permute-done | bytes 196640 | tf_op jit(solution)/shard_map/ppermute | solution.py:569
  52.3 0.9 collective-permute-start.7
  53.5 1.1 pad_maximum_fusion.1
  54.5 3.0 %collective-permute-done.5.own2 = bf16[192,512]{1,0:T(8,128)(2,1)S(1)} collective-permute-done((bf16[192,512]{1,0:T(8,128)(2,1)S(1)}, bf16[192,512]{1,0:T(8,128)(2,1)S(1)}, u32[]{:S(2)}, u32[]{:S(2)}) %collective-permute-start.5) | collective-permute-done | bytes 196640 | tf_op jit(solution)/shard_map/ppermute | solution.py:569
  57.5 2.6 %collective-permute-start.16 = (bf16[256,2048]{1,0:T(8,128)(2,1)}, bf16[256,2048]{1,0:T(8,128)(2,1)}, u32[]{:S(2)}, u32[]{:S(2)}) collective-permute-start(bf16[256,2048]{1,0:T(8,128)(2,1)} %pad_maximum_fusion), channel_id=1, source_target_pairs={{0,2},{2,4},{4,6},{6,0},{1,3},{3,5},{5,7},{7,1},{8,10},{10,12},{12... | collective-permute-start | bytes 3145736 | tf_op jit(solution)/shard_map/ppermute | solution.py:569
  60.1 0.7 collective-permute-start.17
  60.8 1.1 collective-permute-start.9
  62.0 0.3 collective-permute-start.10
  62.3 0.8 copy.20
  63.1 0.7 collective-permute-done.10.two3
  63.8 2.5 %queries.1.qt = bf16[3,128,1536]{2,1,0:T(8,128)(2,1)S(1)} custom-call(bf16[384,256]{1,0:T(8,128)(2,1)} %bitcast.9, bf16[192,512]{1,0:T(8,128)(2,1)} %copy-done.3, bf16[192,512]{1,0:T(8,128)(2,1)} %copy-done.6, bf16[192,512]{1,0:T(8,128)(2,1)} %copy-done.7, bf16[192,512]{1,0:T(8,128)(2,1)} %collective-permute-done.6.own3, bf16[192,512]{1,0:T(8,128)(2,1)} %copy-done.8, ...), custom_call_target="tpu_custom_call" | custom-call | tf_op jit(solution)/shard_map/queries/pallas_call | solution.py:225
  66.3 3.2 %keys.1 = (bf16[3,3072,128]{2,1,0:T(8,128)(2,1)S(1)}, bf16[3,80,3072]{2,1,0:T(8,128)(2,1)S(1)}) custom-call(bf16[4,448,256]{2,1,0:T(8,128)(2,1)} %all-to-all-done.1.refs_0_, bf16[4,448,256]{2,1,0:T(8,128)(2,1)} %collective-permute-done.refs_1_, bf16[384,256]{1,0:T(8,128)(2,1)} %bitcast.10, bf16[96]{0:T(256)(128)(2,1)} %refs_3_.1, ...), custom_call_target="tpu_custom_call" | custom-call | tf_op jit(solution)/shard_map/keys/pallas_call | solution.py:278
  69.5 16.4 %attend.1 = (bf16[16,96,256]{2,1,0:T(8,128)(2,1)}, f32[8,384]{1,0:T(8,128)}, f32[8,384]{1,0:T(8,128)}, f32[8,384]{1,0:T(8,128)}, f32[8,384]{1,0:T(8,128)}) custom-call(bf16[3,3072,128]{2,1,0:T(8,128)(2,1)S(1)} %get-tuple-element.17.kbuf, bf16[3,80,3072]{2,1,0:T(8,128)(2,1)S(1)} %get-tuple-element.18.vbuf, bf16[3,128,1536]{2,1,0:T(8,128)(2,1)S(1)} %queries.1.qt), custom_call_target="tpu_custom_call" | custom-call | tf_op jit(solution)/shard_map/attend/pallas_call | solution.py:397
  85.9 4.7 %all-to-all-start.2 = ((bf16[16,96,256]{2,1,0:T(8,128)(2,1)}), bf16[16,96,256]{2,1,0:T(8,128)(2,1)S(1)}, u32[]{:S(2)}, u32[]{:S(2)}) async-start(bf16[16,96,256]{2,1,0:T(8,128)(2,1)} %get-tuple-element.20), calls=%async_computation.2 | async-start | bytes 1572864 | tf_op jit(solution)/shard_map/all_to_all | solution.py:641
  90.6 0.7 fusion.3
  91.4 4.0 %collective-permute-start.11 = (bf16[8,512]{1,0:T(8,128)(2,1)S(1)}, bf16[8,512]{1,0:T(8,128)(2,1)S(1)}, u32[]{:S(2)}, u32[]{:S(2)}) collective-permute-start(bf16[8,512]{1,0:T(8,128)(2,1)S(1)} %get-tuple-element.31), channel_id=1, source_target_pairs={{0,1},{1,2},{2,3},{3,4},{4,5},{5,6},{6,7},{7,8},{8,9},{9,10},{10,1... | collective-permute-start | bytes 24584 | tf_op jit(solution)/shard_map/ppermute | solution.py:608
  95.4 1.9 %collective-permute-start.12 = (bf16[8,512]{1,0:T(8,128)(2,1)S(1)}, bf16[8,512]{1,0:T(8,128)(2,1)S(1)}, u32[]{:S(2)}, u32[]{:S(2)}) collective-permute-start(bf16[8,512]{1,0:T(8,128)(2,1)S(1)} %get-tuple-element.30), channel_id=1, source_target_pairs={{1,0},{2,1},{3,2},{4,3},{5,4},{6,5},{7,6},{8,7},{9,8},{10,9},{11,1... | collective-permute-start | bytes 24584 | tf_op jit(solution)/shard_map/ppermute | solution.py:611
  97.3 4.1 %collective-permute-done.12.high = bf16[8,512]{1,0:T(8,128)(2,1)S(1)} collective-permute-done((bf16[8,512]{1,0:T(8,128)(2,1)S(1)}, bf16[8,512]{1,0:T(8,128)(2,1)S(1)}, u32[]{:S(2)}, u32[]{:S(2)}) %collective-permute-start.12) | collective-permute-done | bytes 8224 | tf_op jit(solution)/shard_map/ppermute | solution.py:611
  101.4 0.6 copy-done.16
  102.0 1.7 %pooling.1 = (bf16[48,256]{1,0:T(8,128)(2,1)}, bf16[48,256]{1,0:T(8,128)(2,1)}) custom-call(bf16[48,512]{1,0:T(8,128)(2,1)} %get-tuple-element.21.own, bf16[8,512]{1,0:T(8,128)(2,1)} %copy-done.15, bf16[8,512]{1,0:T(8,128)(2,1)} %copy-done.16), custom_call_target="tpu_custom_call" | custom-call | tf_op jit(solution)/shard_map/pooling/pallas_call | solution.py:478
  103.7 1.4 %collective-permute-done.13.theirs = bf16[48,256]{1,0:T(8,128)(2,1)S(1)} collective-permute-done((bf16[48,256]{1,0:T(8,128)(2,1)}, bf16[48,256]{1,0:T(8,128)(2,1)S(1)}, u32[]{:S(2)}, u32[]{:S(2)}) %collective-permute-start.13) | collective-permute-done | bytes 24608 | tf_op jit(solution)/shard_map/ppermute | solution.py:564
  105.1 0.7 copy-done.1
  105.9 2.7 %project.1 = (f32[48,2048]{1,0:T(8,128)S(1)}, bf16[48,2048]{1,0:T(8,128)(2,1)S(1)}) custom-call(bf16[16,96,256]{2,1,0:T(8,128)(2,1)S(1)} %all-to-all-done.2.got, bf16[48,256]{1,0:T(8,128)(2,1)S(1)} %copy-done.1, bf16[48,256]{1,0:T(8,128)(2,1)S(1)} %collective-permute-done.13.theirs, bf16[128,2048]{1,0:T(8,128)(2,1)S(1)} %slice.14.refs_0_, ...), custom_call_target="tpu_custom_call" | custom-call | tf_op jit(solution)/shard_map/project/pallas_call | solution.py:546
  108.6 1.2 collective-permute-start.18
  109.7 2.1 %collective-permute-start.19 = (f32[8,384]{1,0:T(8,128)S(1)}, f32[8,384]{1,0:T(8,128)S(1)}, u32[]{:S(2)}, u32[]{:S(2)}) collective-permute-start(f32[8,384]{1,0:T(8,128)S(1)} %copy-done.19), channel_id=1, source_target_pairs={{0,8},{8,16},{16,24},{24,0},{1,9},{9,17},{17,25},{25,1},{2,10},{10... | collective-permute-start | bytes 36872 | tf_op jit(solution)/shard_map/ppermute | solution.py:569
  111.9 2.5 %collective-permute-start.20 = (f32[8,384]{1,0:T(8,128)S(1)}, f32[8,384]{1,0:T(8,128)S(1)}, u32[]{:S(2)}, u32[]{:S(2)}) collective-permute-start(f32[8,384]{1,0:T(8,128)S(1)} %copy-done.18), channel_id=1, source_target_pairs={{0,16},{8,24},{16,0},{24,8},{1,17},{9,25},{17,1},{25,9},{2,18},{10... | collective-permute-start | bytes 36872 | tf_op jit(solution)/shard_map/ppermute | solution.py:569
  114.4 0.8 collective-permute-start.21
  115.2 0.7 collective-permute-done.20.c
  115.9 1.2 %collective-permute-done.21.d = f32[8,384]{1,0:T(8,128)S(1)} collective-permute-done((f32[8,384]{1,0:T(8,128)S(1)}, f32[8,384]{1,0:T(8,128)S(1)}, u32[]{:S(2)}, u32[]{:S(2)}) %collective-permute-start.21) | collective-permute-done | bytes 12320 | tf_op jit(solution)/shard_map/ppermute | solution.py:569
  117.1 0.6 copy-done.14
  117.7 1.4 %logsums.1 = f32[3,384]{1,0:T(4,128)} custom-call(f32[8,384]{1,0:T(8,128)} %get-tuple-element.26.a, f32[8,384]{1,0:T(8,128)} %copy-done.12, f32[8,384]{1,0:T(8,128)} %copy-done.13, f32[8,384]{1,0:T(8,128)} %copy-done.14), custom_call_target="tpu_custom_call" | custom-call | tf_op jit(solution)/shard_map/logsums/pallas_call | solution.py:427
  119.1 0.7 add_convert_fusion
  (66 shorter events, 0.8 us)
Async XLA Ops:
  0.6 28.5 %copy-start = (bf16[1,64,64]{2,1,0:T(8,128)(2,1)S(1)}, bf16[1,64,64]{2,1,0:T(8,128)(2,1)}, u32[]{:S(2)}) copy-start(bf16[1,64,64]{2,1,0:T(8,128)(2,1)} %param.30) | copy-start | bytes 24580
  0.6 18.3 %copy-start.2 = (bf16[192,2048]{1,0:T(8,128)(2,1)S(1)}, bf16[192,2048]{1,0:T(8,128)(2,1)}, u32[]{:S(2)}) copy-start(bf16[192,2048]{1,0:T(8,128)(2,1)} %param.32) | copy-start | bytes 2359300
  0.7 18.8 %copy-start.20 = (bf16[64]{0:T(256)(128)(2,1)S(1)}, bf16[64]{0:T(256)(128)(2,1)}, u32[]{:S(2)}) copy-start(bf16[64]{0:T(256)(128)(2,1)} %param.31) | copy-start | bytes 388
  4.9 18.8 %all-to-all-start = ((bf16[8,56,256]{2,1,0:T(8,128)(2,1)}), bf16[8,56,256]{2,1,0:T(8,128)(2,1)S(1)}, u32[]{:S(2)}, u32[]{:S(2)}) async-start(bf16[8,56,256]{2,1,0:T(8,128)(2,1)} %get-tuple-element.16), calls=%async_computation | async-start | bytes 458752 | tf_op jit(solution)/shard_map/all_to_all | solution.py:604
  13.9 15.3 %copy-start.4 = (bf16[64,2048]{1,0:T(8,128)(2,1)S(1)}, bf16[64,2048]{1,0:T(8,128)(2,1)}, u32[]{:S(2)}) copy-start(bf16[64,2048]{1,0:T(8,128)(2,1)} %param.33) | copy-start | bytes 786436
  13.9 18.4 %collective-permute-start.1 = (bf16[48,512]{1,0:T(8,128)(2,1)}, bf16[48,512]{1,0:T(8,128)(2,1)S(1)}, u32[]{:S(2)}, u32[]{:S(2)}) collective-permute-start(bf16[48,512]{1,0:T(8,128)(2,1)} %get-tuple-element.19), channel_id=1, source_target_pairs={{0,2},{2,4},{4,6},{6,0},{1,3},{3,5},{5,7},{7,1},{8,10},{10,12},{12... | collective-permute-start | bytes 147464 | tf_op jit(solution)/shard_map/ppermute | solution.py:569
  15.3 17.1 %collective-permute-start.2 = (bf16[48,512]{1,0:T(8,128)(2,1)}, bf16[48,512]{1,0:T(8,128)(2,1)S(1)}, u32[]{:S(2)}, u32[]{:S(2)}) collective-permute-start(bf16[48,512]{1,0:T(8,128)(2,1)} %get-tuple-element.19), channel_id=1, source_target_pairs={{0,4},{2,6},{4,0},{6,2},{1,5},{3,7},{5,1},{7,3},{8,12},{10,14},{12... | collective-permute-start | bytes 147464 | tf_op jit(solution)/shard_map/ppermute | solution.py:569
  17.9 26.7 %collective-permute-start.3 = (bf16[48,512]{1,0:T(8,128)(2,1)}, bf16[48,512]{1,0:T(8,128)(2,1)S(1)}, u32[]{:S(2)}, u32[]{:S(2)}) collective-permute-start(bf16[48,512]{1,0:T(8,128)(2,1)} %get-tuple-element.19), channel_id=1, source_target_pairs={{0,6},{2,0},{4,2},{6,4},{1,7},{3,1},{5,3},{7,5},{8,14},{10,8},{12,... | collective-permute-start | bytes 147464 | tf_op jit(solution)/shard_map/ppermute | solution.py:569
  19.0 29.3 %collective-permute-start.14 = (bf16[128,2048]{1,0:T(8,128)(2,1)S(1)}, bf16[128,2048]{1,0:T(8,128)(2,1)S(1)}, u32[]{:S(2)}, u32[]{:S(2)}) collective-permute-start(bf16[128,2048]{1,0:T(8,128)(2,1)S(1)} %slice.14.refs_0_), channel_id=1, source_target_pairs={{0,2},{2,4},{4,6},{6,0},{1,3},{3,5},{5,7},{7,1},{8,10},{10,12},{12... | collective-permute-start | bytes 1572872 | tf_op jit(solution)/shard_map/ppermute | solution.py:569
  24.8 7.5 %copy-start.11 = (bf16[48,512]{1,0:T(8,128)(2,1)S(1)}, bf16[48,512]{1,0:T(8,128)(2,1)}, u32[]{:S(2)}) copy-start(bf16[48,512]{1,0:T(8,128)(2,1)} %get-tuple-element.19) | copy-start | bytes 147460
  24.8 15.4 %all-to-all-start.1 = ((bf16[4,448,256]{2,1,0:T(8,128)(2,1)}), bf16[4,448,256]{2,1,0:T(8,128)(2,1)}, u32[]{:S(2)}, u32[]{:S(2)}) async-start(bf16[4,448,256]{2,1,0:T(8,128)(2,1)} %broadcast_in_dim.9), calls=%async_computation.1 | async-start | bytes 1835008 | tf_op jit(solution)/shard_map/all_to_all | solution.py:630
  29.5 23.7 %collective-permute-start.15 = (bf16[128,2048]{1,0:T(8,128)(2,1)S(1)}, bf16[128,2048]{1,0:T(8,128)(2,1)S(1)}, u32[]{:S(2)}, u32[]{:S(2)}) collective-permute-start(bf16[128,2048]{1,0:T(8,128)(2,1)S(1)} %pad_maximum_fusion.2.refs_1_), channel_id=1, source_target_pairs={{0,6},{2,0},{4,2},{6,4},{1,7},{3,1},{5,3},{7,5},{8,14},{10,8},{12,... | collective-permute-start | bytes 1572872 | tf_op jit(solution)/shard_map/ppermute | solution.py:569
  40.1 26.2 %collective-permute-start = (bf16[4,448,256]{2,1,0:T(8,128)(2,1)}, bf16[4,448,256]{2,1,0:T(8,128)(2,1)}, u32[]{:S(2)}, u32[]{:S(2)}) collective-permute-start(bf16[4,448,256]{2,1,0:T(8,128)(2,1)} %all-to-all-done.1.refs_0_), channel_id=1, source_target_pairs={{0,1},{1,0},{2,3},{3,2},{4,5},{5,4},{6,7},{7,6},{8,9},{9,8},{10,11... | collective-permute-start | bytes 2752520 | tf_op jit(solution)/shard_map/ppermute | solution.py:564
  44.6 10.0 %copy-start.3 = (bf16[192,512]{1,0:T(8,128)(2,1)}, bf16[192,512]{1,0:T(8,128)(2,1)S(1)}, u32[]{:S(2)}) copy-start(bf16[192,512]{1,0:T(8,128)(2,1)S(1)} %constant_dynamic-update-slice_fusion.own0) | copy-start | bytes 589828
  44.6 17.7 %copy-start.5 = (bf16[256,384]{1,0:T(8,128)(2,1)S(1)}, bf16[256,384]{1,0:T(8,128)(2,1)}, u32[]{:S(2)}) copy-start(bf16[256,384]{1,0:T(8,128)(2,1)} %param.27) | copy-start | bytes 589828
  44.6 7.7 %collective-permute-start.4 = (bf16[192,512]{1,0:T(8,128)(2,1)S(1)}, bf16[192,512]{1,0:T(8,128)(2,1)S(1)}, u32[]{:S(2)}, u32[]{:S(2)}) collective-permute-start(bf16[192,512]{1,0:T(8,128)(2,1)S(1)} %constant_dynamic-update-slice_fusion.own0), channel_id=1, source_target_pairs={{0,8},{8,16},{16,24},{24,0},{1,9},{9,17},{17,25},{25,1},{2,10},{10... | collective-permute-start | bytes 589832 | tf_op jit(solution)/shard_map/ppermute | solution.py:569
  45.9 11.6 %collective-permute-start.5 = (bf16[192,512]{1,0:T(8,128)(2,1)S(1)}, bf16[192,512]{1,0:T(8,128)(2,1)S(1)}, u32[]{:S(2)}, u32[]{:S(2)}) collective-permute-start(bf16[192,512]{1,0:T(8,128)(2,1)S(1)} %constant_dynamic-update-slice_fusion.own0), channel_id=1, source_target_pairs={{0,16},{8,24},{16,0},{24,8},{1,17},{9,25},{17,1},{25,9},{2,18},{10... | collective-permute-start | bytes 589832 | tf_op jit(solution)/shard_map/ppermute | solution.py:569
  48.3 11.8 %collective-permute-start.6 = (bf16[192,512]{1,0:T(8,128)(2,1)S(1)}, bf16[192,512]{1,0:T(8,128)(2,1)}, u32[]{:S(2)}, u32[]{:S(2)}) collective-permute-start(bf16[192,512]{1,0:T(8,128)(2,1)S(1)} %constant_dynamic-update-slice_fusion.own0), channel_id=1, source_target_pairs={{0,24},{8,0},{16,8},{24,16},{1,25},{9,1},{17,9},{25,17},{2,26},{10... | collective-permute-start | bytes 589832 | tf_op jit(solution)/shard_map/ppermute | solution.py:569
  52.3 11.4 %copy-start.6 = (bf16[192,512]{1,0:T(8,128)(2,1)}, bf16[192,512]{1,0:T(8,128)(2,1)S(1)}, u32[]{:S(2)}) copy-start(bf16[192,512]{1,0:T(8,128)(2,1)S(1)} %collective-permute-done.4.own1) | copy-start | bytes 589828
  52.3 8.5 %collective-permute-start.7 = (bf16[192,512]{1,0:T(8,128)(2,1)S(1)}, bf16[192,512]{1,0:T(8,128)(2,1)S(1)}, u32[]{:S(2)}, u32[]{:S(2)}) collective-permute-start(bf16[192,512]{1,0:T(8,128)(2,1)S(1)} %constant_dynamic-update-slice_fusion.own0), channel_id=1, source_target_pairs={{0,1},{1,0},{2,3},{3,2},{4,5},{5,4},{6,7},{7,6},{8,9},{9,8},{10,11... | collective-permute-start | bytes 589832 | tf_op jit(solution)/shard_map/ppermute | solution.py:564
  53.2 8.7 %collective-permute-start.8 = (bf16[192,512]{1,0:T(8,128)(2,1)S(1)}, bf16[192,512]{1,0:T(8,128)(2,1)S(1)}, u32[]{:S(2)}, u32[]{:S(2)}) collective-permute-start(bf16[192,512]{1,0:T(8,128)(2,1)S(1)} %collective-permute-done.4.own1), channel_id=1, source_target_pairs={{0,1},{1,0},{2,3},{3,2},{4,5},{5,4},{6,7},{7,6},{8,9},{9,8},{10,11... | collective-permute-start | bytes 589832 | tf_op jit(solution)/shard_map/ppermute | solution.py:564
  57.5 6.2 %copy-start.7 = (bf16[192,512]{1,0:T(8,128)(2,1)}, bf16[192,512]{1,0:T(8,128)(2,1)S(1)}, u32[]{:S(2)}) copy-start(bf16[192,512]{1,0:T(8,128)(2,1)S(1)} %collective-permute-done.5.own2) | copy-start | bytes 589828
  57.5 47.6 %collective-permute-start.16 = (bf16[256,2048]{1,0:T(8,128)(2,1)}, bf16[256,2048]{1,0:T(8,128)(2,1)}, u32[]{:S(2)}, u32[]{:S(2)}) collective-permute-start(bf16[256,2048]{1,0:T(8,128)(2,1)} %pad_maximum_fusion), channel_id=1, source_target_pairs={{0,2},{2,4},{4,6},{6,0},{1,3},{3,5},{5,7},{7,1},{8,10},{10,12},{12... | collective-permute-start | bytes 3145736 | tf_op jit(solution)/shard_map/ppermute | solution.py:569
  60.1 45.0 %collective-permute-start.17 = (bf16[256,2048]{1,0:T(8,128)(2,1)}, bf16[256,2048]{1,0:T(8,128)(2,1)}, u32[]{:S(2)}, u32[]{:S(2)}) collective-permute-start(bf16[256,2048]{1,0:T(8,128)(2,1)} %pad_maximum_fusion.1), channel_id=1, source_target_pairs={{0,6},{2,0},{4,2},{6,4},{1,7},{3,1},{5,3},{7,5},{8,14},{10,8},{12,... | collective-permute-start | bytes 3145736 | tf_op jit(solution)/shard_map/ppermute | solution.py:569
  60.8 2.9 %copy-start.8 = (bf16[192,512]{1,0:T(8,128)(2,1)}, bf16[192,512]{1,0:T(8,128)(2,1)S(1)}, u32[]{:S(2)}) copy-start(bf16[192,512]{1,0:T(8,128)(2,1)S(1)} %collective-permute-done.7.two0) | copy-start | bytes 589828
  60.8 2.3 %collective-permute-start.9 = (bf16[192,512]{1,0:T(8,128)(2,1)S(1)}, bf16[192,512]{1,0:T(8,128)(2,1)S(1)}, u32[]{:S(2)}, u32[]{:S(2)}) collective-permute-start(bf16[192,512]{1,0:T(8,128)(2,1)S(1)} %collective-permute-done.5.own2), channel_id=1, source_target_pairs={{0,1},{1,0},{2,3},{3,2},{4,5},{5,4},{6,7},{7,6},{8,9},{9,8},{10,11... | collective-permute-start | bytes 589832 | tf_op jit(solution)/shard_map/ppermute | solution.py:564
  62.0 1.8 %copy-start.9 = (bf16[192,512]{1,0:T(8,128)(2,1)}, bf16[192,512]{1,0:T(8,128)(2,1)S(1)}, u32[]{:S(2)}) copy-start(bf16[192,512]{1,0:T(8,128)(2,1)S(1)} %collective-permute-done.8.two1) | copy-start | bytes 589828
  62.0 1.8 %collective-permute-start.10 = (bf16[192,512]{1,0:T(8,128)(2,1)}, bf16[192,512]{1,0:T(8,128)(2,1)}, u32[]{:S(2)}, u32[]{:S(2)}) collective-permute-start(bf16[192,512]{1,0:T(8,128)(2,1)} %collective-permute-done.6.own3), channel_id=1, source_target_pairs={{0,1},{1,0},{2,3},{3,2},{4,5},{5,4},{6,7},{7,6},{8,9},{9,8},{10,11... | collective-permute-start | bytes 589832 | tf_op jit(solution)/shard_map/ppermute | solution.py:564
  63.1 0.7 copy-start.10
  85.9 19.2 %all-to-all-start.2 = ((bf16[16,96,256]{2,1,0:T(8,128)(2,1)}), bf16[16,96,256]{2,1,0:T(8,128)(2,1)S(1)}, u32[]{:S(2)}, u32[]{:S(2)}) async-start(bf16[16,96,256]{2,1,0:T(8,128)(2,1)} %get-tuple-element.20), calls=%async_computation.2 | async-start | bytes 1572864 | tf_op jit(solution)/shard_map/all_to_all | solution.py:641
  91.4 5.9 %collective-permute-start.11 = (bf16[8,512]{1,0:T(8,128)(2,1)S(1)}, bf16[8,512]{1,0:T(8,128)(2,1)S(1)}, u32[]{:S(2)}, u32[]{:S(2)}) collective-permute-start(bf16[8,512]{1,0:T(8,128)(2,1)S(1)} %get-tuple-element.31), channel_id=1, source_target_pairs={{0,1},{1,2},{2,3},{3,4},{4,5},{5,6},{6,7},{7,8},{8,9},{9,10},{10,1... | collective-permute-start | bytes 24584 | tf_op jit(solution)/shard_map/ppermute | solution.py:608
  95.4 6.1 %collective-permute-start.12 = (bf16[8,512]{1,0:T(8,128)(2,1)S(1)}, bf16[8,512]{1,0:T(8,128)(2,1)S(1)}, u32[]{:S(2)}, u32[]{:S(2)}) collective-permute-start(bf16[8,512]{1,0:T(8,128)(2,1)S(1)} %get-tuple-element.30), channel_id=1, source_target_pairs={{1,0},{2,1},{3,2},{4,3},{5,4},{6,5},{7,6},{8,7},{9,8},{10,9},{11,1... | collective-permute-start | bytes 24584 | tf_op jit(solution)/shard_map/ppermute | solution.py:611
  97.3 4.1 %copy-start.15 = (bf16[8,512]{1,0:T(8,128)(2,1)}, bf16[8,512]{1,0:T(8,128)(2,1)S(1)}, u32[]{:S(2)}) copy-start(bf16[8,512]{1,0:T(8,128)(2,1)S(1)} %collective-permute-done.11.low) | copy-start | bytes 24580
  101.4 0.6 copy-start.16
  103.7 1.4 %collective-permute-start.13 = (bf16[48,256]{1,0:T(8,128)(2,1)}, bf16[48,256]{1,0:T(8,128)(2,1)S(1)}, u32[]{:S(2)}, u32[]{:S(2)}) collective-permute-start(bf16[48,256]{1,0:T(8,128)(2,1)} %get-tuple-element.23), channel_id=1, source_target_pairs={{0,1},{1,0},{2,3},{3,2},{4,5},{5,4},{6,7},{7,6},{8,9},{9,8},{10,11... | collective-permute-start | bytes 73736 | tf_op jit(solution)/shard_map/ppermute | solution.py:564
  105.1 0.7 copy-start.1
  105.9 3.9 %copy-start.19 = (f32[8,384]{1,0:T(8,128)S(1)}, f32[8,384]{1,0:T(8,128)}, u32[]{:S(2)}) copy-start(f32[8,384]{1,0:T(8,128)} %get-tuple-element.27) | copy-start | bytes 36868
  105.9 6.0 %copy-start.18 = (f32[8,384]{1,0:T(8,128)S(1)}, f32[8,384]{1,0:T(8,128)}, u32[]{:S(2)}) copy-start(f32[8,384]{1,0:T(8,128)} %get-tuple-element.28) | copy-start | bytes 36868
  105.9 8.5 %copy-start.17 = (f32[8,384]{1,0:T(8,128)S(1)}, f32[8,384]{1,0:T(8,128)}, u32[]{:S(2)}) copy-start(f32[8,384]{1,0:T(8,128)} %get-tuple-element.29) | copy-start | bytes 36868
  108.6 10.5 %collective-permute-start.18 = (bf16[48,2048]{1,0:T(8,128)(2,1)S(1)}, bf16[48,2048]{1,0:T(8,128)(2,1)S(1)}, u32[]{:S(2)}, u32[]{:S(2)}) collective-permute-start(bf16[48,2048]{1,0:T(8,128)(2,1)S(1)} %get-tuple-element.25), channel_id=1, source_target_pairs={{0,1},{1,0},{2,3},{3,2},{4,5},{5,4},{6,7},{7,6},{8,9},{9,8},{10,11... | collective-permute-start | bytes 589832 | tf_op jit(solution)/shard_map/ppermute | solution.py:564
  109.7 5.5 %collective-permute-start.19 = (f32[8,384]{1,0:T(8,128)S(1)}, f32[8,384]{1,0:T(8,128)S(1)}, u32[]{:S(2)}, u32[]{:S(2)}) collective-permute-start(f32[8,384]{1,0:T(8,128)S(1)} %copy-done.19), channel_id=1, source_target_pairs={{0,8},{8,16},{16,24},{24,0},{1,9},{9,17},{17,25},{25,1},{2,10},{10... | collective-permute-start | bytes 36872 | tf_op jit(solution)/shard_map/ppermute | solution.py:569
  111.9 4.0 %collective-permute-start.20 = (f32[8,384]{1,0:T(8,128)S(1)}, f32[8,384]{1,0:T(8,128)S(1)}, u32[]{:S(2)}, u32[]{:S(2)}) collective-permute-start(f32[8,384]{1,0:T(8,128)S(1)} %copy-done.18), channel_id=1, source_target_pairs={{0,16},{8,24},{16,0},{24,8},{1,17},{9,25},{17,1},{25,9},{2,18},{10... | collective-permute-start | bytes 36872 | tf_op jit(solution)/shard_map/ppermute | solution.py:569
  114.4 2.8 %collective-permute-start.21 = (f32[8,384]{1,0:T(8,128)S(1)}, f32[8,384]{1,0:T(8,128)S(1)}, u32[]{:S(2)}, u32[]{:S(2)}) collective-permute-start(f32[8,384]{1,0:T(8,128)S(1)} %copy-done.17), channel_id=1, source_target_pairs={{0,24},{8,0},{16,8},{24,16},{1,25},{9,1},{17,9},{25,17},{2,26},{10... | collective-permute-start | bytes 36872 | tf_op jit(solution)/shard_map/ppermute | solution.py:569
  115.2 1.9 %copy-start.12 = (f32[8,384]{1,0:T(8,128)}, f32[8,384]{1,0:T(8,128)S(1)}, u32[]{:S(2)}) copy-start(f32[8,384]{1,0:T(8,128)S(1)} %collective-permute-done.19.b) | copy-start | bytes 36868
  115.9 1.2 %copy-start.13 = (f32[8,384]{1,0:T(8,128)}, f32[8,384]{1,0:T(8,128)S(1)}, u32[]{:S(2)}) copy-start(f32[8,384]{1,0:T(8,128)S(1)} %collective-permute-done.20.c) | copy-start | bytes 36868
  117.1 0.6 copy-start.14

commit v7 on v6

--- a/solution.py
+++ b/solution.py
@@ -234,7 +234,7 @@
 
 
 def keys_body(count, *refs):
-    own, other, wkvt, gain, table, kbuf, vbuf = refs[count:]
+    own, other, wkv, gain, table, kbuf, vbuf = refs[count:]
     c = lax.axis_index("c")
     x = lax.axis_index("x")
     kgain = column(gain)
@@ -243,6 +243,7 @@
         == lax.broadcasted_iota(jnp.int32, (ROT, KR), 1) % ROT
     ).astype(bf16)
     group = lax.broadcasted_iota(jnp.int32, (8, KR), 1) // ROT
+    wt = wkv[...].T
     ones = (lax.broadcasted_iota(jnp.int32, (VROWS - VAL, BLOCK), 0) == 0).astype(bf16)
     blocks = [(own, k, k, c) for k in range(NY)] + [(other, k, k, 1 - c) for k in range(NY)]
     for b, (ref, at, y_from, c_from) in enumerate(blocks):
@@ -252,7 +253,7 @@
             lat.append(ref[at, row : row + ROWS, :])
             packed = ref[at, row + ROWS : row + ROWS + 8, :].astype(f32)
             spread += [jnp.where(group == g, packed, 0.0) for g in range(ROWS // 8)]
-        kv = nt(wkvt[...], jnp.concatenate(lat, axis=0))
+        kv = nt(wt, jnp.concatenate(lat, axis=0))
         rope = nt(pick, jnp.concatenate(spread, axis=0).astype(bf16))
         rope_square = jnp.sum(rope * rope, axis=0, keepdims=True)
         place = (x * NY + y_from) * 2 + c_from
@@ -480,7 +481,7 @@
         in_specs=[vmem()] * 3,
         out_specs=(vmem(), vmem()),
         out_shape=(
-            jax.ShapeDtypeStruct((ROWS, 256), bf16),
+            pltpu.VMEM((ROWS, 256), bf16),
             jax.ShapeDtypeStruct((ROWS, 256), bf16),
         ),
         scratch_shapes=[pltpu.VMEM((ROWS, 512), bf16)],
@@ -557,7 +558,7 @@
         ],
         compiler_params=params(40),
         name="project",
-    )(near(got), mine, near(theirs), *weights)
+    )(near(got), near(mine), near(theirs), *weights)
 
 
 def across(x):
@@ -588,7 +589,6 @@
     w_out_pool,
 ):
     wqt = query_up_weight.T
-    wkvt = key_value_up_weight.T
 
     q_all, kv_all, pool_in = latents(
         tokens,
@@ -634,8 +634,8 @@
     q_own = [q_side] + [shifted(q_side, "x", k) for k in range(1, NX)]
     q_twin = [across(q) for q in q_own]
     kv_twin = across(kv)
-    qt = queries(wkvt, q_own, q_twin, wqt, query_gain, query_tables())
-    pair = keys_values((), kv, kv_twin, wkvt, key_gain, key_tables())
+    qt = queries(key_value_up_weight, q_own, q_twin, wqt, query_gain, query_tables())
+    pair = keys_values((), kv, kv_twin, key_value_up_weight, key_gain, key_tables())
     message, *logs = attend(*pair, qt)
 
     got = lax.all_to_all(message, ("x", "y"), 0, 0, tiled=True)

time: 121 us -> 120 us (level)
    unnamed x46 -> x45, local copies, waits for them, and re-layouts: 2.83 us -> 1.93 us
  transfers between devices with their start and end apart: 25 -> 25, of which waited for: 9 -> 10; matrix products, arithmetic and copies ran while one was open for 4% -> 4% of each run, Pallas kernels for 21% -> 21%
where the time goes in v7:
time: 120 us; the launch traced here: 119 us
  starting transfers between devices  54 us (45%)
  Pallas kernels  32.1 us (27%)
  waiting for transfers between devices  25.4 us (21%)
  local copies, waits for them, and re-layouts  3.74 us (3%)
  other arithmetic  2.91 us (2%)
    ppermute x13, starting transfers between devices, shifted(): lax.ppermute(x, axis, [(i, (i + places) % count) for i in range(count)])  22 us
    pallas_call x1, Pallas kernels, attend(): pl.pallas_call(attend_body, in_specs=[vmem()] * 3, out_specs=(pl.BlockSpe...  16.4 us
    all_to_all x1, starting transfers between devices, shards(): lax.all_to_all(kv_all, 'z', 0, 0, tiled=True).reshape(NZ * (ROWS + 8), KR)  9 us
    ppermute x7, starting transfers between devices, across(): return lax.ppermute(x, 'c', [(0, 1), (1, 0)])  8.16 us
    all_to_all x1, waiting for transfers between devices, shards(): lax.all_to_all(jnp.broadcast_to(kv_own[None], (NY, *kv_own.shape)), 'y',...  7.79 us
    ppermute x13, waiting for transfers between devices, shifted(): lax.ppermute(x, axis, [(i, (i + places) % count) for i in range(count)])  6.68 us
    all_to_all x1, starting transfers between devices, shards(): got = lax.all_to_all(message, ('x', 'y'), 0, 0, tiled=True)  4.59 us
    all_to_all x1, starting transfers between devices, shards(): lax.all_to_all(jnp.broadcast_to(kv_own[None], (NY, *kv_own.shape)), 'y',...  4.38 us
  transfers between devices with their start and end apart: 25, of which 10 were waited for; matrix products, arithmetic and copies ran while one was open for 4% of the time, Pallas kernels for 21%

profile of v7, /device:TPU:1, one launch (start us, length us, event | category | flops | bytes accessed | tf_op | source)
XLA Modules:
  0.0 119.3 jit_solution(11796429960703416440)
XLA Ops:
  0.7 4.2 %latents.1 = (bf16[48,512]{1,0:T(8,128)(2,1)}, bf16[8,56,256]{2,1,0:T(8,128)(2,1)}, bf16[48,512]{1,0:T(8,128)(2,1)}) custom-call(bf16[48,2048]{1,0:T(8,128)(2,1)} %tok.1, bf16[2048]{0:T(1024)(128)(2,1)} %gain.2, bf16[2048,512]{1,0:T(8,128)(2,1)} %qdw.1, bf16[512]{0:T(512)(128)(2,1)} %qg.1, bf16[2048,256]{1,0:T(8,128)(2,1)} %kdw.1, bf16[256]{0:T(256)(128)(2,1)} %kg.1, ...), custom_call_target="tpu_custom_call" | custom-call | tf_op jit(solution)/shard_map/latents/pallas_call | solution.py:128
  4.9 9.0 %all-to-all-start = ((bf16[8,56,256]{2,1,0:T(8,128)(2,1)}), bf16[8,56,256]{2,1,0:T(8,128)(2,1)S(1)}, u32[]{:S(2)}, u32[]{:S(2)}) async-start(bf16[8,56,256]{2,1,0:T(8,128)(2,1)} %get-tuple-element.16), calls=%async_computation | async-start | bytes 458752 | tf_op jit(solution)/shard_map/all_to_all | solution.py:604
  13.9 1.4 %collective-permute-start.1 = (bf16[48,512]{1,0:T(8,128)(2,1)}, bf16[48,512]{1,0:T(8,128)(2,1)S(1)}, u32[]{:S(2)}, u32[]{:S(2)}) collective-permute-start(bf16[48,512]{1,0:T(8,128)(2,1)} %get-tuple-element.19), channel_id=1, source_target_pairs={{0,2},{2,4},{4,6},{6,0},{1,3},{3,5},{5,7},{7,1},{8,10},{10,12},{12... | collective-permute-start | bytes 147464 | tf_op jit(solution)/shard_map/ppermute | solution.py:570
  15.3 2.6 %collective-permute-start.2 = (bf16[48,512]{1,0:T(8,128)(2,1)}, bf16[48,512]{1,0:T(8,128)(2,1)S(1)}, u32[]{:S(2)}, u32[]{:S(2)}) collective-permute-start(bf16[48,512]{1,0:T(8,128)(2,1)} %get-tuple-element.19), channel_id=1, source_target_pairs={{0,4},{2,6},{4,0},{6,2},{1,5},{3,7},{5,1},{7,3},{8,12},{10,14},{12... | collective-permute-start | bytes 147464 | tf_op jit(solution)/shard_map/ppermute | solution.py:570
  17.9 1.1 collective-permute-start.3
  19.0 0.5 collective-permute-start.14
  19.5 4.2 %all-to-all-done = bf16[8,56,256]{2,1,0:T(8,128)(2,1)S(1)} async-done(((bf16[8,56,256]{2,1,0:T(8,128)(2,1)}), bf16[8,56,256]{2,1,0:T(8,128)(2,1)S(1)}, u32[]{:S(2)}, u32[]{:S(2)}) %all-to-all-start) | async-done | bytes 229408 | tf_op jit(solution)/shard_map/all_to_all | solution.py:604
  23.7 1.0 broadcast_in_dim.9
  24.8 4.4 %all-to-all-start.1 = ((bf16[4,448,256]{2,1,0:T(8,128)(2,1)}), bf16[4,448,256]{2,1,0:T(8,128)(2,1)}, u32[]{:S(2)}, u32[]{:S(2)}) async-start(bf16[4,448,256]{2,1,0:T(8,128)(2,1)} %broadcast_in_dim.9), calls=%async_computation.1 | async-start | bytes 1835008 | tf_op jit(solution)/shard_map/all_to_all | solution.py:630
  29.5 2.8 %collective-permute-start.15 = (bf16[128,2048]{1,0:T(8,128)(2,1)S(1)}, bf16[128,2048]{1,0:T(8,128)(2,1)S(1)}, u32[]{:S(2)}, u32[]{:S(2)}) collective-permute-start(bf16[128,2048]{1,0:T(8,128)(2,1)S(1)} %pad_maximum_fusion.2.refs_1_), channel_id=1, source_target_pairs={{0,6},{2,0},{4,2},{6,4},{1,7},{3,1},{5,3},{7,5},{8,14},{10,8},{12,... | collective-permute-start | bytes 1572872 | tf_op jit(solution)/shard_map/ppermute | solution.py:570
  32.4 7.8 %all-to-all-done.1.refs_0_ = bf16[4,448,256]{2,1,0:T(8,128)(2,1)} async-done(((bf16[4,448,256]{2,1,0:T(8,128)(2,1)}), bf16[4,448,256]{2,1,0:T(8,128)(2,1)}, u32[]{:S(2)}, u32[]{:S(2)}) %all-to-all-start.1) | async-done | bytes 917536 | tf_op jit(solution)/shard_map/all_to_all | solution.py:630
  40.1 4.4 %collective-permute-start = (bf16[4,448,256]{2,1,0:T(8,128)(2,1)}, bf16[4,448,256]{2,1,0:T(8,128)(2,1)}, u32[]{:S(2)}, u32[]{:S(2)}) collective-permute-start(bf16[4,448,256]{2,1,0:T(8,128)(2,1)} %all-to-all-done.1.refs_0_), channel_id=1, source_target_pairs={{0,1},{1,0},{2,3},{3,2},{4,5},{5,4},{6,7},{7,6},{8,9},{9,8},{10,11... | collective-permute-start | bytes 2752520 | tf_op jit(solution)/shard_map/ppermute | solution.py:565
  44.6 1.3 %collective-permute-start.4 = (bf16[192,512]{1,0:T(8,128)(2,1)S(1)}, bf16[192,512]{1,0:T(8,128)(2,1)S(1)}, u32[]{:S(2)}, u32[]{:S(2)}) collective-permute-start(bf16[192,512]{1,0:T(8,128)(2,1)S(1)} %constant_dynamic-update-slice_fusion.own0), channel_id=1, source_target_pairs={{0,8},{8,16},{16,24},{24,0},{1,9},{9,17},{17,25},{25,1},{2,10},{10... | collective-permute-start | bytes 589832 | tf_op jit(solution)/shard_map/ppermute | solution.py:570
  45.9 2.4 %collective-permute-start.5 = (bf16[192,512]{1,0:T(8,128)(2,1)S(1)}, bf16[192,512]{1,0:T(8,128)(2,1)S(1)}, u32[]{:S(2)}, u32[]{:S(2)}) collective-permute-start(bf16[192,512]{1,0:T(8,128)(2,1)S(1)} %constant_dynamic-update-slice_fusion.own0), channel_id=1, source_target_pairs={{0,16},{8,24},{16,0},{24,8},{1,17},{9,25},{17,1},{25,9},{2,18},{10... | collective-permute-start | bytes 589832 | tf_op jit(solution)/shard_map/ppermute | solution.py:570
  48.3 1.2 collective-permute-start.6
  49.5 1.1 pad_maximum_fusion
  50.6 1.8 %collective-permute-done.4.own1 = bf16[192,512]{1,0:T(8,128)(2,1)S(1)} collective-permute-done((bf16[192,512]{1,0:T(8,128)(2,1)S(1)}, bf16[192,512]{1,0:T(8,128)(2,1)S(1)}, u32[]{:S(2)}, u32[]{:S(2)}) %collective-permute-start.4) | collective-permute-done | bytes 196640 | tf_op jit(solution)/shard_map/ppermute | solution.py:570
  52.3 0.9 collective-permute-start.7
  53.5 1.1 pad_maximum_fusion.1
  54.5 3.0 %collective-permute-done.5.own2 = bf16[192,512]{1,0:T(8,128)(2,1)S(1)} collective-permute-done((bf16[192,512]{1,0:T(8,128)(2,1)S(1)}, bf16[192,512]{1,0:T(8,128)(2,1)S(1)}, u32[]{:S(2)}, u32[]{:S(2)}) %collective-permute-start.5) | collective-permute-done | bytes 196640 | tf_op jit(solution)/shard_map/ppermute | solution.py:570
  57.5 2.6 %collective-permute-start.16 = (bf16[256,2048]{1,0:T(8,128)(2,1)}, bf16[256,2048]{1,0:T(8,128)(2,1)}, u32[]{:S(2)}, u32[]{:S(2)}) collective-permute-start(bf16[256,2048]{1,0:T(8,128)(2,1)} %pad_maximum_fusion), channel_id=1, source_target_pairs={{0,2},{2,4},{4,6},{6,0},{1,3},{3,5},{5,7},{7,1},{8,10},{10,12},{12... | collective-permute-start | bytes 3145736 | tf_op jit(solution)/shard_map/ppermute | solution.py:570
  60.1 0.7 collective-permute-start.17
  60.8 1.1 collective-permute-start.9
  62.0 0.3 collective-permute-start.10
  62.2 0.8 collective-permute-done.9.two2
  63.0 0.4 collective-permute-done.10.two3
  63.7 0.4 copy-done.10
  64.1 2.5 %queries.1.qt = bf16[3,128,1536]{2,1,0:T(8,128)(2,1)S(1)} custom-call(bf16[256,384]{1,0:T(8,128)(2,1)} %early.1, bf16[192,512]{1,0:T(8,128)(2,1)} %copy-done.2, bf16[192,512]{1,0:T(8,128)(2,1)} %copy-done.4, bf16[192,512]{1,0:T(8,128)(2,1)} %copy-done.5, bf16[192,512]{1,0:T(8,128)(2,1)} %copy-done.6, bf16[192,512]{1,0:T(8,128)(2,1)} %copy-done.7, ...), custom_call_target="tpu_custom_call" | custom-call | tf_op jit(solution)/shard_map/queries/pallas_call | solution.py:225
  66.6 3.2 %keys.1 = (bf16[3,3072,128]{2,1,0:T(8,128)(2,1)S(1)}, bf16[3,80,3072]{2,1,0:T(8,128)(2,1)S(1)}) custom-call(bf16[4,448,256]{2,1,0:T(8,128)(2,1)} %all-to-all-done.1.refs_0_, bf16[4,448,256]{2,1,0:T(8,128)(2,1)} %collective-permute-done.refs_1_, bf16[256,384]{1,0:T(8,128)(2,1)} %early.1, bf16[96]{0:T(256)(128)(2,1)} %refs_3_.1, f32[16,1024]{1,0:T(8,128)} %constant.5.clone.refs_4_), custom_call_target="tpu_custom_call" | custom-call | tf_op jit(solution)/shard_map/keys/pallas_call | solution.py:279
  69.9 16.4 %attend.1 = (bf16[16,96,256]{2,1,0:T(8,128)(2,1)}, f32[8,384]{1,0:T(8,128)}, f32[8,384]{1,0:T(8,128)}, f32[8,384]{1,0:T(8,128)}, f32[8,384]{1,0:T(8,128)}) custom-call(bf16[3,3072,128]{2,1,0:T(8,128)(2,1)S(1)} %get-tuple-element.17.kbuf, bf16[3,80,3072]{2,1,0:T(8,128)(2,1)S(1)} %get-tuple-element.18.vbuf, bf16[3,128,1536]{2,1,0:T(8,128)(2,1)S(1)} %queries.1.qt), custom_call_target="tpu_custom_call" | custom-call | tf_op jit(solution)/shard_map/attend/pallas_call | solution.py:398
  86.2 4.6 %all-to-all-start.2 = ((bf16[16,96,256]{2,1,0:T(8,128)(2,1)}), bf16[16,96,256]{2,1,0:T(8,128)(2,1)S(1)}, u32[]{:S(2)}, u32[]{:S(2)}) async-start(bf16[16,96,256]{2,1,0:T(8,128)(2,1)} %get-tuple-element.20), calls=%async_computation.2 | async-start | bytes 1572864 | tf_op jit(solution)/shard_map/all_to_all | solution.py:641
  90.8 0.7 fusion.3
  91.5 4.0 %collective-permute-start.11 = (bf16[8,512]{1,0:T(8,128)(2,1)S(1)}, bf16[8,512]{1,0:T(8,128)(2,1)S(1)}, u32[]{:S(2)}, u32[]{:S(2)}) collective-permute-start(bf16[8,512]{1,0:T(8,128)(2,1)S(1)} %get-tuple-element.31), channel_id=1, source_target_pairs={{0,1},{1,2},{2,3},{3,4},{4,5},{5,6},{6,7},{7,8},{8,9},{9,10},{10,1... | collective-permute-start | bytes 24584 | tf_op jit(solution)/shard_map/ppermute | solution.py:608
  95.5 1.9 %collective-permute-start.12 = (bf16[8,512]{1,0:T(8,128)(2,1)S(1)}, bf16[8,512]{1,0:T(8,128)(2,1)S(1)}, u32[]{:S(2)}, u32[]{:S(2)}) collective-permute-start(bf16[8,512]{1,0:T(8,128)(2,1)S(1)} %get-tuple-element.30), channel_id=1, source_target_pairs={{1,0},{2,1},{3,2},{4,3},{5,4},{6,5},{7,6},{8,7},{9,8},{10,9},{11,1... | collective-permute-start | bytes 24584 | tf_op jit(solution)/shard_map/ppermute | solution.py:611
  97.5 4.1 %collective-permute-done.12.high = bf16[8,512]{1,0:T(8,128)(2,1)S(1)} collective-permute-done((bf16[8,512]{1,0:T(8,128)(2,1)S(1)}, bf16[8,512]{1,0:T(8,128)(2,1)S(1)}, u32[]{:S(2)}, u32[]{:S(2)}) %collective-permute-start.12) | collective-permute-done | bytes 8224 | tf_op jit(solution)/shard_map/ppermute | solution.py:611
  101.6 0.6 copy-done.16
  102.2 1.7 %pooling.1 = (bf16[48,256]{1,0:T(8,128)(2,1)S(1)}, bf16[48,256]{1,0:T(8,128)(2,1)}) custom-call(bf16[48,512]{1,0:T(8,128)(2,1)} %get-tuple-element.21.own, bf16[8,512]{1,0:T(8,128)(2,1)} %copy-done.15, bf16[8,512]{1,0:T(8,128)(2,1)} %copy-done.16), custom_call_target="tpu_custom_call" | custom-call | tf_op jit(solution)/shard_map/pooling/pallas_call | solution.py:479
  103.9 1.4 %collective-permute-done.13.theirs = bf16[48,256]{1,0:T(8,128)(2,1)S(1)} collective-permute-done((bf16[48,256]{1,0:T(8,128)(2,1)}, bf16[48,256]{1,0:T(8,128)(2,1)S(1)}, u32[]{:S(2)}, u32[]{:S(2)}) %collective-permute-start.13) | collective-permute-done | bytes 24608 | tf_op jit(solution)/shard_map/ppermute | solution.py:565
  105.3 2.7 %project.1 = (f32[48,2048]{1,0:T(8,128)S(1)}, bf16[48,2048]{1,0:T(8,128)(2,1)S(1)}) custom-call(bf16[16,96,256]{2,1,0:T(8,128)(2,1)S(1)} %all-to-all-done.2.got, bf16[48,256]{1,0:T(8,128)(2,1)S(1)} %get-tuple-element.22.mine, bf16[48,256]{1,0:T(8,128)(2,1)S(1)} %collective-permute-done.13.theirs, bf16[128,2048]{1,0:T(8,128)(2,1)S(1)} %slice.14.refs_0_, ...), custom_call_target="tpu_custom_call" | custom-call | tf_op jit(solution)/shard_map/project/pallas_call | solution.py:547
  108.0 1.2 collective-permute-start.18
  109.2 2.2 %collective-permute-start.19 = (f32[8,384]{1,0:T(8,128)S(1)}, f32[8,384]{1,0:T(8,128)S(1)}, u32[]{:S(2)}, u32[]{:S(2)}) collective-permute-start(f32[8,384]{1,0:T(8,128)S(1)} %copy-done.19), channel_id=1, source_target_pairs={{0,8},{8,16},{16,24},{24,0},{1,9},{9,17},{17,25},{25,1},{2,10},{10... | collective-permute-start | bytes 36872 | tf_op jit(solution)/shard_map/ppermute | solution.py:570
  111.4 2.5 %collective-permute-start.20 = (f32[8,384]{1,0:T(8,128)S(1)}, f32[8,384]{1,0:T(8,128)S(1)}, u32[]{:S(2)}, u32[]{:S(2)}) collective-permute-start(f32[8,384]{1,0:T(8,128)S(1)} %copy-done.18), channel_id=1, source_target_pairs={{0,16},{8,24},{16,0},{24,8},{1,17},{9,25},{17,1},{25,9},{2,18},{10... | collective-permute-start | bytes 36872 | tf_op jit(solution)/shard_map/ppermute | solution.py:570
  113.9 0.8 collective-permute-start.21
  114.7 0.7 collective-permute-done.20.c
  115.4 1.2 %collective-permute-done.21.d = f32[8,384]{1,0:T(8,128)S(1)} collective-permute-done((f32[8,384]{1,0:T(8,128)S(1)}, f32[8,384]{1,0:T(8,128)S(1)}, u32[]{:S(2)}, u32[]{:S(2)}) %collective-permute-start.21) | collective-permute-done | bytes 12320 | tf_op jit(solution)/shard_map/ppermute | solution.py:570
  116.6 0.6 copy-done.14
  117.2 1.4 %logsums.1 = f32[3,384]{1,0:T(4,128)} custom-call(f32[8,384]{1,0:T(8,128)} %get-tuple-element.26.a, f32[8,384]{1,0:T(8,128)} %copy-done.12, f32[8,384]{1,0:T(8,128)} %copy-done.13, f32[8,384]{1,0:T(8,128)} %copy-done.14), custom_call_target="tpu_custom_call" | custom-call | tf_op jit(solution)/shard_map/logsums/pallas_call | solution.py:428
  118.6 0.7 add_convert_fusion
  (65 shorter events, 1.1 us)
Async XLA Ops:
  0.6 28.5 %copy-start = (bf16[1,64,64]{2,1,0:T(8,128)(2,1)S(1)}, bf16[1,64,64]{2,1,0:T(8,128)(2,1)}, u32[]{:S(2)}) copy-start(bf16[1,64,64]{2,1,0:T(8,128)(2,1)} %param.30) | copy-start | bytes 24580
  0.6 18.3 %copy-start.1 = (bf16[192,2048]{1,0:T(8,128)(2,1)S(1)}, bf16[192,2048]{1,0:T(8,128)(2,1)}, u32[]{:S(2)}) copy-start(bf16[192,2048]{1,0:T(8,128)(2,1)} %param.32) | copy-start | bytes 2359300
  0.7 18.8 %copy-start.20 = (bf16[64]{0:T(256)(128)(2,1)S(1)}, bf16[64]{0:T(256)(128)(2,1)}, u32[]{:S(2)}) copy-start(bf16[64]{0:T(256)(128)(2,1)} %param.31) | copy-start | bytes 388
  4.9 18.8 %all-to-all-start = ((bf16[8,56,256]{2,1,0:T(8,128)(2,1)}), bf16[8,56,256]{2,1,0:T(8,128)(2,1)S(1)}, u32[]{:S(2)}, u32[]{:S(2)}) async-start(bf16[8,56,256]{2,1,0:T(8,128)(2,1)} %get-tuple-element.16), calls=%async_computation | async-start | bytes 458752 | tf_op jit(solution)/shard_map/all_to_all | solution.py:604
  13.9 15.3 %copy-start.3 = (bf16[64,2048]{1,0:T(8,128)(2,1)S(1)}, bf16[64,2048]{1,0:T(8,128)(2,1)}, u32[]{:S(2)}) copy-start(bf16[64,2048]{1,0:T(8,128)(2,1)} %param.33) | copy-start | bytes 786436
  13.9 18.4 %collective-permute-start.1 = (bf16[48,512]{1,0:T(8,128)(2,1)}, bf16[48,512]{1,0:T(8,128)(2,1)S(1)}, u32[]{:S(2)}, u32[]{:S(2)}) collective-permute-start(bf16[48,512]{1,0:T(8,128)(2,1)} %get-tuple-element.19), channel_id=1, source_target_pairs={{0,2},{2,4},{4,6},{6,0},{1,3},{3,5},{5,7},{7,1},{8,10},{10,12},{12... | collective-permute-start | bytes 147464 | tf_op jit(solution)/shard_map/ppermute | solution.py:570
  15.3 17.1 %collective-permute-start.2 = (bf16[48,512]{1,0:T(8,128)(2,1)}, bf16[48,512]{1,0:T(8,128)(2,1)S(1)}, u32[]{:S(2)}, u32[]{:S(2)}) collective-permute-start(bf16[48,512]{1,0:T(8,128)(2,1)} %get-tuple-element.19), channel_id=1, source_target_pairs={{0,4},{2,6},{4,0},{6,2},{1,5},{3,7},{5,1},{7,3},{8,12},{10,14},{12... | collective-permute-start | bytes 147464 | tf_op jit(solution)/shard_map/ppermute | solution.py:570
  17.9 26.7 %collective-permute-start.3 = (bf16[48,512]{1,0:T(8,128)(2,1)}, bf16[48,512]{1,0:T(8,128)(2,1)S(1)}, u32[]{:S(2)}, u32[]{:S(2)}) collective-permute-start(bf16[48,512]{1,0:T(8,128)(2,1)} %get-tuple-element.19), channel_id=1, source_target_pairs={{0,6},{2,0},{4,2},{6,4},{1,7},{3,1},{5,3},{7,5},{8,14},{10,8},{12,... | collective-permute-start | bytes 147464 | tf_op jit(solution)/shard_map/ppermute | solution.py:570
  19.0 29.3 %collective-permute-start.14 = (bf16[128,2048]{1,0:T(8,128)(2,1)S(1)}, bf16[128,2048]{1,0:T(8,128)(2,1)S(1)}, u32[]{:S(2)}, u32[]{:S(2)}) collective-permute-start(bf16[128,2048]{1,0:T(8,128)(2,1)S(1)} %slice.14.refs_0_), channel_id=1, source_target_pairs={{0,2},{2,4},{4,6},{6,0},{1,3},{3,5},{5,7},{7,1},{8,10},{10,12},{12... | collective-permute-start | bytes 1572872 | tf_op jit(solution)/shard_map/ppermute | solution.py:570
  24.8 7.5 %copy-start.11 = (bf16[48,512]{1,0:T(8,128)(2,1)S(1)}, bf16[48,512]{1,0:T(8,128)(2,1)}, u32[]{:S(2)}) copy-start(bf16[48,512]{1,0:T(8,128)(2,1)} %get-tuple-element.19) | copy-start | bytes 147460
  24.8 15.4 %all-to-all-start.1 = ((bf16[4,448,256]{2,1,0:T(8,128)(2,1)}), bf16[4,448,256]{2,1,0:T(8,128)(2,1)}, u32[]{:S(2)}, u32[]{:S(2)}) async-start(bf16[4,448,256]{2,1,0:T(8,128)(2,1)} %broadcast_in_dim.9), calls=%async_computation.1 | async-start | bytes 1835008 | tf_op jit(solution)/shard_map/all_to_all | solution.py:630
  29.5 23.7 %collective-permute-start.15 = (bf16[128,2048]{1,0:T(8,128)(2,1)S(1)}, bf16[128,2048]{1,0:T(8,128)(2,1)S(1)}, u32[]{:S(2)}, u32[]{:S(2)}) collective-permute-start(bf16[128,2048]{1,0:T(8,128)(2,1)S(1)} %pad_maximum_fusion.2.refs_1_), channel_id=1, source_target_pairs={{0,6},{2,0},{4,2},{6,4},{1,7},{3,1},{5,3},{7,5},{8,14},{10,8},{12,... | collective-permute-start | bytes 1572872 | tf_op jit(solution)/shard_map/ppermute | solution.py:570
  40.1 26.5 %collective-permute-start = (bf16[4,448,256]{2,1,0:T(8,128)(2,1)}, bf16[4,448,256]{2,1,0:T(8,128)(2,1)}, u32[]{:S(2)}, u32[]{:S(2)}) collective-permute-start(bf16[4,448,256]{2,1,0:T(8,128)(2,1)} %all-to-all-done.1.refs_0_), channel_id=1, source_target_pairs={{0,1},{1,0},{2,3},{3,2},{4,5},{5,4},{6,7},{7,6},{8,9},{9,8},{10,11... | collective-permute-start | bytes 2752520 | tf_op jit(solution)/shard_map/ppermute | solution.py:565
  44.6 10.0 %copy-start.2 = (bf16[192,512]{1,0:T(8,128)(2,1)}, bf16[192,512]{1,0:T(8,128)(2,1)S(1)}, u32[]{:S(2)}) copy-start(bf16[192,512]{1,0:T(8,128)(2,1)S(1)} %constant_dynamic-update-slice_fusion.own0) | copy-start | bytes 589828
  44.6 7.7 %collective-permute-start.4 = (bf16[192,512]{1,0:T(8,128)(2,1)S(1)}, bf16[192,512]{1,0:T(8,128)(2,1)S(1)}, u32[]{:S(2)}, u32[]{:S(2)}) collective-permute-start(bf16[192,512]{1,0:T(8,128)(2,1)S(1)} %constant_dynamic-update-slice_fusion.own0), channel_id=1, source_target_pairs={{0,8},{8,16},{16,24},{24,0},{1,9},{9,17},{17,25},{25,1},{2,10},{10... | collective-permute-start | bytes 589832 | tf_op jit(solution)/shard_map/ppermute | solution.py:570
  45.9 11.6 %collective-permute-start.5 = (bf16[192,512]{1,0:T(8,128)(2,1)S(1)}, bf16[192,512]{1,0:T(8,128)(2,1)S(1)}, u32[]{:S(2)}, u32[]{:S(2)}) collective-permute-start(bf16[192,512]{1,0:T(8,128)(2,1)S(1)} %constant_dynamic-update-slice_fusion.own0), channel_id=1, source_target_pairs={{0,16},{8,24},{16,0},{24,8},{1,17},{9,25},{17,1},{25,9},{2,18},{10... | collective-permute-start | bytes 589832 | tf_op jit(solution)/shard_map/ppermute | solution.py:570
  48.3 11.8 %collective-permute-start.6 = (bf16[192,512]{1,0:T(8,128)(2,1)S(1)}, bf16[192,512]{1,0:T(8,128)(2,1)S(1)}, u32[]{:S(2)}, u32[]{:S(2)}) collective-permute-start(bf16[192,512]{1,0:T(8,128)(2,1)S(1)} %constant_dynamic-update-slice_fusion.own0), channel_id=1, source_target_pairs={{0,24},{8,0},{16,8},{24,16},{1,25},{9,1},{17,9},{25,17},{2,26},{10... | collective-permute-start | bytes 589832 | tf_op jit(solution)/shard_map/ppermute | solution.py:570
  52.3 11.1 %copy-start.4 = (bf16[192,512]{1,0:T(8,128)(2,1)}, bf16[192,512]{1,0:T(8,128)(2,1)S(1)}, u32[]{:S(2)}) copy-start(bf16[192,512]{1,0:T(8,128)(2,1)S(1)} %collective-permute-done.4.own1) | copy-start | bytes 589828
  52.3 8.5 %collective-permute-start.7 = (bf16[192,512]{1,0:T(8,128)(2,1)S(1)}, bf16[192,512]{1,0:T(8,128)(2,1)S(1)}, u32[]{:S(2)}, u32[]{:S(2)}) collective-permute-start(bf16[192,512]{1,0:T(8,128)(2,1)S(1)} %constant_dynamic-update-slice_fusion.own0), channel_id=1, source_target_pairs={{0,1},{1,0},{2,3},{3,2},{4,5},{5,4},{6,7},{7,6},{8,9},{9,8},{10,11... | collective-permute-start | bytes 589832 | tf_op jit(solution)/shard_map/ppermute | solution.py:565
  53.2 8.8 %collective-permute-start.8 = (bf16[192,512]{1,0:T(8,128)(2,1)S(1)}, bf16[192,512]{1,0:T(8,128)(2,1)S(1)}, u32[]{:S(2)}, u32[]{:S(2)}) collective-permute-start(bf16[192,512]{1,0:T(8,128)(2,1)S(1)} %collective-permute-done.4.own1), channel_id=1, source_target_pairs={{0,1},{1,0},{2,3},{3,2},{4,5},{5,4},{6,7},{7,6},{8,9},{9,8},{10,11... | collective-permute-start | bytes 589832 | tf_op jit(solution)/shard_map/ppermute | solution.py:565
  57.5 5.9 %copy-start.5 = (bf16[192,512]{1,0:T(8,128)(2,1)}, bf16[192,512]{1,0:T(8,128)(2,1)S(1)}, u32[]{:S(2)}) copy-start(bf16[192,512]{1,0:T(8,128)(2,1)S(1)} %collective-permute-done.5.own2) | copy-start | bytes 589828
  57.5 47.7 %collective-permute-start.16 = (bf16[256,2048]{1,0:T(8,128)(2,1)}, bf16[256,2048]{1,0:T(8,128)(2,1)}, u32[]{:S(2)}, u32[]{:S(2)}) collective-permute-start(bf16[256,2048]{1,0:T(8,128)(2,1)} %pad_maximum_fusion), channel_id=1, source_target_pairs={{0,2},{2,4},{4,6},{6,0},{1,3},{3,5},{5,7},{7,1},{8,10},{10,12},{12... | collective-permute-start | bytes 3145736 | tf_op jit(solution)/shard_map/ppermute | solution.py:570
  60.1 3.3 %copy-start.6 = (bf16[192,512]{1,0:T(8,128)(2,1)}, bf16[192,512]{1,0:T(8,128)(2,1)S(1)}, u32[]{:S(2)}) copy-start(bf16[192,512]{1,0:T(8,128)(2,1)S(1)} %collective-permute-done.6.own3) | copy-start | bytes 589828
  60.1 45.2 %collective-permute-start.17 = (bf16[256,2048]{1,0:T(8,128)(2,1)}, bf16[256,2048]{1,0:T(8,128)(2,1)}, u32[]{:S(2)}, u32[]{:S(2)}) collective-permute-start(bf16[256,2048]{1,0:T(8,128)(2,1)} %pad_maximum_fusion.1), channel_id=1, source_target_pairs={{0,6},{2,0},{4,2},{6,4},{1,7},{3,1},{5,3},{7,5},{8,14},{10,8},{12,... | collective-permute-start | bytes 3145736 | tf_op jit(solution)/shard_map/ppermute | solution.py:570
  60.8 2.6 %copy-start.7 = (bf16[192,512]{1,0:T(8,128)(2,1)}, bf16[192,512]{1,0:T(8,128)(2,1)S(1)}, u32[]{:S(2)}) copy-start(bf16[192,512]{1,0:T(8,128)(2,1)S(1)} %collective-permute-done.7.two0) | copy-start | bytes 589828
  60.8 2.2 %collective-permute-start.9 = (bf16[192,512]{1,0:T(8,128)(2,1)S(1)}, bf16[192,512]{1,0:T(8,128)(2,1)S(1)}, u32[]{:S(2)}, u32[]{:S(2)}) collective-permute-start(bf16[192,512]{1,0:T(8,128)(2,1)S(1)} %collective-permute-done.5.own2), channel_id=1, source_target_pairs={{0,1},{1,0},{2,3},{3,2},{4,5},{5,4},{6,7},{7,6},{8,9},{9,8},{10,11... | collective-permute-start | bytes 589832 | tf_op jit(solution)/shard_map/ppermute | solution.py:565
  62.0 1.5 %copy-start.8 = (bf16[192,512]{1,0:T(8,128)(2,1)}, bf16[192,512]{1,0:T(8,128)(2,1)S(1)}, u32[]{:S(2)}) copy-start(bf16[192,512]{1,0:T(8,128)(2,1)S(1)} %collective-permute-done.8.two1) | copy-start | bytes 589828
  62.0 1.4 %collective-permute-start.10 = (bf16[192,512]{1,0:T(8,128)(2,1)S(1)}, bf16[192,512]{1,0:T(8,128)(2,1)S(1)}, u32[]{:S(2)}, u32[]{:S(2)}) collective-permute-start(bf16[192,512]{1,0:T(8,128)(2,1)S(1)} %collective-permute-done.6.own3), channel_id=1, source_target_pairs={{0,1},{1,0},{2,3},{3,2},{4,5},{5,4},{6,7},{7,6},{8,9},{9,8},{10,11... | collective-permute-start | bytes 589832 | tf_op jit(solution)/shard_map/ppermute | solution.py:565
  63.0 0.7 copy-start.9
  63.4 0.7 copy-start.10
  86.2 19.0 %all-to-all-start.2 = ((bf16[16,96,256]{2,1,0:T(8,128)(2,1)}), bf16[16,96,256]{2,1,0:T(8,128)(2,1)S(1)}, u32[]{:S(2)}, u32[]{:S(2)}) async-start(bf16[16,96,256]{2,1,0:T(8,128)(2,1)} %get-tuple-element.20), calls=%async_computation.2 | async-start | bytes 1572864 | tf_op jit(solution)/shard_map/all_to_all | solution.py:641
  91.5 5.9 %collective-permute-start.11 = (bf16[8,512]{1,0:T(8,128)(2,1)S(1)}, bf16[8,512]{1,0:T(8,128)(2,1)S(1)}, u32[]{:S(2)}, u32[]{:S(2)}) collective-permute-start(bf16[8,512]{1,0:T(8,128)(2,1)S(1)} %get-tuple-element.31), channel_id=1, source_target_pairs={{0,1},{1,2},{2,3},{3,4},{4,5},{5,6},{6,7},{7,8},{8,9},{9,10},{10,1... | collective-permute-start | bytes 24584 | tf_op jit(solution)/shard_map/ppermute | solution.py:608
  95.5 6.1 %collective-permute-start.12 = (bf16[8,512]{1,0:T(8,128)(2,1)S(1)}, bf16[8,512]{1,0:T(8,128)(2,1)S(1)}, u32[]{:S(2)}, u32[]{:S(2)}) collective-permute-start(bf16[8,512]{1,0:T(8,128)(2,1)S(1)} %get-tuple-element.30), channel_id=1, source_target_pairs={{1,0},{2,1},{3,2},{4,3},{5,4},{6,5},{7,6},{8,7},{9,8},{10,9},{11,1... | collective-permute-start | bytes 24584 | tf_op jit(solution)/shard_map/ppermute | solution.py:611
  97.5 4.1 %copy-start.15 = (bf16[8,512]{1,0:T(8,128)(2,1)}, bf16[8,512]{1,0:T(8,128)(2,1)S(1)}, u32[]{:S(2)}) copy-start(bf16[8,512]{1,0:T(8,128)(2,1)S(1)} %collective-permute-done.11.low) | copy-start | bytes 24580
  101.6 0.6 copy-start.16
  103.9 1.4 %collective-permute-start.13 = (bf16[48,256]{1,0:T(8,128)(2,1)}, bf16[48,256]{1,0:T(8,128)(2,1)S(1)}, u32[]{:S(2)}, u32[]{:S(2)}) collective-permute-start(bf16[48,256]{1,0:T(8,128)(2,1)} %get-tuple-element.23), channel_id=1, source_target_pairs={{0,1},{1,0},{2,3},{3,2},{4,5},{5,4},{6,7},{7,6},{8,9},{9,8},{10,11... | collective-permute-start | bytes 73736 | tf_op jit(solution)/shard_map/ppermute | solution.py:565
  105.3 3.9 %copy-start.19 = (f32[8,384]{1,0:T(8,128)S(1)}, f32[8,384]{1,0:T(8,128)}, u32[]{:S(2)}) copy-start(f32[8,384]{1,0:T(8,128)} %get-tuple-element.27) | copy-start | bytes 36868
  105.3 6.1 %copy-start.18 = (f32[8,384]{1,0:T(8,128)S(1)}, f32[8,384]{1,0:T(8,128)}, u32[]{:S(2)}) copy-start(f32[8,384]{1,0:T(8,128)} %get-tuple-element.28) | copy-start | bytes 36868
  105.3 8.6 %copy-start.17 = (f32[8,384]{1,0:T(8,128)S(1)}, f32[8,384]{1,0:T(8,128)}, u32[]{:S(2)}) copy-start(f32[8,384]{1,0:T(8,128)} %get-tuple-element.29) | copy-start | bytes 36868
  108.0 10.6 %collective-permute-start.18 = (bf16[48,2048]{1,0:T(8,128)(2,1)S(1)}, bf16[48,2048]{1,0:T(8,128)(2,1)S(1)}, u32[]{:S(2)}, u32[]{:S(2)}) collective-permute-start(bf16[48,2048]{1,0:T(8,128)(2,1)S(1)} %get-tuple-element.25), channel_id=1, source_target_pairs={{0,1},{1,0},{2,3},{3,2},{4,5},{5,4},{6,7},{7,6},{8,9},{9,8},{10,11... | collective-permute-start | bytes 589832 | tf_op jit(solution)/shard_map/ppermute | solution.py:565
  109.2 5.5 %collective-permute-start.19 = (f32[8,384]{1,0:T(8,128)S(1)}, f32[8,384]{1,0:T(8,128)S(1)}, u32[]{:S(2)}, u32[]{:S(2)}) collective-permute-start(f32[8,384]{1,0:T(8,128)S(1)} %copy-done.19), channel_id=1, source_target_pairs={{0,8},{8,16},{16,24},{24,0},{1,9},{9,17},{17,25},{25,1},{2,10},{10... | collective-permute-start | bytes 36872 | tf_op jit(solution)/shard_map/ppermute | solution.py:570
  111.4 4.0 %collective-permute-start.20 = (f32[8,384]{1,0:T(8,128)S(1)}, f32[8,384]{1,0:T(8,128)S(1)}, u32[]{:S(2)}, u32[]{:S(2)}) collective-permute-start(f32[8,384]{1,0:T(8,128)S(1)} %copy-done.18), channel_id=1, source_target_pairs={{0,16},{8,24},{16,0},{24,8},{1,17},{9,25},{17,1},{25,9},{2,18},{10... | collective-permute-start | bytes 36872 | tf_op jit(solution)/shard_map/ppermute | solution.py:570
  113.9 2.8 %collective-permute-start.21 = (f32[8,384]{1,0:T(8,128)S(1)}, f32[8,384]{1,0:T(8,128)S(1)}, u32[]{:S(2)}, u32[]{:S(2)}) collective-permute-start(f32[8,384]{1,0:T(8,128)S(1)} %copy-done.17), channel_id=1, source_target_pairs={{0,24},{8,0},{16,8},{24,16},{1,25},{9,1},{17,9},{25,17},{2,26},{10... | collective-permute-start | bytes 36872 | tf_op jit(solution)/shard_map/ppermute | solution.py:570
  114.7 1.9 %copy-start.12 = (f32[8,384]{1,0:T(8,128)}, f32[8,384]{1,0:T(8,128)S(1)}, u32[]{:S(2)}) copy-start(f32[8,384]{1,0:T(8,128)S(1)} %collective-permute-done.19.b) | copy-start | bytes 36868
  115.4 1.2 %copy-start.13 = (f32[8,384]{1,0:T(8,128)}, f32[8,384]{1,0:T(8,128)S(1)}, u32[]{:S(2)}) copy-start(f32[8,384]{1,0:T(8,128)S(1)} %collective-permute-done.20.c) | copy-start | bytes 36868
  116.6 0.6 copy-start.14
